TPU v7x, 512 devices: a whole 4x8x8 slice. The times are simulated.
512 devices in a mesh: sp: 64 (over z, y), tp: 8 (over x, core).
Axes of the slice: x: 4, y: 8, z: 8, core: 2. Of those that a mesh axis runs over, the one named last changes fastest.
Arguments:
- tokens: bfloat16 [16384, 2048], P(('sp', 'tp')), may hold values from -6 to 6
- norm_gain: float32 [2048], replicated, may hold values from 0.1 to 1.9
- w_query: bfloat16 [2048, 1024], P('sp', 'tp'), may hold values from -0.125 to 0.125
- w_forget: bfloat16 [2048, 1024], P('sp', 'tp'), may hold values from -0.125 to 0.125
- w_value: bfloat16 [2048, 1024], P('sp', 'tp'), may hold values from -0.125 to 0.125
- w_outgate: bfloat16 [2048, 1024], P('sp', 'tp'), may hold values from -0.125 to 0.125
- leak: float32 [1024], P('tp'), may hold values from 1.2207031e-05 to 6.1035156e-05
- decay_shift: float32 [16384, 1024], P('sp', 'tp'), may hold values from -1 to 0
- head_gain: float32 [128], replicated, may hold values from 0.1 to 1.9
- w_glu_value: bfloat16 [2048, 2048], P('sp', 'tp'), may hold values from -0.125 to 0.125
- w_glu_gate: bfloat16 [2048, 2048], P('sp', 'tp'), may hold values from -0.125 to 0.125
- conv_kernel: float32 [31, 2048], P(None, 'tp'), may hold values from -20 to 20
- ln_gain: float32 [2048], P('tp'), may hold values from 0.1 to 1.9
- ln_bias: float32 [2048], P('tp'), may hold values from -3 to 3
- w_out_rec: bfloat16 [1024, 2048], P('tp', 'sp'), may hold values from -0.125 to 0.125
- w_out_conv: bfloat16 [2048, 2048], P('tp', 'sp'), may hold values from -0.09375 to 0.09375
Outputs:
- mixed: bfloat16 [16384, 2048], P(('sp', 'tp'))
All inputs are finite; a program needn't handle non-finite values.
Results may differ from a plain program's by a relative error of at most 0.019.
Values may be sent and summed in bfloat16 or wider, within the bound.
No kernel may reach another device: no remote copies, remote signals or barrier semaphores. Data moves between devices by JAX's collectives and lax.ppermute only.
A program may use at most 64 MiB of HBM per device.

v0:
```python
import jax
import jax.numpy as jnp
from jax import lax
from jax.sharding import Mesh
from jax.sharding import PartitionSpec as P

HEAD_K = 128
HEAD_V = 128
KERNEL = 31
BLOCK = 64
SP = ("sp_0", "sp_1")
SP_TP = ("sp_0", "sp_1", "tp")


def turned_gather(arrays, axis, dims):
    turned = [jnp.moveaxis(a, dim, 0) for a, dim in zip(arrays, dims)]
    widths = [t[0].size for t in turned]
    both = jnp.concatenate([t.reshape(-1, w) for t, w in zip(turned, widths)], axis=1)
    filled = lax.all_gather(both, axis, axis=0, tiled=True)
    pieces = jnp.split(filled, [sum(widths[:k]) for k in range(1, len(widths))], axis=1)
    return tuple(
        (
            jnp.moveaxis(b.reshape(-1, *t.shape[1:]), 0, dim)
            for b, t, dim in zip(pieces, turned, dims)
        )
    )


def from_everyone(value, axis):
    copies = jnp.broadcast_to(value, (lax.axis_size(axis), *value.shape))
    return lax.all_to_all(copies, axis, split_axis=0, concat_axis=0, tiled=True)


def laid_out(pieces, dim):
    lengths = list(pieces.shape[1:])
    lengths[dim] *= pieces.shape[0]
    return jnp.moveaxis(pieces, 0, dim).reshape(lengths)


def gather_directly(value, axis, dim):
    pieces = from_everyone(value, axis)
    return laid_out(pieces, dim)


def neutral_like(value, identity):
    return jax.tree.map(
        lambda a, e: jnp.broadcast_to(jnp.asarray(e, a.dtype), a.shape), value, identity
    )


def collected_together(value, axis):
    leaves = jax.tree.leaves(value)
    order = sorted(range(len(leaves)), key=lambda k: -leaves[k].size)
    width = (1, *leaves[order[0]].shape)[-1]
    lines = [
        jnp.pad(leaves[k].reshape(-1), (0, -leaves[k].size % width)).reshape(-1, width)
        for k in order
    ]
    both, at, found = (lax.all_gather(jnp.concatenate(lines), axis), 0, {})
    for k, line in zip(order, lines):
        piece = both[:, at : at + len(line)].reshape(len(both), -1)
        found[k] = piece[:, : leaves[k].size].reshape(-1, *leaves[k].shape)
        at += len(line)
    numbers = iter(range(len(leaves)))
    return jax.tree.map(lambda _: found[next(numbers)], value)


def entering(value, axes, combine, identity):
    before = start = neutral_like(value, identity)
    subtotal = value
    for axis in reversed(axes):
        peers, position = (lax.axis_size(axis), lax.axis_index(axis))
        pieces = collected_together(
            jax.tree.map(
                lambda part, kind: part.astype(kind), subtotal, (jnp.bfloat16, jnp.bfloat16)
            ),
            axis,
        )
        inside, subtotal = (start, start)
        for k in range(peers):
            passed = k < position
            subtotal = combine(
                subtotal, jax.tree.map(lambda part, own: part[k].astype(own.dtype), pieces, value)
            )
            inside = jax.tree.map(lambda new, old: jnp.where(passed, new, old), subtotal, inside)
        before = combine(inside, before)
    return before


def from_behind(value, axis, steps):
    count = lax.axis_size(axis)
    initial, last = (max(0, -steps), min(count, count - steps))
    return lax.ppermute(value, axis, [(source, source + steps) for source in range(initial, last)])


def over_copies(value, axis):
    return from_everyone(value, axis).sum(axis=0)


def in_one(arrays, axis):
    ravelled, at, done = (jnp.concatenate([a.reshape(-1) for a in arrays]), 0, [])
    subtotal = over_copies(ravelled, axis)
    for a in arrays:
        done.append(subtotal[at : at + a.size].reshape(a.shape))
        at += a.size
    return tuple(done)


def split_up(value, dim, peers):
    before, after = (value.shape[:dim], value.shape[dim + 1 :])
    return jnp.moveaxis(value.reshape(*before, peers, -1, *after), dim, 0)


def sent_and_summed(value, axis, dim):
    pieces = split_up(value, dim, lax.axis_size(axis))
    arrived = lax.all_to_all(pieces, axis, split_axis=0, concat_axis=0, tiled=True)
    return arrived.astype(jnp.float32).sum(axis=0)


def normalize(row_block, norm_gain):
    values_in = row_block.astype(jnp.float32)
    row_scale = lax.rsqrt(jnp.mean(values_in * values_in, axis=1, keepdims=True) + 1e-06)
    return (values_in * row_scale * norm_gain).astype(jnp.bfloat16)


def combine_states(earlier, later):
    return (earlier[0] + later[0], jnp.exp(later[0])[..., None] * earlier[1] + later[1])


def local_recurrence(queries, in_gate, payload_matrix_lines, log_decay):
    row_count, head_count, key_width = queries.shape
    value_width = payload_matrix_lines.shape[2]
    block_count = row_count // BLOCK

    def split_blocks(tensor):
        return tensor.reshape(block_count, BLOCK, head_count, tensor.shape[-1])

    q_blocks = split_blocks(queries)
    k_blocks = split_blocks(in_gate)
    v_blocks = split_blocks(payload_matrix_lines)
    cumulative_sum = jnp.cumsum(split_blocks(log_decay), axis=1)
    causal = jnp.tril(jnp.ones((BLOCK, BLOCK), jnp.float32))
    scores = jnp.einsum(
        "nthk,nshk->nhts", q_blocks * jnp.exp(cumulative_sum), k_blocks * jnp.exp(-cumulative_sum)
    )
    within = jnp.einsum("nhts,nshv->nthv", scores * causal, v_blocks)
    block_finish = cumulative_sum[:, -1]
    contrib = jnp.einsum(
        "nshk,nshv->nhkv", k_blocks * jnp.exp(block_finish[:, None] - cumulative_sum), v_blocks
    )

    def advance(carried_in, inputs):
        state_list, before = carried_in
        query_block, column_block, e_block, added_terms = inputs
        carried_state = jnp.einsum("aub,ubd->aud", query_block * jnp.exp(column_block), state_list)
        device_query = query_block * jnp.exp(column_block + before[None])
        state_list = jnp.exp(e_block)[..., None] * state_list + added_terms
        return ((state_list, before + e_block), (carried_state, device_query))

    initial = (
        jnp.zeros((head_count, key_width, value_width), jnp.float32),
        jnp.zeros((head_count, key_width), jnp.float32),
    )
    (state_list, totals), (carried_state, device_query) = lax.scan(
        advance, initial, (q_blocks, cumulative_sum, block_finish, contrib)
    )
    recurrence_step = (within + carried_state).reshape(row_count, head_count, value_width)
    return (
        recurrence_step,
        device_query.reshape(row_count, head_count, key_width),
        state_list,
        totals,
    )


def on_device(
    tokens,
    norm_gain,
    w_query,
    w_forget,
    w_value,
    w_outgate,
    leak,
    decay_shift,
    head_gain,
    w_glu_value,
    w_glu_gate,
    conv_kernel,
    ln_gain,
    ln_bias,
    w_out_rec,
    w_out_conv,
):
    widths = [
        w_query.shape[1],
        w_forget.shape[1],
        w_value.shape[1],
        w_outgate.shape[1],
        w_glu_value.shape[1],
        w_glu_gate.shape[1],
    ]
    gathered = turned_gather(
        (w_query, w_forget, w_value, w_outgate, w_glu_value, w_glu_gate, w_out_rec, w_out_conv),
        SP,
        (0, 0, 0, 0, 0, 0, 1, 1),
    )
    full_in = gathered[:6]
    out_rec = gathered[6]
    out_conv = gathered[7]
    normed = normalize(gather_directly(tokens, "tp", 0), norm_gain)
    joined = jnp.concatenate(
        [
            jnp.dot(normed, weight, preferred_element_type=jnp.float32).astype(jnp.bfloat16)
            for weight in full_in
        ],
        axis=1,
    )
    projections = []
    column = 0
    for width_now in widths:
        projections.append(joined[:, column : column + width_now])
        column = column + width_now
    query_pre, forget_pre, value_pre, gate_pre, glu_value_pre, glu_gate_pre = projections
    row_count = query_pre.shape[0]
    head_count = query_pre.shape[1] // HEAD_K
    queries = jax.nn.silu(query_pre.astype(jnp.float32))
    in_gate = leak * jax.nn.sigmoid(-forget_pre.astype(jnp.float32))
    log_decay = jnp.log1p(-in_gate) + decay_shift
    recurrence_step, device_query, state_list, totals = local_recurrence(
        queries.reshape(row_count, head_count, HEAD_K),
        in_gate.reshape(row_count, head_count, HEAD_K),
        value_pre.astype(jnp.float32).reshape(row_count, head_count, HEAD_V),
        log_decay.reshape(row_count, head_count, HEAD_K),
    )
    _, incoming_state = entering(
        (totals, state_list),
        SP,
        combine_states,
        (jnp.zeros_like(totals), jnp.zeros_like(state_list)),
    )
    recurrence_step = recurrence_step + jnp.einsum("aub,ubd->aud", device_query, incoming_state)
    scaling = lax.rsqrt(jnp.mean(recurrence_step * recurrence_step, axis=2, keepdims=True) + 1e-06)
    gate_act = jax.nn.silu(gate_pre.astype(jnp.float32)).reshape(row_count, head_count, HEAD_V)
    head_out = (
        (recurrence_step * scaling * head_gain * gate_act)
        .reshape(row_count, head_count * HEAD_V)
        .astype(jnp.bfloat16)
    )
    glu = (
        glu_value_pre.astype(jnp.float32) * jax.nn.sigmoid(glu_gate_pre.astype(jnp.float32))
    ).astype(jnp.bfloat16)
    left_rim = from_behind(glu[row_count - (KERNEL - 1) :], SP, 1)
    extended = jnp.concatenate([left_rim, glu], axis=0).astype(jnp.float32)

    def add_tap(tap_index, accum):
        taps = lax.dynamic_slice_in_dim(conv_kernel, tap_index, 1, 0)
        return accum + taps * lax.dynamic_slice_in_dim(extended, tap_index, row_count, 0)

    conv_sum = lax.fori_loop(0, KERNEL, add_tap, jnp.zeros((row_count, glu.shape[1]), jnp.float32))
    channel_count = conv_sum.shape[1] * lax.axis_size("tp")
    sum_rows, square_rows = in_one(
        (
            jnp.sum(conv_sum, axis=1, keepdims=True),
            jnp.sum(conv_sum * conv_sum, axis=1, keepdims=True),
        ),
        "tp",
    )
    row_mean = sum_rows / channel_count
    centered = conv_sum - row_mean
    row_var = square_rows / channel_count - row_mean * row_mean
    conv_out = jax.nn.silu(centered * lax.rsqrt(row_var + 1e-05) * ln_gain + ln_bias).astype(
        jnp.bfloat16
    )
    mixed = sent_and_summed(
        (
            jnp.dot(head_out, out_rec, preferred_element_type=jnp.float32)
            + jnp.dot(conv_out, out_conv, preferred_element_type=jnp.float32)
        ).astype(jnp.bfloat16),
        "tp",
        0,
    )
    return mixed.astype(jnp.bfloat16)


def solution(mesh):
    torus = Mesh(mesh.devices.reshape(8, 8, mesh.shape["tp"]), ("sp_0", "sp_1", "tp"))
    placed = (
        P(SP_TP, None),
        P(),
        P(SP, "tp"),
        P(SP, "tp"),
        P(SP, "tp"),
        P(SP, "tp"),
        P("tp"),
        P(SP, "tp"),
        P(),
        P(SP, "tp"),
        P(SP, "tp"),
        P(None, "tp"),
        P("tp"),
        P("tp"),
        P("tp", SP),
        P("tp", SP),
    )
    return jax.shard_map(
        on_device, mesh=torus, in_specs=placed, out_specs=P(SP_TP, None), check_vma=False
    )
```

profile of v0, /device:TPU:64, one launch (start us, length us, event | category | flops | bytes accessed | tf_op | source)
XLA Modules:
  0.0 237.1 jit_solution(12225472231829536616)
XLA Ops:
  6.5 0.7 constant_dynamic-update-slice_fusion.7
  9.4 0.7 constant_dynamic-update-slice_fusion.3
  10.1 0.7 constant_dynamic-update-slice_fusion.2
  11.5 0.7 constant_dynamic-update-slice_fusion
  12.9 2.0 broadcast_in_dim.19
  14.9 4.3 %all-to-all-start = ((bf16[8,32,2048]{2,1,0:T(8,128)(2,1)}), bf16[8,32,2048]{2,1,0:T(8,128)(2,1)S(1)}, u32[]{:S(2)}, u32[]{:S(2)}) async-start(bf16[8,32,2048]{2,1,0:T(8,128)(2,1)} %broadcast_in_dim.19), calls=%async_computation | async-start | bytes 2097152 | tf_op jit(solution)/shard_map/all_to_all | solution.py:31
  19.3 15.8 %all-to-all-done = bf16[8,32,2048]{2,1,0:T(8,128)(2,1)S(1)} async-done(((bf16[8,32,2048]{2,1,0:T(8,128)(2,1)}), bf16[8,32,2048]{2,1,0:T(8,128)(2,1)S(1)}, u32[]{:S(2)}, u32[]{:S(2)}) %all-to-all-start) | async-done | bytes 1048608 | tf_op jit(solution)/shard_map/all_to_all | solution.py:31
  35.5 1.0 fusion.9
  36.6 69.1 %all-gather.6.cloned.1.call-done = bf16[2048,1408]{1,0:T(8,128)(2,1)} async-done(((bf16[32,1408]{1,0:T(8,128)(2,1)}), bf16[2048,1408]{1,0:T(8,128)(2,1)}) %all-gather.6.cloned.1.call-update) | async-done | bytes 5767184 | tf_op jit(solution)/shard_map/all_gather | solution.py:19
  105.7 1.5 log-plus-one_add_fusion
  107.3 1.5 convolution_convert_fusion.5
  109.0 1.5 divide_multiply_fusion
  110.5 1.5 while.31
  112.1 25.0 %all-gather.2 = bf16[8,129,128]{2,1,0:T(8,128)(2,1)S(1)} all-gather(bf16[1,129,128]{2,1,0:T(8,128)(2,1)S(1)} %maximum_bitcast_fusion), channel_id=2, replica_groups=mesh['sp_0'=8,'sp_1'=8,'tp'=8] {'sp_1'}, dimensions={0}, use_global_device_ids=true | all-gather | bytes 297216 | tf_op jit(solution)/shard_map/all_gather | solution.py:59
  137.3 24.6 %all-gather.3 = bf16[8,129,128]{2,1,0:T(8,128)(2,1)S(1)} all-gather(bf16[1,129,128]{2,1,0:T(8,128)(2,1)S(1)} %maximum_bitcast_fusion.1), channel_id=3, replica_groups=mesh['sp_0'=8,'sp_1'=8,'tp'=8] {'sp_0'}, dimensions={0}, use_global_device_ids=true | all-gather | bytes 297216 | tf_op jit(solution)/shard_map/all_gather | solution.py:59
  162.0 1.7 fusion.17
  163.6 1.7 fusion.16
  165.3 2.7 %collective-permute-start = (bf16[30,256]{1,0:T(8,128)(2,1)S(1)}, bf16[30,256]{1,0:T(8,128)(2,1)S(1)}, u32[]{:S(2)}, u32[]{:S(2)}) collective-permute-start(bf16[30,256]{1,0:T(8,128)(2,1)S(1)} %slice.229), channel_id=1, source_target_pairs={{0,8},{8,16},{16,24},{24,32},{32,40},{40,48},{48,56},{56,64},{64,7... | collective-permute-start | bytes 46088 | tf_op jit(solution)/shard_map/ppermute | solution.py:93
  169.6 3.5 %collective-permute-done = bf16[30,256]{1,0:T(8,128)(2,1)S(1)} collective-permute-done((bf16[30,256]{1,0:T(8,128)(2,1)S(1)}, bf16[30,256]{1,0:T(8,128)(2,1)S(1)}, u32[]{:S(2)}, u32[]{:S(2)}) %collective-permute-start) | collective-permute-done | bytes 15392 | tf_op jit(solution)/shard_map/ppermute | solution.py:93
  173.1 25.7 %while.32 = (s32[]{:T(128)}, f32[256,256]{1,0:T(8,128)S(1)}, f32[31,256]{1,0:T(8,128)}, f32[286,256]{1,0:T(8,128)S(1)}, s32[]{:T(128)}, /*index=5*/s32[]{:T(128)}) while((s32[]{:T(128)}, f32[256,256]{1,0:T(8,128)S(1)}, f32[31,256]{1,0:T(8,128)}, f32[286,256]{1,0:T(8,128)S(1)}, s32[]{:T(128)}, /*index=5*/s32[]{:T(128)}) %tuple.82), condition=%wide.region_6.7_spmd.clone, body=%wide.region_5.6_spmd.clone.sunk | while | flops 196611 | bytes 789591 | solution.py:259
  173.1 0.7 constant_dynamic-slice_fusion.3
  174.0 0.7 constant_dynamic-slice_fusion.3
  174.8 0.7 constant_dynamic-slice_fusion.3
  175.6 0.7 constant_dynamic-slice_fusion.3
  176.4 0.7 constant_dynamic-slice_fusion.3
  177.3 0.7 constant_dynamic-slice_fusion.3
  178.1 0.7 constant_dynamic-slice_fusion.3
  178.9 0.7 constant_dynamic-slice_fusion.3
  179.8 0.7 constant_dynamic-slice_fusion.3
  180.6 0.7 constant_dynamic-slice_fusion.3
  181.4 0.7 constant_dynamic-slice_fusion.3
  182.3 0.7 constant_dynamic-slice_fusion.3
  183.1 0.7 constant_dynamic-slice_fusion.3
  183.9 0.7 constant_dynamic-slice_fusion.3
  184.7 0.7 constant_dynamic-slice_fusion.3
  186.4 0.7 constant_dynamic-slice_fusion.3
  188.9 0.7 constant_dynamic-slice_fusion.3
  191.4 0.7 constant_dynamic-slice_fusion.3
  193.9 0.7 constant_dynamic-slice_fusion.3
  194.7 0.7 constant_dynamic-slice_fusion.3
  196.4 0.7 constant_dynamic-slice_fusion.3
  197.2 0.7 constant_dynamic-slice_fusion.3
  199.6 4.3 %all-to-all-start.1 = ((f32[8,1,512]{2,1,0:T(1,128)}), f32[8,1,512]{2,1,0:T(1,128)S(1)}, u32[]{:S(2)}, u32[]{:S(2)}) async-start(f32[8,1,512]{2,1,0:T(1,128)} %broadcast_in_dim.23), calls=%async_computation.1 | async-start | bytes 32768 | tf_op jit(solution)/shard_map/all_to_all | solution.py:31
  203.9 2.0 fusion.30
  205.9 3.3 %all-to-all-done.1 = f32[8,1,512]{2,1,0:T(1,128)S(1)} async-done(((f32[8,1,512]{2,1,0:T(1,128)}), f32[8,1,512]{2,1,0:T(1,128)S(1)}, u32[]{:S(2)}, u32[]{:S(2)}) %all-to-all-start.1) | async-done | bytes 16416 | tf_op jit(solution)/shard_map/all_to_all | solution.py:31
  209.3 1.8 fusion.7
  211.1 18.4 %all_to_all.16 = bf16[8,32,2048]{2,1,0:T(8,128)(2,1)S(1)} all-to-all(bf16[8,32,2048]{2,1,0:T(8,128)(2,1)S(1)} %bitcast.158), channel_id=1, replica_groups=mesh['sp_0'=8,'sp_1'=8,'tp'=8] {'tp'}, dimensions={0} | all-to-all | bytes 2097152 | tf_op jit(solution)/shard_map/all_to_all | solution.py:116
  229.4 0.8 reduce_sum.62
  (102 shorter events, 17.9 us)
Async XLA Ops:
  6.5 99.2 %copy-start.2 = (f32[128]{0:T(128)S(1)}, f32[128]{0:T(128)}, u32[]{:S(2)}) copy-start(f32[128]{0:T(128)} %param.26) | copy-start | bytes 1540
  6.5 99.2 %copy-start.1 = (f32[256,128]{1,0:T(8,128)S(1)}, f32[256,128]{1,0:T(8,128)}, u32[]{:S(2)}) copy-start(f32[256,128]{1,0:T(8,128)} %param.27) | copy-start | bytes 393220
  6.5 99.2 %all-gather.6.cloned.1.call-start = ((), (), s32[]{:S(2)}) async-start(), calls=%async_computation.3 | async-start | bytes 5857280 | tf_op jit(solution)/shard_map/all_gather | solution.py:19
  12.3 0.6 copy-start
  14.9 20.2 %all-to-all-start = ((bf16[8,32,2048]{2,1,0:T(8,128)(2,1)}), bf16[8,32,2048]{2,1,0:T(8,128)(2,1)S(1)}, u32[]{:S(2)}, u32[]{:S(2)}) async-start(bf16[8,32,2048]{2,1,0:T(8,128)(2,1)} %broadcast_in_dim.19), calls=%async_computation | async-start | bytes 2097152 | tf_op jit(solution)/shard_map/all_to_all | solution.py:31
  165.3 7.7 %collective-permute-start = (bf16[30,256]{1,0:T(8,128)(2,1)S(1)}, bf16[30,256]{1,0:T(8,128)(2,1)S(1)}, u32[]{:S(2)}, u32[]{:S(2)}) collective-permute-start(bf16[30,256]{1,0:T(8,128)(2,1)S(1)} %slice.229), channel_id=1, source_target_pairs={{0,8},{8,16},{16,24},{24,32},{32,40},{40,48},{48,56},{56,64},{64,7... | collective-permute-start | bytes 46088 | tf_op jit(solution)/shard_map/ppermute | solution.py:93
  199.6 9.6 %all-to-all-start.1 = ((f32[8,1,512]{2,1,0:T(1,128)}), f32[8,1,512]{2,1,0:T(1,128)S(1)}, u32[]{:S(2)}, u32[]{:S(2)}) async-start(f32[8,1,512]{2,1,0:T(1,128)} %broadcast_in_dim.23), calls=%async_computation.1 | async-start | bytes 32768 | tf_op jit(solution)/shard_map/all_to_all | solution.py:31
Sparse Core Ops, SparseCore 0:
  13.0 92.6 all-gather.5
where the time goes:
time: 240 us; the launch traced here: 237 us
  waiting for transfers between devices  91.9 us (38%)
  blocking collectives  68 us (28%)
  local copies, waits for them, and re-layouts  31 us (13%)
  between operations  13.7 us (6%)
  matrix products  13.2 us (6%)
  starting transfers between devices  11.2 us (5%)
  other arithmetic  7.44 us (3%)
    all_gather x1, waiting for transfers between devices, turned_gather(): filled = lax.all_gather(both, axis, axis=0, tiled=True)  69.1 us
    all_gather x2, blocking collectives, collected_together(): both, at, found = (lax.all_gather(jnp.concatenate(lines), axis), 0, {})  49.6 us
    dynamic_slice x31, local copies, waits for them, and re-layouts, add_tap(): taps = lax.dynamic_slice_in_dim(conv_kernel, tap_index, 1, 0)  21.9 us
    all_to_all x2, waiting for transfers between devices, from_everyone(): return lax.all_to_all(copies, axis, split_axis=0, concat_axis=0, tiled=True)  19.2 us
    all_to_all x1, blocking collectives, sent_and_summed(): lax.all_to_all(pieces, axis, split_axis=0, concat_axis=0, tiled=True)  18.4 us
    all_to_all x2, starting transfers between devices, from_everyone(): return lax.all_to_all(copies, axis, split_axis=0, concat_axis=0, tiled=True)  8.55 us
    dot_general x5, matrix products, on_device(): jnp.dot(normed, weight, preferred_element_type=jnp.float32)  7.78 us
    unnamed x14, local copies, waits for them, and re-layouts  5.64 us
  transfers between devices with their start and end apart: 4, of which 4 were waited for; matrix products, arithmetic and copies ran while one was open for 3% of the time, Pallas kernels for 0%

commit v1 on v0

v1 whole, which is shorter than its diff:
```python
import jax
import jax.numpy as jnp
from jax import lax
from jax.experimental import pallas as pl
from jax.experimental.pallas import tpu as pltpu
from jax.sharding import Mesh
from jax.sharding import PartitionSpec as P

HEAD_K = 128
KERNEL = 31
BLOCK = 64
HALO = 32
SP = ("sp_0", "sp_1")
SP_TP = ("sp_0", "sp_1", "tp")
F32 = jnp.float32
BF16 = jnp.bfloat16
EXACT = lax.Precision.HIGHEST
ANY = pl.BlockSpec(memory_space=pl.ANY)


def dot_nt(a, b):
    return lax.dot_general(a, b, (((1,), (1,)), ((), ())), preferred_element_type=F32)


def dot_tn(a, b):
    return lax.dot_general(a, b, (((0,), (0,)), ((), ())), preferred_element_type=F32)


def call(body, outs, *args, grid=None, in_specs=None, out_specs=None, scratch=()):
    specs = {}
    if in_specs is not None:
        specs["in_specs"] = in_specs
    if out_specs is not None:
        specs["out_specs"] = out_specs
    if grid is not None:
        specs["grid"] = grid
    return pl.pallas_call(body, out_shape=outs, scratch_shapes=scratch, **specs)(*args)


def whole(count):
    return [pl.BlockSpec(memory_space=pltpu.VMEM)] * count


def rec_weights_body(q, f, v, g, out):
    joined = jnp.concatenate([q[...], f[...], v[...], g[...]], axis=1)
    for k in range(out.shape[0]):
        out[k] = joined


def rest_weights_body(gv, gg, wr, wc, _, out):
    turned = [w[...].astype(F32).T.astype(BF16) for w in (wr, wc)]
    joined = jnp.concatenate([gv[...], gg[...], *turned], axis=1)
    for k in range(out.shape[0]):
        out[k] = joined


def copies_body(value, _, out):
    out[0] = value[...]


def norm_body(halo, tokens, gain, out):
    def scaled(rows):
        values_in = rows.astype(F32)
        row_scale = lax.rsqrt(jnp.mean(values_in * values_in, axis=1, keepdims=True) + 1e-06)
        return (values_in * row_scale * gain[...]).astype(BF16)

    out[:HALO] = scaled(halo[...])
    for k in range(tokens.shape[0]):
        width = tokens.shape[1]
        out[HALO + k * width : HALO + (k + 1) * width] = scaled(tokens[k])


def pack_state(out, state, total):
    high = total.astype(BF16).astype(F32)
    row = lax.broadcasted_iota(jnp.int32, (8, total.shape[1]), 0)
    tail = jnp.where(row == 0, high, jnp.where(row == 1, total - high, 0.0)).astype(BF16)
    state = state.astype(BF16)
    width = state.shape[0]
    for k in range(out.shape[0]):
        out[k, :width] = state
        out[k, width:] = tail


def rec_body(normed, weights, leak, shift, sent, local, device_query, gate_act):
    rows = normed.shape[0] - HALO
    projected = jnp.dot(normed[HALO:], weights[...], preferred_element_type=F32)
    projected = projected.astype(BF16).astype(F32)
    query_pre, forget_pre, value, gate_pre = [
        projected[:, k * HEAD_K : (k + 1) * HEAD_K] for k in range(4)
    ]
    gate_act[...] = jax.nn.silu(gate_pre)
    queries = jax.nn.silu(query_pre)
    in_gate = leak[...] * jax.nn.sigmoid(-forget_pre)
    log_decay = jnp.log1p(-in_gate) + shift[...]
    at_row = lax.broadcasted_iota(jnp.int32, (BLOCK, BLOCK), 0)
    at_col = lax.broadcasted_iota(jnp.int32, (BLOCK, BLOCK), 1)
    causal = at_row >= at_col
    triangle = jnp.where(causal, 1.0, 0.0).astype(F32)
    value = value.astype(BF16)
    state = jnp.zeros((HEAD_K, HEAD_K), F32)
    before = jnp.zeros((1, HEAD_K), F32)
    for n in range(rows // BLOCK):
        at = slice(n * BLOCK, (n + 1) * BLOCK)
        total = jnp.dot(triangle, log_decay[at], precision=EXACT, preferred_element_type=F32)
        last = total[BLOCK - 1 :]
        grown = queries[at] * jnp.exp(total)
        query = grown.astype(BF16)
        key = (in_gate[at] * jnp.exp(-total)).astype(BF16)
        scores = jnp.where(causal, dot_nt(query, key), 0.0).astype(BF16)
        within = jnp.dot(scores, value[at], preferred_element_type=F32)
        local[at] = within + dot_nt(query, state.astype(BF16))
        device_query[at] = (grown * jnp.exp(before)).astype(BF16)
        late_key = (in_gate[at] * jnp.exp(last - total)).astype(BF16)
        state = jnp.exp(last) * state + dot_tn(value[at], late_key)
        before = before + last
    pack_state(sent, state, before)


def unpack(got, k):
    tail = got[k, HEAD_K:].astype(F32)
    return got[k, :HEAD_K].astype(F32), tail[0:1] + tail[1:2]


def gathered_before(got, position):
    state = inside_state = jnp.zeros((HEAD_K, HEAD_K), F32)
    total = inside_total = jnp.zeros((1, HEAD_K), F32)
    for k in range(got.shape[0]):
        passed = k < position
        new_state, new_total = unpack(got, k)
        state = jnp.exp(new_total) * state + new_state
        total = total + new_total
        inside_state = jnp.where(passed, state, inside_state)
        inside_total = jnp.where(passed, total, inside_total)
    return inside_state, inside_total, state, total


def inner_body(position, got, sent, inner_state, inner_total):
    inside_state, inside_total, state, total = gathered_before(got, position[0])
    inner_state[...] = inside_state
    inner_total[...] = jnp.broadcast_to(inside_total, inner_total.shape)
    pack_state(sent, state, total)


def outer_body(position, got, inner_state, inner_total, device_query, local, gate_act, gain, out):
    outside_state = gathered_before(got, position[0])[0]
    incoming = jnp.exp(inner_total[0:1]) * outside_state + inner_state[...]
    recur = local[...] + dot_nt(device_query[...], incoming.astype(BF16))
    scaling = lax.rsqrt(jnp.mean(recur * recur, axis=1, keepdims=True) + 1e-06)
    out[...] = (recur * scaling * gain[...] * gate_act[...]).astype(BF16)


def conv_body(normed, weights, taps, conv, stats, shifted):
    channels = conv.shape[1]
    rows = conv.shape[0]
    filled = normed.shape[0]
    projected = jnp.dot(normed[...], weights[...], preferred_element_type=F32)
    projected = projected.astype(BF16).astype(F32)
    glu = projected[:, :channels] * jax.nn.sigmoid(projected[:, channels:])
    shifted[0, :filled] = glu.astype(BF16).astype(F32)
    for r in range(1, 8):
        shifted[r, : filled - 8] = shifted[0, r : filled - 8 + r]
    first = HALO - (KERNEL - 1)
    step = 32
    for row in range(0, rows, step):
        accum = jnp.zeros((step, channels), F32)
        for tap in range(KERNEL):
            off = row + first + tap
            base = off // 8 * 8
            accum = accum + taps[tap : tap + 1] * shifted[off - base, base : base + step]
        conv[row : row + step] = accum
    summed = conv[...]
    ones = jnp.ones((8, channels), F32)

    def over_channels(value):
        return lax.dot_general(
            ones, value, (((1,), (1,)), ((), ())), precision=EXACT, preferred_element_type=F32
        )

    row = lax.broadcasted_iota(jnp.int32, (8, rows), 0)
    both = jnp.where(row == 0, over_channels(summed), over_channels(summed * summed))[0:2]
    for k in range(stats.shape[0]):
        stats[k] = both


def out_body(stats, conv, head_out, ln_gain, ln_bias, w_rec, w_low, w_high, out):
    channels = conv.shape[1]
    both = stats[0]
    for k in range(1, stats.shape[0]):
        both = both + stats[k]
    both = both / (channels * stats.shape[0])
    mean = both[0:1]
    inverse = lax.rsqrt(both[1:2] - mean * mean + 1e-05)
    row = lax.broadcasted_iota(jnp.int32, (8, both.shape[1]), 0)
    paired = jnp.where(row == 0, mean, jnp.where(row == 1, inverse, 0.0))

    def column(k):
        chosen = jnp.where(lax.broadcasted_iota(jnp.int32, (8, channels), 0) == k, 1.0, 0.0)
        return lax.dot_general(
            paired,
            chosen.astype(F32),
            (((0,), (0,)), ((), ())),
            precision=EXACT,
            preferred_element_type=F32,
        )

    normal = (conv[...] - column(0)) * column(1) * ln_gain[...] + ln_bias[...]
    conv_out = jax.nn.silu(normal).astype(BF16)
    half = channels // 2
    mixed = dot_nt(head_out[...], w_rec[...])
    mixed = mixed + dot_nt(conv_out[:, :half], w_low[...])
    mixed = mixed + dot_nt(conv_out[:, half:], w_high[...])
    out[...] = mixed.astype(BF16)


def swap(value, axis):
    return lax.all_to_all(value, axis, split_axis=0, concat_axis=0, tiled=True)


def two_stage(copies):
    inner = swap(copies, SP[1])
    peers, rows, width = inner.shape
    return inner, lax.all_gather(inner.reshape(peers * rows, width), SP[0], axis=0, tiled=True)


def on_device(
    tokens,
    norm_gain,
    w_query,
    w_forget,
    w_value,
    w_outgate,
    leak,
    decay_shift,
    head_gain,
    w_glu_value,
    w_glu_gate,
    conv_kernel,
    ln_gain,
    ln_bias,
    w_out_rec,
    w_out_conv,
):
    shape = jax.ShapeDtypeStruct
    inner_count = lax.axis_size(SP[1])
    group = lax.axis_size("tp")
    depth, width = w_query.shape[0], 4 * HEAD_K
    copies = call(
        rec_weights_body,
        shape((inner_count, depth, width), BF16),
        w_query,
        w_forget,
        w_value,
        w_outgate,
    )
    staged, rec_weights = two_stage(copies)
    glu_width = w_glu_value.shape[1] + w_glu_gate.shape[1]
    rest = glu_width + w_out_rec.shape[0] + w_out_conv.shape[0]
    copies = call(
        rest_weights_body,
        shape((inner_count, depth, rest), BF16),
        w_glu_value,
        w_glu_gate,
        w_out_rec,
        w_out_conv,
        staged,
        in_specs=whole(4) + [ANY],
    )
    staged, rest_weights = two_stage(copies)
    share, features = tokens.shape
    copies = call(
        copies_body,
        shape((group, share, features), BF16),
        tokens,
        staged,
        grid=(group,),
        in_specs=[pl.BlockSpec((share, features), lambda k: (0, 0)), ANY],
        out_specs=pl.BlockSpec((1, share, features), lambda k: (k, 0, 0)),
    )
    block = swap(copies, "tp")
    count = lax.axis_size(SP)
    halo = lax.ppermute(block[group - 1], SP, [(k, k + 1) for k in range(count - 1)])
    rows = group * share
    normed = call(
        norm_body, shape((HALO + rows, features), BF16), halo, block, norm_gain.reshape(1, -1)
    )
    message = shape((inner_count, HEAD_K + 8, HEAD_K), BF16)
    sent, local, device_query, gate_act = call(
        rec_body,
        (message, shape((rows, HEAD_K), F32), shape((rows, HEAD_K), BF16), shape((rows, HEAD_K), F32)),
        normed,
        rec_weights,
        leak.reshape(1, -1),
        decay_shift,
    )
    smem = pl.BlockSpec(memory_space=pltpu.SMEM)
    sent, inner_state, inner_total = call(
        inner_body,
        (message, shape((HEAD_K, HEAD_K), F32), shape((8, HEAD_K), F32)),
        lax.axis_index(SP[1]).reshape(1),
        swap(sent, SP[1]),
        in_specs=[smem] + whole(1),
    )
    head_out = call(
        outer_body,
        shape((rows, HEAD_K), BF16),
        lax.axis_index(SP[0]).reshape(1),
        swap(sent, SP[0]),
        inner_state,
        inner_total,
        device_query,
        local,
        gate_act,
        head_gain.reshape(1, -1),
        in_specs=[smem] + whole(7),
    )
    channels = conv_kernel.shape[1]

    def part(size, at):
        return pl.BlockSpec((rest_weights.shape[0], size), lambda k: (0, at))

    def full(*lengths):
        return pl.BlockSpec(lengths, lambda k: (0,) * len(lengths))

    conv, stats = call(
        conv_body,
        (shape((rows, channels), F32), shape((group, 2, rows), F32)),
        normed,
        rest_weights,
        conv_kernel,
        grid=(1,),
        in_specs=[full(*normed.shape), part(glu_width, 0), full(*conv_kernel.shape)],
        out_specs=(full(rows, channels), full(group, 2, rows)),
        scratch=(pltpu.VMEM((8, HALO + rows, channels), F32),),
    )
    stats = swap(stats, "tp")
    mixed = call(
        out_body,
        shape((rows, features), BF16),
        stats,
        conv,
        head_out,
        ln_gain.reshape(1, -1),
        ln_bias.reshape(1, -1),
        rest_weights,
        rest_weights,
        rest_weights,
        grid=(1,),
        in_specs=[
            full(*stats.shape),
            full(rows, channels),
            full(rows, HEAD_K),
            full(1, channels),
            full(1, channels),
            *[part(HEAD_K, glu_width // HEAD_K + k) for k in range(3)],
        ],
        out_specs=full(rows, features),
    )
    arrived = swap(mixed.reshape(group, share, features), "tp")
    return arrived.astype(F32).sum(axis=0).astype(BF16)


def solution(mesh):
    torus = Mesh(mesh.devices.reshape(8, 8, mesh.shape["tp"]), SP_TP)
    placed = (
        P(SP_TP, None),
        P(),
        P(SP, "tp"),
        P(SP, "tp"),
        P(SP, "tp"),
        P(SP, "tp"),
        P("tp"),
        P(SP, "tp"),
        P(),
        P(SP, "tp"),
        P(SP, "tp"),
        P(None, "tp"),
        P("tp"),
        P("tp"),
        P("tp", SP),
        P("tp", SP),
    )
    return jax.shard_map(
        on_device, mesh=torus, in_specs=placed, out_specs=P(SP_TP, None), check_vma=False
    )
```

time: 240 us -> 177 us (0.74)
  the two profiles are of different devices: /device:TPU:64 before, /device:TPU:32 now
where the time goes in v1:
time: 177 us; the launch traced here: 176 us
  blocking collectives  72.3 us (41%)
  starting transfers between devices  28.9 us (16%)
  waiting for transfers between devices  28.8 us (16%)
  Pallas kernels  26.8 us (15%)
  between operations  13.4 us (8%)
  local copies, waits for them, and re-layouts  4.82 us (3%)
    all_to_all x4, blocking collectives, swap(): return lax.all_to_all(value, axis, split_axis=0, concat_axis=0, tiled=True)  72.3 us
    pallas_call x9, Pallas kernels, call(): pl.pallas_call(body, out_shape=outs, scratch_shapes=scratch, **specs)(*args)  26.8 us
    all_to_all x3, starting transfers between devices, swap(): return lax.all_to_all(value, axis, split_axis=0, concat_axis=0, tiled=True)  25.5 us
    all_gather x2, waiting for transfers between devices, two_stage(): lax.all_gather(inner.reshape(peers * rows, width), SP[0], axis=0, tiled=T...  15.2 us
    all_to_all x3, waiting for transfers between devices, swap(): return lax.all_to_all(value, axis, split_axis=0, concat_axis=0, tiled=True)  8.8 us
    unnamed x12, local copies, waits for them, and re-layouts  4.81 us
    ppermute x1, waiting for transfers between devices, on_device(): lax.ppermute(block[group - 1], SP, [(k, k + 1) for k in range(count - 1)])  4.7 us
  transfers between devices with their start and end apart: 6, of which 4 were waited for; matrix products, arithmetic and copies ran while one was open for 2% of the time, Pallas kernels for 12%

profile of v1, /device:TPU:32, one launch (start us, length us, event | category | flops | bytes accessed | tf_op | source)
XLA Modules:
  0.0 175.8 jit_solution(4655950846684313045)
XLA Ops:
  6.5 0.0 all-gather.5.cloned.1.call-start
  6.5 1.5 shard_map.154
  8.0 14.6 %all_to_all.35._ = bf16[8,32,512]{2,1,0:T(8,128)(2,1)} all-to-all(bf16[8,32,512]{2,1,0:T(8,128)(2,1)} %shard_map.154), channel_id=1, replica_groups=mesh['sp_0'=8,'sp_1'=8,'tp'=8] {'sp_1'}, dimensions={0} | all-to-all | bytes 524288 | tf_op jit(solution)/shard_map/all_to_all | solution.py:216
  22.6 0.0 all-gather.5.cloned.1.call-update
  22.6 0.0 all-gather.3.cloned.1.call-start
  22.7 1.5 copy.18.wc
  24.1 1.4 copy.17.wr
  25.5 1.8 %shard_map.155 = bf16[8,32,896]{2,1,0:T(8,128)(2,1)} custom-call(bf16[32,256]{1,0:T(8,128)(2,1)} %gv.1, bf16[32,256]{1,0:T(8,128)(2,1)} %gg.1, bf16[128,32]{1,0:T(8,128)(2,1)} %copy.17.wr, bf16[256,32]{1,0:T(8,128)(2,1)} %copy.18.wc, bf16[8,32,512]{2,1,0:T(8,128)(2,1)} %all_to_all.35._), custom_call_target="tpu_custom_call" | custom-call | tf_op jit(solution)/shard_map/pallas_call | solution.py:37
  27.3 17.0 %all_to_all.36._ = bf16[8,32,896]{2,1,0:T(8,128)(2,1)} all-to-all(bf16[8,32,896]{2,1,0:T(8,128)(2,1)} %shard_map.155), channel_id=1, replica_groups=mesh['sp_0'=8,'sp_1'=8,'tp'=8] {'sp_1'}, dimensions={0} | all-to-all | bytes 917504 | tf_op jit(solution)/shard_map/all_to_all | solution.py:216
  44.3 0.0 all-gather.3.cloned.1.call-update
  44.3 3.7 %shard_map.156 = bf16[8,32,2048]{2,1,0:T(8,128)(2,1)} custom-call(bf16[32,2048]{1,0:T(8,128)(2,1)} %value.1, bf16[8,32,896]{2,1,0:T(8,128)(2,1)} %all_to_all.36._), custom_call_target="tpu_custom_call" | custom-call | tf_op jit(solution)/shard_map/pallas_call | solution.py:37
  48.0 21.3 %all_to_all.37.tokens = bf16[8,32,2048]{2,1,0:T(8,128)(2,1)S(1)} all-to-all(bf16[8,32,2048]{2,1,0:T(8,128)(2,1)} %shard_map.156), channel_id=1, replica_groups=mesh['sp_0'=8,'sp_1'=8,'tp'=8] {'tp'}, dimensions={0} | all-to-all | bytes 2097152 | tf_op jit(solution)/shard_map/all_to_all | solution.py:216
  69.3 0.0 copy-start
  69.3 3.4 %collective-permute-start = (bf16[32,2048]{1,0:T(8,128)(2,1)S(1)}, bf16[32,2048]{1,0:T(8,128)(2,1)S(1)}, u32[]{:S(2)}, u32[]{:S(2)}) collective-permute-start(bf16[32,2048]{1,0:T(8,128)(2,1)S(1)} %slice_bitcast_fusion), channel_id=1, source_target_pairs={{0,8},{8,16},{16,24},{24,32},{32,40},{40,48},{48,56},{56,64},{64,7... | collective-permute-start | bytes 393224 | tf_op jit(solution)/shard_map/ppermute | solution.py:281
  72.7 4.7 %collective-permute-done.halo = bf16[32,2048]{1,0:T(8,128)(2,1)S(1)} collective-permute-done((bf16[32,2048]{1,0:T(8,128)(2,1)S(1)}, bf16[32,2048]{1,0:T(8,128)(2,1)S(1)}, u32[]{:S(2)}, u32[]{:S(2)}) %collective-permute-start) | collective-permute-done | bytes 131104 | tf_op jit(solution)/shard_map/ppermute | solution.py:281
  77.4 0.0 copy-start.3
  77.4 0.0 copy-done
  77.4 0.7 copy-done.3
  78.1 2.7 %shard_map.157.normed = bf16[288,2048]{1,0:T(8,128)(2,1)} custom-call(bf16[32,2048]{1,0:T(8,128)(2,1)} %copy-done.3, bf16[8,32,2048]{2,1,0:T(8,128)(2,1)} %copy-done, f32[1,2048]{1,0:T(1,128)} %bitcast.15), custom_call_target="tpu_custom_call" | custom-call | tf_op jit(solution)/shard_map/pallas_call | solution.py:37
  80.8 0.0 all-gather.5.cloned.1.call-done.weights
  80.8 4.7 %shard_map.159 = (bf16[8,136,128]{2,1,0:T(8,128)(2,1)}, f32[256,128]{1,0:T(8,128)}, bf16[256,128]{1,0:T(8,128)(2,1)}, f32[256,128]{1,0:T(8,128)}) custom-call(bf16[288,2048]{1,0:T(8,128)(2,1)} %shard_map.157.normed, bf16[2048,512]{1,0:T(8,128)(2,1)} %all-gather.5.cloned.1.call-done.weights, f32[1,128]{1,0:T(1,128)} %bitcast.18, f32[256,128]{1,0:T(8,128)} %shift.1), custom_call_target="tpu_custom_call" | custom-call | tf_op jit(solution)/shard_map/pallas_call | solution.py:37
  85.4 8.1 %all-to-all-start.4 = ((bf16[8,136,128]{2,1,0:T(8,128)(2,1)}), bf16[8,136,128]{2,1,0:T(8,128)(2,1)S(1)}, u32[]{:S(2)}, u32[]{:S(2)}) async-start(bf16[8,136,128]{2,1,0:T(8,128)(2,1)} %get-tuple-element.16), calls=%async_computation.4 | async-start | bytes 557056 | tf_op jit(solution)/shard_map/all_to_all | solution.py:216
  93.6 5.5 %all-to-all-done.4.got = bf16[8,136,128]{2,1,0:T(8,128)(2,1)S(1)} async-done(((bf16[8,136,128]{2,1,0:T(8,128)(2,1)}), bf16[8,136,128]{2,1,0:T(8,128)(2,1)S(1)}, u32[]{:S(2)}, u32[]{:S(2)}) %all-to-all-start.4) | async-done | bytes 278560 | tf_op jit(solution)/shard_map/all_to_all | solution.py:216
  99.1 0.0 copy-start.1
  99.1 0.7 copy-done.1
  99.8 1.8 %shard_map.160 = (bf16[8,136,128]{2,1,0:T(8,128)(2,1)}, f32[128,128]{1,0:T(8,128)}, f32[8,128]{1,0:T(8,128)}) custom-call(s32[1]{0:T(128)} %bitcast.4.position, bf16[8,136,128]{2,1,0:T(8,128)(2,1)} %copy-done.1), custom_call_target="tpu_custom_call" | custom-call | tf_op jit(solution)/shard_map/pallas_call | solution.py:37
  101.6 13.1 %all-to-all-start.5 = ((bf16[8,136,128]{2,1,0:T(8,128)(2,1)}), bf16[8,136,128]{2,1,0:T(8,128)(2,1)S(1)}, u32[]{:S(2)}, u32[]{:S(2)}) async-start(bf16[8,136,128]{2,1,0:T(8,128)(2,1)} %get-tuple-element.17), calls=%async_computation.5 | async-start | bytes 557056 | tf_op jit(solution)/shard_map/all_to_all | solution.py:216
  114.7 15.2 %all-gather.3.cloned.1.call-done.weights.w_rec.w_low.w_high = bf16[2048,896]{1,0:T(8,128)(2,1)} async-done(((bf16[256,896]{1,0:T(8,128)(2,1)}), bf16[2048,896]{1,0:T(8,128)(2,1)}) %all-gather.3.cloned.1.call-update) | async-done | bytes 3670032 | tf_op jit(solution)/shard_map/all_gather | solution.py:222
  129.9 4.5 %shard_map.158 = (f32[256,256]{1,0:T(8,128)}, f32[8,2,256]{2,1,0:T(2,128)}) custom-call(bf16[288,2048]{1,0:T(8,128)(2,1)} %shard_map.157.normed, bf16[2048,896]{1,0:T(8,128)(2,1)} %all-gather.3.cloned.1.call-done.weights.w_rec.w_low.w_high, f32[31,256]{1,0:T(8,128)} %taps.1), custom_call_target="tpu_custom_call" | custom-call | tf_op jit(solution)/shard_map/pallas_call | solution.py:37
  134.4 0.0 all-to-all-done.5.got
  134.4 0.0 copy-start.2
  134.4 4.3 %all-to-all-start.3 = ((f32[8,2,256]{2,1,0:T(2,128)}), f32[8,2,256]{2,1,0:T(2,128)S(1)}, u32[]{:S(2)}, u32[]{:S(2)}) async-start(f32[8,2,256]{2,1,0:T(2,128)} %get-tuple-element.14), calls=%async_computation.3 | async-start | bytes 32768 | tf_op jit(solution)/shard_map/all_to_all | solution.py:216
  138.7 0.0 copy-done.2
  138.7 2.1 %shard_map.161.head_out = bf16[256,128]{1,0:T(8,128)(2,1)} custom-call(s32[1]{0:T(128)} %bitcast.3.position, bf16[8,136,128]{2,1,0:T(8,128)(2,1)} %copy-done.2, f32[128,128]{1,0:T(8,128)} %get-tuple-element.18.inner_state, f32[8,128]{1,0:T(8,128)} %get-tuple-element.19.inner_total, bf16[256,128]{1,0:T(8,128)(2,1)} %get-tuple-element.20.device_query, ...), custom_call_target="tpu_custom_call" | custom-call | tf_op jit(solution)/shard_map/pallas_call | solution.py:37
  140.8 3.3 %all-to-all-done.3.stats = f32[8,2,256]{2,1,0:T(2,128)S(1)} async-done(((f32[8,2,256]{2,1,0:T(2,128)}), f32[8,2,256]{2,1,0:T(2,128)S(1)}, u32[]{:S(2)}, u32[]{:S(2)}) %all-to-all-start.3) | async-done | bytes 16416 | tf_op jit(solution)/shard_map/all_to_all | solution.py:216
  144.1 0.0 copy-start.4
  144.1 0.6 copy-done.4
  144.7 4.1 %shard_map.162 = bf16[256,2048]{1,0:T(8,128)(2,1)} custom-call(f32[8,2,256]{2,1,0:T(2,128)} %copy-done.4, f32[256,256]{1,0:T(8,128)} %get-tuple-element.15.conv, bf16[256,128]{1,0:T(8,128)(2,1)} %shard_map.161.head_out, f32[1,256]{1,0:T(1,128)} %bitcast.16, f32[1,256]{1,0:T(1,128)} %bitcast.17, ...), custom_call_target="tpu_custom_call" | custom-call | tf_op jit(solution)/shard_map/pallas_call | solution.py:37
  148.8 19.4 %all_to_all.38 = bf16[8,32,2048]{2,1,0:T(8,128)(2,1)S(1)} all-to-all(bf16[8,32,2048]{2,1,0:T(8,128)(2,1)} %bitcast.12), channel_id=1, replica_groups=mesh['sp_0'=8,'sp_1'=8,'tp'=8] {'tp'}, dimensions={0} | all-to-all | bytes 2097152 | tf_op jit(solution)/shard_map/all_to_all | solution.py:216
  168.2 0.8 reduce_sum.12
  (1 shorter events, 0.0 us)
Async XLA Ops:
  6.5 74.2 %all-gather.5.cloned.1.call-start = ((), (), s32[]{:S(2)}) async-start(), calls=%async_computation.8 | async-start | bytes 2359296 | tf_op jit(solution)/shard_map/all_gather | solution.py:222
  22.6 107.3 %all-gather.3.cloned.1.call-start = ((), (), s32[]{:S(2)}) async-start(), calls=%async_computation.7 | async-start | bytes 4128768 | tf_op jit(solution)/shard_map/all_gather | solution.py:222
  69.3 8.1 %copy-start = (bf16[8,32,2048]{2,1,0:T(8,128)(2,1)}, bf16[8,32,2048]{2,1,0:T(8,128)(2,1)S(1)}, u32[]{:S(2)}) copy-start(bf16[8,32,2048]{2,1,0:T(8,128)(2,1)S(1)} %all_to_all.37.tokens) | copy-start | bytes 3145732
  69.3 8.1 %collective-permute-start = (bf16[32,2048]{1,0:T(8,128)(2,1)S(1)}, bf16[32,2048]{1,0:T(8,128)(2,1)S(1)}, u32[]{:S(2)}, u32[]{:S(2)}) collective-permute-start(bf16[32,2048]{1,0:T(8,128)(2,1)S(1)} %slice_bitcast_fusion), channel_id=1, source_target_pairs={{0,8},{8,16},{16,24},{24,32},{32,40},{40,48},{48,56},{56,64},{64,7... | collective-permute-start | bytes 393224 | tf_op jit(solution)/shard_map/ppermute | solution.py:281
  77.4 0.7 copy-start.3
  85.4 13.7 %all-to-all-start.4 = ((bf16[8,136,128]{2,1,0:T(8,128)(2,1)}), bf16[8,136,128]{2,1,0:T(8,128)(2,1)S(1)}, u32[]{:S(2)}, u32[]{:S(2)}) async-start(bf16[8,136,128]{2,1,0:T(8,128)(2,1)} %get-tuple-element.16), calls=%async_computation.4 | async-start | bytes 557056 | tf_op jit(solution)/shard_map/all_to_all | solution.py:216
  99.1 0.7 copy-start.1
  101.6 32.8 %all-to-all-start.5 = ((bf16[8,136,128]{2,1,0:T(8,128)(2,1)}), bf16[8,136,128]{2,1,0:T(8,128)(2,1)S(1)}, u32[]{:S(2)}, u32[]{:S(2)}) async-start(bf16[8,136,128]{2,1,0:T(8,128)(2,1)} %get-tuple-element.17), calls=%async_computation.5 | async-start | bytes 557056 | tf_op jit(solution)/shard_map/all_to_all | solution.py:216
  134.4 4.3 %copy-start.2 = (bf16[8,136,128]{2,1,0:T(8,128)(2,1)}, bf16[8,136,128]{2,1,0:T(8,128)(2,1)S(1)}, u32[]{:S(2)}) copy-start(bf16[8,136,128]{2,1,0:T(8,128)(2,1)S(1)} %all-to-all-done.5.got) | copy-start | bytes 835588
  134.4 9.6 %all-to-all-start.3 = ((f32[8,2,256]{2,1,0:T(2,128)}), f32[8,2,256]{2,1,0:T(2,128)S(1)}, u32[]{:S(2)}, u32[]{:S(2)}) async-start(f32[8,2,256]{2,1,0:T(2,128)} %get-tuple-element.14), calls=%async_computation.3 | async-start | bytes 32768 | tf_op jit(solution)/shard_map/all_to_all | solution.py:216
  144.1 0.6 copy-start.4
Sparse Core Ops, SparseCore 0:
  22.7 47.5 all-gather.4
  72.4 57.4 all-gather.2

commit v2 on v1

v2 whole, which is shorter than its diff:
```python
import jax
import jax.numpy as jnp
from jax import lax
from jax.experimental import pallas as pl
from jax.experimental.pallas import tpu as pltpu
from jax.sharding import Mesh
from jax.sharding import PartitionSpec as P

HEAD_K = 128
KERNEL = 31
BLOCK = 64
HALO = 32
SP = ("sp_0", "sp_1")
TP = ("x", "core")
SP_TP = SP + TP
F32 = jnp.float32
BF16 = jnp.bfloat16
EXACT = lax.Precision.HIGHEST
ANY = pl.BlockSpec(memory_space=pl.ANY)


def dot_nt(a, b):
    return lax.dot_general(a, b, (((1,), (1,)), ((), ())), preferred_element_type=F32)


def dot_tn(a, b):
    return lax.dot_general(a, b, (((0,), (0,)), ((), ())), preferred_element_type=F32)


def call(body, outs, *args, grid=None, in_specs=None, out_specs=None, scratch=()):
    specs = {}
    if in_specs is not None:
        specs["in_specs"] = in_specs
    if out_specs is not None:
        specs["out_specs"] = out_specs
    if grid is not None:
        specs["grid"] = grid
    return pl.pallas_call(body, out_shape=outs, scratch_shapes=scratch, **specs)(*args)


def whole(count):
    return [pl.BlockSpec(memory_space=pltpu.VMEM)] * count


def first_body(gv, gg, q, g, wr, wc, tokens, operand, copies):
    operand[...] = jnp.concatenate([w[...] for w in (gv, gg, q, g, wr, wc)], axis=1)
    for k in range(copies.shape[0]):
        copies[k] = tokens[...]


def second_body(f, v, _, copies):
    joined = jnp.concatenate([f[...], v[...]], axis=1)
    for k in range(copies.shape[0]):
        copies[k] = joined


def norm_body(core, own, other, gain, out, tail):
    peers, share, _ = own.shape

    def scaled(rows):
        values_in = rows.astype(F32)
        row_scale = lax.rsqrt(jnp.mean(values_in * values_in, axis=1, keepdims=True) + 1e-06)
        return (values_in * row_scale * gain[...]).astype(BF16)

    def place(even, odd):
        for k in range(peers):
            out[2 * k * share : (2 * k + 1) * share] = scaled(even[k])
            done = scaled(odd[k])
            out[(2 * k + 1) * share : (2 * k + 2) * share] = done
        tail[...] = done

    @pl.when(core[0] == 0)
    def _():
        place(own, other)

    @pl.when(core[0] != 0)
    def _():
        place(other, own)


def pack_state(out, state, total):
    high = total.astype(BF16).astype(F32)
    row = lax.broadcasted_iota(jnp.int32, (8, total.shape[1]), 0)
    tail = jnp.where(row == 0, high, jnp.where(row == 1, total - high, 0.0)).astype(BF16)
    state = state.astype(BF16)
    width = state.shape[0]
    for k in range(out.shape[0]):
        out[k, :width] = state
        out[k, width:] = tail


def causal_mask():
    at_row = lax.broadcasted_iota(jnp.int32, (BLOCK, BLOCK), 0)
    at_col = lax.broadcasted_iota(jnp.int32, (BLOCK, BLOCK), 1)
    return at_row >= at_col


def state_body(normed, weights, leak, shift, sent, value_out, key, totals, starts, befores):
    rows = normed.shape[0]
    projected = jnp.dot(normed[...], weights[...], preferred_element_type=F32).astype(BF16)
    value = projected[:, HEAD_K:]
    value_out[...] = value
    in_gate = leak[...] * jax.nn.sigmoid(-projected[:, :HEAD_K].astype(F32))
    log_decay = jnp.log1p(-in_gate) + shift[...]
    triangle = jnp.where(causal_mask(), 1.0, 0.0).astype(F32)
    state = jnp.zeros((HEAD_K, HEAD_K), F32)
    before = jnp.zeros((1, HEAD_K), F32)
    kept = []
    for n in range(rows // BLOCK):
        at = slice(n * BLOCK, (n + 1) * BLOCK)
        total = jnp.dot(triangle, log_decay[at], precision=EXACT, preferred_element_type=F32)
        last = total[BLOCK - 1 :]
        totals[at] = total
        key[at] = (in_gate[at] * jnp.exp(-total)).astype(BF16)
        starts[n] = state.astype(BF16)
        kept.append(before)
        late_key = (in_gate[at] * jnp.exp(last - total)).astype(BF16)
        state = jnp.exp(last) * state + dot_tn(value[at], late_key)
        before = before + last
    befores[...] = jnp.concatenate(kept, axis=0)
    pack_state(sent, state, before)


def unpack(got, k):
    tail = got[k, HEAD_K:].astype(F32)
    return got[k, :HEAD_K].astype(F32), tail[0:1] + tail[1:2]


def gathered_before(got, position):
    state = inside_state = jnp.zeros((HEAD_K, HEAD_K), F32)
    total = inside_total = jnp.zeros((1, HEAD_K), F32)
    for k in range(got.shape[0]):
        passed = k < position
        new_state, new_total = unpack(got, k)
        state = jnp.exp(new_total) * state + new_state
        total = total + new_total
        inside_state = jnp.where(passed, state, inside_state)
        inside_total = jnp.where(passed, total, inside_total)
    return inside_state, inside_total, state, total


def inner_body(position, got, sent, inner_state, inner_total):
    inside_state, inside_total, state, total = gathered_before(got, position[0])
    inner_state[...] = inside_state
    inner_total[...] = jnp.broadcast_to(inside_total, inner_total.shape)
    pack_state(sent, state, total)


def outer_body(
    position,
    got,
    inner_state,
    inner_total,
    normed,
    weights,
    value,
    key,
    totals,
    starts,
    befores,
    gain,
    out,
):
    outside_state = gathered_before(got, position[0])[0]
    incoming = jnp.exp(inner_total[0:1]) * outside_state + inner_state[...]
    projected = jnp.dot(normed[...], weights[...], preferred_element_type=F32)
    projected = projected.astype(BF16).astype(F32)
    queries = jax.nn.silu(projected[:, :HEAD_K])
    gate_act = jax.nn.silu(projected[:, HEAD_K:])
    causal = causal_mask()
    for n in range(starts.shape[0]):
        at = slice(n * BLOCK, (n + 1) * BLOCK)
        query = (queries[at] * jnp.exp(totals[at])).astype(BF16)
        scores = jnp.where(causal, dot_nt(query, key[at]), 0.0).astype(BF16)
        state = jnp.exp(befores[n : n + 1]) * incoming + starts[n].astype(F32)
        recur = jnp.dot(scores, value[at], preferred_element_type=F32)
        recur = recur + dot_nt(query, state.astype(BF16))
        scaling = lax.rsqrt(jnp.mean(recur * recur, axis=1, keepdims=True) + 1e-06)
        out[at] = (recur * scaling * gain[...] * gate_act[at]).astype(BF16)


def conv_body(halo, normed, weights, taps, conv, stats, shifted):
    channels = conv.shape[1]
    rows = conv.shape[0]
    filled = HALO + rows
    extended = jnp.concatenate([halo[...], normed[...]], axis=0)
    projected = jnp.dot(extended, weights[...], preferred_element_type=F32)
    projected = projected.astype(BF16).astype(F32)
    glu = projected[:, :channels] * jax.nn.sigmoid(projected[:, channels:])
    shifted[0, :filled] = glu.astype(BF16).astype(F32)
    for r in range(1, 8):
        shifted[r, : filled - 8] = shifted[0, r : filled - 8 + r]
    first = HALO - (KERNEL - 1)
    step = 32
    for row in range(0, rows, step):
        accum = jnp.zeros((step, channels), F32)
        for tap in range(KERNEL):
            off = row + first + tap
            base = off // 8 * 8
            accum = accum + taps[tap : tap + 1] * shifted[off - base, base : base + step]
        conv[row : row + step] = accum
    summed = conv[...]
    ones = jnp.ones((8, channels), F32)

    def over_channels(value):
        return lax.dot_general(
            ones, value, (((1,), (1,)), ((), ())), precision=EXACT, preferred_element_type=F32
        )

    row = lax.broadcasted_iota(jnp.int32, (8, rows), 0)
    both = jnp.where(row == 0, over_channels(summed), over_channels(summed * summed))[0:2]
    for k in range(stats.shape[0]):
        stats[k] = both


def out_body(stats, conv, head_out, ln_gain, ln_bias, w_rec, w_low, w_high, out, conv_out):
    channels = conv.shape[1]

    @pl.when(pl.program_id(0) == 0)
    def _():
        both = stats[0]
        for k in range(1, stats.shape[0]):
            both = both + stats[k]
        both = both / (channels * stats.shape[0])
        mean = both[0:1]
        inverse = lax.rsqrt(both[1:2] - mean * mean + 1e-05)
        row = lax.broadcasted_iota(jnp.int32, (8, both.shape[1]), 0)
        paired = jnp.where(row == 0, mean, jnp.where(row == 1, inverse, 0.0))

        def column(k):
            chosen = jnp.where(lax.broadcasted_iota(jnp.int32, (8, channels), 0) == k, 1.0, 0.0)
            return lax.dot_general(
                paired,
                chosen.astype(F32),
                (((0,), (0,)), ((), ())),
                precision=EXACT,
                preferred_element_type=F32,
            )

        normal = (conv[...] - column(0)) * column(1) * ln_gain[...] + ln_bias[...]
        conv_out[...] = jax.nn.silu(normal).astype(BF16)

    half = channels // 2
    mixed = dot_nt(head_out[...], w_rec[...])
    mixed = mixed + dot_nt(conv_out[:, :half], w_low[...])
    mixed = mixed + dot_nt(conv_out[:, half:], w_high[...])
    out[...] = mixed.astype(BF16)


def swap(value, axis):
    return lax.all_to_all(value, axis, split_axis=0, concat_axis=0, tiled=True)


def on_device(
    tokens,
    norm_gain,
    w_query,
    w_forget,
    w_value,
    w_outgate,
    leak,
    decay_shift,
    head_gain,
    w_glu_value,
    w_glu_gate,
    conv_kernel,
    ln_gain,
    ln_bias,
    w_out_rec,
    w_out_conv,
):
    shape = jax.ShapeDtypeStruct
    smem = pl.BlockSpec(memory_space=pltpu.SMEM)
    inner_count = lax.axis_size(SP[1])
    group = lax.axis_size(TP)
    share, features = tokens.shape
    depth = w_query.shape[0]
    channels = conv_kernel.shape[1]
    columns = (w_glu_value, w_glu_gate, w_query, w_outgate, w_out_rec.T, w_out_conv.T)
    glu_width = 2 * channels
    all_width = sum(w.shape[1] for w in columns)
    operand, copies = call(
        first_body,
        (
            shape((depth, all_width), BF16),
            shape((lax.axis_size(TP[0]), share, features), BF16),
        ),
        *columns,
        tokens,
    )
    gathered = lax.all_gather(operand, SP, axis=0, tiled=True)
    own = swap(copies, TP[0])
    other = lax.ppermute(own, TP[1], [(0, 1), (1, 0)])
    rows = group * share
    normed, tail = call(
        norm_body,
        (shape((rows, features), BF16), shape((share, features), BF16)),
        lax.axis_index(TP[1]).reshape(1),
        own,
        other,
        norm_gain.reshape(1, -1),
        in_specs=[smem] + whole(3),
    )
    count = lax.axis_size(SP)
    copies = call(
        second_body,
        shape((count, depth, 2 * HEAD_K), BF16),
        w_forget,
        w_value,
        other,
        in_specs=whole(2) + [ANY],
    )
    state_weights = swap(copies, SP).reshape(count * depth, 2 * HEAD_K)
    halo = lax.ppermute(tail, SP, [(k, k + 1) for k in range(count - 1)])
    message = shape((inner_count, HEAD_K + 8, HEAD_K), BF16)
    blocks = rows // BLOCK
    sent, *kept = call(
        state_body,
        (
            message,
            shape((rows, HEAD_K), BF16),
            shape((rows, HEAD_K), BF16),
            shape((rows, HEAD_K), F32),
            shape((blocks, HEAD_K, HEAD_K), BF16),
            shape((blocks, HEAD_K), F32),
        ),
        normed,
        state_weights,
        leak.reshape(1, -1),
        decay_shift,
    )
    sent, inner_state, inner_total = call(
        inner_body,
        (message, shape((HEAD_K, HEAD_K), F32), shape((8, HEAD_K), F32)),
        lax.axis_index(SP[1]).reshape(1),
        swap(sent, SP[1]),
        in_specs=[smem] + whole(1),
    )

    def part(size, at):
        return pl.BlockSpec((gathered.shape[0], size), lambda k: (0, at))

    def full(*lengths):
        return pl.BlockSpec(lengths, lambda k: (0,) * len(lengths))

    conv, stats = call(
        conv_body,
        (shape((rows, channels), F32), shape((group, 2, rows), F32)),
        halo,
        normed,
        gathered,
        conv_kernel,
        grid=(1,),
        in_specs=[
            full(*halo.shape),
            full(*normed.shape),
            part(glu_width, 0),
            full(*conv_kernel.shape),
        ],
        out_specs=(full(rows, channels), full(group, 2, rows)),
        scratch=(pltpu.VMEM((8, HALO + rows, channels), F32),),
    )
    stats = swap(stats, TP)
    outer_sent = swap(sent, SP[0])
    head_gain = head_gain.reshape(1, -1)
    head_out = call(
        outer_body,
        shape((rows, HEAD_K), BF16),
        lax.axis_index(SP[0]).reshape(1),
        outer_sent,
        inner_state,
        inner_total,
        normed,
        gathered,
        *kept,
        head_gain,
        grid=(1,),
        in_specs=[
            smem,
            *[full(*a.shape) for a in (outer_sent, inner_state, inner_total, normed)],
            part(2 * HEAD_K, glu_width // (2 * HEAD_K)),
            *[full(*a.shape) for a in kept],
            full(*head_gain.shape),
        ],
        out_specs=full(rows, HEAD_K),
    )
    first = glu_width // HEAD_K + 2
    step = 512
    mixed = call(
        out_body,
        shape((rows, features), BF16),
        stats,
        conv,
        head_out,
        ln_gain.reshape(1, -1),
        ln_bias.reshape(1, -1),
        gathered,
        gathered,
        gathered,
        grid=(features // step,),
        in_specs=[
            full(*stats.shape),
            full(rows, channels),
            full(rows, HEAD_K),
            full(1, channels),
            full(1, channels),
            pl.BlockSpec((step, HEAD_K), lambda k: (k, first)),
            pl.BlockSpec((step, HEAD_K), lambda k: (k, first + 1)),
            pl.BlockSpec((step, HEAD_K), lambda k: (k, first + 2)),
        ],
        out_specs=pl.BlockSpec((rows, step), lambda k: (0, k)),
        scratch=(pltpu.VMEM((rows, channels), BF16),),
    )
    arrived = swap(mixed.reshape(group, share, features), TP)
    return arrived.astype(F32).sum(axis=0).astype(BF16)


def solution(mesh):
    torus = Mesh(mesh.devices.reshape(8, 8, mesh.shape["tp"] // 2, 2), SP_TP)
    placed = (
        P(SP_TP, None),
        P(),
        P(SP, TP),
        P(SP, TP),
        P(SP, TP),
        P(SP, TP),
        P(TP),
        P(SP, TP),
        P(),
        P(SP, TP),
        P(SP, TP),
        P(None, TP),
        P(TP),
        P(TP),
        P(TP, SP),
        P(TP, SP),
    )
    return jax.shard_map(
        on_device, mesh=torus, in_specs=placed, out_specs=P(SP_TP, None), check_vma=False
    )
```

time: 177 us -> 175 us (0.989)
  the two profiles are of different devices: /device:TPU:32 before, /device:TPU:1 now
where the time goes in v2:
time: 175 us
  waiting for transfers between devices  62.5 us (36%)
  starting transfers between devices  38.6 us (22%)
  blocking collectives  30.9 us (18%)
  Pallas kernels  25.2 us (14%)
  between operations  13.4 us (8%)
  local copies, waits for them, and re-layouts  3.1 us (2%)
    all_to_all x4, waiting for transfers between devices, swap(): return lax.all_to_all(value, axis, split_axis=0, concat_axis=0, tiled=True)  37.9 us
    all_to_all x2, blocking collectives, swap(): return lax.all_to_all(value, axis, split_axis=0, concat_axis=0, tiled=True)  30.9 us
    all_to_all x4, starting transfers between devices, swap(): return lax.all_to_all(value, axis, split_axis=0, concat_axis=0, tiled=True)  28.5 us
    pallas_call x8, Pallas kernels, call(): pl.pallas_call(body, out_shape=outs, scratch_shapes=scratch, **specs)(*args)  25.2 us
    all_gather x1, waiting for transfers between devices, on_device(): gathered = lax.all_gather(operand, SP, axis=0, tiled=True)  18.3 us
    ppermute x1, starting transfers between devices, on_device(): other = lax.ppermute(own, TP[1], [(0, 1), (1, 0)])  8.49 us
    ppermute x1, waiting for transfers between devices, on_device(): halo = lax.ppermute(tail, SP, [(k, k + 1) for k in range(count - 1)])  4.81 us
  transfers between devices with their start and end apart: 7, of which 6 were waited for; matrix products, arithmetic and copies ran while one was open for 0% of the time, Pallas kernels for 10%

profile of v2, /device:TPU:1, one launch (start us, length us, event | category | flops | bytes accessed | tf_op | source)
XLA Modules:
  0.0 174.6 jit_solution(14733150355085791853)
XLA Ops:
  6.5 0.0 all-gather.2.cloned.1.call-start
  6.5 1.8 %shard_map.154 = (bf16[32,1152]{1,0:T(8,128)(2,1)}, bf16[4,32,2048]{2,1,0:T(8,128)(2,1)}) custom-call(bf16[32,256]{1,0:T(8,128)(2,1)} %gv.1, bf16[32,256]{1,0:T(8,128)(2,1)} %gg.1, bf16[32,128]{1,0:T(8,128)(2,1)} %q.1, bf16[32,128]{1,0:T(8,128)(2,1)} %g.1, bf16[32,128]{1,0:T(8,128)(2,1)} %bitcast.16, bf16[32,256]{1,0:T(8,128)(2,1)} %bitcast.14, ...), custom_call_target="tpu_custom_call" | custom-call | tf_op jit(solution)/shard_map/pallas_call | solution.py:38
  8.4 0.0 all-gather.2.cloned.1.call-update
  8.4 11.8 %all_to_all.30.own = bf16[4,32,2048]{2,1,0:T(8,128)(2,1)S(1)} all-to-all(bf16[4,32,2048]{2,1,0:T(8,128)(2,1)} %get-tuple-element.20), channel_id=1, replica_groups=mesh['sp_0'=8,'sp_1'=8,'x'=4,'core'=2] {'x'}, dimensions={0} | all-to-all | bytes 1048576 | tf_op jit(solution)/shard_map/all_to_all | solution.py:251
  20.2 0.0 copy-start.2
  20.2 8.5 %collective-permute-start = (bf16[4,32,2048]{2,1,0:T(8,128)(2,1)S(1)}, bf16[4,32,2048]{2,1,0:T(8,128)(2,1)S(1)}, u32[]{:S(2)}, u32[]{:S(2)}) collective-permute-start(bf16[4,32,2048]{2,1,0:T(8,128)(2,1)S(1)} %all_to_all.30.own), channel_id=1, source_target_pairs={{0,1},{1,0},{2,3},{3,2},{4,5},{5,4},{6,7},{7,6},{8,9},{9,8},{10,11... | collective-permute-start | bytes 1572872 | tf_op jit(solution)/shard_map/ppermute | solution.py:293
  28.7 1.5 collective-permute-done.other._
  30.2 0.0 copy-start.1
  30.2 0.8 copy-done.1
  31.0 1.8 %shard_map.157 = bf16[64,32,256]{2,1,0:T(8,128)(2,1)} custom-call(bf16[32,128]{1,0:T(8,128)(2,1)} %f.1, bf16[32,128]{1,0:T(8,128)(2,1)} %v.1, bf16[4,32,2048]{2,1,0:T(8,128)(2,1)} %copy-done.1), custom_call_target="tpu_custom_call" | custom-call | tf_op jit(solution)/shard_map/pallas_call | solution.py:38
  32.8 13.2 %all-to-all-start.2 = ((bf16[64,32,256]{2,1,0:T(8,128)(2,1)}), bf16[64,32,256]{2,1,0:T(8,128)(2,1)S(1)}, u32[]{:S(2)}, u32[]{:S(2)}) async-start(bf16[64,32,256]{2,1,0:T(8,128)(2,1)} %shard_map.157), calls=%async_computation.2 | async-start | bytes 2097152 | tf_op jit(solution)/shard_map/all_to_all | solution.py:251
  46.1 0.0 copy-done.2
  46.1 2.6 %shard_map.155 = (bf16[256,2048]{1,0:T(8,128)(2,1)}, bf16[32,2048]{1,0:T(8,128)(2,1)}) custom-call(s32[1]{0:T(128)} %bitcast.core, bf16[4,32,2048]{2,1,0:T(8,128)(2,1)} %copy-done.2, bf16[4,32,2048]{2,1,0:T(8,128)(2,1)} %copy-done.1, f32[1,2048]{1,0:T(1,128)} %bitcast.15), custom_call_target="tpu_custom_call" | custom-call | tf_op jit(solution)/shard_map/pallas_call | solution.py:38
  48.7 26.5 %all-to-all-done.2 = bf16[64,32,256]{2,1,0:T(8,128)(2,1)S(1)} async-done(((bf16[64,32,256]{2,1,0:T(8,128)(2,1)}), bf16[64,32,256]{2,1,0:T(8,128)(2,1)S(1)}, u32[]{:S(2)}, u32[]{:S(2)}) %all-to-all-start.2) | async-done | bytes 1048608 | tf_op jit(solution)/shard_map/all_to_all | solution.py:251
  75.2 0.0 copy-start
  75.2 1.0 copy-done
  76.2 3.7 %shard_map.158 = (bf16[8,136,128]{2,1,0:T(8,128)(2,1)}, bf16[256,128]{1,0:T(8,128)(2,1)}, bf16[256,128]{1,0:T(8,128)(2,1)}, f32[256,128]{1,0:T(8,128)}, bf16[4,128,128]{2,1,0:T(8,128)(2,1)}, /*index=5*/f32[4,128]{1,0:T(4,128)}) custom-call(bf16[256,2048]{1,0:T(8,128)(2,1)} %get-tuple-element.22.normed, bf16[2048,256]{1,0:T(8,128)(2,1)} %bitcast.13, ...), custom_call_target="tpu_custom_call" | custom-call | tf_op jit(solution)/shard_map/pallas_call | solution.py:38
  80.0 4.8 %all-to-all-start.3 = ((bf16[8,136,128]{2,1,0:T(8,128)(2,1)}), bf16[8,136,128]{2,1,0:T(8,128)(2,1)S(1)}, u32[]{:S(2)}, u32[]{:S(2)}) async-start(bf16[8,136,128]{2,1,0:T(8,128)(2,1)} %get-tuple-element.26), calls=%async_computation.3 | async-start | bytes 557056 | tf_op jit(solution)/shard_map/all_to_all | solution.py:251
  84.7 10.3 %all-to-all-done.3.got = bf16[8,136,128]{2,1,0:T(8,128)(2,1)S(1)} async-done(((bf16[8,136,128]{2,1,0:T(8,128)(2,1)}), bf16[8,136,128]{2,1,0:T(8,128)(2,1)S(1)}, u32[]{:S(2)}, u32[]{:S(2)}) %all-to-all-start.3) | async-done | bytes 278560 | tf_op jit(solution)/shard_map/all_to_all | solution.py:251
  95.0 0.0 copy-start.4
  95.0 0.7 copy-done.4
  95.7 1.8 %shard_map.159 = (bf16[8,136,128]{2,1,0:T(8,128)(2,1)}, f32[128,128]{1,0:T(8,128)}, f32[8,128]{1,0:T(8,128)}) custom-call(s32[1]{0:T(128)} %bitcast.5.position, bf16[8,136,128]{2,1,0:T(8,128)(2,1)} %copy-done.4), custom_call_target="tpu_custom_call" | custom-call | tf_op jit(solution)/shard_map/pallas_call | solution.py:38
  97.5 3.4 %all-to-all-start.4 = ((bf16[8,136,128]{2,1,0:T(8,128)(2,1)}), bf16[8,136,128]{2,1,0:T(8,128)(2,1)S(1)}, u32[]{:S(2)}, u32[]{:S(2)}) async-start(bf16[8,136,128]{2,1,0:T(8,128)(2,1)} %get-tuple-element.27), calls=%async_computation.4 | async-start | bytes 557056 | tf_op jit(solution)/shard_map/all_to_all | solution.py:251
  100.9 1.6 collective-permute-start.1
  102.6 4.8 %collective-permute-done.1.halo = bf16[32,2048]{1,0:T(8,128)(2,1)S(1)} collective-permute-done((bf16[32,2048]{1,0:T(8,128)(2,1)}, bf16[32,2048]{1,0:T(8,128)(2,1)S(1)}, u32[]{:S(2)}, u32[]{:S(2)}) %collective-permute-start.1) | collective-permute-done | bytes 131104 | tf_op jit(solution)/shard_map/ppermute | solution.py:314
  107.4 0.0 copy-start.5
  107.4 18.3 %all-gather.2.cloned.1.call-done.weights.w_rec.w_low.w_high = bf16[2048,1152]{1,0:T(8,128)(2,1)} async-done(((bf16[32,1152]{1,0:T(8,128)(2,1)}), bf16[2048,1152]{1,0:T(8,128)(2,1)}) %all-gather.2.cloned.1.call-update) | async-done | bytes 4718608 | tf_op jit(solution)/shard_map/all_gather | solution.py:291
  125.7 0.0 copy-done.5
  125.7 4.6 %shard_map.156 = (f32[256,256]{1,0:T(8,128)}, f32[8,2,256]{2,1,0:T(2,128)}) custom-call(bf16[32,2048]{1,0:T(8,128)(2,1)} %copy-done.5, bf16[256,2048]{1,0:T(8,128)(2,1)} %get-tuple-element.22.normed, bf16[2048,1152]{1,0:T(8,128)(2,1)} %all-gather.2.cloned.1.call-done.weights.w_rec.w_low.w_high, f32[31,256]{1,0:T(8,128)} %taps.1), custom_call_target="tpu_custom_call" | custom-call | tf_op jit(solution)/shard_map/pallas_call | solution.py:38
  130.2 0.0 all-to-all-done.4.got
  130.2 0.0 copy-start.3
  130.2 7.1 %all-to-all-start.1 = ((f32[8,2,256]{2,1,0:T(2,128)}), f32[8,2,256]{2,1,0:T(2,128)S(1)}, u32[]{:S(2)}, u32[]{:S(2)}) async-start(f32[8,2,256]{2,1,0:T(2,128)} %get-tuple-element.24), calls=%async_computation.1 | async-start | bytes 32768 | tf_op jit(solution)/shard_map/all_to_all | solution.py:251
  137.4 0.0 copy-done.3
  137.4 3.6 %shard_map.160.head_out = bf16[256,128]{1,0:T(8,128)(2,1)} custom-call(s32[1]{0:T(128)} %bitcast.4.position, bf16[8,136,128]{2,1,0:T(8,128)(2,1)} %copy-done.3, f32[128,128]{1,0:T(8,128)} %get-tuple-element.28.inner_state, f32[8,128]{1,0:T(8,128)} %get-tuple-element.29.inner_total, bf16[256,2048]{1,0:T(8,128)(2,1)} %get-tuple-element.22.normed, ...), custom_call_target="tpu_custom_call" | custom-call | tf_op jit(solution)/shard_map/pallas_call | solution.py:38
  141.0 1.0 all-to-all-done.1.stats
  142.0 0.0 copy-start.6
  142.0 0.6 copy-done.6
  142.6 5.2 %shard_map.161 = bf16[256,2048]{1,0:T(8,128)(2,1)} custom-call(f32[8,2,256]{2,1,0:T(2,128)} %copy-done.6, f32[256,256]{1,0:T(8,128)} %get-tuple-element.25.conv, bf16[256,128]{1,0:T(8,128)(2,1)} %shard_map.160.head_out, f32[1,256]{1,0:T(1,128)} %bitcast.17, f32[1,256]{1,0:T(1,128)} %bitcast.18, ...), custom_call_target="tpu_custom_call" | custom-call | tf_op jit(solution)/shard_map/pallas_call | solution.py:38
  147.8 19.1 %all_to_all.31 = bf16[8,32,2048]{2,1,0:T(8,128)(2,1)S(1)} all-to-all(bf16[8,32,2048]{2,1,0:T(8,128)(2,1)} %bitcast.12), channel_id=1, replica_groups=mesh['sp_0'=8,'sp_1'=8,'x'=4,'core'=2] {'x','core'}, dimensions={0} | all-to-all | bytes 2097152 | tf_op jit(solution)/shard_map/all_to_all | solution.py:251
  166.9 0.8 reduce_sum.12
Async XLA Ops:
  6.5 119.1 %all-gather.2.cloned.1.call-start = ((), (), s32[]{:S(2)}) async-start(), calls=%async_computation.6 | async-start | bytes 4792320 | tf_op jit(solution)/shard_map/all_gather | solution.py:291
  20.2 25.9 %copy-start.2 = (bf16[4,32,2048]{2,1,0:T(8,128)(2,1)}, bf16[4,32,2048]{2,1,0:T(8,128)(2,1)S(1)}, u32[]{:S(2)}) copy-start(bf16[4,32,2048]{2,1,0:T(8,128)(2,1)S(1)} %all_to_all.30.own) | copy-start | bytes 1572868
  20.2 10.0 %collective-permute-start = (bf16[4,32,2048]{2,1,0:T(8,128)(2,1)S(1)}, bf16[4,32,2048]{2,1,0:T(8,128)(2,1)S(1)}, u32[]{:S(2)}, u32[]{:S(2)}) collective-permute-start(bf16[4,32,2048]{2,1,0:T(8,128)(2,1)S(1)} %all_to_all.30.own), channel_id=1, source_target_pairs={{0,1},{1,0},{2,3},{3,2},{4,5},{5,4},{6,7},{7,6},{8,9},{9,8},{10,11... | collective-permute-start | bytes 1572872 | tf_op jit(solution)/shard_map/ppermute | solution.py:293
  30.2 0.8 copy-start.1
  32.8 42.4 %all-to-all-start.2 = ((bf16[64,32,256]{2,1,0:T(8,128)(2,1)}), bf16[64,32,256]{2,1,0:T(8,128)(2,1)S(1)}, u32[]{:S(2)}, u32[]{:S(2)}) async-start(bf16[64,32,256]{2,1,0:T(8,128)(2,1)} %shard_map.157), calls=%async_computation.2 | async-start | bytes 2097152 | tf_op jit(solution)/shard_map/all_to_all | solution.py:251
  75.2 1.0 copy-start
  80.0 15.1 %all-to-all-start.3 = ((bf16[8,136,128]{2,1,0:T(8,128)(2,1)}), bf16[8,136,128]{2,1,0:T(8,128)(2,1)S(1)}, u32[]{:S(2)}, u32[]{:S(2)}) async-start(bf16[8,136,128]{2,1,0:T(8,128)(2,1)} %get-tuple-element.26), calls=%async_computation.3 | async-start | bytes 557056 | tf_op jit(solution)/shard_map/all_to_all | solution.py:251
  95.0 0.7 copy-start.4
  97.5 32.7 %all-to-all-start.4 = ((bf16[8,136,128]{2,1,0:T(8,128)(2,1)}), bf16[8,136,128]{2,1,0:T(8,128)(2,1)S(1)}, u32[]{:S(2)}, u32[]{:S(2)}) async-start(bf16[8,136,128]{2,1,0:T(8,128)(2,1)} %get-tuple-element.27), calls=%async_computation.4 | async-start | bytes 557056 | tf_op jit(solution)/shard_map/all_to_all | solution.py:251
  100.9 6.4 %collective-permute-start.1 = (bf16[32,2048]{1,0:T(8,128)(2,1)}, bf16[32,2048]{1,0:T(8,128)(2,1)S(1)}, u32[]{:S(2)}, u32[]{:S(2)}) collective-permute-start(bf16[32,2048]{1,0:T(8,128)(2,1)} %get-tuple-element.21), channel_id=1, source_target_pairs={{0,8},{8,16},{16,24},{24,32},{32,40},{40,48},{48,56},{56,64},{64,7... | collective-permute-start | bytes 393224 | tf_op jit(solution)/shard_map/ppermute | solution.py:314
  107.4 18.3 %copy-start.5 = (bf16[32,2048]{1,0:T(8,128)(2,1)}, bf16[32,2048]{1,0:T(8,128)(2,1)S(1)}, u32[]{:S(2)}) copy-start(bf16[32,2048]{1,0:T(8,128)(2,1)S(1)} %collective-permute-done.1.halo) | copy-start | bytes 393220
  130.2 7.1 %copy-start.3 = (bf16[8,136,128]{2,1,0:T(8,128)(2,1)}, bf16[8,136,128]{2,1,0:T(8,128)(2,1)S(1)}, u32[]{:S(2)}) copy-start(bf16[8,136,128]{2,1,0:T(8,128)(2,1)S(1)} %all-to-all-done.4.got) | copy-start | bytes 835588
  130.2 11.8 %all-to-all-start.1 = ((f32[8,2,256]{2,1,0:T(2,128)}), f32[8,2,256]{2,1,0:T(2,128)S(1)}, u32[]{:S(2)}, u32[]{:S(2)}) async-start(f32[8,2,256]{2,1,0:T(2,128)} %get-tuple-element.24), calls=%async_computation.1 | async-start | bytes 32768 | tf_op jit(solution)/shard_map/all_to_all | solution.py:251
  142.0 0.6 copy-start.6
Sparse Core Ops, SparseCore 0:
  10.3 115.2 all-gather.1

commit v3 on v2

--- a/solution.py
+++ b/solution.py
@@ -42,10 +42,10 @@
     return [pl.BlockSpec(memory_space=pltpu.VMEM)] * count
 
 
-def first_body(gv, gg, q, g, wr, wc, tokens, operand, copies):
-    operand[...] = jnp.concatenate([w[...] for w in (gv, gg, q, g, wr, wc)], axis=1)
+def first_body(gv, gg, q, g, wr, wc, copies):
+    joined = jnp.concatenate([w[...] for w in (gv, gg, q, g, wr, wc)], axis=1)
     for k in range(copies.shape[0]):
-        copies[k] = tokens[...]
+        copies[k] = joined
 
 
 def second_body(f, v, _, copies):
@@ -54,28 +54,17 @@
         copies[k] = joined
 
 
-def norm_body(core, own, other, gain, out, tail):
-    peers, share, _ = own.shape
-
-    def scaled(rows):
-        values_in = rows.astype(F32)
-        row_scale = lax.rsqrt(jnp.mean(values_in * values_in, axis=1, keepdims=True) + 1e-06)
-        return (values_in * row_scale * gain[...]).astype(BF16)
-
-    def place(even, odd):
-        for k in range(peers):
-            out[2 * k * share : (2 * k + 1) * share] = scaled(even[k])
-            done = scaled(odd[k])
-            out[(2 * k + 1) * share : (2 * k + 2) * share] = done
-        tail[...] = done
-
-    @pl.when(core[0] == 0)
-    def _():
-        place(own, other)
-
-    @pl.when(core[0] != 0)
-    def _():
-        place(other, own)
+def again_body(value, copies):
+    for k in range(copies.shape[0]):
+        copies[k] = value[...]
+
+
+def norm_body(tokens, gain, out, tail):
+    values_in = tokens[...].astype(F32)
+    row_scale = lax.rsqrt(jnp.mean(values_in * values_in, axis=1, keepdims=True) + 1e-06)
+    scaled = (values_in * row_scale * gain[...]).astype(BF16)
+    out[...] = scaled
+    tail[...] = scaled[scaled.shape[0] - HALO :]
 
 
 def pack_state(out, state, total):
@@ -97,7 +86,12 @@
 
 def state_body(normed, weights, leak, shift, sent, value_out, key, totals, starts, befores):
     rows = normed.shape[0]
-    projected = jnp.dot(normed[...], weights[...], preferred_element_type=F32).astype(BF16)
+    peers = weights.shape[0]
+    ordered = jnp.concatenate(
+        [weights[inner, outer] for outer in range(weights.shape[1]) for inner in range(peers)],
+        axis=0,
+    )
+    projected = jnp.dot(normed[...], ordered, preferred_element_type=F32).astype(BF16)
     value = projected[:, HEAD_K:]
     value_out[...] = value
     in_gate = leak[...] * jax.nn.sigmoid(-projected[:, :HEAD_K].astype(F32))
@@ -213,33 +207,30 @@
         stats[k] = both
 
 
-def out_body(stats, conv, head_out, ln_gain, ln_bias, w_rec, w_low, w_high, out, conv_out):
+def out_body(stats, conv, head_out, ln_gain, ln_bias, w_rec, w_low, w_high, out):
     channels = conv.shape[1]
 
-    @pl.when(pl.program_id(0) == 0)
-    def _():
-        both = stats[0]
-        for k in range(1, stats.shape[0]):
-            both = both + stats[k]
-        both = both / (channels * stats.shape[0])
-        mean = both[0:1]
-        inverse = lax.rsqrt(both[1:2] - mean * mean + 1e-05)
-        row = lax.broadcasted_iota(jnp.int32, (8, both.shape[1]), 0)
-        paired = jnp.where(row == 0, mean, jnp.where(row == 1, inverse, 0.0))
-
-        def column(k):
-            chosen = jnp.where(lax.broadcasted_iota(jnp.int32, (8, channels), 0) == k, 1.0, 0.0)
-            return lax.dot_general(
-                paired,
-                chosen.astype(F32),
-                (((0,), (0,)), ((), ())),
-                precision=EXACT,
-                preferred_element_type=F32,
-            )
-
-        normal = (conv[...] - column(0)) * column(1) * ln_gain[...] + ln_bias[...]
-        conv_out[...] = jax.nn.silu(normal).astype(BF16)
-
+    both = stats[0]
+    for k in range(1, stats.shape[0]):
+        both = both + stats[k]
+    both = both / (channels * stats.shape[0])
+    mean = both[0:1]
+    inverse = lax.rsqrt(both[1:2] - mean * mean + 1e-05)
+    row = lax.broadcasted_iota(jnp.int32, (8, both.shape[1]), 0)
+    paired = jnp.where(row == 0, mean, jnp.where(row == 1, inverse, 0.0))
+
+    def column(k):
+        chosen = jnp.where(lax.broadcasted_iota(jnp.int32, (8, channels), 0) == k, 1.0, 0.0)
+        return lax.dot_general(
+            paired,
+            chosen.astype(F32),
+            (((0,), (0,)), ((), ())),
+            precision=EXACT,
+            preferred_element_type=F32,
+        )
+
+    normal = (conv[...] - column(0)) * column(1) * ln_gain[...] + ln_bias[...]
+    conv_out = jax.nn.silu(normal).astype(BF16)
     half = channels // 2
     mixed = dot_nt(head_out[...], w_rec[...])
     mixed = mixed + dot_nt(conv_out[:, :half], w_low[...])
@@ -279,38 +270,30 @@
     columns = (w_glu_value, w_glu_gate, w_query, w_outgate, w_out_rec.T, w_out_conv.T)
     glu_width = 2 * channels
     all_width = sum(w.shape[1] for w in columns)
-    operand, copies = call(
-        first_body,
-        (
-            shape((depth, all_width), BF16),
-            shape((lax.axis_size(TP[0]), share, features), BF16),
-        ),
-        *columns,
-        tokens,
-    )
-    gathered = lax.all_gather(operand, SP, axis=0, tiled=True)
-    own = swap(copies, TP[0])
-    other = lax.ppermute(own, TP[1], [(0, 1), (1, 0)])
+    outer_count = lax.axis_size(SP[0])
+    copies = call(first_body, shape((inner_count, depth, all_width), BF16), *columns)
+    block = lax.all_gather(tokens, TP, axis=0, tiled=True)
+    staged = swap(copies, SP[1]).reshape(inner_count * depth, all_width)
+    gathered = lax.all_gather(staged, SP[0], axis=0, tiled=True)
+    copies = call(
+        second_body,
+        shape((outer_count, depth, 2 * HEAD_K), BF16),
+        w_forget,
+        w_value,
+        staged,
+        in_specs=whole(2) + [ANY],
+    )
+    column = swap(copies, SP[0]).reshape(outer_count * depth, 2 * HEAD_K)
+    copies = call(again_body, shape((inner_count, *column.shape), BF16), column)
+    state_weights = swap(copies, SP[1]).reshape(inner_count, outer_count, depth, 2 * HEAD_K)
     rows = group * share
     normed, tail = call(
         norm_body,
         (shape((rows, features), BF16), shape((share, features), BF16)),
-        lax.axis_index(TP[1]).reshape(1),
-        own,
-        other,
+        block,
         norm_gain.reshape(1, -1),
-        in_specs=[smem] + whole(3),
     )
     count = lax.axis_size(SP)
-    copies = call(
-        second_body,
-        shape((count, depth, 2 * HEAD_K), BF16),
-        w_forget,
-        w_value,
-        other,
-        in_specs=whole(2) + [ANY],
-    )
-    state_weights = swap(copies, SP).reshape(count * depth, 2 * HEAD_K)
     halo = lax.ppermute(tail, SP, [(k, k + 1) for k in range(count - 1)])
     message = shape((inner_count, HEAD_K + 8, HEAD_K), BF16)
     blocks = rows // BLOCK
@@ -385,7 +368,7 @@
         out_specs=full(rows, HEAD_K),
     )
     first = glu_width // HEAD_K + 2
-    step = 512
+    step = features
     mixed = call(
         out_body,
         shape((rows, features), BF16),
@@ -409,7 +392,6 @@
             pl.BlockSpec((step, HEAD_K), lambda k: (k, first + 2)),
         ],
         out_specs=pl.BlockSpec((rows, step), lambda k: (0, k)),
-        scratch=(pltpu.VMEM((rows, channels), BF16),),
     )
     arrived = swap(mixed.reshape(group, share, features), TP)
     return arrived.astype(F32).sum(axis=0).astype(BF16)

time: 175 us -> 169 us (0.966)
  the two profiles are of different devices: /device:TPU:1 before, /device:TPU:64 now
where the time goes in v3:
time: 169 us; the launch traced here: 168 us
  blocking collectives  63.2 us (37%)
  waiting for transfers between devices  43.7 us (26%)
  Pallas kernels  25.4 us (15%)
  starting transfers between devices  18.2 us (11%)
  between operations  13.5 us (8%)
  local copies, waits for them, and re-layouts  2.94 us (2%)
    all_to_all x3, blocking collectives, swap(): return lax.all_to_all(value, axis, split_axis=0, concat_axis=0, tiled=True)  63.2 us
    all_to_all x4, waiting for transfers between devices, swap(): return lax.all_to_all(value, axis, split_axis=0, concat_axis=0, tiled=True)  35.5 us
    pallas_call x9, Pallas kernels, call(): pl.pallas_call(body, out_shape=outs, scratch_shapes=scratch, **specs)(*args)  25.4 us
    all_to_all x4, starting transfers between devices, swap(): return lax.all_to_all(value, axis, split_axis=0, concat_axis=0, tiled=True)  16.1 us
    ppermute x1, waiting for transfers between devices, on_device(): halo = lax.ppermute(tail, SP, [(k, k + 1) for k in range(count - 1)])  7.43 us
  transfers between devices with their start and end apart: 7, of which 4 were waited for; matrix products, arithmetic and copies ran while one was open for 0% of the time, Pallas kernels for 13%

profile of v3, /device:TPU:64, one launch (start us, length us, event | category | flops | bytes accessed | tf_op | source)
XLA Modules:
  0.0 167.8 jit_solution(2595828305937533613)
XLA Ops:
  6.5 0.0 all-gather.3.cloned.1.call-start
  6.5 0.7 all-gather.3.cloned.1.call-update
  7.3 0.0 all-gather.5.cloned.1.call-start
  7.3 1.7 shard_map.155
  9.0 26.1 %all_to_all.35 = bf16[8,32,1152]{2,1,0:T(8,128)(2,1)} all-to-all(bf16[8,32,1152]{2,1,0:T(8,128)(2,1)} %shard_map.155), channel_id=1, replica_groups=mesh['sp_0'=8,'sp_1'=8,'x'=4,'core'=2] {'sp_1'}, dimensions={0} | all-to-all | bytes 1179648 | tf_op jit(solution)/shard_map/all_to_all | solution.py:242
  35.1 0.0 all-gather.5.cloned.1.call-update
  35.1 1.4 shard_map.157
  36.5 17.7 %all_to_all.36 = bf16[8,32,256]{2,1,0:T(8,128)(2,1)} all-to-all(bf16[8,32,256]{2,1,0:T(8,128)(2,1)} %shard_map.157), channel_id=1, replica_groups=mesh['sp_0'=8,'sp_1'=8,'x'=4,'core'=2] {'sp_0'}, dimensions={0} | all-to-all | bytes 262144 | tf_op jit(solution)/shard_map/all_to_all | solution.py:242
  54.2 1.9 %shard_map.158 = bf16[8,256,256]{2,1,0:T(8,128)(2,1)} custom-call(bf16[256,256]{1,0:T(8,128)(2,1)} %bitcast.17), custom_call_target="tpu_custom_call" | custom-call | tf_op jit(solution)/shard_map/pallas_call | solution.py:38
  56.1 3.6 %all-to-all-start.3 = ((bf16[8,256,256]{2,1,0:T(8,128)(2,1)}), bf16[8,256,256]{2,1,0:T(8,128)(2,1)S(1)}, u32[]{:S(2)}, u32[]{:S(2)}) async-start(bf16[8,256,256]{2,1,0:T(8,128)(2,1)} %shard_map.158), calls=%async_computation.3 | async-start | bytes 2097152 | tf_op jit(solution)/shard_map/all_to_all | solution.py:242
  59.7 0.0 all-gather.3.cloned.1.call-done.tokens
  59.7 2.6 %shard_map.154 = (bf16[256,2048]{1,0:T(8,128)(2,1)}, bf16[32,2048]{1,0:T(8,128)(2,1)}) custom-call(bf16[256,2048]{1,0:T(8,128)(2,1)} %all-gather.3.cloned.1.call-done.tokens, f32[1,2048]{1,0:T(1,128)} %bitcast.19), custom_call_target="tpu_custom_call" | custom-call | tf_op jit(solution)/shard_map/pallas_call | solution.py:38
  62.4 23.2 %all-to-all-done.3 = bf16[8,256,256]{2,1,0:T(8,128)(2,1)S(1)} async-done(((bf16[8,256,256]{2,1,0:T(8,128)(2,1)}), bf16[8,256,256]{2,1,0:T(8,128)(2,1)S(1)}, u32[]{:S(2)}, u32[]{:S(2)}) %all-to-all-start.3) | async-done | bytes 1048608 | tf_op jit(solution)/shard_map/all_to_all | solution.py:242
  85.6 0.0 copy-start
  85.6 1.0 copy-done
  86.6 3.8 %shard_map.159 = (bf16[8,136,128]{2,1,0:T(8,128)(2,1)}, bf16[256,128]{1,0:T(8,128)(2,1)}, bf16[256,128]{1,0:T(8,128)(2,1)}, f32[256,128]{1,0:T(8,128)}, bf16[4,128,128]{2,1,0:T(8,128)(2,1)}, /*index=5*/f32[4,128]{1,0:T(4,128)}) custom-call(bf16[256,2048]{1,0:T(8,128)(2,1)} %get-tuple-element.19.normed, bf16[8,8,32,256]{3,2,1,0:T(8,128)(2,1)} %bitcast.16, ...), custom_call_target="tpu_custom_call" | custom-call | tf_op jit(solution)/shard_map/pallas_call | solution.py:38
  90.3 3.4 %all-to-all-start.4 = ((bf16[8,136,128]{2,1,0:T(8,128)(2,1)}), bf16[8,136,128]{2,1,0:T(8,128)(2,1)S(1)}, u32[]{:S(2)}, u32[]{:S(2)}) async-start(bf16[8,136,128]{2,1,0:T(8,128)(2,1)} %get-tuple-element.22), calls=%async_computation.4 | async-start | bytes 557056 | tf_op jit(solution)/shard_map/all_to_all | solution.py:242
  93.8 10.6 %all-to-all-done.4.got = bf16[8,136,128]{2,1,0:T(8,128)(2,1)S(1)} async-done(((bf16[8,136,128]{2,1,0:T(8,128)(2,1)}), bf16[8,136,128]{2,1,0:T(8,128)(2,1)S(1)}, u32[]{:S(2)}, u32[]{:S(2)}) %all-to-all-start.4) | async-done | bytes 278560 | tf_op jit(solution)/shard_map/all_to_all | solution.py:242
  104.3 0.0 copy-start.2
  104.3 0.7 copy-done.2
  105.0 1.8 %shard_map.160 = (bf16[8,136,128]{2,1,0:T(8,128)(2,1)}, f32[128,128]{1,0:T(8,128)}, f32[8,128]{1,0:T(8,128)}) custom-call(s32[1]{0:T(128)} %bitcast.5.position, bf16[8,136,128]{2,1,0:T(8,128)(2,1)} %copy-done.2), custom_call_target="tpu_custom_call" | custom-call | tf_op jit(solution)/shard_map/pallas_call | solution.py:38
  106.8 4.8 %all-to-all-start.5 = ((bf16[8,136,128]{2,1,0:T(8,128)(2,1)}), bf16[8,136,128]{2,1,0:T(8,128)(2,1)S(1)}, u32[]{:S(2)}, u32[]{:S(2)}) async-start(bf16[8,136,128]{2,1,0:T(8,128)(2,1)} %get-tuple-element.23), calls=%async_computation.5 | async-start | bytes 557056 | tf_op jit(solution)/shard_map/all_to_all | solution.py:242
  111.6 2.1 %collective-permute-start = (bf16[32,2048]{1,0:T(8,128)(2,1)}, bf16[32,2048]{1,0:T(8,128)(2,1)S(1)}, u32[]{:S(2)}, u32[]{:S(2)}) collective-permute-start(bf16[32,2048]{1,0:T(8,128)(2,1)} %get-tuple-element.18), channel_id=1, source_target_pairs={{0,8},{8,16},{16,24},{24,32},{32,40},{40,48},{48,56},{56,64},{64,7... | collective-permute-start | bytes 393224 | tf_op jit(solution)/shard_map/ppermute | solution.py:297
  113.7 7.4 %collective-permute-done.halo = bf16[32,2048]{1,0:T(8,128)(2,1)S(1)} collective-permute-done((bf16[32,2048]{1,0:T(8,128)(2,1)}, bf16[32,2048]{1,0:T(8,128)(2,1)S(1)}, u32[]{:S(2)}, u32[]{:S(2)}) %collective-permute-start) | collective-permute-done | bytes 131104 | tf_op jit(solution)/shard_map/ppermute | solution.py:297
  121.1 0.0 copy-start.3
  121.1 0.0 all-gather.5.cloned.1.call-done.weights.w_rec.w_low.w_high
  121.1 0.7 copy-done.3
  121.8 4.6 %shard_map.156 = (f32[256,256]{1,0:T(8,128)}, f32[8,2,256]{2,1,0:T(2,128)}) custom-call(bf16[32,2048]{1,0:T(8,128)(2,1)} %copy-done.3, bf16[256,2048]{1,0:T(8,128)(2,1)} %get-tuple-element.19.normed, bf16[2048,1152]{1,0:T(8,128)(2,1)} %all-gather.5.cloned.1.call-done.weights.w_rec.w_low.w_high, f32[31,256]{1,0:T(8,128)} %taps.1), custom_call_target="tpu_custom_call" | custom-call | tf_op jit(solution)/shard_map/pallas_call | solution.py:38
  126.3 0.0 all-to-all-done.5.got
  126.3 0.0 copy-start.1
  126.3 4.3 %all-to-all-start.1 = ((f32[8,2,256]{2,1,0:T(2,128)}), f32[8,2,256]{2,1,0:T(2,128)S(1)}, u32[]{:S(2)}, u32[]{:S(2)}) async-start(f32[8,2,256]{2,1,0:T(2,128)} %get-tuple-element.20), calls=%async_computation.1 | async-start | bytes 32768 | tf_op jit(solution)/shard_map/all_to_all | solution.py:242
  130.7 0.0 copy-done.1
  130.7 3.6 %shard_map.161.head_out = bf16[256,128]{1,0:T(8,128)(2,1)} custom-call(s32[1]{0:T(128)} %bitcast.4.position, bf16[8,136,128]{2,1,0:T(8,128)(2,1)} %copy-done.1, f32[128,128]{1,0:T(8,128)} %get-tuple-element.24.inner_state, f32[8,128]{1,0:T(8,128)} %get-tuple-element.25.inner_total, bf16[256,2048]{1,0:T(8,128)(2,1)} %get-tuple-element.19.normed, ...), custom_call_target="tpu_custom_call" | custom-call | tf_op jit(solution)/shard_map/pallas_call | solution.py:38
  134.3 1.7 %all-to-all-done.1.stats = f32[8,2,256]{2,1,0:T(2,128)S(1)} async-done(((f32[8,2,256]{2,1,0:T(2,128)}), f32[8,2,256]{2,1,0:T(2,128)S(1)}, u32[]{:S(2)}, u32[]{:S(2)}) %all-to-all-start.1) | async-done | bytes 16416 | tf_op jit(solution)/shard_map/all_to_all | solution.py:242
  136.0 0.0 copy-start.4
  136.0 0.6 copy-done.4
  136.6 4.1 %shard_map.162 = bf16[256,2048]{1,0:T(8,128)(2,1)} custom-call(f32[8,2,256]{2,1,0:T(2,128)} %copy-done.4, f32[256,256]{1,0:T(8,128)} %get-tuple-element.21.conv, bf16[256,128]{1,0:T(8,128)(2,1)} %shard_map.161.head_out, f32[1,256]{1,0:T(1,128)} %bitcast.21, f32[1,256]{1,0:T(1,128)} %bitcast.22, ...), custom_call_target="tpu_custom_call" | custom-call | tf_op jit(solution)/shard_map/pallas_call | solution.py:38
  140.7 19.4 %all_to_all.37 = bf16[8,32,2048]{2,1,0:T(8,128)(2,1)S(1)} all-to-all(bf16[8,32,2048]{2,1,0:T(8,128)(2,1)} %bitcast.15), channel_id=1, replica_groups=mesh['sp_0'=8,'sp_1'=8,'x'=4,'core'=2] {'x','core'}, dimensions={0} | all-to-all | bytes 2097152 | tf_op jit(solution)/shard_map/all_to_all | solution.py:242
  160.1 0.8 reduce_sum.12
Async XLA Ops:
  6.5 53.2 %all-gather.3.cloned.1.call-start = ((), (), s32[]{:S(2)}) async-start(), calls=%async_computation.7 | async-start | bytes 1179648 | tf_op jit(solution)/shard_map/all_gather | solution.py:275
  7.3 113.9 %all-gather.5.cloned.1.call-start = ((), (), s32[]{:S(2)}) async-start(), calls=%async_computation.8 | async-start | bytes 5308416 | tf_op jit(solution)/shard_map/all_gather | solution.py:277
  56.1 29.5 %all-to-all-start.3 = ((bf16[8,256,256]{2,1,0:T(8,128)(2,1)}), bf16[8,256,256]{2,1,0:T(8,128)(2,1)S(1)}, u32[]{:S(2)}, u32[]{:S(2)}) async-start(bf16[8,256,256]{2,1,0:T(8,128)(2,1)} %shard_map.158), calls=%async_computation.3 | async-start | bytes 2097152 | tf_op jit(solution)/shard_map/all_to_all | solution.py:242
  85.6 1.0 copy-start
  90.3 14.0 %all-to-all-start.4 = ((bf16[8,136,128]{2,1,0:T(8,128)(2,1)}), bf16[8,136,128]{2,1,0:T(8,128)(2,1)S(1)}, u32[]{:S(2)}, u32[]{:S(2)}) async-start(bf16[8,136,128]{2,1,0:T(8,128)(2,1)} %get-tuple-element.22), calls=%async_computation.4 | async-start | bytes 557056 | tf_op jit(solution)/shard_map/all_to_all | solution.py:242
  104.3 0.7 copy-start.2
  106.8 19.5 %all-to-all-start.5 = ((bf16[8,136,128]{2,1,0:T(8,128)(2,1)}), bf16[8,136,128]{2,1,0:T(8,128)(2,1)S(1)}, u32[]{:S(2)}, u32[]{:S(2)}) async-start(bf16[8,136,128]{2,1,0:T(8,128)(2,1)} %get-tuple-element.23), calls=%async_computation.5 | async-start | bytes 557056 | tf_op jit(solution)/shard_map/all_to_all | solution.py:242
  111.6 9.5 %collective-permute-start = (bf16[32,2048]{1,0:T(8,128)(2,1)}, bf16[32,2048]{1,0:T(8,128)(2,1)S(1)}, u32[]{:S(2)}, u32[]{:S(2)}) collective-permute-start(bf16[32,2048]{1,0:T(8,128)(2,1)} %get-tuple-element.18), channel_id=1, source_target_pairs={{0,8},{8,16},{16,24},{24,32},{32,40},{40,48},{48,56},{56,64},{64,7... | collective-permute-start | bytes 393224 | tf_op jit(solution)/shard_map/ppermute | solution.py:297
  121.1 0.7 copy-start.3
  126.3 4.3 %copy-start.1 = (bf16[8,136,128]{2,1,0:T(8,128)(2,1)}, bf16[8,136,128]{2,1,0:T(8,128)(2,1)S(1)}, u32[]{:S(2)}) copy-start(bf16[8,136,128]{2,1,0:T(8,128)(2,1)S(1)} %all-to-all-done.5.got) | copy-start | bytes 835588
  126.3 9.7 %all-to-all-start.1 = ((f32[8,2,256]{2,1,0:T(2,128)}), f32[8,2,256]{2,1,0:T(2,128)S(1)}, u32[]{:S(2)}, u32[]{:S(2)}) async-start(f32[8,2,256]{2,1,0:T(2,128)} %get-tuple-element.20), calls=%async_computation.1 | async-start | bytes 32768 | tf_op jit(solution)/shard_map/all_to_all | solution.py:242
  136.0 0.6 copy-start.4
Sparse Core Ops, SparseCore 0:
  9.5 32.4 all-gather.2
  44.1 60.6 all-gather.4

commit v4 on v3

--- a/solution.py
+++ b/solution.py
@@ -42,19 +42,19 @@
     return [pl.BlockSpec(memory_space=pltpu.VMEM)] * count
 
 
-def first_body(gv, gg, q, g, wr, wc, copies):
+def first_body(f, v, copies):
+    joined = jnp.concatenate([f[...], v[...]], axis=1)
+    for k in range(copies.shape[0]):
+        copies[k] = joined
+
+
+def second_body(gv, gg, q, g, wr, wc, _, copies):
     joined = jnp.concatenate([w[...] for w in (gv, gg, q, g, wr, wc)], axis=1)
     for k in range(copies.shape[0]):
         copies[k] = joined
 
 
-def second_body(f, v, _, copies):
-    joined = jnp.concatenate([f[...], v[...]], axis=1)
-    for k in range(copies.shape[0]):
-        copies[k] = joined
-
-
-def again_body(value, copies):
+def again_body(value, _, copies):
     for k in range(copies.shape[0]):
         copies[k] = value[...]
 
@@ -207,9 +207,9 @@
         stats[k] = both
 
 
-def out_body(stats, conv, head_out, ln_gain, ln_bias, w_rec, w_low, w_high, out):
+def out_body(core, stats, conv, head_out, ln_gain, ln_bias, w_rec, w_low, w_high, rows_out, out):
     channels = conv.shape[1]
-
+    share = conv.shape[0] // stats.shape[0]
     both = stats[0]
     for k in range(1, stats.shape[0]):
         both = both + stats[k]
@@ -231,11 +231,23 @@
 
     normal = (conv[...] - column(0)) * column(1) * ln_gain[...] + ln_bias[...]
     conv_out = jax.nn.silu(normal).astype(BF16)
-    half = channels // 2
-    mixed = dot_nt(head_out[...], w_rec[...])
-    mixed = mixed + dot_nt(conv_out[:, :half], w_low[...])
-    mixed = mixed + dot_nt(conv_out[:, half:], w_high[...])
-    out[...] = mixed.astype(BF16)
+    for k in range(stats.shape[0]):
+        piece = slice(k * share, (k + 1) * share)
+        at = slice(k // 2 * share, (k // 2 + 1) * share)
+        rows_out[k % 2, at, :HEAD_K] = head_out[piece]
+        rows_out[k % 2, at, HEAD_K:] = conv_out[piece]
+    out[...] = product(rows_out[1 - core[0]], w_rec, w_low, w_high)
+
+
+def product(rows, w_rec, w_low, w_high):
+    mixed = dot_nt(rows[:, :HEAD_K], w_rec[...])
+    mixed = mixed + dot_nt(rows[:, HEAD_K : 2 * HEAD_K], w_low[...])
+    mixed = mixed + dot_nt(rows[:, 2 * HEAD_K :], w_high[...])
+    return mixed.astype(BF16)
+
+
+def own_body(core, rows, w_rec, w_low, w_high, out):
+    out[...] = product(rows[core[0]], w_rec, w_low, w_high)
 
 
 def swap(value, axis):
@@ -271,20 +283,27 @@
     glu_width = 2 * channels
     all_width = sum(w.shape[1] for w in columns)
     outer_count = lax.axis_size(SP[0])
-    copies = call(first_body, shape((inner_count, depth, all_width), BF16), *columns)
+    copies = call(
+        first_body, shape((outer_count, depth, 2 * HEAD_K), BF16), w_forget, w_value
+    )
     block = lax.all_gather(tokens, TP, axis=0, tiled=True)
+    column = swap(copies, SP[0]).reshape(outer_count * depth, 2 * HEAD_K)
+    copies = call(
+        second_body,
+        shape((inner_count, depth, all_width), BF16),
+        *columns,
+        column,
+        in_specs=whole(len(columns)) + [ANY],
+    )
     staged = swap(copies, SP[1]).reshape(inner_count * depth, all_width)
     gathered = lax.all_gather(staged, SP[0], axis=0, tiled=True)
     copies = call(
-        second_body,
-        shape((outer_count, depth, 2 * HEAD_K), BF16),
-        w_forget,
-        w_value,
+        again_body,
+        shape((inner_count, *column.shape), BF16),
+        column,
         staged,
-        in_specs=whole(2) + [ANY],
-    )
-    column = swap(copies, SP[0]).reshape(outer_count * depth, 2 * HEAD_K)
-    copies = call(again_body, shape((inner_count, *column.shape), BF16), column)
+        in_specs=whole(1) + [ANY],
+    )
     state_weights = swap(copies, SP[1]).reshape(inner_count, outer_count, depth, 2 * HEAD_K)
     rows = group * share
     normed, tail = call(
@@ -368,32 +387,46 @@
         out_specs=full(rows, HEAD_K),
     )
     first = glu_width // HEAD_K + 2
-    step = features
-    mixed = call(
+    half = rows // 2
+    width = HEAD_K + channels
+    core = lax.axis_index(TP[1]).reshape(1)
+    weights = [gathered] * 3
+    weight_specs = [part(HEAD_K, first + k) for k in range(3)]
+    mixed_rows, sent = call(
         out_body,
-        shape((rows, features), BF16),
+        (shape((2, half, width), BF16), shape((half, features), BF16)),
+        core,
         stats,
         conv,
         head_out,
         ln_gain.reshape(1, -1),
         ln_bias.reshape(1, -1),
-        gathered,
-        gathered,
-        gathered,
-        grid=(features // step,),
+        *weights,
+        grid=(1,),
         in_specs=[
+            smem,
             full(*stats.shape),
             full(rows, channels),
             full(rows, HEAD_K),
             full(1, channels),
             full(1, channels),
-            pl.BlockSpec((step, HEAD_K), lambda k: (k, first)),
-            pl.BlockSpec((step, HEAD_K), lambda k: (k, first + 1)),
-            pl.BlockSpec((step, HEAD_K), lambda k: (k, first + 2)),
+            *weight_specs,
         ],
-        out_specs=pl.BlockSpec((rows, step), lambda k: (0, k)),
-    )
-    arrived = swap(mixed.reshape(group, share, features), TP)
+        out_specs=(full(2, half, width), full(half, features)),
+    )
+    received = lax.ppermute(sent, TP[1], [(0, 1), (1, 0)])
+    own = call(
+        own_body,
+        shape((half, features), BF16),
+        core,
+        mixed_rows,
+        *weights,
+        grid=(1,),
+        in_specs=[smem, full(2, half, width), *weight_specs],
+        out_specs=full(half, features),
+    )
+    pair = (own.astype(F32) + received.astype(F32)).astype(BF16)
+    arrived = swap(pair.reshape(group // 2, share, features), TP[0])
     return arrived.astype(F32).sum(axis=0).astype(BF16)
 
 

time: 169 us -> 166 us (0.982)
  blocking collectives: 63.2 us -> 55.4 us
  starting transfers between devices: 18.2 us -> 20.6 us
  Pallas kernels: 25.4 us -> 27.7 us
    all_to_all x3, blocking collectives: 63.2 us -> 55.4 us  [swap(): return lax.all_to_all(value, axis, split_axis=0, concat_axis=0, tiled=True)]
    pallas_call x9 -> x10, Pallas kernels: 25.4 us -> 27.7 us  [call(): pl.pallas_call(body, out_shape=outs, scratch_shapes=scratch, **specs)(*args)]
    ppermute x0 -> x1, starting transfers between devices: none -> 1.91 us  [on_device(): received = lax.ppermute(sent, TP[1], [(0, 1), (1, 0)])]
  transfers between devices with their start and end apart: 7 -> 8, of which waited for: 4 -> 4; matrix products, arithmetic and copies ran while one was open for 0% -> 0% of each run, Pallas kernels for 13% -> 15%
where the time goes in v4:
time: 166 us; the launch traced here: 165 us
  blocking collectives  55.4 us (33%)
  waiting for transfers between devices  43 us (26%)
  Pallas kernels  27.7 us (17%)
  starting transfers between devices  20.6 us (12%)
  between operations  13.5 us (8%)
  local copies, waits for them, and re-layouts  2.94 us (2%)
  other arithmetic  1.91 us (1%)
    all_to_all x3, blocking collectives, swap(): return lax.all_to_all(value, axis, split_axis=0, concat_axis=0, tiled=True)  55.4 us
    all_to_all x4, waiting for transfers between devices, swap(): return lax.all_to_all(value, axis, split_axis=0, concat_axis=0, tiled=True)  35.2 us
    pallas_call x10, Pallas kernels, call(): pl.pallas_call(body, out_shape=outs, scratch_shapes=scratch, **specs)(*args)  27.7 us
    all_to_all x4, starting transfers between devices, swap(): return lax.all_to_all(value, axis, split_axis=0, concat_axis=0, tiled=True)  16.2 us
    ppermute x1, waiting for transfers between devices, on_device(): halo = lax.ppermute(tail, SP, [(k, k + 1) for k in range(count - 1)])  7.07 us
  transfers between devices with their start and end apart: 8, of which 4 were waited for; matrix products, arithmetic and copies ran while one was open for 0% of the time, Pallas kernels for 15%

profile of v4, /device:TPU:64, one launch (start us, length us, event | category | flops | bytes accessed | tf_op | source)
XLA Modules:
  0.0 164.9 jit_solution(6571892405603465094)
XLA Ops:
  6.5 0.0 all-gather.3.cloned.1.call-start
  6.5 0.7 all-gather.3.cloned.1.call-update
  7.3 0.0 all-gather.5.cloned.1.call-start
  7.3 1.4 shard_map.155
  8.7 17.5 %all_to_all.35 = bf16[8,32,256]{2,1,0:T(8,128)(2,1)} all-to-all(bf16[8,32,256]{2,1,0:T(8,128)(2,1)} %shard_map.155), channel_id=1, replica_groups=mesh['sp_0'=8,'sp_1'=8,'x'=4,'core'=2] {'sp_0'}, dimensions={0} | all-to-all | bytes 262144 | tf_op jit(solution)/shard_map/all_to_all | solution.py:254
  26.2 1.7 %shard_map.156 = bf16[8,32,1152]{2,1,0:T(8,128)(2,1)} custom-call(bf16[32,256]{1,0:T(8,128)(2,1)} %gv.1, bf16[32,256]{1,0:T(8,128)(2,1)} %gg.1, bf16[32,128]{1,0:T(8,128)(2,1)} %q.1, bf16[32,128]{1,0:T(8,128)(2,1)} %g.1, bf16[32,128]{1,0:T(8,128)(2,1)} %bitcast.21, bf16[32,256]{1,0:T(8,128)(2,1)} %bitcast.20, bf16[256,256]{1,0:T(8,128)(2,1)} %bitcast.18), custom_call_target="tpu_custom_call" | custom-call | tf_op jit(solution)/shard_map/pallas_call | solution.py:38
  27.9 24.8 %all_to_all.36 = bf16[8,32,1152]{2,1,0:T(8,128)(2,1)} all-to-all(bf16[8,32,1152]{2,1,0:T(8,128)(2,1)} %shard_map.156), channel_id=1, replica_groups=mesh['sp_0'=8,'sp_1'=8,'x'=4,'core'=2] {'sp_1'}, dimensions={0} | all-to-all | bytes 1179648 | tf_op jit(solution)/shard_map/all_to_all | solution.py:254
  52.7 0.0 all-gather.5.cloned.1.call-update
  52.7 1.9 %shard_map.158 = bf16[8,256,256]{2,1,0:T(8,128)(2,1)} custom-call(bf16[256,256]{1,0:T(8,128)(2,1)} %bitcast.19, bf16[256,1152]{1,0:T(8,128)(2,1)} %bitcast.15), custom_call_target="tpu_custom_call" | custom-call | tf_op jit(solution)/shard_map/pallas_call | solution.py:38
  54.7 3.6 %all-to-all-start.3 = ((bf16[8,256,256]{2,1,0:T(8,128)(2,1)}), bf16[8,256,256]{2,1,0:T(8,128)(2,1)S(1)}, u32[]{:S(2)}, u32[]{:S(2)}) async-start(bf16[8,256,256]{2,1,0:T(8,128)(2,1)} %shard_map.158), calls=%async_computation.3 | async-start | bytes 2097152 | tf_op jit(solution)/shard_map/all_to_all | solution.py:254
  58.2 0.0 all-gather.3.cloned.1.call-done.tokens
  58.3 2.6 %shard_map.154 = (bf16[256,2048]{1,0:T(8,128)(2,1)}, bf16[32,2048]{1,0:T(8,128)(2,1)}) custom-call(bf16[256,2048]{1,0:T(8,128)(2,1)} %all-gather.3.cloned.1.call-done.tokens, f32[1,2048]{1,0:T(1,128)} %bitcast.22), custom_call_target="tpu_custom_call" | custom-call | tf_op jit(solution)/shard_map/pallas_call | solution.py:38
  60.9 22.9 %all-to-all-done.3 = bf16[8,256,256]{2,1,0:T(8,128)(2,1)S(1)} async-done(((bf16[8,256,256]{2,1,0:T(8,128)(2,1)}), bf16[8,256,256]{2,1,0:T(8,128)(2,1)S(1)}, u32[]{:S(2)}, u32[]{:S(2)}) %all-to-all-start.3) | async-done | bytes 1048608 | tf_op jit(solution)/shard_map/all_to_all | solution.py:254
  83.8 0.0 copy-start
  83.8 1.0 copy-done
  84.8 3.8 %shard_map.159 = (bf16[8,136,128]{2,1,0:T(8,128)(2,1)}, bf16[256,128]{1,0:T(8,128)(2,1)}, bf16[256,128]{1,0:T(8,128)(2,1)}, f32[256,128]{1,0:T(8,128)}, bf16[4,128,128]{2,1,0:T(8,128)(2,1)}, /*index=5*/f32[4,128]{1,0:T(4,128)}) custom-call(bf16[256,2048]{1,0:T(8,128)(2,1)} %get-tuple-element.21.normed, bf16[8,8,32,256]{3,2,1,0:T(8,128)(2,1)} %bitcast.16, ...), custom_call_target="tpu_custom_call" | custom-call | tf_op jit(solution)/shard_map/pallas_call | solution.py:38
  88.5 3.4 %all-to-all-start.4 = ((bf16[8,136,128]{2,1,0:T(8,128)(2,1)}), bf16[8,136,128]{2,1,0:T(8,128)(2,1)S(1)}, u32[]{:S(2)}, u32[]{:S(2)}) async-start(bf16[8,136,128]{2,1,0:T(8,128)(2,1)} %get-tuple-element.24), calls=%async_computation.4 | async-start | bytes 557056 | tf_op jit(solution)/shard_map/all_to_all | solution.py:254
  91.9 10.6 %all-to-all-done.4.got = bf16[8,136,128]{2,1,0:T(8,128)(2,1)S(1)} async-done(((bf16[8,136,128]{2,1,0:T(8,128)(2,1)}), bf16[8,136,128]{2,1,0:T(8,128)(2,1)S(1)}, u32[]{:S(2)}, u32[]{:S(2)}) %all-to-all-start.4) | async-done | bytes 278560 | tf_op jit(solution)/shard_map/all_to_all | solution.py:254
  102.5 0.0 copy-start.2
  102.5 0.7 copy-done.2
  103.2 1.8 %shard_map.160 = (bf16[8,136,128]{2,1,0:T(8,128)(2,1)}, f32[128,128]{1,0:T(8,128)}, f32[8,128]{1,0:T(8,128)}) custom-call(s32[1]{0:T(128)} %bitcast.7.position, bf16[8,136,128]{2,1,0:T(8,128)(2,1)} %copy-done.2), custom_call_target="tpu_custom_call" | custom-call | tf_op jit(solution)/shard_map/pallas_call | solution.py:38
  105.0 4.9 %all-to-all-start.5 = ((bf16[8,136,128]{2,1,0:T(8,128)(2,1)}), bf16[8,136,128]{2,1,0:T(8,128)(2,1)S(1)}, u32[]{:S(2)}, u32[]{:S(2)}) async-start(bf16[8,136,128]{2,1,0:T(8,128)(2,1)} %get-tuple-element.25), calls=%async_computation.5 | async-start | bytes 557056 | tf_op jit(solution)/shard_map/all_to_all | solution.py:254
  109.9 2.5 %collective-permute-start = (bf16[32,2048]{1,0:T(8,128)(2,1)}, bf16[32,2048]{1,0:T(8,128)(2,1)S(1)}, u32[]{:S(2)}, u32[]{:S(2)}) collective-permute-start(bf16[32,2048]{1,0:T(8,128)(2,1)} %get-tuple-element.20), channel_id=1, source_target_pairs={{0,8},{8,16},{16,24},{24,32},{32,40},{40,48},{48,56},{56,64},{64,7... | collective-permute-start | bytes 393224 | tf_op jit(solution)/shard_map/ppermute | solution.py:316
  112.3 7.1 %collective-permute-done.halo = bf16[32,2048]{1,0:T(8,128)(2,1)S(1)} collective-permute-done((bf16[32,2048]{1,0:T(8,128)(2,1)}, bf16[32,2048]{1,0:T(8,128)(2,1)S(1)}, u32[]{:S(2)}, u32[]{:S(2)}) %collective-permute-start) | collective-permute-done | bytes 131104 | tf_op jit(solution)/shard_map/ppermute | solution.py:316
  119.4 0.0 copy-start.3
  119.4 0.0 all-gather.5.cloned.1.call-done.weights.w_rec.w_low.w_high
  119.4 0.7 copy-done.3
  120.1 4.6 %shard_map.157 = (f32[256,256]{1,0:T(8,128)}, f32[8,2,256]{2,1,0:T(2,128)}) custom-call(bf16[32,2048]{1,0:T(8,128)(2,1)} %copy-done.3, bf16[256,2048]{1,0:T(8,128)(2,1)} %get-tuple-element.21.normed, bf16[2048,1152]{1,0:T(8,128)(2,1)} %all-gather.5.cloned.1.call-done.weights.w_rec.w_low.w_high, f32[31,256]{1,0:T(8,128)} %taps.1), custom_call_target="tpu_custom_call" | custom-call | tf_op jit(solution)/shard_map/pallas_call | solution.py:38
  124.6 0.0 all-to-all-done.5.got
  124.6 0.0 copy-start.1
  124.6 4.3 %all-to-all-start.2 = ((f32[8,2,256]{2,1,0:T(2,128)}), f32[8,2,256]{2,1,0:T(2,128)S(1)}, u32[]{:S(2)}, u32[]{:S(2)}) async-start(f32[8,2,256]{2,1,0:T(2,128)} %get-tuple-element.22), calls=%async_computation.2 | async-start | bytes 32768 | tf_op jit(solution)/shard_map/all_to_all | solution.py:254
  128.9 0.0 copy-done.1
  128.9 3.6 %shard_map.161.head_out = bf16[256,128]{1,0:T(8,128)(2,1)} custom-call(s32[1]{0:T(128)} %bitcast.6.position, bf16[8,136,128]{2,1,0:T(8,128)(2,1)} %copy-done.1, f32[128,128]{1,0:T(8,128)} %get-tuple-element.26.inner_state, f32[8,128]{1,0:T(8,128)} %get-tuple-element.27.inner_total, bf16[256,2048]{1,0:T(8,128)(2,1)} %get-tuple-element.21.normed, ...), custom_call_target="tpu_custom_call" | custom-call | tf_op jit(solution)/shard_map/pallas_call | solution.py:38
  132.5 1.7 %all-to-all-done.2.stats = f32[8,2,256]{2,1,0:T(2,128)S(1)} async-done(((f32[8,2,256]{2,1,0:T(2,128)}), f32[8,2,256]{2,1,0:T(2,128)S(1)}, u32[]{:S(2)}, u32[]{:S(2)}) %all-to-all-start.2) | async-done | bytes 16416 | tf_op jit(solution)/shard_map/all_to_all | solution.py:254
  134.3 0.0 copy-start.4
  134.3 0.6 copy-done.4
  134.9 3.5 %shard_map.162 = (bf16[2,128,384]{2,1,0:T(8,128)(2,1)}, bf16[128,2048]{1,0:T(8,128)(2,1)}) custom-call(s32[1]{0:T(128)} %bitcast.core, f32[8,2,256]{2,1,0:T(2,128)} %copy-done.4, f32[256,256]{1,0:T(8,128)} %get-tuple-element.23.conv, bf16[256,128]{1,0:T(8,128)(2,1)} %shard_map.161.head_out, f32[1,256]{1,0:T(1,128)} %bitcast.23, f32[1,256]{1,0:T(1,128)} %bitcast.24, ...), custom_call_target="tpu_custom_call" | custom-call | tf_op jit(solution)/shard_map/pallas_call | solution.py:38
  138.4 1.9 %collective-permute-start.1 = (bf16[128,2048]{1,0:T(8,128)(2,1)}, bf16[128,2048]{1,0:T(8,128)(2,1)S(1)}, u32[]{:S(2)}, u32[]{:S(2)}) collective-permute-start(bf16[128,2048]{1,0:T(8,128)(2,1)} %get-tuple-element.34), channel_id=1, source_target_pairs={{0,1},{1,0},{2,3},{3,2},{4,5},{5,4},{6,7},{7,6},{8,9},{9,8},{10,11... | collective-permute-start | bytes 1572872 | tf_op jit(solution)/shard_map/ppermute | solution.py:417
  140.3 2.8 %shard_map.163 = bf16[128,2048]{1,0:T(8,128)(2,1)} custom-call(s32[1]{0:T(128)} %bitcast.core, bf16[2,128,384]{2,1,0:T(8,128)(2,1)} %get-tuple-element.33.rows, bf16[2048,1152]{1,0:T(8,128)(2,1)} %all-gather.5.cloned.1.call-done.weights.w_rec.w_low.w_high, bf16[2048,1152]{1,0:T(8,128)(2,1)} %all-gather.5.cloned.1.call-done.weights.w_rec.w_low.w_high, ...), custom_call_target="tpu_custom_call" | custom-call | tf_op jit(solution)/shard_map/pallas_call | solution.py:38
  143.1 0.0 collective-permute-done.1
  143.1 1.2 add_convert_fusion
  144.3 13.0 %all_to_all.37 = bf16[4,32,2048]{2,1,0:T(8,128)(2,1)S(1)} all-to-all(bf16[4,32,2048]{2,1,0:T(8,128)(2,1)S(1)} %bitcast.17), channel_id=1, replica_groups=mesh['sp_0'=8,'sp_1'=8,'x'=4,'core'=2] {'x'}, dimensions={0} | all-to-all | bytes 1048576 | tf_op jit(solution)/shard_map/all_to_all | solution.py:254
  157.3 0.7 reduce_sum.12
Async XLA Ops:
  6.5 51.7 %all-gather.3.cloned.1.call-start = ((), (), s32[]{:S(2)}) async-start(), calls=%async_computation.7 | async-start | bytes 1179648 | tf_op jit(solution)/shard_map/all_gather | solution.py:289
  7.3 112.1 %all-gather.5.cloned.1.call-start = ((), (), s32[]{:S(2)}) async-start(), calls=%async_computation.8 | async-start | bytes 5308416 | tf_op jit(solution)/shard_map/all_gather | solution.py:299
  54.7 29.1 %all-to-all-start.3 = ((bf16[8,256,256]{2,1,0:T(8,128)(2,1)}), bf16[8,256,256]{2,1,0:T(8,128)(2,1)S(1)}, u32[]{:S(2)}, u32[]{:S(2)}) async-start(bf16[8,256,256]{2,1,0:T(8,128)(2,1)} %shard_map.158), calls=%async_computation.3 | async-start | bytes 2097152 | tf_op jit(solution)/shard_map/all_to_all | solution.py:254
  83.8 1.0 copy-start
  88.5 14.0 %all-to-all-start.4 = ((bf16[8,136,128]{2,1,0:T(8,128)(2,1)}), bf16[8,136,128]{2,1,0:T(8,128)(2,1)S(1)}, u32[]{:S(2)}, u32[]{:S(2)}) async-start(bf16[8,136,128]{2,1,0:T(8,128)(2,1)} %get-tuple-element.24), calls=%async_computation.4 | async-start | bytes 557056 | tf_op jit(solution)/shard_map/all_to_all | solution.py:254
  102.5 0.7 copy-start.2
  105.0 19.6 %all-to-all-start.5 = ((bf16[8,136,128]{2,1,0:T(8,128)(2,1)}), bf16[8,136,128]{2,1,0:T(8,128)(2,1)S(1)}, u32[]{:S(2)}, u32[]{:S(2)}) async-start(bf16[8,136,128]{2,1,0:T(8,128)(2,1)} %get-tuple-element.25), calls=%async_computation.5 | async-start | bytes 557056 | tf_op jit(solution)/shard_map/all_to_all | solution.py:254
  109.9 9.5 %collective-permute-start = (bf16[32,2048]{1,0:T(8,128)(2,1)}, bf16[32,2048]{1,0:T(8,128)(2,1)S(1)}, u32[]{:S(2)}, u32[]{:S(2)}) collective-permute-start(bf16[32,2048]{1,0:T(8,128)(2,1)} %get-tuple-element.20), channel_id=1, source_target_pairs={{0,8},{8,16},{16,24},{24,32},{32,40},{40,48},{48,56},{56,64},{64,7... | collective-permute-start | bytes 393224 | tf_op jit(solution)/shard_map/ppermute | solution.py:316
  119.4 0.7 copy-start.3
  124.6 4.3 %copy-start.1 = (bf16[8,136,128]{2,1,0:T(8,128)(2,1)}, bf16[8,136,128]{2,1,0:T(8,128)(2,1)S(1)}, u32[]{:S(2)}) copy-start(bf16[8,136,128]{2,1,0:T(8,128)(2,1)S(1)} %all-to-all-done.5.got) | copy-start | bytes 835588
  124.6 9.7 %all-to-all-start.2 = ((f32[8,2,256]{2,1,0:T(2,128)}), f32[8,2,256]{2,1,0:T(2,128)S(1)}, u32[]{:S(2)}, u32[]{:S(2)}) async-start(f32[8,2,256]{2,1,0:T(2,128)} %get-tuple-element.22), calls=%async_computation.2 | async-start | bytes 32768 | tf_op jit(solution)/shard_map/all_to_all | solution.py:254
  134.3 0.6 copy-start.4
  138.4 4.7 %collective-permute-start.1 = (bf16[128,2048]{1,0:T(8,128)(2,1)}, bf16[128,2048]{1,0:T(8,128)(2,1)S(1)}, u32[]{:S(2)}, u32[]{:S(2)}) collective-permute-start(bf16[128,2048]{1,0:T(8,128)(2,1)} %get-tuple-element.34), channel_id=1, source_target_pairs={{0,1},{1,0},{2,3},{3,2},{4,5},{5,4},{6,7},{7,6},{8,9},{9,8},{10,11... | collective-permute-start | bytes 1572872 | tf_op jit(solution)/shard_map/ppermute | solution.py:417
Sparse Core Ops, SparseCore 0:
  9.5 32.4 all-gather.2
  52.9 53.2 all-gather.4

commit v5 on v4

--- a/solution.py
+++ b/solution.py
@@ -16,7 +16,6 @@
 F32 = jnp.float32
 BF16 = jnp.bfloat16
 EXACT = lax.Precision.HIGHEST
-ANY = pl.BlockSpec(memory_space=pl.ANY)
 
 
 def dot_nt(a, b):
@@ -42,29 +41,30 @@
     return [pl.BlockSpec(memory_space=pltpu.VMEM)] * count
 
 
-def first_body(f, v, copies):
-    joined = jnp.concatenate([f[...], v[...]], axis=1)
+def first_body(gv, gg, q, g, wr, wc, f, v, copies, joined):
+    together = jnp.concatenate([w[...] for w in (gv, gg, q, g, wr, wc)], axis=1)
     for k in range(copies.shape[0]):
-        copies[k] = joined
-
-
-def second_body(gv, gg, q, g, wr, wc, _, copies):
-    joined = jnp.concatenate([w[...] for w in (gv, gg, q, g, wr, wc)], axis=1)
-    for k in range(copies.shape[0]):
-        copies[k] = joined
-
-
-def again_body(value, _, copies):
-    for k in range(copies.shape[0]):
-        copies[k] = value[...]
-
-
-def norm_body(tokens, gain, out, tail):
-    values_in = tokens[...].astype(F32)
-    row_scale = lax.rsqrt(jnp.mean(values_in * values_in, axis=1, keepdims=True) + 1e-06)
-    scaled = (values_in * row_scale * gain[...]).astype(BF16)
-    out[...] = scaled
-    tail[...] = scaled[scaled.shape[0] - HALO :]
+        copies[k] = together
+    joined[...] = jnp.concatenate([f[...], v[...]], axis=1)
+
+
+def again_body(places, *refs):
+    *pieces, copies = refs
+    for n, piece in enumerate(pieces):
+        value = piece[...]
+        for k in range(copies.shape[0]):
+            copies[k, places[n]] = value
+
+
+def norm_body(places, gain, *refs):
+    *pieces, out, tail = refs
+    share = tail.shape[0]
+    for n, piece in enumerate(pieces):
+        values_in = piece[...].astype(F32)
+        row_scale = lax.rsqrt(jnp.mean(values_in * values_in, axis=1, keepdims=True) + 1e-06)
+        scaled = (values_in * row_scale * gain[...]).astype(BF16)
+        out[pl.ds(pl.multiple_of(places[n] * share, share), share)] = scaled
+    tail[...] = out[out.shape[0] - share :]
 
 
 def pack_state(out, state, total):
@@ -254,6 +254,14 @@
     return lax.all_to_all(value, axis, split_axis=0, concat_axis=0, tiled=True)
 
 
+def shifted_around(value, axis):
+    count = lax.axis_size(axis)
+    pieces = [value]
+    for k in range(1, count):
+        pieces.append(lax.ppermute(value, axis, [(n, (n + k) % count) for n in range(count)]))
+    return pieces, (lax.axis_index(axis) + count - jnp.arange(count, dtype=jnp.int32)) % count
+
+
 def on_device(
     tokens,
     norm_gain,
@@ -283,34 +291,36 @@
     glu_width = 2 * channels
     all_width = sum(w.shape[1] for w in columns)
     outer_count = lax.axis_size(SP[0])
-    copies = call(
-        first_body, shape((outer_count, depth, 2 * HEAD_K), BF16), w_forget, w_value
-    )
-    block = lax.all_gather(tokens, TP, axis=0, tiled=True)
-    column = swap(copies, SP[0]).reshape(outer_count * depth, 2 * HEAD_K)
-    copies = call(
-        second_body,
-        shape((inner_count, depth, all_width), BF16),
+    copies, joined = call(
+        first_body,
+        (
+            shape((inner_count, depth, all_width), BF16),
+            shape((depth, 2 * HEAD_K), BF16),
+        ),
         *columns,
-        column,
-        in_specs=whole(len(columns)) + [ANY],
+        w_forget,
+        w_value,
     )
     staged = swap(copies, SP[1]).reshape(inner_count * depth, all_width)
     gathered = lax.all_gather(staged, SP[0], axis=0, tiled=True)
+    pieces, places = shifted_around(joined, SP[0])
     copies = call(
         again_body,
-        shape((inner_count, *column.shape), BF16),
-        column,
-        staged,
-        in_specs=whole(1) + [ANY],
-    )
-    state_weights = swap(copies, SP[1]).reshape(inner_count, outer_count, depth, 2 * HEAD_K)
+        shape((inner_count, outer_count, depth, 2 * HEAD_K), BF16),
+        places,
+        *pieces,
+        in_specs=[smem] + whole(len(pieces)),
+    )
+    state_weights = swap(copies, SP[1])
+    pieces, places = shifted_around(tokens, TP)
     rows = group * share
     normed, tail = call(
         norm_body,
         (shape((rows, features), BF16), shape((share, features), BF16)),
-        block,
+        places,
         norm_gain.reshape(1, -1),
+        *pieces,
+        in_specs=[smem] + whole(1 + len(pieces)),
     )
     count = lax.axis_size(SP)
     halo = lax.ppermute(tail, SP, [(k, k + 1) for k in range(count - 1)])
@@ -450,6 +460,7 @@
         P(TP, SP),
         P(TP, SP),
     )
+
     return jax.shard_map(
         on_device, mesh=torus, in_specs=placed, out_specs=P(SP_TP, None), check_vma=False
     )

time: 166 us -> 194 us (1.17)
  the two profiles are of different devices: /device:TPU:64 before, /device:TPU:1 now
where the time goes in v5:
time: 194 us; the launch traced here: 192 us
  starting transfers between devices  82 us (42%)
  blocking collectives  34.1 us (18%)
  waiting for transfers between devices  28.8 us (15%)
  Pallas kernels  26.5 us (14%)
  between operations  13.8 us (7%)
  local copies, waits for them, and re-layouts  4.2 us (2%)
  other arithmetic  3.05 us (2%)
    ppermute x14, starting transfers between devices, shifted_around(): lax.ppermute(value, axis, [(n, (n + k) % count) for n in range(count)])  56.2 us
    all_to_all x2, blocking collectives, swap(): return lax.all_to_all(value, axis, split_axis=0, concat_axis=0, tiled=True)  34.1 us
    pallas_call x9, Pallas kernels, call(): pl.pallas_call(body, out_shape=outs, scratch_shapes=scratch, **specs)(*args)  26.5 us
    all_to_all x4, starting transfers between devices, swap(): return lax.all_to_all(value, axis, split_axis=0, concat_axis=0, tiled=True)  21.3 us
    all_to_all x4, waiting for transfers between devices, swap(): return lax.all_to_all(value, axis, split_axis=0, concat_axis=0, tiled=True)  18.9 us
    ppermute x14, waiting for transfers between devices, shifted_around(): lax.ppermute(value, axis, [(n, (n + k) % count) for n in range(count)])  7.66 us
    unnamed x40, local copies, waits for them, and re-layouts  4.2 us
  transfers between devices with their start and end apart: 21, of which 7 were waited for; matrix products, arithmetic and copies ran while one was open for 1% of the time, Pallas kernels for 11%

profile of v5, /device:TPU:1, one launch (start us, length us, event | category | flops | bytes accessed | tf_op | source)
XLA Modules:
  0.0 192.5 jit_solution(7554689178604285098)
XLA Ops:
  6.5 1.7 shard_map.155
  8.3 22.4 %all_to_all.30 = bf16[8,32,1152]{2,1,0:T(8,128)(2,1)} all-to-all(bf16[8,32,1152]{2,1,0:T(8,128)(2,1)} %get-tuple-element.24), channel_id=1, replica_groups=mesh['sp_0'=8,'sp_1'=8,'x'=4,'core'=2] {'sp_1'}, dimensions={0} | all-to-all | bytes 1179648 | tf_op jit(solution)/shard_map/all_to_all | solution.py:254
  30.7 10.5 %collective-permute-start.10 = (bf16[32,256]{1,0:T(8,128)(2,1)}, bf16[32,256]{1,0:T(8,128)(2,1)S(1)}, u32[]{:S(2)}, u32[]{:S(2)}) collective-permute-start(bf16[32,256]{1,0:T(8,128)(2,1)} %get-tuple-element.27.refs_0_), channel_id=1, source_target_pairs={{0,192},{64,256},{128,320},{192,384},{256,448},{320,0},{384,64},{4... | collective-permute-start | bytes 49160 | tf_op jit(solution)/shard_map/ppermute | solution.py:261
  41.2 7.9 %collective-permute-start.11 = (bf16[32,256]{1,0:T(8,128)(2,1)}, bf16[32,256]{1,0:T(8,128)(2,1)S(1)}, u32[]{:S(2)}, u32[]{:S(2)}) collective-permute-start(bf16[32,256]{1,0:T(8,128)(2,1)} %get-tuple-element.27.refs_0_), channel_id=1, source_target_pairs={{0,256},{64,320},{128,384},{192,448},{256,0},{320,64},{384,128},{4... | collective-permute-start | bytes 49160 | tf_op jit(solution)/shard_map/ppermute | solution.py:261
  49.2 3.4 %collective-permute-start.12 = (bf16[32,256]{1,0:T(8,128)(2,1)}, bf16[32,256]{1,0:T(8,128)(2,1)S(1)}, u32[]{:S(2)}, u32[]{:S(2)}) collective-permute-start(bf16[32,256]{1,0:T(8,128)(2,1)} %get-tuple-element.27.refs_0_), channel_id=1, source_target_pairs={{0,320},{64,384},{128,448},{192,0},{256,64},{320,128},{384,192},{4... | collective-permute-start | bytes 49160 | tf_op jit(solution)/shard_map/ppermute | solution.py:261
  52.5 2.9 %collective-permute-start.13 = (bf16[32,256]{1,0:T(8,128)(2,1)}, bf16[32,256]{1,0:T(8,128)(2,1)S(1)}, u32[]{:S(2)}, u32[]{:S(2)}) collective-permute-start(bf16[32,256]{1,0:T(8,128)(2,1)} %get-tuple-element.27.refs_0_), channel_id=1, source_target_pairs={{0,384},{64,448},{128,0},{192,64},{256,128},{320,192},{384,256},{4... | collective-permute-start | bytes 49160 | tf_op jit(solution)/shard_map/ppermute | solution.py:261
  55.4 2.2 %collective-permute-start.14 = (bf16[32,256]{1,0:T(8,128)(2,1)}, bf16[32,256]{1,0:T(8,128)(2,1)S(1)}, u32[]{:S(2)}, u32[]{:S(2)}) collective-permute-start(bf16[32,256]{1,0:T(8,128)(2,1)} %get-tuple-element.27.refs_0_), channel_id=1, source_target_pairs={{0,448},{64,0},{128,64},{192,128},{256,192},{320,256},{384,320},{4... | collective-permute-start | bytes 49160 | tf_op jit(solution)/shard_map/ppermute | solution.py:261
  57.6 3.1 %collective-permute-start.8 = (bf16[32,256]{1,0:T(8,128)(2,1)}, bf16[32,256]{1,0:T(8,128)(2,1)S(1)}, u32[]{:S(2)}, u32[]{:S(2)}) collective-permute-start(bf16[32,256]{1,0:T(8,128)(2,1)} %get-tuple-element.27.refs_0_), channel_id=1, source_target_pairs={{0,64},{64,128},{128,192},{192,256},{256,320},{320,384},{384,448},... | collective-permute-start | bytes 49160 | tf_op jit(solution)/shard_map/ppermute | solution.py:261
  60.7 3.3 %collective-permute-start.9 = (bf16[32,256]{1,0:T(8,128)(2,1)}, bf16[32,256]{1,0:T(8,128)(2,1)S(1)}, u32[]{:S(2)}, u32[]{:S(2)}) collective-permute-start(bf16[32,256]{1,0:T(8,128)(2,1)} %get-tuple-element.27.refs_0_), channel_id=1, source_target_pairs={{0,128},{64,192},{128,256},{192,320},{256,384},{320,448},{384,0},{... | collective-permute-start | bytes 49160 | tf_op jit(solution)/shard_map/ppermute | solution.py:261
  64.1 0.6 and_select_fusion.places
  64.7 3.6 %collective-permute-done.9.refs_2_ = bf16[32,256]{1,0:T(8,128)(2,1)S(1)} collective-permute-done((bf16[32,256]{1,0:T(8,128)(2,1)}, bf16[32,256]{1,0:T(8,128)(2,1)S(1)}, u32[]{:S(2)}, u32[]{:S(2)}) %collective-permute-start.9) | collective-permute-done | bytes 16416 | tf_op jit(solution)/shard_map/ppermute | solution.py:261
  68.4 0.6 copy-done.19
  69.0 1.9 shard_map.157
  70.9 3.6 %all-to-all-start.2 = ((bf16[8,8,32,256]{3,2,1,0:T(8,128)(2,1)}), bf16[8,8,32,256]{3,2,1,0:T(8,128)(2,1)S(1)}, u32[]{:S(2)}, u32[]{:S(2)}) async-start(bf16[8,8,32,256]{3,2,1,0:T(8,128)(2,1)} %shard_map.157), calls=%async_computation.2 | async-start | bytes 2097152 | tf_op jit(solution)/shard_map/all_to_all | solution.py:254
  74.5 5.8 %collective-permute-start = (bf16[32,2048]{1,0:T(8,128)(2,1)S(1)}, bf16[32,2048]{1,0:T(8,128)(2,1)S(1)}, u32[]{:S(2)}, u32[]{:S(2)}) collective-permute-start(bf16[32,2048]{1,0:T(8,128)(2,1)S(1)} %copy-done.4), channel_id=1, source_target_pairs={{0,1},{1,2},{2,3},{3,4},{4,5},{5,6},{6,7},{7,0},{8,9},{9,10},{10,1... | collective-permute-start | bytes 393224 | tf_op jit(solution)/shard_map/ppermute | solution.py:261
  80.3 3.1 %collective-permute-start.1 = (bf16[32,2048]{1,0:T(8,128)(2,1)S(1)}, bf16[32,2048]{1,0:T(8,128)(2,1)S(1)}, u32[]{:S(2)}, u32[]{:S(2)}) collective-permute-start(bf16[32,2048]{1,0:T(8,128)(2,1)S(1)} %copy-done.4), channel_id=1, source_target_pairs={{0,2},{1,3},{2,4},{3,5},{4,6},{5,7},{6,0},{7,1},{8,10},{9,11},{10,... | collective-permute-start | bytes 393224 | tf_op jit(solution)/shard_map/ppermute | solution.py:261
  83.4 3.5 %collective-permute-start.2 = (bf16[32,2048]{1,0:T(8,128)(2,1)S(1)}, bf16[32,2048]{1,0:T(8,128)(2,1)S(1)}, u32[]{:S(2)}, u32[]{:S(2)}) collective-permute-start(bf16[32,2048]{1,0:T(8,128)(2,1)S(1)} %copy-done.4), channel_id=1, source_target_pairs={{0,3},{1,4},{2,5},{3,6},{4,7},{5,0},{6,1},{7,2},{8,11},{9,12},{10,... | collective-permute-start | bytes 393224 | tf_op jit(solution)/shard_map/ppermute | solution.py:261
  86.8 2.4 %collective-permute-start.3 = (bf16[32,2048]{1,0:T(8,128)(2,1)S(1)}, bf16[32,2048]{1,0:T(8,128)(2,1)S(1)}, u32[]{:S(2)}, u32[]{:S(2)}) collective-permute-start(bf16[32,2048]{1,0:T(8,128)(2,1)S(1)} %copy-done.4), channel_id=1, source_target_pairs={{0,4},{1,5},{2,6},{3,7},{4,0},{5,1},{6,2},{7,3},{8,12},{9,13},{10,... | collective-permute-start | bytes 393224 | tf_op jit(solution)/shard_map/ppermute | solution.py:261
  89.3 3.9 %collective-permute-start.4 = (bf16[32,2048]{1,0:T(8,128)(2,1)S(1)}, bf16[32,2048]{1,0:T(8,128)(2,1)S(1)}, u32[]{:S(2)}, u32[]{:S(2)}) collective-permute-start(bf16[32,2048]{1,0:T(8,128)(2,1)S(1)} %copy-done.4), channel_id=1, source_target_pairs={{0,5},{1,6},{2,7},{3,0},{4,1},{5,2},{6,3},{7,4},{8,13},{9,14},{10,... | collective-permute-start | bytes 393224 | tf_op jit(solution)/shard_map/ppermute | solution.py:261
  93.2 2.6 %collective-permute-start.5 = (bf16[32,2048]{1,0:T(8,128)(2,1)S(1)}, bf16[32,2048]{1,0:T(8,128)(2,1)S(1)}, u32[]{:S(2)}, u32[]{:S(2)}) collective-permute-start(bf16[32,2048]{1,0:T(8,128)(2,1)S(1)} %copy-done.4), channel_id=1, source_target_pairs={{0,6},{1,7},{2,0},{3,1},{4,2},{5,3},{6,4},{7,5},{8,14},{9,15},{10,... | collective-permute-start | bytes 393224 | tf_op jit(solution)/shard_map/ppermute | solution.py:261
  95.8 1.6 collective-permute-start.6
  97.4 0.5 and_select_fusion.1.places
  98.0 1.3 collective-permute-done.5.refs_6_
  99.3 2.7 %collective-permute-done.6.refs_7_ = bf16[32,2048]{1,0:T(8,128)(2,1)S(1)} collective-permute-done((bf16[32,2048]{1,0:T(8,128)(2,1)S(1)}, bf16[32,2048]{1,0:T(8,128)(2,1)S(1)}, u32[]{:S(2)}, u32[]{:S(2)}) %collective-permute-start.6) | collective-permute-done | bytes 131104 | tf_op jit(solution)/shard_map/ppermute | solution.py:261
  102.1 0.6 copy-done.11
  102.7 2.8 %shard_map.154 = (bf16[256,2048]{1,0:T(8,128)(2,1)}, bf16[32,2048]{1,0:T(8,128)(2,1)}) custom-call(s32[8]{0:T(128)} %and_select_fusion.1.places, f32[1,2048]{1,0:T(1,128)} %bitcast.15, bf16[32,2048]{1,0:T(8,128)(2,1)} %refs_0_.1, bf16[32,2048]{1,0:T(8,128)(2,1)} %copy-done.5, bf16[32,2048]{1,0:T(8,128)(2,1)} %copy-done.6, bf16[32,2048]{1,0:T(8,128)(2,1)} %copy-done.7, ...), custom_call_target="tpu_custom_call" | custom-call | tf_op jit(solution)/shard_map/pallas_call | solution.py:37
  105.5 1.0 copy-done
  106.4 3.8 %shard_map.158 = (bf16[8,136,128]{2,1,0:T(8,128)(2,1)}, bf16[256,128]{1,0:T(8,128)(2,1)}, bf16[256,128]{1,0:T(8,128)(2,1)}, f32[256,128]{1,0:T(8,128)}, bf16[4,128,128]{2,1,0:T(8,128)(2,1)}, /*index=5*/f32[4,128]{1,0:T(4,128)}) custom-call(bf16[256,2048]{1,0:T(8,128)(2,1)} %get-tuple-element.23.normed, bf16[8,8,32,256]{3,2,1,0:T(8,128)(2,1)} %copy-done, ...), custom_call_target="tpu_custom_call" | custom-call | tf_op jit(solution)/shard_map/pallas_call | solution.py:37
  110.2 6.5 %all-to-all-start.3 = ((bf16[8,136,128]{2,1,0:T(8,128)(2,1)}), bf16[8,136,128]{2,1,0:T(8,128)(2,1)S(1)}, u32[]{:S(2)}, u32[]{:S(2)}) async-start(bf16[8,136,128]{2,1,0:T(8,128)(2,1)} %get-tuple-element.28), calls=%async_computation.3 | async-start | bytes 557056 | tf_op jit(solution)/shard_map/all_to_all | solution.py:254
  116.7 12.8 %all-to-all-done.3.got = bf16[8,136,128]{2,1,0:T(8,128)(2,1)S(1)} async-done(((bf16[8,136,128]{2,1,0:T(8,128)(2,1)}), bf16[8,136,128]{2,1,0:T(8,128)(2,1)S(1)}, u32[]{:S(2)}, u32[]{:S(2)}) %all-to-all-start.3) | async-done | bytes 278560 | tf_op jit(solution)/shard_map/all_to_all | solution.py:254
  129.5 0.7 copy-done.2
  130.2 1.8 shard_map.159
  132.0 6.0 %all-to-all-start.4 = ((bf16[8,136,128]{2,1,0:T(8,128)(2,1)}), bf16[8,136,128]{2,1,0:T(8,128)(2,1)S(1)}, u32[]{:S(2)}, u32[]{:S(2)}) async-start(bf16[8,136,128]{2,1,0:T(8,128)(2,1)} %get-tuple-element.29), calls=%async_computation.4 | async-start | bytes 557056 | tf_op jit(solution)/shard_map/all_to_all | solution.py:254
  138.0 1.9 %collective-permute-start.7 = (bf16[32,2048]{1,0:T(8,128)(2,1)}, bf16[32,2048]{1,0:T(8,128)(2,1)S(1)}, u32[]{:S(2)}, u32[]{:S(2)}) collective-permute-start(bf16[32,2048]{1,0:T(8,128)(2,1)} %get-tuple-element.22), channel_id=1, source_target_pairs={{0,8},{8,16},{16,24},{24,32},{32,40},{40,48},{48,56},{56,64},{64,7... | collective-permute-start | bytes 393224 | tf_op jit(solution)/shard_map/ppermute | solution.py:326
  140.0 2.2 %collective-permute-done.7.halo = bf16[32,2048]{1,0:T(8,128)(2,1)S(1)} collective-permute-done((bf16[32,2048]{1,0:T(8,128)(2,1)}, bf16[32,2048]{1,0:T(8,128)(2,1)S(1)}, u32[]{:S(2)}, u32[]{:S(2)}) %collective-permute-start.7) | collective-permute-done | bytes 131104 | tf_op jit(solution)/shard_map/ppermute | solution.py:326
  142.2 0.7 copy-done.3
  142.9 4.6 %shard_map.156 = (f32[256,256]{1,0:T(8,128)}, f32[8,2,256]{2,1,0:T(2,128)}) custom-call(bf16[32,2048]{1,0:T(8,128)(2,1)} %copy-done.3, bf16[256,2048]{1,0:T(8,128)(2,1)} %get-tuple-element.23.normed, bf16[2048,1152]{1,0:T(8,128)(2,1)} %all-gather.2.cloned.1.call-done.weights.w_rec.w_low.w_high, f32[31,256]{1,0:T(8,128)} %taps.1), custom_call_target="tpu_custom_call" | custom-call | tf_op jit(solution)/shard_map/pallas_call | solution.py:37
  147.4 5.1 %all-to-all-done.4.got = bf16[8,136,128]{2,1,0:T(8,128)(2,1)S(1)} async-done(((bf16[8,136,128]{2,1,0:T(8,128)(2,1)}), bf16[8,136,128]{2,1,0:T(8,128)(2,1)S(1)}, u32[]{:S(2)}, u32[]{:S(2)}) %all-to-all-start.4) | async-done | bytes 278560 | tf_op jit(solution)/shard_map/all_to_all | solution.py:254
  152.5 5.2 %all-to-all-start.1 = ((f32[8,2,256]{2,1,0:T(2,128)}), f32[8,2,256]{2,1,0:T(2,128)S(1)}, u32[]{:S(2)}, u32[]{:S(2)}) async-start(f32[8,2,256]{2,1,0:T(2,128)} %get-tuple-element.25), calls=%async_computation.1 | async-start | bytes 32768 | tf_op jit(solution)/shard_map/all_to_all | solution.py:254
  157.7 3.6 %shard_map.160.head_out = bf16[256,128]{1,0:T(8,128)(2,1)} custom-call(s32[1]{0:T(128)} %bitcast.5.position, bf16[8,136,128]{2,1,0:T(8,128)(2,1)} %copy-done.1, f32[128,128]{1,0:T(8,128)} %get-tuple-element.30.inner_state, f32[8,128]{1,0:T(8,128)} %get-tuple-element.31.inner_total, bf16[256,2048]{1,0:T(8,128)(2,1)} %get-tuple-element.23.normed, ...), custom_call_target="tpu_custom_call" | custom-call | tf_op jit(solution)/shard_map/pallas_call | solution.py:37
  161.3 1.0 all-to-all-done.1.stats
  162.4 0.6 copy-done.12
  163.0 3.6 %shard_map.161 = (bf16[2,128,384]{2,1,0:T(8,128)(2,1)}, bf16[128,2048]{1,0:T(8,128)(2,1)}) custom-call(s32[1]{0:T(128)} %bitcast.core, f32[8,2,256]{2,1,0:T(2,128)} %copy-done.12, f32[256,256]{1,0:T(8,128)} %get-tuple-element.26.conv, bf16[256,128]{1,0:T(8,128)(2,1)} %shard_map.160.head_out, f32[1,256]{1,0:T(1,128)} %bitcast.17, f32[1,256]{1,0:T(1,128)} %bitcast.18, ...), custom_call_target="tpu_custom_call" | custom-call | tf_op jit(solution)/shard_map/pallas_call | solution.py:37
  166.5 2.6 %collective-permute-start.15 = (bf16[128,2048]{1,0:T(8,128)(2,1)}, bf16[128,2048]{1,0:T(8,128)(2,1)S(1)}, u32[]{:S(2)}, u32[]{:S(2)}) collective-permute-start(bf16[128,2048]{1,0:T(8,128)(2,1)} %get-tuple-element.38), channel_id=1, source_target_pairs={{0,1},{1,0},{2,3},{3,2},{4,5},{5,4},{6,7},{7,6},{8,9},{9,8},{10,11... | collective-permute-start | bytes 1572872 | tf_op jit(solution)/shard_map/ppermute | solution.py:427
  169.1 2.8 %shard_map.162 = bf16[128,2048]{1,0:T(8,128)(2,1)} custom-call(s32[1]{0:T(128)} %bitcast.core, bf16[2,128,384]{2,1,0:T(8,128)(2,1)} %get-tuple-element.37.rows, bf16[2048,1152]{1,0:T(8,128)(2,1)} %all-gather.2.cloned.1.call-done.weights.w_rec.w_low.w_high, bf16[2048,1152]{1,0:T(8,128)(2,1)} %all-gather.2.cloned.1.call-done.weights.w_rec.w_low.w_high, ...), custom_call_target="tpu_custom_call" | custom-call | tf_op jit(solution)/shard_map/pallas_call | solution.py:37
  172.0 1.2 add_convert_fusion
  173.2 11.7 %all_to_all.31 = bf16[4,32,2048]{2,1,0:T(8,128)(2,1)S(1)} all-to-all(bf16[4,32,2048]{2,1,0:T(8,128)(2,1)S(1)} %bitcast.13), channel_id=1, replica_groups=mesh['sp_0'=8,'sp_1'=8,'x'=4,'core'=2] {'x'}, dimensions={0} | all-to-all | bytes 1048576 | tf_op jit(solution)/shard_map/all_to_all | solution.py:254
  184.9 0.7 reduce_sum.12
  (50 shorter events, 0.1 us)
Async XLA Ops:
  6.5 67.9 %copy-start.4 = (bf16[32,2048]{1,0:T(8,128)(2,1)S(1)}, bf16[32,2048]{1,0:T(8,128)(2,1)}, u32[]{:S(2)}) copy-start(bf16[32,2048]{1,0:T(8,128)(2,1)} %refs_0_.1) | copy-start | bytes 393220
  6.5 135.7 %all-gather.2.cloned.1.call-start = ((), (), s32[]{:S(2)}) async-start(), calls=%async_computation.6 | async-start | bytes 5308416 | tf_op jit(solution)/shard_map/all_gather | solution.py:305
  30.7 26.9 %collective-permute-start.10 = (bf16[32,256]{1,0:T(8,128)(2,1)}, bf16[32,256]{1,0:T(8,128)(2,1)S(1)}, u32[]{:S(2)}, u32[]{:S(2)}) collective-permute-start(bf16[32,256]{1,0:T(8,128)(2,1)} %get-tuple-element.27.refs_0_), channel_id=1, source_target_pairs={{0,192},{64,256},{128,320},{192,384},{256,448},{320,0},{384,64},{4... | collective-permute-start | bytes 49160 | tf_op jit(solution)/shard_map/ppermute | solution.py:261
  41.2 19.5 %collective-permute-start.11 = (bf16[32,256]{1,0:T(8,128)(2,1)}, bf16[32,256]{1,0:T(8,128)(2,1)S(1)}, u32[]{:S(2)}, u32[]{:S(2)}) collective-permute-start(bf16[32,256]{1,0:T(8,128)(2,1)} %get-tuple-element.27.refs_0_), channel_id=1, source_target_pairs={{0,256},{64,320},{128,384},{192,448},{256,0},{320,64},{384,128},{4... | collective-permute-start | bytes 49160 | tf_op jit(solution)/shard_map/ppermute | solution.py:261
  49.2 15.5 %collective-permute-start.12 = (bf16[32,256]{1,0:T(8,128)(2,1)}, bf16[32,256]{1,0:T(8,128)(2,1)S(1)}, u32[]{:S(2)}, u32[]{:S(2)}) collective-permute-start(bf16[32,256]{1,0:T(8,128)(2,1)} %get-tuple-element.27.refs_0_), channel_id=1, source_target_pairs={{0,320},{64,384},{128,448},{192,0},{256,64},{320,128},{384,192},{4... | collective-permute-start | bytes 49160 | tf_op jit(solution)/shard_map/ppermute | solution.py:261
  52.5 12.1 %collective-permute-start.13 = (bf16[32,256]{1,0:T(8,128)(2,1)}, bf16[32,256]{1,0:T(8,128)(2,1)S(1)}, u32[]{:S(2)}, u32[]{:S(2)}) collective-permute-start(bf16[32,256]{1,0:T(8,128)(2,1)} %get-tuple-element.27.refs_0_), channel_id=1, source_target_pairs={{0,384},{64,448},{128,0},{192,64},{256,128},{320,192},{384,256},{4... | collective-permute-start | bytes 49160 | tf_op jit(solution)/shard_map/ppermute | solution.py:261
  55.4 9.3 %collective-permute-start.14 = (bf16[32,256]{1,0:T(8,128)(2,1)}, bf16[32,256]{1,0:T(8,128)(2,1)S(1)}, u32[]{:S(2)}, u32[]{:S(2)}) collective-permute-start(bf16[32,256]{1,0:T(8,128)(2,1)} %get-tuple-element.27.refs_0_), channel_id=1, source_target_pairs={{0,448},{64,0},{128,64},{192,128},{256,192},{320,256},{384,320},{4... | collective-permute-start | bytes 49160 | tf_op jit(solution)/shard_map/ppermute | solution.py:261
  57.6 10.8 %copy-start.13 = (bf16[32,256]{1,0:T(8,128)(2,1)}, bf16[32,256]{1,0:T(8,128)(2,1)S(1)}, u32[]{:S(2)}) copy-start(bf16[32,256]{1,0:T(8,128)(2,1)S(1)} %collective-permute-done.10.refs_3_) | copy-start | bytes 49156
  57.6 7.1 %collective-permute-start.8 = (bf16[32,256]{1,0:T(8,128)(2,1)}, bf16[32,256]{1,0:T(8,128)(2,1)S(1)}, u32[]{:S(2)}, u32[]{:S(2)}) collective-permute-start(bf16[32,256]{1,0:T(8,128)(2,1)} %get-tuple-element.27.refs_0_), channel_id=1, source_target_pairs={{0,64},{64,128},{128,192},{192,256},{256,320},{320,384},{384,448},... | collective-permute-start | bytes 49160 | tf_op jit(solution)/shard_map/ppermute | solution.py:261
  60.7 7.6 %copy-start.14 = (bf16[32,256]{1,0:T(8,128)(2,1)}, bf16[32,256]{1,0:T(8,128)(2,1)S(1)}, u32[]{:S(2)}) copy-start(bf16[32,256]{1,0:T(8,128)(2,1)S(1)} %collective-permute-done.11.refs_4_) | copy-start | bytes 49156
  60.7 7.6 %collective-permute-start.9 = (bf16[32,256]{1,0:T(8,128)(2,1)}, bf16[32,256]{1,0:T(8,128)(2,1)S(1)}, u32[]{:S(2)}, u32[]{:S(2)}) collective-permute-start(bf16[32,256]{1,0:T(8,128)(2,1)} %get-tuple-element.27.refs_0_), channel_id=1, source_target_pairs={{0,128},{64,192},{128,256},{192,320},{256,384},{320,448},{384,0},{... | collective-permute-start | bytes 49160 | tf_op jit(solution)/shard_map/ppermute | solution.py:261
  64.7 3.7 %copy-start.15 = (bf16[32,256]{1,0:T(8,128)(2,1)}, bf16[32,256]{1,0:T(8,128)(2,1)S(1)}, u32[]{:S(2)}) copy-start(bf16[32,256]{1,0:T(8,128)(2,1)S(1)} %collective-permute-done.12.refs_5_) | copy-start | bytes 49156
  64.7 3.7 %copy-start.16 = (bf16[32,256]{1,0:T(8,128)(2,1)}, bf16[32,256]{1,0:T(8,128)(2,1)S(1)}, u32[]{:S(2)}) copy-start(bf16[32,256]{1,0:T(8,128)(2,1)S(1)} %collective-permute-done.13.refs_6_) | copy-start | bytes 49156
  64.7 3.7 %copy-start.17 = (bf16[32,256]{1,0:T(8,128)(2,1)}, bf16[32,256]{1,0:T(8,128)(2,1)S(1)}, u32[]{:S(2)}) copy-start(bf16[32,256]{1,0:T(8,128)(2,1)S(1)} %collective-permute-done.14.refs_7_) | copy-start | bytes 49156
  64.7 3.7 %copy-start.18 = (bf16[32,256]{1,0:T(8,128)(2,1)}, bf16[32,256]{1,0:T(8,128)(2,1)S(1)}, u32[]{:S(2)}) copy-start(bf16[32,256]{1,0:T(8,128)(2,1)S(1)} %collective-permute-done.8.refs_1_) | copy-start | bytes 49156
  68.4 0.6 copy-start.19
  70.9 34.6 %all-to-all-start.2 = ((bf16[8,8,32,256]{3,2,1,0:T(8,128)(2,1)}), bf16[8,8,32,256]{3,2,1,0:T(8,128)(2,1)S(1)}, u32[]{:S(2)}, u32[]{:S(2)}) async-start(bf16[8,8,32,256]{3,2,1,0:T(8,128)(2,1)} %shard_map.157), calls=%async_computation.2 | async-start | bytes 2097152 | tf_op jit(solution)/shard_map/all_to_all | solution.py:254
  74.5 18.7 %collective-permute-start = (bf16[32,2048]{1,0:T(8,128)(2,1)S(1)}, bf16[32,2048]{1,0:T(8,128)(2,1)S(1)}, u32[]{:S(2)}, u32[]{:S(2)}) collective-permute-start(bf16[32,2048]{1,0:T(8,128)(2,1)S(1)} %copy-done.4), channel_id=1, source_target_pairs={{0,1},{1,2},{2,3},{3,4},{4,5},{5,6},{6,7},{7,0},{8,9},{9,10},{10,1... | collective-permute-start | bytes 393224 | tf_op jit(solution)/shard_map/ppermute | solution.py:261
  80.3 15.5 %collective-permute-start.1 = (bf16[32,2048]{1,0:T(8,128)(2,1)S(1)}, bf16[32,2048]{1,0:T(8,128)(2,1)S(1)}, u32[]{:S(2)}, u32[]{:S(2)}) collective-permute-start(bf16[32,2048]{1,0:T(8,128)(2,1)S(1)} %copy-done.4), channel_id=1, source_target_pairs={{0,2},{1,3},{2,4},{3,5},{4,6},{5,7},{6,0},{7,1},{8,10},{9,11},{10,... | collective-permute-start | bytes 393224 | tf_op jit(solution)/shard_map/ppermute | solution.py:261
  83.4 14.6 %collective-permute-start.2 = (bf16[32,2048]{1,0:T(8,128)(2,1)S(1)}, bf16[32,2048]{1,0:T(8,128)(2,1)S(1)}, u32[]{:S(2)}, u32[]{:S(2)}) collective-permute-start(bf16[32,2048]{1,0:T(8,128)(2,1)S(1)} %copy-done.4), channel_id=1, source_target_pairs={{0,3},{1,4},{2,5},{3,6},{4,7},{5,0},{6,1},{7,2},{8,11},{9,12},{10,... | collective-permute-start | bytes 393224 | tf_op jit(solution)/shard_map/ppermute | solution.py:261
  86.8 11.1 %collective-permute-start.3 = (bf16[32,2048]{1,0:T(8,128)(2,1)S(1)}, bf16[32,2048]{1,0:T(8,128)(2,1)S(1)}, u32[]{:S(2)}, u32[]{:S(2)}) collective-permute-start(bf16[32,2048]{1,0:T(8,128)(2,1)S(1)} %copy-done.4), channel_id=1, source_target_pairs={{0,4},{1,5},{2,6},{3,7},{4,0},{5,1},{6,2},{7,3},{8,12},{9,13},{10,... | collective-permute-start | bytes 393224 | tf_op jit(solution)/shard_map/ppermute | solution.py:261
  89.3 8.7 %collective-permute-start.4 = (bf16[32,2048]{1,0:T(8,128)(2,1)S(1)}, bf16[32,2048]{1,0:T(8,128)(2,1)S(1)}, u32[]{:S(2)}, u32[]{:S(2)}) collective-permute-start(bf16[32,2048]{1,0:T(8,128)(2,1)S(1)} %copy-done.4), channel_id=1, source_target_pairs={{0,5},{1,6},{2,7},{3,0},{4,1},{5,2},{6,3},{7,4},{8,13},{9,14},{10,... | collective-permute-start | bytes 393224 | tf_op jit(solution)/shard_map/ppermute | solution.py:261
  93.2 8.8 %copy-start.5 = (bf16[32,2048]{1,0:T(8,128)(2,1)}, bf16[32,2048]{1,0:T(8,128)(2,1)S(1)}, u32[]{:S(2)}) copy-start(bf16[32,2048]{1,0:T(8,128)(2,1)S(1)} %collective-permute-done.refs_1_) | copy-start | bytes 393220
  93.2 6.1 %collective-permute-start.5 = (bf16[32,2048]{1,0:T(8,128)(2,1)S(1)}, bf16[32,2048]{1,0:T(8,128)(2,1)S(1)}, u32[]{:S(2)}, u32[]{:S(2)}) collective-permute-start(bf16[32,2048]{1,0:T(8,128)(2,1)S(1)} %copy-done.4), channel_id=1, source_target_pairs={{0,6},{1,7},{2,0},{3,1},{4,2},{5,3},{6,4},{7,5},{8,14},{9,15},{10,... | collective-permute-start | bytes 393224 | tf_op jit(solution)/shard_map/ppermute | solution.py:261
  95.8 6.2 %copy-start.6 = (bf16[32,2048]{1,0:T(8,128)(2,1)}, bf16[32,2048]{1,0:T(8,128)(2,1)S(1)}, u32[]{:S(2)}) copy-start(bf16[32,2048]{1,0:T(8,128)(2,1)S(1)} %collective-permute-done.1.refs_2_) | copy-start | bytes 393220
  95.8 6.2 %collective-permute-start.6 = (bf16[32,2048]{1,0:T(8,128)(2,1)S(1)}, bf16[32,2048]{1,0:T(8,128)(2,1)S(1)}, u32[]{:S(2)}, u32[]{:S(2)}) collective-permute-start(bf16[32,2048]{1,0:T(8,128)(2,1)S(1)} %copy-done.4), channel_id=1, source_target_pairs={{0,7},{1,0},{2,1},{3,2},{4,3},{5,4},{6,5},{7,6},{8,15},{9,8},{10,9... | collective-permute-start | bytes 393224 | tf_op jit(solution)/shard_map/ppermute | solution.py:261
  98.0 4.1 %copy-start.7 = (bf16[32,2048]{1,0:T(8,128)(2,1)}, bf16[32,2048]{1,0:T(8,128)(2,1)S(1)}, u32[]{:S(2)}) copy-start(bf16[32,2048]{1,0:T(8,128)(2,1)S(1)} %collective-permute-done.2.refs_3_) | copy-start | bytes 393220
  98.0 4.1 %copy-start.8 = (bf16[32,2048]{1,0:T(8,128)(2,1)}, bf16[32,2048]{1,0:T(8,128)(2,1)S(1)}, u32[]{:S(2)}) copy-start(bf16[32,2048]{1,0:T(8,128)(2,1)S(1)} %collective-permute-done.3.refs_4_) | copy-start | bytes 393220
  98.0 4.1 %copy-start.9 = (bf16[32,2048]{1,0:T(8,128)(2,1)}, bf16[32,2048]{1,0:T(8,128)(2,1)S(1)}, u32[]{:S(2)}) copy-start(bf16[32,2048]{1,0:T(8,128)(2,1)S(1)} %collective-permute-done.4.refs_5_) | copy-start | bytes 393220
  99.3 2.7 %copy-start.10 = (bf16[32,2048]{1,0:T(8,128)(2,1)}, bf16[32,2048]{1,0:T(8,128)(2,1)S(1)}, u32[]{:S(2)}) copy-start(bf16[32,2048]{1,0:T(8,128)(2,1)S(1)} %collective-permute-done.5.refs_6_) | copy-start | bytes 393220
  102.0 0.7 copy-start.11
  105.5 1.0 copy-start
  110.2 19.3 %all-to-all-start.3 = ((bf16[8,136,128]{2,1,0:T(8,128)(2,1)}), bf16[8,136,128]{2,1,0:T(8,128)(2,1)S(1)}, u32[]{:S(2)}, u32[]{:S(2)}) async-start(bf16[8,136,128]{2,1,0:T(8,128)(2,1)} %get-tuple-element.28), calls=%async_computation.3 | async-start | bytes 557056 | tf_op jit(solution)/shard_map/all_to_all | solution.py:254
  129.5 0.7 copy-start.2
  132.0 20.5 %all-to-all-start.4 = ((bf16[8,136,128]{2,1,0:T(8,128)(2,1)}), bf16[8,136,128]{2,1,0:T(8,128)(2,1)S(1)}, u32[]{:S(2)}, u32[]{:S(2)}) async-start(bf16[8,136,128]{2,1,0:T(8,128)(2,1)} %get-tuple-element.29), calls=%async_computation.4 | async-start | bytes 557056 | tf_op jit(solution)/shard_map/all_to_all | solution.py:254
  138.0 4.2 %collective-permute-start.7 = (bf16[32,2048]{1,0:T(8,128)(2,1)}, bf16[32,2048]{1,0:T(8,128)(2,1)S(1)}, u32[]{:S(2)}, u32[]{:S(2)}) collective-permute-start(bf16[32,2048]{1,0:T(8,128)(2,1)} %get-tuple-element.22), channel_id=1, source_target_pairs={{0,8},{8,16},{16,24},{24,32},{32,40},{40,48},{48,56},{56,64},{64,7... | collective-permute-start | bytes 393224 | tf_op jit(solution)/shard_map/ppermute | solution.py:326
  142.2 0.7 copy-start.3
  152.5 5.2 %copy-start.1 = (bf16[8,136,128]{2,1,0:T(8,128)(2,1)}, bf16[8,136,128]{2,1,0:T(8,128)(2,1)S(1)}, u32[]{:S(2)}) copy-start(bf16[8,136,128]{2,1,0:T(8,128)(2,1)S(1)} %all-to-all-done.4.got) | copy-start | bytes 835588
  152.5 9.8 %all-to-all-start.1 = ((f32[8,2,256]{2,1,0:T(2,128)}), f32[8,2,256]{2,1,0:T(2,128)S(1)}, u32[]{:S(2)}, u32[]{:S(2)}) async-start(f32[8,2,256]{2,1,0:T(2,128)} %get-tuple-element.25), calls=%async_computation.1 | async-start | bytes 32768 | tf_op jit(solution)/shard_map/all_to_all | solution.py:254
  162.4 0.6 copy-start.12
  166.5 5.5 %collective-permute-start.15 = (bf16[128,2048]{1,0:T(8,128)(2,1)}, bf16[128,2048]{1,0:T(8,128)(2,1)S(1)}, u32[]{:S(2)}, u32[]{:S(2)}) collective-permute-start(bf16[128,2048]{1,0:T(8,128)(2,1)} %get-tuple-element.38), channel_id=1, source_target_pairs={{0,1},{1,0},{2,3},{3,2},{4,5},{5,4},{6,7},{7,6},{8,9},{9,8},{10,11... | collective-permute-start | bytes 1572872 | tf_op jit(solution)/shard_map/ppermute | solution.py:427
Sparse Core Ops, SparseCore 0:
  30.8 68.4 all-gather.1

commit v6 on v5

--- a/solution.py
+++ b/solution.py
@@ -41,19 +41,16 @@
     return [pl.BlockSpec(memory_space=pltpu.VMEM)] * count
 
 
-def first_body(gv, gg, q, g, wr, wc, f, v, copies, joined):
-    together = jnp.concatenate([w[...] for w in (gv, gg, q, g, wr, wc)], axis=1)
+def first_body(gv, gg, q, g, wr, wc, f, v, operand, copies):
+    operand[...] = jnp.concatenate([w[...] for w in (gv, gg, q, g, wr, wc)], axis=1)
+    joined = jnp.concatenate([f[...], v[...]], axis=1)
     for k in range(copies.shape[0]):
-        copies[k] = together
-    joined[...] = jnp.concatenate([f[...], v[...]], axis=1)
-
-
-def again_body(places, *refs):
-    *pieces, copies = refs
-    for n, piece in enumerate(pieces):
-        value = piece[...]
-        for k in range(copies.shape[0]):
-            copies[k, places[n]] = value
+        copies[k] = joined
+
+
+def again_body(value, copies):
+    for k in range(copies.shape[0]):
+        copies[k] = value[...]
 
 
 def norm_body(places, gain, *refs):
@@ -291,26 +288,19 @@
     glu_width = 2 * channels
     all_width = sum(w.shape[1] for w in columns)
     outer_count = lax.axis_size(SP[0])
-    copies, joined = call(
+    operand, copies = call(
         first_body,
         (
-            shape((inner_count, depth, all_width), BF16),
-            shape((depth, 2 * HEAD_K), BF16),
+            shape((depth, all_width), BF16),
+            shape((outer_count, depth, 2 * HEAD_K), BF16),
         ),
         *columns,
         w_forget,
         w_value,
     )
-    staged = swap(copies, SP[1]).reshape(inner_count * depth, all_width)
-    gathered = lax.all_gather(staged, SP[0], axis=0, tiled=True)
-    pieces, places = shifted_around(joined, SP[0])
-    copies = call(
-        again_body,
-        shape((inner_count, outer_count, depth, 2 * HEAD_K), BF16),
-        places,
-        *pieces,
-        in_specs=[smem] + whole(len(pieces)),
-    )
+    gathered = lax.all_gather(operand, SP, axis=0, tiled=True)
+    column = swap(copies, SP[0])
+    copies = call(again_body, shape((inner_count, *column.shape), BF16), column)
     state_weights = swap(copies, SP[1])
     pieces, places = shifted_around(tokens, TP)
     rows = group * share

time: 194 us -> 163 us (0.84)
  starting transfers between devices: 82 us -> 48.8 us
  waiting for transfers between devices: 28.8 us -> 37.7 us
  blocking collectives: 34.1 us -> 30.5 us
    ppermute x14 -> x7, starting transfers between devices: 56.2 us -> 20.8 us  [shifted_around(): lax.ppermute(value, axis, [(n, (n + k) % count) for n in range(count)])]
    all_gather x1, waiting for transfers between devices: 0.01 us -> 8.62 us  [on_device(): gathered = lax.all_gather(operand, SP, axis=0, tiled=True)]
    ppermute x1, waiting for transfers between devices: 2.24 us -> 5.93 us  [on_device(): halo = lax.ppermute(tail, SP, [(k, k + 1) for k in range(count - 1)])]
    all_to_all x2, blocking collectives: 34.1 us -> 30.5 us  [swap(): return lax.all_to_all(value, axis, split_axis=0, concat_axis=0, tiled=True)]
    ppermute x14 -> x7, waiting for transfers between devices: 7.66 us -> 4.31 us  [shifted_around(): lax.ppermute(value, axis, [(n, (n + k) % count) for n in range(count)])]
    all_to_all x4, starting transfers between devices: 21.3 us -> 23.4 us  [swap(): return lax.all_to_all(value, axis, split_axis=0, concat_axis=0, tiled=True)]
    unnamed x40 -> x24, local copies, waits for them, and re-layouts: 4.2 us -> 2.98 us
  transfers between devices with their start and end apart: 21 -> 14, of which waited for: 7 -> 7; matrix products, arithmetic and copies ran while one was open for 1% -> 0% of each run, Pallas kernels for 11% -> 13%
where the time goes in v6:
time: 163 us; the launch traced here: 162 us
  starting transfers between devices  48.8 us (30%)
  waiting for transfers between devices  37.7 us (23%)
  blocking collectives  30.5 us (19%)
  Pallas kernels  26.3 us (16%)
  between operations  13.6 us (8%)
  local copies, waits for them, and re-layouts  2.98 us (2%)
  other arithmetic  2.48 us (2%)
    all_to_all x2, blocking collectives, swap(): return lax.all_to_all(value, axis, split_axis=0, concat_axis=0, tiled=True)  30.5 us
    pallas_call x9, Pallas kernels, call(): pl.pallas_call(body, out_shape=outs, scratch_shapes=scratch, **specs)(*args)  26.3 us
    all_to_all x4, starting transfers between devices, swap(): return lax.all_to_all(value, axis, split_axis=0, concat_axis=0, tiled=True)  23.4 us
    ppermute x7, starting transfers between devices, shifted_around(): lax.ppermute(value, axis, [(n, (n + k) % count) for n in range(count)])  20.8 us
    all_to_all x4, waiting for transfers between devices, swap(): return lax.all_to_all(value, axis, split_axis=0, concat_axis=0, tiled=True)  18.8 us
    all_gather x1, waiting for transfers between devices, on_device(): gathered = lax.all_gather(operand, SP, axis=0, tiled=True)  8.62 us
    ppermute x1, waiting for transfers between devices, on_device(): halo = lax.ppermute(tail, SP, [(k, k + 1) for k in range(count - 1)])  5.93 us
    ppermute x7, waiting for transfers between devices, shifted_around(): lax.ppermute(value, axis, [(n, (n + k) % count) for n in range(count)])  4.31 us
  transfers between devices with their start and end apart: 14, of which 7 were waited for; matrix products, arithmetic and copies ran while one was open for 0% of the time, Pallas kernels for 13%

profile of v6, /device:TPU:1, one launch (start us, length us, event | category | flops | bytes accessed | tf_op | source)
XLA Modules:
  0.0 162.3 jit_solution(12733882161357385682)
XLA Ops:
  6.5 1.5 shard_map.155
  8.0 0.0 all-gather.2.cloned.1.call-update
  8.1 18.7 %all_to_all.30.value = bf16[8,32,256]{2,1,0:T(8,128)(2,1)} all-to-all(bf16[8,32,256]{2,1,0:T(8,128)(2,1)} %get-tuple-element.27), channel_id=1, replica_groups=mesh['sp_0'=8,'sp_1'=8,'x'=4,'core'=2] {'sp_0'}, dimensions={0} | all-to-all | bytes 262144 | tf_op jit(solution)/shard_map/all_to_all | solution.py:251
  26.8 2.0 %shard_map.157 = bf16[8,8,32,256]{3,2,1,0:T(8,128)(2,1)} custom-call(bf16[8,32,256]{2,1,0:T(8,128)(2,1)} %all_to_all.30.value), custom_call_target="tpu_custom_call" | custom-call | tf_op jit(solution)/shard_map/pallas_call | solution.py:37
  28.8 6.8 %all-to-all-start.2 = ((bf16[8,8,32,256]{3,2,1,0:T(8,128)(2,1)}), bf16[8,8,32,256]{3,2,1,0:T(8,128)(2,1)S(1)}, u32[]{:S(2)}, u32[]{:S(2)}) async-start(bf16[8,8,32,256]{3,2,1,0:T(8,128)(2,1)} %shard_map.157), calls=%async_computation.2 | async-start | bytes 2097152 | tf_op jit(solution)/shard_map/all_to_all | solution.py:251
  35.6 3.7 %collective-permute-start = (bf16[32,2048]{1,0:T(8,128)(2,1)}, bf16[32,2048]{1,0:T(8,128)(2,1)S(1)}, u32[]{:S(2)}, u32[]{:S(2)}) collective-permute-start(bf16[32,2048]{1,0:T(8,128)(2,1)} %refs_0_.1), channel_id=1, source_target_pairs={{0,1},{1,2},{2,3},{3,4},{4,5},{5,6},{6,7},{7,0},{8,9},{9,10},{10,1... | collective-permute-start | bytes 393224 | tf_op jit(solution)/shard_map/ppermute | solution.py:258
  39.3 3.1 %collective-permute-start.1 = (bf16[32,2048]{1,0:T(8,128)(2,1)}, bf16[32,2048]{1,0:T(8,128)(2,1)S(1)}, u32[]{:S(2)}, u32[]{:S(2)}) collective-permute-start(bf16[32,2048]{1,0:T(8,128)(2,1)} %refs_0_.1), channel_id=1, source_target_pairs={{0,2},{1,3},{2,4},{3,5},{4,6},{5,7},{6,0},{7,1},{8,10},{9,11},{10,... | collective-permute-start | bytes 393224 | tf_op jit(solution)/shard_map/ppermute | solution.py:258
  42.4 3.5 %collective-permute-start.2 = (bf16[32,2048]{1,0:T(8,128)(2,1)}, bf16[32,2048]{1,0:T(8,128)(2,1)S(1)}, u32[]{:S(2)}, u32[]{:S(2)}) collective-permute-start(bf16[32,2048]{1,0:T(8,128)(2,1)} %refs_0_.1), channel_id=1, source_target_pairs={{0,3},{1,4},{2,5},{3,6},{4,7},{5,0},{6,1},{7,2},{8,11},{9,12},{10,... | collective-permute-start | bytes 393224 | tf_op jit(solution)/shard_map/ppermute | solution.py:258
  45.8 2.4 %collective-permute-start.3 = (bf16[32,2048]{1,0:T(8,128)(2,1)}, bf16[32,2048]{1,0:T(8,128)(2,1)S(1)}, u32[]{:S(2)}, u32[]{:S(2)}) collective-permute-start(bf16[32,2048]{1,0:T(8,128)(2,1)} %refs_0_.1), channel_id=1, source_target_pairs={{0,4},{1,5},{2,6},{3,7},{4,0},{5,1},{6,2},{7,3},{8,12},{9,13},{10,... | collective-permute-start | bytes 393224 | tf_op jit(solution)/shard_map/ppermute | solution.py:258
  48.3 3.9 %collective-permute-start.4 = (bf16[32,2048]{1,0:T(8,128)(2,1)}, bf16[32,2048]{1,0:T(8,128)(2,1)S(1)}, u32[]{:S(2)}, u32[]{:S(2)}) collective-permute-start(bf16[32,2048]{1,0:T(8,128)(2,1)} %refs_0_.1), channel_id=1, source_target_pairs={{0,5},{1,6},{2,7},{3,0},{4,1},{5,2},{6,3},{7,4},{8,13},{9,14},{10,... | collective-permute-start | bytes 393224 | tf_op jit(solution)/shard_map/ppermute | solution.py:258
  52.2 0.0 collective-permute-done.refs_1_
  52.2 0.0 copy-start.4
  52.2 2.6 %collective-permute-start.5 = (bf16[32,2048]{1,0:T(8,128)(2,1)}, bf16[32,2048]{1,0:T(8,128)(2,1)S(1)}, u32[]{:S(2)}, u32[]{:S(2)}) collective-permute-start(bf16[32,2048]{1,0:T(8,128)(2,1)} %refs_0_.1), channel_id=1, source_target_pairs={{0,6},{1,7},{2,0},{3,1},{4,2},{5,3},{6,4},{7,5},{8,14},{9,15},{10,... | collective-permute-start | bytes 393224 | tf_op jit(solution)/shard_map/ppermute | solution.py:258
  54.8 0.0 collective-permute-done.1.refs_2_
  54.8 0.0 copy-start.5
  54.8 1.6 collective-permute-start.6
  56.4 0.6 and_select_fusion.places
  57.0 0.0 collective-permute-done.2.refs_3_
  57.0 0.0 collective-permute-done.3.refs_4_
  57.0 0.0 collective-permute-done.4.refs_5_
  57.1 1.6 collective-permute-done.5.refs_6_
  58.7 2.7 %collective-permute-done.6.refs_7_ = bf16[32,2048]{1,0:T(8,128)(2,1)S(1)} collective-permute-done((bf16[32,2048]{1,0:T(8,128)(2,1)}, bf16[32,2048]{1,0:T(8,128)(2,1)S(1)}, u32[]{:S(2)}, u32[]{:S(2)}) %collective-permute-start.6) | collective-permute-done | bytes 131104 | tf_op jit(solution)/shard_map/ppermute | solution.py:258
  61.4 0.6 copy-done.10
  62.0 2.7 %shard_map.154 = (bf16[256,2048]{1,0:T(8,128)(2,1)}, bf16[32,2048]{1,0:T(8,128)(2,1)}) custom-call(s32[8]{0:T(128)} %and_select_fusion.places, f32[1,2048]{1,0:T(1,128)} %bitcast.13, bf16[32,2048]{1,0:T(8,128)(2,1)} %refs_0_.1, bf16[32,2048]{1,0:T(8,128)(2,1)} %copy-done.4, bf16[32,2048]{1,0:T(8,128)(2,1)} %copy-done.5, bf16[32,2048]{1,0:T(8,128)(2,1)} %copy-done.6, ...), custom_call_target="tpu_custom_call" | custom-call | tf_op jit(solution)/shard_map/pallas_call | solution.py:37
  64.8 2.1 %all-to-all-done.2.weights = bf16[8,8,32,256]{3,2,1,0:T(8,128)(2,1)S(1)} async-done(((bf16[8,8,32,256]{3,2,1,0:T(8,128)(2,1)}), bf16[8,8,32,256]{3,2,1,0:T(8,128)(2,1)S(1)}, u32[]{:S(2)}, u32[]{:S(2)}) %all-to-all-start.2) | async-done | bytes 1048608 | tf_op jit(solution)/shard_map/all_to_all | solution.py:251
  66.9 1.0 copy-done
  67.9 3.7 %shard_map.158 = (bf16[8,136,128]{2,1,0:T(8,128)(2,1)}, bf16[256,128]{1,0:T(8,128)(2,1)}, bf16[256,128]{1,0:T(8,128)(2,1)}, f32[256,128]{1,0:T(8,128)}, bf16[4,128,128]{2,1,0:T(8,128)(2,1)}, /*index=5*/f32[4,128]{1,0:T(4,128)}) custom-call(bf16[256,2048]{1,0:T(8,128)(2,1)} %get-tuple-element.23.normed, bf16[8,8,32,256]{3,2,1,0:T(8,128)(2,1)} %copy-done, ...), custom_call_target="tpu_custom_call" | custom-call | tf_op jit(solution)/shard_map/pallas_call | solution.py:37
  71.6 4.8 %all-to-all-start.3 = ((bf16[8,136,128]{2,1,0:T(8,128)(2,1)}), bf16[8,136,128]{2,1,0:T(8,128)(2,1)S(1)}, u32[]{:S(2)}, u32[]{:S(2)}) async-start(bf16[8,136,128]{2,1,0:T(8,128)(2,1)} %get-tuple-element.28), calls=%async_computation.3 | async-start | bytes 557056 | tf_op jit(solution)/shard_map/all_to_all | solution.py:251
  76.4 15.7 %all-to-all-done.3.got = bf16[8,136,128]{2,1,0:T(8,128)(2,1)S(1)} async-done(((bf16[8,136,128]{2,1,0:T(8,128)(2,1)}), bf16[8,136,128]{2,1,0:T(8,128)(2,1)S(1)}, u32[]{:S(2)}, u32[]{:S(2)}) %all-to-all-start.3) | async-done | bytes 278560 | tf_op jit(solution)/shard_map/all_to_all | solution.py:251
  92.1 0.7 copy-done.2
  92.8 1.8 %shard_map.159 = (bf16[8,136,128]{2,1,0:T(8,128)(2,1)}, f32[128,128]{1,0:T(8,128)}, f32[8,128]{1,0:T(8,128)}) custom-call(s32[1]{0:T(128)} %bitcast.5.position, bf16[8,136,128]{2,1,0:T(8,128)(2,1)} %copy-done.2), custom_call_target="tpu_custom_call" | custom-call | tf_op jit(solution)/shard_map/pallas_call | solution.py:37
  94.6 3.4 %all-to-all-start.4 = ((bf16[8,136,128]{2,1,0:T(8,128)(2,1)}), bf16[8,136,128]{2,1,0:T(8,128)(2,1)S(1)}, u32[]{:S(2)}, u32[]{:S(2)}) async-start(bf16[8,136,128]{2,1,0:T(8,128)(2,1)} %get-tuple-element.29), calls=%async_computation.4 | async-start | bytes 557056 | tf_op jit(solution)/shard_map/all_to_all | solution.py:251
  98.1 2.0 %collective-permute-start.7 = (bf16[32,2048]{1,0:T(8,128)(2,1)}, bf16[32,2048]{1,0:T(8,128)(2,1)S(1)}, u32[]{:S(2)}, u32[]{:S(2)}) collective-permute-start(bf16[32,2048]{1,0:T(8,128)(2,1)} %get-tuple-element.22), channel_id=1, source_target_pairs={{0,8},{8,16},{16,24},{24,32},{32,40},{40,48},{48,56},{56,64},{64,7... | collective-permute-start | bytes 393224 | tf_op jit(solution)/shard_map/ppermute | solution.py:316
  100.1 5.9 %collective-permute-done.7.halo = bf16[32,2048]{1,0:T(8,128)(2,1)S(1)} collective-permute-done((bf16[32,2048]{1,0:T(8,128)(2,1)}, bf16[32,2048]{1,0:T(8,128)(2,1)S(1)}, u32[]{:S(2)}, u32[]{:S(2)}) %collective-permute-start.7) | collective-permute-done | bytes 131104 | tf_op jit(solution)/shard_map/ppermute | solution.py:316
  106.0 8.6 %all-gather.2.cloned.1.call-done.weights.w_rec.w_low.w_high = bf16[2048,1152]{1,0:T(8,128)(2,1)} async-done(((bf16[32,1152]{1,0:T(8,128)(2,1)}), bf16[2048,1152]{1,0:T(8,128)(2,1)}) %all-gather.2.cloned.1.call-update) | async-done | bytes 4718608 | tf_op jit(solution)/shard_map/all_gather | solution.py:301
  114.6 4.6 %shard_map.156 = (f32[256,256]{1,0:T(8,128)}, f32[8,2,256]{2,1,0:T(2,128)}) custom-call(bf16[32,2048]{1,0:T(8,128)(2,1)} %copy-done.3, bf16[256,2048]{1,0:T(8,128)(2,1)} %get-tuple-element.23.normed, bf16[2048,1152]{1,0:T(8,128)(2,1)} %all-gather.2.cloned.1.call-done.weights.w_rec.w_low.w_high, f32[31,256]{1,0:T(8,128)} %taps.1), custom_call_target="tpu_custom_call" | custom-call | tf_op jit(solution)/shard_map/pallas_call | solution.py:37
  119.2 0.0 all-to-all-done.4.got
  119.2 8.3 %all-to-all-start = ((f32[8,2,256]{2,1,0:T(2,128)}), f32[8,2,256]{2,1,0:T(2,128)S(1)}, u32[]{:S(2)}, u32[]{:S(2)}) async-start(f32[8,2,256]{2,1,0:T(2,128)} %get-tuple-element.25), calls=%async_computation | async-start | bytes 32768 | tf_op jit(solution)/shard_map/all_to_all | solution.py:251
  127.5 3.6 %shard_map.160.head_out = bf16[256,128]{1,0:T(8,128)(2,1)} custom-call(s32[1]{0:T(128)} %bitcast.4.position, bf16[8,136,128]{2,1,0:T(8,128)(2,1)} %copy-done.1, f32[128,128]{1,0:T(8,128)} %get-tuple-element.30.inner_state, f32[8,128]{1,0:T(8,128)} %get-tuple-element.31.inner_total, bf16[256,2048]{1,0:T(8,128)(2,1)} %get-tuple-element.23.normed, ...), custom_call_target="tpu_custom_call" | custom-call | tf_op jit(solution)/shard_map/pallas_call | solution.py:37
  131.2 1.0 all-to-all-done.stats
  132.2 0.6 copy-done.11
  132.8 3.6 %shard_map.161 = (bf16[2,128,384]{2,1,0:T(8,128)(2,1)}, bf16[128,2048]{1,0:T(8,128)(2,1)}) custom-call(s32[1]{0:T(128)} %bitcast.core, f32[8,2,256]{2,1,0:T(2,128)} %copy-done.11, f32[256,256]{1,0:T(8,128)} %get-tuple-element.26.conv, bf16[256,128]{1,0:T(8,128)(2,1)} %shard_map.160.head_out, f32[1,256]{1,0:T(1,128)} %bitcast.15, f32[1,256]{1,0:T(1,128)} %bitcast.16, ...), custom_call_target="tpu_custom_call" | custom-call | tf_op jit(solution)/shard_map/pallas_call | solution.py:37
  136.3 2.6 %collective-permute-start.8 = (bf16[128,2048]{1,0:T(8,128)(2,1)}, bf16[128,2048]{1,0:T(8,128)(2,1)S(1)}, u32[]{:S(2)}, u32[]{:S(2)}) collective-permute-start(bf16[128,2048]{1,0:T(8,128)(2,1)} %get-tuple-element.38), channel_id=1, source_target_pairs={{0,1},{1,0},{2,3},{3,2},{4,5},{5,4},{6,7},{7,6},{8,9},{9,8},{10,11... | collective-permute-start | bytes 1572872 | tf_op jit(solution)/shard_map/ppermute | solution.py:417
  139.0 2.8 %shard_map.162 = bf16[128,2048]{1,0:T(8,128)(2,1)} custom-call(s32[1]{0:T(128)} %bitcast.core, bf16[2,128,384]{2,1,0:T(8,128)(2,1)} %get-tuple-element.37.rows, bf16[2048,1152]{1,0:T(8,128)(2,1)} %all-gather.2.cloned.1.call-done.weights.w_rec.w_low.w_high, bf16[2048,1152]{1,0:T(8,128)(2,1)} %all-gather.2.cloned.1.call-done.weights.w_rec.w_low.w_high, ...), custom_call_target="tpu_custom_call" | custom-call | tf_op jit(solution)/shard_map/pallas_call | solution.py:37
  141.8 0.0 collective-permute-done.8
  141.8 1.2 add_convert_fusion
  142.9 11.7 %all_to_all.31 = bf16[4,32,2048]{2,1,0:T(8,128)(2,1)S(1)} all-to-all(bf16[4,32,2048]{2,1,0:T(8,128)(2,1)S(1)} %bitcast.11), channel_id=1, replica_groups=mesh['sp_0'=8,'sp_1'=8,'x'=4,'core'=2] {'x'}, dimensions={0} | all-to-all | bytes 1048576 | tf_op jit(solution)/shard_map/all_to_all | solution.py:251
  154.7 0.7 reduce_sum.12
  (19 shorter events, 0.0 us)
Async XLA Ops:
  6.5 108.1 %all-gather.2.cloned.1.call-start = ((), (), s32[]{:S(2)}) async-start(), calls=%async_computation.6 | async-start | bytes 4792320 | tf_op jit(solution)/shard_map/all_gather | solution.py:301
  28.8 38.1 %all-to-all-start.2 = ((bf16[8,8,32,256]{3,2,1,0:T(8,128)(2,1)}), bf16[8,8,32,256]{3,2,1,0:T(8,128)(2,1)S(1)}, u32[]{:S(2)}, u32[]{:S(2)}) async-start(bf16[8,8,32,256]{3,2,1,0:T(8,128)(2,1)} %shard_map.157), calls=%async_computation.2 | async-start | bytes 2097152 | tf_op jit(solution)/shard_map/all_to_all | solution.py:251
  35.6 16.6 %collective-permute-start = (bf16[32,2048]{1,0:T(8,128)(2,1)}, bf16[32,2048]{1,0:T(8,128)(2,1)S(1)}, u32[]{:S(2)}, u32[]{:S(2)}) collective-permute-start(bf16[32,2048]{1,0:T(8,128)(2,1)} %refs_0_.1), channel_id=1, source_target_pairs={{0,1},{1,2},{2,3},{3,4},{4,5},{5,6},{6,7},{7,0},{8,9},{9,10},{10,1... | collective-permute-start | bytes 393224 | tf_op jit(solution)/shard_map/ppermute | solution.py:258
  39.3 15.5 %collective-permute-start.1 = (bf16[32,2048]{1,0:T(8,128)(2,1)}, bf16[32,2048]{1,0:T(8,128)(2,1)S(1)}, u32[]{:S(2)}, u32[]{:S(2)}) collective-permute-start(bf16[32,2048]{1,0:T(8,128)(2,1)} %refs_0_.1), channel_id=1, source_target_pairs={{0,2},{1,3},{2,4},{3,5},{4,6},{5,7},{6,0},{7,1},{8,10},{9,11},{10,... | collective-permute-start | bytes 393224 | tf_op jit(solution)/shard_map/ppermute | solution.py:258
  42.4 14.6 %collective-permute-start.2 = (bf16[32,2048]{1,0:T(8,128)(2,1)}, bf16[32,2048]{1,0:T(8,128)(2,1)S(1)}, u32[]{:S(2)}, u32[]{:S(2)}) collective-permute-start(bf16[32,2048]{1,0:T(8,128)(2,1)} %refs_0_.1), channel_id=1, source_target_pairs={{0,3},{1,4},{2,5},{3,6},{4,7},{5,0},{6,1},{7,2},{8,11},{9,12},{10,... | collective-permute-start | bytes 393224 | tf_op jit(solution)/shard_map/ppermute | solution.py:258
  45.8 11.2 %collective-permute-start.3 = (bf16[32,2048]{1,0:T(8,128)(2,1)}, bf16[32,2048]{1,0:T(8,128)(2,1)S(1)}, u32[]{:S(2)}, u32[]{:S(2)}) collective-permute-start(bf16[32,2048]{1,0:T(8,128)(2,1)} %refs_0_.1), channel_id=1, source_target_pairs={{0,4},{1,5},{2,6},{3,7},{4,0},{5,1},{6,2},{7,3},{8,12},{9,13},{10,... | collective-permute-start | bytes 393224 | tf_op jit(solution)/shard_map/ppermute | solution.py:258
  48.3 8.8 %collective-permute-start.4 = (bf16[32,2048]{1,0:T(8,128)(2,1)}, bf16[32,2048]{1,0:T(8,128)(2,1)S(1)}, u32[]{:S(2)}, u32[]{:S(2)}) collective-permute-start(bf16[32,2048]{1,0:T(8,128)(2,1)} %refs_0_.1), channel_id=1, source_target_pairs={{0,5},{1,6},{2,7},{3,0},{4,1},{5,2},{6,3},{7,4},{8,13},{9,14},{10,... | collective-permute-start | bytes 393224 | tf_op jit(solution)/shard_map/ppermute | solution.py:258
  52.2 9.2 %copy-start.4 = (bf16[32,2048]{1,0:T(8,128)(2,1)}, bf16[32,2048]{1,0:T(8,128)(2,1)S(1)}, u32[]{:S(2)}) copy-start(bf16[32,2048]{1,0:T(8,128)(2,1)S(1)} %collective-permute-done.refs_1_) | copy-start | bytes 393220
  52.2 6.4 %collective-permute-start.5 = (bf16[32,2048]{1,0:T(8,128)(2,1)}, bf16[32,2048]{1,0:T(8,128)(2,1)S(1)}, u32[]{:S(2)}, u32[]{:S(2)}) collective-permute-start(bf16[32,2048]{1,0:T(8,128)(2,1)} %refs_0_.1), channel_id=1, source_target_pairs={{0,6},{1,7},{2,0},{3,1},{4,2},{5,3},{6,4},{7,5},{8,14},{9,15},{10,... | collective-permute-start | bytes 393224 | tf_op jit(solution)/shard_map/ppermute | solution.py:258
  54.8 6.6 %copy-start.5 = (bf16[32,2048]{1,0:T(8,128)(2,1)}, bf16[32,2048]{1,0:T(8,128)(2,1)S(1)}, u32[]{:S(2)}) copy-start(bf16[32,2048]{1,0:T(8,128)(2,1)S(1)} %collective-permute-done.1.refs_2_) | copy-start | bytes 393220
  54.8 6.5 %collective-permute-start.6 = (bf16[32,2048]{1,0:T(8,128)(2,1)}, bf16[32,2048]{1,0:T(8,128)(2,1)S(1)}, u32[]{:S(2)}, u32[]{:S(2)}) collective-permute-start(bf16[32,2048]{1,0:T(8,128)(2,1)} %refs_0_.1), channel_id=1, source_target_pairs={{0,7},{1,0},{2,1},{3,2},{4,3},{5,4},{6,5},{7,6},{8,15},{9,8},{10,9... | collective-permute-start | bytes 393224 | tf_op jit(solution)/shard_map/ppermute | solution.py:258
  57.0 4.4 %copy-start.6 = (bf16[32,2048]{1,0:T(8,128)(2,1)}, bf16[32,2048]{1,0:T(8,128)(2,1)S(1)}, u32[]{:S(2)}) copy-start(bf16[32,2048]{1,0:T(8,128)(2,1)S(1)} %collective-permute-done.2.refs_3_) | copy-start | bytes 393220
  57.0 4.3 %copy-start.7 = (bf16[32,2048]{1,0:T(8,128)(2,1)}, bf16[32,2048]{1,0:T(8,128)(2,1)S(1)}, u32[]{:S(2)}) copy-start(bf16[32,2048]{1,0:T(8,128)(2,1)S(1)} %collective-permute-done.3.refs_4_) | copy-start | bytes 393220
  57.0 4.3 %copy-start.8 = (bf16[32,2048]{1,0:T(8,128)(2,1)}, bf16[32,2048]{1,0:T(8,128)(2,1)S(1)}, u32[]{:S(2)}) copy-start(bf16[32,2048]{1,0:T(8,128)(2,1)S(1)} %collective-permute-done.4.refs_5_) | copy-start | bytes 393220
  58.7 2.7 %copy-start.9 = (bf16[32,2048]{1,0:T(8,128)(2,1)}, bf16[32,2048]{1,0:T(8,128)(2,1)S(1)}, u32[]{:S(2)}) copy-start(bf16[32,2048]{1,0:T(8,128)(2,1)S(1)} %collective-permute-done.5.refs_6_) | copy-start | bytes 393220
  61.4 0.7 copy-start.10
  66.9 1.0 copy-start
  71.6 20.5 %all-to-all-start.3 = ((bf16[8,136,128]{2,1,0:T(8,128)(2,1)}), bf16[8,136,128]{2,1,0:T(8,128)(2,1)S(1)}, u32[]{:S(2)}, u32[]{:S(2)}) async-start(bf16[8,136,128]{2,1,0:T(8,128)(2,1)} %get-tuple-element.28), calls=%async_computation.3 | async-start | bytes 557056 | tf_op jit(solution)/shard_map/all_to_all | solution.py:251
  92.1 0.7 copy-start.2
  94.6 24.6 %all-to-all-start.4 = ((bf16[8,136,128]{2,1,0:T(8,128)(2,1)}), bf16[8,136,128]{2,1,0:T(8,128)(2,1)S(1)}, u32[]{:S(2)}, u32[]{:S(2)}) async-start(bf16[8,136,128]{2,1,0:T(8,128)(2,1)} %get-tuple-element.29), calls=%async_computation.4 | async-start | bytes 557056 | tf_op jit(solution)/shard_map/all_to_all | solution.py:251
  98.1 8.0 %collective-permute-start.7 = (bf16[32,2048]{1,0:T(8,128)(2,1)}, bf16[32,2048]{1,0:T(8,128)(2,1)S(1)}, u32[]{:S(2)}, u32[]{:S(2)}) collective-permute-start(bf16[32,2048]{1,0:T(8,128)(2,1)} %get-tuple-element.22), channel_id=1, source_target_pairs={{0,8},{8,16},{16,24},{24,32},{32,40},{40,48},{48,56},{56,64},{64,7... | collective-permute-start | bytes 393224 | tf_op jit(solution)/shard_map/ppermute | solution.py:316
  106.0 8.6 %copy-start.3 = (bf16[32,2048]{1,0:T(8,128)(2,1)}, bf16[32,2048]{1,0:T(8,128)(2,1)S(1)}, u32[]{:S(2)}) copy-start(bf16[32,2048]{1,0:T(8,128)(2,1)S(1)} %collective-permute-done.7.halo) | copy-start | bytes 393220
  119.2 8.3 %copy-start.1 = (bf16[8,136,128]{2,1,0:T(8,128)(2,1)}, bf16[8,136,128]{2,1,0:T(8,128)(2,1)S(1)}, u32[]{:S(2)}) copy-start(bf16[8,136,128]{2,1,0:T(8,128)(2,1)S(1)} %all-to-all-done.4.got) | copy-start | bytes 835588
  119.2 13.0 %all-to-all-start = ((f32[8,2,256]{2,1,0:T(2,128)}), f32[8,2,256]{2,1,0:T(2,128)S(1)}, u32[]{:S(2)}, u32[]{:S(2)}) async-start(f32[8,2,256]{2,1,0:T(2,128)} %get-tuple-element.25), calls=%async_computation | async-start | bytes 32768 | tf_op jit(solution)/shard_map/all_to_all | solution.py:251
  132.2 0.6 copy-start.11
  136.3 5.4 %collective-permute-start.8 = (bf16[128,2048]{1,0:T(8,128)(2,1)}, bf16[128,2048]{1,0:T(8,128)(2,1)S(1)}, u32[]{:S(2)}, u32[]{:S(2)}) collective-permute-start(bf16[128,2048]{1,0:T(8,128)(2,1)} %get-tuple-element.38), channel_id=1, source_target_pairs={{0,1},{1,0},{2,3},{3,2},{4,5},{5,4},{6,7},{7,6},{8,9},{9,8},{10,11... | collective-permute-start | bytes 1572872 | tf_op jit(solution)/shard_map/ppermute | solution.py:417
Sparse Core Ops, SparseCore 0:
  10.3 104.2 all-gather.1

commit v7 on v6

--- a/solution.py
+++ b/solution.py
@@ -42,10 +42,16 @@
 
 
 def first_body(gv, gg, q, g, wr, wc, f, v, operand, copies):
-    operand[...] = jnp.concatenate([w[...] for w in (gv, gg, q, g, wr, wc)], axis=1)
+    together = jnp.concatenate([w[...] for w in (gv, gg, q, g, wr, wc)], axis=1)
+    operand[:, : together.shape[1]] = together
+    operand[:, together.shape[1] :] = jnp.zeros_like(operand[:, together.shape[1] :])
     joined = jnp.concatenate([f[...], v[...]], axis=1)
     for k in range(copies.shape[0]):
         copies[k] = joined
+
+
+def trim_body(value, out):
+    out[...] = value[...]
 
 
 def again_body(value, copies):
@@ -291,14 +297,24 @@
     operand, copies = call(
         first_body,
         (
-            shape((depth, all_width), BF16),
+            shape((depth, features), BF16),
             shape((outer_count, depth, 2 * HEAD_K), BF16),
         ),
         *columns,
         w_forget,
         w_value,
     )
-    gathered = lax.all_gather(operand, SP, axis=0, tiled=True)
+    inner = lax.all_gather(operand, SP[1], axis=0, tiled=True)
+    piece = pl.BlockSpec((inner_count * depth, all_width), lambda k: (0, 0))
+    inner = call(
+        trim_body,
+        shape((inner_count * depth, all_width), BF16),
+        inner,
+        grid=(1,),
+        in_specs=[piece],
+        out_specs=piece,
+    )
+    gathered = lax.all_gather(inner, SP[0], axis=0, tiled=True)
     column = swap(copies, SP[0])
     copies = call(again_body, shape((inner_count, *column.shape), BF16), column)
     state_weights = swap(copies, SP[1])

time: 163 us -> 193 us (1.18)
  waiting for transfers between devices: 37.7 us -> 68.5 us
  blocking collectives: 30.5 us -> 26.9 us
  Pallas kernels: 26.3 us -> 28.4 us
    all_gather x1 -> x2, waiting for transfers between devices: 8.62 us -> 42.7 us  [the longest x1 42.7 us: on_device(): inner = lax.all_gather(operand, SP[1], axis=0, tiled=True)]
    all_to_all x4, starting transfers between devices: 23.4 us -> 18.8 us  [swap(): return lax.all_to_all(value, axis, split_axis=0, concat_axis=0, tiled=True)]
    ppermute x7, starting transfers between devices: 20.8 us -> 25.2 us  [shifted_around(): lax.ppermute(value, axis, [(n, (n + k) % count) for n in range(count)])]
    all_to_all x2, blocking collectives: 30.5 us -> 26.9 us  [swap(): return lax.all_to_all(value, axis, split_axis=0, concat_axis=0, tiled=True)]
    ppermute x1, waiting for transfers between devices: 5.93 us -> 2.75 us  [on_device(): halo = lax.ppermute(tail, SP, [(k, k + 1) for k in range(count - 1)])]
    pallas_call x9 -> x10, Pallas kernels: 26.3 us -> 28.4 us  [call(): pl.pallas_call(body, out_shape=outs, scratch_shapes=scratch, **specs)(*args)]
  transfers between devices with their start and end apart: 14 -> 15, of which waited for: 7 -> 7; matrix products, arithmetic and copies ran while one was open for 0% -> 0% of each run, Pallas kernels for 13% -> 11%
where the time goes in v7:
time: 193 us; the launch traced here: 192 us
  waiting for transfers between devices  68.5 us (35%)
  starting transfers between devices  48.7 us (25%)
  Pallas kernels  28.4 us (15%)
  blocking collectives  26.9 us (14%)
  between operations  13.6 us (7%)
  local copies, waits for them, and re-layouts  3.62 us (2%)
  other arithmetic  2.43 us (1%)
    all_gather x1, waiting for transfers between devices, on_device(): inner = lax.all_gather(operand, SP[1], axis=0, tiled=True)  42.7 us
    pallas_call x10, Pallas kernels, call(): pl.pallas_call(body, out_shape=outs, scratch_shapes=scratch, **specs)(*args)  28.4 us
    all_to_all x2, blocking collectives, swap(): return lax.all_to_all(value, axis, split_axis=0, concat_axis=0, tiled=True)  26.9 us
    ppermute x7, starting transfers between devices, shifted_around(): lax.ppermute(value, axis, [(n, (n + k) % count) for n in range(count)])  25.2 us
    all_to_all x4, waiting for transfers between devices, swap(): return lax.all_to_all(value, axis, split_axis=0, concat_axis=0, tiled=True)  18.8 us
    all_to_all x4, starting transfers between devices, swap(): return lax.all_to_all(value, axis, split_axis=0, concat_axis=0, tiled=True)  18.8 us
    ppermute x7, waiting for transfers between devices, shifted_around(): lax.ppermute(value, axis, [(n, (n + k) % count) for n in range(count)])  4.19 us
  transfers between devices with their start and end apart: 15, of which 7 were waited for; matrix products, arithmetic and copies ran while one was open for 0% of the time, Pallas kernels for 11%

profile of v7, /device:TPU:1, one launch (start us, length us, event | category | flops | bytes accessed | tf_op | source)
XLA Modules:
  0.0 192.0 jit_solution(14749248293702855190)
XLA Ops:
  6.5 1.6 shard_map.155
  8.1 0.0 all-gather.3.cloned.1.call-update
  8.1 0.0 all-gather.5.cloned.1.call-start
  8.2 42.7 %all-gather.3.cloned.1.call-done.value = bf16[256,2048]{1,0:T(8,128)(2,1)} async-done(((bf16[32,2048]{1,0:T(8,128)(2,1)}), bf16[256,2048]{1,0:T(8,128)(2,1)}) %all-gather.3.cloned.1.call-update) | async-done | bytes 1048592 | tf_op jit(solution)/shard_map/all_gather | solution.py:307
  50.9 1.9 %shard_map.156 = bf16[256,1152]{1,0:T(8,128)(2,1)} custom-call(bf16[256,2048]{1,0:T(8,128)(2,1)} %all-gather.3.cloned.1.call-done.value), custom_call_target="tpu_custom_call" | custom-call | tf_op jit(solution)/shard_map/pallas_call | solution.py:37
  52.8 0.0 all-gather.5.cloned.1.call-update
  52.8 15.1 %all_to_all.30.value = bf16[8,32,256]{2,1,0:T(8,128)(2,1)} all-to-all(bf16[8,32,256]{2,1,0:T(8,128)(2,1)} %get-tuple-element.27), channel_id=1, replica_groups=mesh['sp_0'=8,'sp_1'=8,'x'=4,'core'=2] {'sp_0'}, dimensions={0} | all-to-all | bytes 262144 | tf_op jit(solution)/shard_map/all_to_all | solution.py:257
  67.9 2.0 %shard_map.158 = bf16[8,8,32,256]{3,2,1,0:T(8,128)(2,1)} custom-call(bf16[8,32,256]{2,1,0:T(8,128)(2,1)} %all_to_all.30.value), custom_call_target="tpu_custom_call" | custom-call | tf_op jit(solution)/shard_map/pallas_call | solution.py:37
  69.9 4.3 %all-to-all-start.2 = ((bf16[8,8,32,256]{3,2,1,0:T(8,128)(2,1)}), bf16[8,8,32,256]{3,2,1,0:T(8,128)(2,1)S(1)}, u32[]{:S(2)}, u32[]{:S(2)}) async-start(bf16[8,8,32,256]{3,2,1,0:T(8,128)(2,1)} %shard_map.158), calls=%async_computation.2 | async-start | bytes 2097152 | tf_op jit(solution)/shard_map/all_to_all | solution.py:257
  74.2 8.1 %collective-permute-start = (bf16[32,2048]{1,0:T(8,128)(2,1)S(1)}, bf16[32,2048]{1,0:T(8,128)(2,1)S(1)}, u32[]{:S(2)}, u32[]{:S(2)}) collective-permute-start(bf16[32,2048]{1,0:T(8,128)(2,1)S(1)} %copy-done.4), channel_id=1, source_target_pairs={{0,1},{1,2},{2,3},{3,4},{4,5},{5,6},{6,7},{7,0},{8,9},{9,10},{10,1... | collective-permute-start | bytes 393224 | tf_op jit(solution)/shard_map/ppermute | solution.py:264
  82.3 3.1 %collective-permute-start.1 = (bf16[32,2048]{1,0:T(8,128)(2,1)S(1)}, bf16[32,2048]{1,0:T(8,128)(2,1)S(1)}, u32[]{:S(2)}, u32[]{:S(2)}) collective-permute-start(bf16[32,2048]{1,0:T(8,128)(2,1)S(1)} %copy-done.4), channel_id=1, source_target_pairs={{0,2},{1,3},{2,4},{3,5},{4,6},{5,7},{6,0},{7,1},{8,10},{9,11},{10,... | collective-permute-start | bytes 393224 | tf_op jit(solution)/shard_map/ppermute | solution.py:264
  85.4 3.4 %collective-permute-start.2 = (bf16[32,2048]{1,0:T(8,128)(2,1)S(1)}, bf16[32,2048]{1,0:T(8,128)(2,1)S(1)}, u32[]{:S(2)}, u32[]{:S(2)}) collective-permute-start(bf16[32,2048]{1,0:T(8,128)(2,1)S(1)} %copy-done.4), channel_id=1, source_target_pairs={{0,3},{1,4},{2,5},{3,6},{4,7},{5,0},{6,1},{7,2},{8,11},{9,12},{10,... | collective-permute-start | bytes 393224 | tf_op jit(solution)/shard_map/ppermute | solution.py:264
  88.9 2.5 %collective-permute-start.3 = (bf16[32,2048]{1,0:T(8,128)(2,1)S(1)}, bf16[32,2048]{1,0:T(8,128)(2,1)S(1)}, u32[]{:S(2)}, u32[]{:S(2)}) collective-permute-start(bf16[32,2048]{1,0:T(8,128)(2,1)S(1)} %copy-done.4), channel_id=1, source_target_pairs={{0,4},{1,5},{2,6},{3,7},{4,0},{5,1},{6,2},{7,3},{8,12},{9,13},{10,... | collective-permute-start | bytes 393224 | tf_op jit(solution)/shard_map/ppermute | solution.py:264
  91.4 3.9 %collective-permute-start.4 = (bf16[32,2048]{1,0:T(8,128)(2,1)S(1)}, bf16[32,2048]{1,0:T(8,128)(2,1)S(1)}, u32[]{:S(2)}, u32[]{:S(2)}) collective-permute-start(bf16[32,2048]{1,0:T(8,128)(2,1)S(1)} %copy-done.4), channel_id=1, source_target_pairs={{0,5},{1,6},{2,7},{3,0},{4,1},{5,2},{6,3},{7,4},{8,13},{9,14},{10,... | collective-permute-start | bytes 393224 | tf_op jit(solution)/shard_map/ppermute | solution.py:264
  95.3 0.0 collective-permute-done.refs_1_
  95.3 0.0 copy-start.5
  95.3 2.5 %collective-permute-start.5 = (bf16[32,2048]{1,0:T(8,128)(2,1)S(1)}, bf16[32,2048]{1,0:T(8,128)(2,1)S(1)}, u32[]{:S(2)}, u32[]{:S(2)}) collective-permute-start(bf16[32,2048]{1,0:T(8,128)(2,1)S(1)} %copy-done.4), channel_id=1, source_target_pairs={{0,6},{1,7},{2,0},{3,1},{4,2},{5,3},{6,4},{7,5},{8,14},{9,15},{10,... | collective-permute-start | bytes 393224 | tf_op jit(solution)/shard_map/ppermute | solution.py:264
  97.8 0.0 collective-permute-done.1.refs_2_
  97.9 1.6 collective-permute-start.6
  99.5 0.5 and_select_fusion.places
  100.0 0.0 collective-permute-done.3.refs_4_
  100.0 0.0 collective-permute-done.4.refs_5_
  100.1 1.5 collective-permute-done.5.refs_6_
  101.6 2.6 %collective-permute-done.6.refs_7_ = bf16[32,2048]{1,0:T(8,128)(2,1)S(1)} collective-permute-done((bf16[32,2048]{1,0:T(8,128)(2,1)S(1)}, bf16[32,2048]{1,0:T(8,128)(2,1)S(1)}, u32[]{:S(2)}, u32[]{:S(2)}) %collective-permute-start.6) | collective-permute-done | bytes 131104 | tf_op jit(solution)/shard_map/ppermute | solution.py:264
  104.3 0.6 copy-done.11
  104.9 2.8 %shard_map.154 = (bf16[256,2048]{1,0:T(8,128)(2,1)}, bf16[32,2048]{1,0:T(8,128)(2,1)}) custom-call(s32[8]{0:T(128)} %and_select_fusion.places, f32[1,2048]{1,0:T(1,128)} %bitcast.13, bf16[32,2048]{1,0:T(8,128)(2,1)} %refs_0_.1, bf16[32,2048]{1,0:T(8,128)(2,1)} %copy-done.5, bf16[32,2048]{1,0:T(8,128)(2,1)} %copy-done.6, bf16[32,2048]{1,0:T(8,128)(2,1)} %copy-done.7, ...), custom_call_target="tpu_custom_call" | custom-call | tf_op jit(solution)/shard_map/pallas_call | solution.py:37
  107.7 1.0 copy-done
  108.7 3.8 %shard_map.159 = (bf16[8,136,128]{2,1,0:T(8,128)(2,1)}, bf16[256,128]{1,0:T(8,128)(2,1)}, bf16[256,128]{1,0:T(8,128)(2,1)}, f32[256,128]{1,0:T(8,128)}, bf16[4,128,128]{2,1,0:T(8,128)(2,1)}, /*index=5*/f32[4,128]{1,0:T(4,128)}) custom-call(bf16[256,2048]{1,0:T(8,128)(2,1)} %get-tuple-element.23.normed, bf16[8,8,32,256]{3,2,1,0:T(8,128)(2,1)} %copy-done, ...), custom_call_target="tpu_custom_call" | custom-call | tf_op jit(solution)/shard_map/pallas_call | solution.py:37
  112.5 6.9 %all-to-all-start.3 = ((bf16[8,136,128]{2,1,0:T(8,128)(2,1)}), bf16[8,136,128]{2,1,0:T(8,128)(2,1)S(1)}, u32[]{:S(2)}, u32[]{:S(2)}) async-start(bf16[8,136,128]{2,1,0:T(8,128)(2,1)} %get-tuple-element.28), calls=%async_computation.3 | async-start | bytes 557056 | tf_op jit(solution)/shard_map/all_to_all | solution.py:257
  119.4 12.6 %all-to-all-done.3.got = bf16[8,136,128]{2,1,0:T(8,128)(2,1)S(1)} async-done(((bf16[8,136,128]{2,1,0:T(8,128)(2,1)}), bf16[8,136,128]{2,1,0:T(8,128)(2,1)S(1)}, u32[]{:S(2)}, u32[]{:S(2)}) %all-to-all-start.3) | async-done | bytes 278560 | tf_op jit(solution)/shard_map/all_to_all | solution.py:257
  132.1 0.7 copy-done.2
  132.8 1.8 shard_map.160
  134.5 3.4 %all-to-all-start.4 = ((bf16[8,136,128]{2,1,0:T(8,128)(2,1)}), bf16[8,136,128]{2,1,0:T(8,128)(2,1)S(1)}, u32[]{:S(2)}, u32[]{:S(2)}) async-start(bf16[8,136,128]{2,1,0:T(8,128)(2,1)} %get-tuple-element.29), calls=%async_computation.4 | async-start | bytes 557056 | tf_op jit(solution)/shard_map/all_to_all | solution.py:257
  138.0 2.0 %collective-permute-start.7 = (bf16[32,2048]{1,0:T(8,128)(2,1)}, bf16[32,2048]{1,0:T(8,128)(2,1)S(1)}, u32[]{:S(2)}, u32[]{:S(2)}) collective-permute-start(bf16[32,2048]{1,0:T(8,128)(2,1)} %get-tuple-element.22), channel_id=1, source_target_pairs={{0,8},{8,16},{16,24},{24,32},{32,40},{40,48},{48,56},{56,64},{64,7... | collective-permute-start | bytes 393224 | tf_op jit(solution)/shard_map/ppermute | solution.py:332
  140.0 2.8 %collective-permute-done.7.halo = bf16[32,2048]{1,0:T(8,128)(2,1)S(1)} collective-permute-done((bf16[32,2048]{1,0:T(8,128)(2,1)}, bf16[32,2048]{1,0:T(8,128)(2,1)S(1)}, u32[]{:S(2)}, u32[]{:S(2)}) %collective-permute-start.7) | collective-permute-done | bytes 131104 | tf_op jit(solution)/shard_map/ppermute | solution.py:332
  142.8 0.7 copy-done.3
  143.4 4.6 %shard_map.157 = (f32[256,256]{1,0:T(8,128)}, f32[8,2,256]{2,1,0:T(2,128)}) custom-call(bf16[32,2048]{1,0:T(8,128)(2,1)} %copy-done.3, bf16[256,2048]{1,0:T(8,128)(2,1)} %get-tuple-element.23.normed, bf16[2048,1152]{1,0:T(8,128)(2,1)} %all-gather.5.cloned.1.call-done.weights.w_rec.w_low.w_high, f32[31,256]{1,0:T(8,128)} %taps.1), custom_call_target="tpu_custom_call" | custom-call | tf_op jit(solution)/shard_map/pallas_call | solution.py:37
  148.0 5.1 %all-to-all-done.4.got = bf16[8,136,128]{2,1,0:T(8,128)(2,1)S(1)} async-done(((bf16[8,136,128]{2,1,0:T(8,128)(2,1)}), bf16[8,136,128]{2,1,0:T(8,128)(2,1)S(1)}, u32[]{:S(2)}, u32[]{:S(2)}) %all-to-all-start.4) | async-done | bytes 278560 | tf_op jit(solution)/shard_map/all_to_all | solution.py:257
  153.1 4.2 %all-to-all-start = ((f32[8,2,256]{2,1,0:T(2,128)}), f32[8,2,256]{2,1,0:T(2,128)S(1)}, u32[]{:S(2)}, u32[]{:S(2)}) async-start(f32[8,2,256]{2,1,0:T(2,128)} %get-tuple-element.25), calls=%async_computation | async-start | bytes 32768 | tf_op jit(solution)/shard_map/all_to_all | solution.py:257
  157.3 3.6 %shard_map.161.head_out = bf16[256,128]{1,0:T(8,128)(2,1)} custom-call(s32[1]{0:T(128)} %bitcast.4.position, bf16[8,136,128]{2,1,0:T(8,128)(2,1)} %copy-done.1, f32[128,128]{1,0:T(8,128)} %get-tuple-element.30.inner_state, f32[8,128]{1,0:T(8,128)} %get-tuple-element.31.inner_total, bf16[256,2048]{1,0:T(8,128)(2,1)} %get-tuple-element.23.normed, ...), custom_call_target="tpu_custom_call" | custom-call | tf_op jit(solution)/shard_map/pallas_call | solution.py:37
  160.9 1.0 all-to-all-done.stats
  161.9 0.6 copy-done.12
  162.5 3.5 %shard_map.162 = (bf16[2,128,384]{2,1,0:T(8,128)(2,1)}, bf16[128,2048]{1,0:T(8,128)(2,1)}) custom-call(s32[1]{0:T(128)} %bitcast.core, f32[8,2,256]{2,1,0:T(2,128)} %copy-done.12, f32[256,256]{1,0:T(8,128)} %get-tuple-element.26.conv, bf16[256,128]{1,0:T(8,128)(2,1)} %shard_map.161.head_out, f32[1,256]{1,0:T(1,128)} %bitcast.15, f32[1,256]{1,0:T(1,128)} %bitcast.16, ...), custom_call_target="tpu_custom_call" | custom-call | tf_op jit(solution)/shard_map/pallas_call | solution.py:37
  166.1 2.6 %collective-permute-start.8 = (bf16[128,2048]{1,0:T(8,128)(2,1)}, bf16[128,2048]{1,0:T(8,128)(2,1)S(1)}, u32[]{:S(2)}, u32[]{:S(2)}) collective-permute-start(bf16[128,2048]{1,0:T(8,128)(2,1)} %get-tuple-element.38), channel_id=1, source_target_pairs={{0,1},{1,0},{2,3},{3,2},{4,5},{5,4},{6,7},{7,6},{8,9},{9,8},{10,11... | collective-permute-start | bytes 1572872 | tf_op jit(solution)/shard_map/ppermute | solution.py:433
  168.7 2.8 %shard_map.163 = bf16[128,2048]{1,0:T(8,128)(2,1)} custom-call(s32[1]{0:T(128)} %bitcast.core, bf16[2,128,384]{2,1,0:T(8,128)(2,1)} %get-tuple-element.37.rows, bf16[2048,1152]{1,0:T(8,128)(2,1)} %all-gather.5.cloned.1.call-done.weights.w_rec.w_low.w_high, bf16[2048,1152]{1,0:T(8,128)(2,1)} %all-gather.5.cloned.1.call-done.weights.w_rec.w_low.w_high, ...), custom_call_target="tpu_custom_call" | custom-call | tf_op jit(solution)/shard_map/pallas_call | solution.py:37
  171.5 1.2 add_convert_fusion
  172.7 11.8 %all_to_all.31 = bf16[4,32,2048]{2,1,0:T(8,128)(2,1)S(1)} all-to-all(bf16[4,32,2048]{2,1,0:T(8,128)(2,1)S(1)} %bitcast.11), channel_id=1, replica_groups=mesh['sp_0'=8,'sp_1'=8,'x'=4,'core'=2] {'x'}, dimensions={0} | all-to-all | bytes 1048576 | tf_op jit(solution)/shard_map/all_to_all | solution.py:257
  184.4 0.7 reduce_sum.12
  (25 shorter events, 0.0 us)
Async XLA Ops:
  6.5 67.7 %copy-start.4 = (bf16[32,2048]{1,0:T(8,128)(2,1)S(1)}, bf16[32,2048]{1,0:T(8,128)(2,1)}, u32[]{:S(2)}) copy-start(bf16[32,2048]{1,0:T(8,128)(2,1)} %refs_0_.1) | copy-start | bytes 393220
  6.5 44.3 %all-gather.3.cloned.1.call-start = ((), (), s32[]{:S(2)}) async-start(), calls=%async_computation.6 | async-start | bytes 1179648 | tf_op jit(solution)/shard_map/all_gather | solution.py:307
  8.1 134.7 %all-gather.5.cloned.1.call-start = ((), (), s32[]{:S(2)}) async-start(), calls=%async_computation.7 | async-start | bytes 5308416 | tf_op jit(solution)/shard_map/all_gather | solution.py:317
  69.9 37.8 %all-to-all-start.2 = ((bf16[8,8,32,256]{3,2,1,0:T(8,128)(2,1)}), bf16[8,8,32,256]{3,2,1,0:T(8,128)(2,1)S(1)}, u32[]{:S(2)}, u32[]{:S(2)}) async-start(bf16[8,8,32,256]{3,2,1,0:T(8,128)(2,1)} %shard_map.158), calls=%async_computation.2 | async-start | bytes 2097152 | tf_op jit(solution)/shard_map/all_to_all | solution.py:257
  74.2 21.1 %collective-permute-start = (bf16[32,2048]{1,0:T(8,128)(2,1)S(1)}, bf16[32,2048]{1,0:T(8,128)(2,1)S(1)}, u32[]{:S(2)}, u32[]{:S(2)}) collective-permute-start(bf16[32,2048]{1,0:T(8,128)(2,1)S(1)} %copy-done.4), channel_id=1, source_target_pairs={{0,1},{1,2},{2,3},{3,4},{4,5},{5,6},{6,7},{7,0},{8,9},{9,10},{10,1... | collective-permute-start | bytes 393224 | tf_op jit(solution)/shard_map/ppermute | solution.py:264
  82.3 15.5 %collective-permute-start.1 = (bf16[32,2048]{1,0:T(8,128)(2,1)S(1)}, bf16[32,2048]{1,0:T(8,128)(2,1)S(1)}, u32[]{:S(2)}, u32[]{:S(2)}) collective-permute-start(bf16[32,2048]{1,0:T(8,128)(2,1)S(1)} %copy-done.4), channel_id=1, source_target_pairs={{0,2},{1,3},{2,4},{3,5},{4,6},{5,7},{6,0},{7,1},{8,10},{9,11},{10,... | collective-permute-start | bytes 393224 | tf_op jit(solution)/shard_map/ppermute | solution.py:264
  85.4 14.6 %collective-permute-start.2 = (bf16[32,2048]{1,0:T(8,128)(2,1)S(1)}, bf16[32,2048]{1,0:T(8,128)(2,1)S(1)}, u32[]{:S(2)}, u32[]{:S(2)}) collective-permute-start(bf16[32,2048]{1,0:T(8,128)(2,1)S(1)} %copy-done.4), channel_id=1, source_target_pairs={{0,3},{1,4},{2,5},{3,6},{4,7},{5,0},{6,1},{7,2},{8,11},{9,12},{10,... | collective-permute-start | bytes 393224 | tf_op jit(solution)/shard_map/ppermute | solution.py:264
  88.9 11.2 %collective-permute-start.3 = (bf16[32,2048]{1,0:T(8,128)(2,1)S(1)}, bf16[32,2048]{1,0:T(8,128)(2,1)S(1)}, u32[]{:S(2)}, u32[]{:S(2)}) collective-permute-start(bf16[32,2048]{1,0:T(8,128)(2,1)S(1)} %copy-done.4), channel_id=1, source_target_pairs={{0,4},{1,5},{2,6},{3,7},{4,0},{5,1},{6,2},{7,3},{8,12},{9,13},{10,... | collective-permute-start | bytes 393224 | tf_op jit(solution)/shard_map/ppermute | solution.py:264
  91.4 8.7 %collective-permute-start.4 = (bf16[32,2048]{1,0:T(8,128)(2,1)S(1)}, bf16[32,2048]{1,0:T(8,128)(2,1)S(1)}, u32[]{:S(2)}, u32[]{:S(2)}) collective-permute-start(bf16[32,2048]{1,0:T(8,128)(2,1)S(1)} %copy-done.4), channel_id=1, source_target_pairs={{0,5},{1,6},{2,7},{3,0},{4,1},{5,2},{6,3},{7,4},{8,13},{9,14},{10,... | collective-permute-start | bytes 393224 | tf_op jit(solution)/shard_map/ppermute | solution.py:264
  95.3 8.9 %copy-start.5 = (bf16[32,2048]{1,0:T(8,128)(2,1)}, bf16[32,2048]{1,0:T(8,128)(2,1)S(1)}, u32[]{:S(2)}) copy-start(bf16[32,2048]{1,0:T(8,128)(2,1)S(1)} %collective-permute-done.refs_1_) | copy-start | bytes 393220
  95.3 6.3 %collective-permute-start.5 = (bf16[32,2048]{1,0:T(8,128)(2,1)S(1)}, bf16[32,2048]{1,0:T(8,128)(2,1)S(1)}, u32[]{:S(2)}, u32[]{:S(2)}) collective-permute-start(bf16[32,2048]{1,0:T(8,128)(2,1)S(1)} %copy-done.4), channel_id=1, source_target_pairs={{0,6},{1,7},{2,0},{3,1},{4,2},{5,3},{6,4},{7,5},{8,14},{9,15},{10,... | collective-permute-start | bytes 393224 | tf_op jit(solution)/shard_map/ppermute | solution.py:264
  97.8 6.4 %copy-start.6 = (bf16[32,2048]{1,0:T(8,128)(2,1)}, bf16[32,2048]{1,0:T(8,128)(2,1)S(1)}, u32[]{:S(2)}) copy-start(bf16[32,2048]{1,0:T(8,128)(2,1)S(1)} %collective-permute-done.1.refs_2_) | copy-start | bytes 393220
  97.9 6.4 %collective-permute-start.6 = (bf16[32,2048]{1,0:T(8,128)(2,1)S(1)}, bf16[32,2048]{1,0:T(8,128)(2,1)S(1)}, u32[]{:S(2)}, u32[]{:S(2)}) collective-permute-start(bf16[32,2048]{1,0:T(8,128)(2,1)S(1)} %copy-done.4), channel_id=1, source_target_pairs={{0,7},{1,0},{2,1},{3,2},{4,3},{5,4},{6,5},{7,6},{8,15},{9,8},{10,9... | collective-permute-start | bytes 393224 | tf_op jit(solution)/shard_map/ppermute | solution.py:264
  100.0 4.2 %copy-start.7 = (bf16[32,2048]{1,0:T(8,128)(2,1)}, bf16[32,2048]{1,0:T(8,128)(2,1)S(1)}, u32[]{:S(2)}) copy-start(bf16[32,2048]{1,0:T(8,128)(2,1)S(1)} %collective-permute-done.2.refs_3_) | copy-start | bytes 393220
  100.0 4.2 %copy-start.8 = (bf16[32,2048]{1,0:T(8,128)(2,1)}, bf16[32,2048]{1,0:T(8,128)(2,1)S(1)}, u32[]{:S(2)}) copy-start(bf16[32,2048]{1,0:T(8,128)(2,1)S(1)} %collective-permute-done.3.refs_4_) | copy-start | bytes 393220
  100.1 4.2 %copy-start.9 = (bf16[32,2048]{1,0:T(8,128)(2,1)}, bf16[32,2048]{1,0:T(8,128)(2,1)S(1)}, u32[]{:S(2)}) copy-start(bf16[32,2048]{1,0:T(8,128)(2,1)S(1)} %collective-permute-done.4.refs_5_) | copy-start | bytes 393220
  101.6 2.7 %copy-start.10 = (bf16[32,2048]{1,0:T(8,128)(2,1)}, bf16[32,2048]{1,0:T(8,128)(2,1)S(1)}, u32[]{:S(2)}) copy-start(bf16[32,2048]{1,0:T(8,128)(2,1)S(1)} %collective-permute-done.5.refs_6_) | copy-start | bytes 393220
  104.2 0.7 copy-start.11
  107.7 1.0 copy-start
  112.5 19.5 %all-to-all-start.3 = ((bf16[8,136,128]{2,1,0:T(8,128)(2,1)}), bf16[8,136,128]{2,1,0:T(8,128)(2,1)S(1)}, u32[]{:S(2)}, u32[]{:S(2)}) async-start(bf16[8,136,128]{2,1,0:T(8,128)(2,1)} %get-tuple-element.28), calls=%async_computation.3 | async-start | bytes 557056 | tf_op jit(solution)/shard_map/all_to_all | solution.py:257
  132.1 0.7 copy-start.2
  134.5 18.6 %all-to-all-start.4 = ((bf16[8,136,128]{2,1,0:T(8,128)(2,1)}), bf16[8,136,128]{2,1,0:T(8,128)(2,1)S(1)}, u32[]{:S(2)}, u32[]{:S(2)}) async-start(bf16[8,136,128]{2,1,0:T(8,128)(2,1)} %get-tuple-element.29), calls=%async_computation.4 | async-start | bytes 557056 | tf_op jit(solution)/shard_map/all_to_all | solution.py:257
  138.0 4.8 %collective-permute-start.7 = (bf16[32,2048]{1,0:T(8,128)(2,1)}, bf16[32,2048]{1,0:T(8,128)(2,1)S(1)}, u32[]{:S(2)}, u32[]{:S(2)}) collective-permute-start(bf16[32,2048]{1,0:T(8,128)(2,1)} %get-tuple-element.22), channel_id=1, source_target_pairs={{0,8},{8,16},{16,24},{24,32},{32,40},{40,48},{48,56},{56,64},{64,7... | collective-permute-start | bytes 393224 | tf_op jit(solution)/shard_map/ppermute | solution.py:332
  142.8 0.7 copy-start.3
  153.1 4.2 %copy-start.1 = (bf16[8,136,128]{2,1,0:T(8,128)(2,1)}, bf16[8,136,128]{2,1,0:T(8,128)(2,1)S(1)}, u32[]{:S(2)}) copy-start(bf16[8,136,128]{2,1,0:T(8,128)(2,1)S(1)} %all-to-all-done.4.got) | copy-start | bytes 835588
  153.1 8.8 %all-to-all-start = ((f32[8,2,256]{2,1,0:T(2,128)}), f32[8,2,256]{2,1,0:T(2,128)S(1)}, u32[]{:S(2)}, u32[]{:S(2)}) async-start(f32[8,2,256]{2,1,0:T(2,128)} %get-tuple-element.25), calls=%async_computation | async-start | bytes 32768 | tf_op jit(solution)/shard_map/all_to_all | solution.py:257
  161.9 0.6 copy-start.12
  166.1 5.4 %collective-permute-start.8 = (bf16[128,2048]{1,0:T(8,128)(2,1)}, bf16[128,2048]{1,0:T(8,128)(2,1)S(1)}, u32[]{:S(2)}, u32[]{:S(2)}) collective-permute-start(bf16[128,2048]{1,0:T(8,128)(2,1)} %get-tuple-element.38), channel_id=1, source_target_pairs={{0,1},{1,0},{2,3},{3,2},{4,5},{5,4},{6,7},{7,6},{8,9},{9,8},{10,11... | collective-permute-start | bytes 1572872 | tf_op jit(solution)/shard_map/ppermute | solution.py:433
Sparse Core Ops, SparseCore 0:
  9.4 41.4 all-gather.2
  52.9 66.7 all-gather.4

commit v8 on v6

--- a/solution.py
+++ b/solution.py
@@ -41,16 +41,16 @@
     return [pl.BlockSpec(memory_space=pltpu.VMEM)] * count
 
 
-def first_body(gv, gg, q, g, wr, wc, f, v, operand, copies):
-    operand[...] = jnp.concatenate([w[...] for w in (gv, gg, q, g, wr, wc)], axis=1)
+def first_body(gv, gg, q, g, wr, wc, copies):
+    together = jnp.concatenate([w[...] for w in (gv, gg, q, g, wr, wc)], axis=1)
+    for k in range(copies.shape[0]):
+        copies[k] = together
+
+
+def second_body(f, v, copies):
     joined = jnp.concatenate([f[...], v[...]], axis=1)
     for k in range(copies.shape[0]):
         copies[k] = joined
-
-
-def again_body(value, copies):
-    for k in range(copies.shape[0]):
-        copies[k] = value[...]
 
 
 def norm_body(places, gain, *refs):
@@ -83,12 +83,7 @@
 
 def state_body(normed, weights, leak, shift, sent, value_out, key, totals, starts, befores):
     rows = normed.shape[0]
-    peers = weights.shape[0]
-    ordered = jnp.concatenate(
-        [weights[inner, outer] for outer in range(weights.shape[1]) for inner in range(peers)],
-        axis=0,
-    )
-    projected = jnp.dot(normed[...], ordered, preferred_element_type=F32).astype(BF16)
+    projected = jnp.dot(normed[...], weights[...], preferred_element_type=F32).astype(BF16)
     value = projected[:, HEAD_K:]
     value_out[...] = value
     in_gate = leak[...] * jax.nn.sigmoid(-projected[:, :HEAD_K].astype(F32))
@@ -287,21 +282,14 @@
     columns = (w_glu_value, w_glu_gate, w_query, w_outgate, w_out_rec.T, w_out_conv.T)
     glu_width = 2 * channels
     all_width = sum(w.shape[1] for w in columns)
-    outer_count = lax.axis_size(SP[0])
-    operand, copies = call(
-        first_body,
-        (
-            shape((depth, all_width), BF16),
-            shape((outer_count, depth, 2 * HEAD_K), BF16),
-        ),
-        *columns,
-        w_forget,
-        w_value,
-    )
-    gathered = lax.all_gather(operand, SP, axis=0, tiled=True)
-    column = swap(copies, SP[0])
-    copies = call(again_body, shape((inner_count, *column.shape), BF16), column)
-    state_weights = swap(copies, SP[1])
+    copies = call(first_body, shape((inner_count, depth, all_width), BF16), *columns)
+    staged = swap(copies, SP[1]).reshape(inner_count * depth, all_width)
+    gathered = lax.all_gather(staged, SP[0], axis=0, tiled=True)
+    count = lax.axis_size(SP)
+    copies = call(
+        second_body, shape((count, depth, 2 * HEAD_K), BF16), w_forget, w_value
+    )
+    state_weights = swap(copies, SP).reshape(count * depth, 2 * HEAD_K)
     pieces, places = shifted_around(tokens, TP)
     rows = group * share
     normed, tail = call(

time: 163 us -> 170 us (1.043)
  the two profiles are of different devices: /device:TPU:1 before, /device:TPU:24 now
where the time goes in v8:
time: 170 us; the launch traced here: 169 us
  starting transfers between devices  54.7 us (32%)
  blocking collectives  35.9 us (21%)
  waiting for transfers between devices  32.7 us (19%)
  Pallas kernels  26.4 us (16%)
  between operations  13.6 us (8%)
  local copies, waits for them, and re-layouts  2.97 us (2%)
  other arithmetic  2.42 us (1%)
    all_to_all x2, blocking collectives, swap(): return lax.all_to_all(value, axis, split_axis=0, concat_axis=0, tiled=True)  35.9 us
    all_to_all x4, starting transfers between devices, swap(): return lax.all_to_all(value, axis, split_axis=0, concat_axis=0, tiled=True)  31.5 us
    pallas_call x9, Pallas kernels, call(): pl.pallas_call(body, out_shape=outs, scratch_shapes=scratch, **specs)(*args)  26.4 us
    ppermute x7, starting transfers between devices, shifted_around(): lax.ppermute(value, axis, [(n, (n + k) % count) for n in range(count)])  18.2 us
    all_gather x1, waiting for transfers between devices, on_device(): gathered = lax.all_gather(staged, SP[0], axis=0, tiled=True)  12.6 us
    all_to_all x4, waiting for transfers between devices, swap(): return lax.all_to_all(value, axis, split_axis=0, concat_axis=0, tiled=True)  12.5 us
    ppermute x1, waiting for transfers between devices, on_device(): halo = lax.ppermute(tail, SP, [(k, k + 1) for k in range(count - 1)])  4.28 us
  transfers between devices with their start and end apart: 14, of which 8 were waited for; matrix products, arithmetic and copies ran while one was open for 0% of the time, Pallas kernels for 13%

profile of v8, /device:TPU:24, one launch (start us, length us, event | category | flops | bytes accessed | tf_op | source)
XLA Modules:
  0.0 168.7 jit_solution(5042471833820633650)
XLA Ops:
  6.5 1.7 %shard_map.155 = bf16[8,32,1152]{2,1,0:T(8,128)(2,1)} custom-call(bf16[32,256]{1,0:T(8,128)(2,1)} %gv.1, bf16[32,256]{1,0:T(8,128)(2,1)} %gg.1, bf16[32,128]{1,0:T(8,128)(2,1)} %q.1, bf16[32,128]{1,0:T(8,128)(2,1)} %g.1, bf16[32,128]{1,0:T(8,128)(2,1)} %bitcast.18, bf16[32,256]{1,0:T(8,128)(2,1)} %bitcast.16), custom_call_target="tpu_custom_call" | custom-call | tf_op jit(solution)/shard_map/pallas_call | solution.py:37
  8.2 22.9 %all_to_all.30 = bf16[8,32,1152]{2,1,0:T(8,128)(2,1)} all-to-all(bf16[8,32,1152]{2,1,0:T(8,128)(2,1)} %shard_map.155), channel_id=1, replica_groups=mesh['sp_0'=8,'sp_1'=8,'x'=4,'core'=2] {'sp_1'}, dimensions={0} | all-to-all | bytes 1179648 | tf_op jit(solution)/shard_map/all_to_all | solution.py:246
  31.1 0.0 all-gather.2.cloned.1.call-update
  31.1 1.8 %shard_map.157 = bf16[64,32,256]{2,1,0:T(8,128)(2,1)} custom-call(bf16[32,128]{1,0:T(8,128)(2,1)} %f.1, bf16[32,128]{1,0:T(8,128)(2,1)} %v.1), custom_call_target="tpu_custom_call" | custom-call | tf_op jit(solution)/shard_map/pallas_call | solution.py:37
  33.0 14.3 %all-to-all-start.2 = ((bf16[64,32,256]{2,1,0:T(8,128)(2,1)}), bf16[64,32,256]{2,1,0:T(8,128)(2,1)S(1)}, u32[]{:S(2)}, u32[]{:S(2)}) async-start(bf16[64,32,256]{2,1,0:T(8,128)(2,1)} %shard_map.157), calls=%async_computation.2 | async-start | bytes 2097152 | tf_op jit(solution)/shard_map/all_to_all | solution.py:246
  47.3 0.0 collective-permute-start
  47.3 3.4 %collective-permute-start.1 = (bf16[32,2048]{1,0:T(8,128)(2,1)S(1)}, bf16[32,2048]{1,0:T(8,128)(2,1)S(1)}, u32[]{:S(2)}, u32[]{:S(2)}) collective-permute-start(bf16[32,2048]{1,0:T(8,128)(2,1)S(1)} %copy-done.4), channel_id=1, source_target_pairs={{0,2},{1,3},{2,4},{3,5},{4,6},{5,7},{6,0},{7,1},{8,10},{9,11},{10,... | collective-permute-start | bytes 393224 | tf_op jit(solution)/shard_map/ppermute | solution.py:253
  50.7 4.0 %collective-permute-start.2 = (bf16[32,2048]{1,0:T(8,128)(2,1)S(1)}, bf16[32,2048]{1,0:T(8,128)(2,1)S(1)}, u32[]{:S(2)}, u32[]{:S(2)}) collective-permute-start(bf16[32,2048]{1,0:T(8,128)(2,1)S(1)} %copy-done.4), channel_id=1, source_target_pairs={{0,3},{1,4},{2,5},{3,6},{4,7},{5,0},{6,1},{7,2},{8,11},{9,12},{10,... | collective-permute-start | bytes 393224 | tf_op jit(solution)/shard_map/ppermute | solution.py:253
  54.8 3.9 %collective-permute-start.3 = (bf16[32,2048]{1,0:T(8,128)(2,1)S(1)}, bf16[32,2048]{1,0:T(8,128)(2,1)S(1)}, u32[]{:S(2)}, u32[]{:S(2)}) collective-permute-start(bf16[32,2048]{1,0:T(8,128)(2,1)S(1)} %copy-done.4), channel_id=1, source_target_pairs={{0,4},{1,5},{2,6},{3,7},{4,0},{5,1},{6,2},{7,3},{8,12},{9,13},{10,... | collective-permute-start | bytes 393224 | tf_op jit(solution)/shard_map/ppermute | solution.py:253
  58.7 3.5 %collective-permute-start.4 = (bf16[32,2048]{1,0:T(8,128)(2,1)S(1)}, bf16[32,2048]{1,0:T(8,128)(2,1)S(1)}, u32[]{:S(2)}, u32[]{:S(2)}) collective-permute-start(bf16[32,2048]{1,0:T(8,128)(2,1)S(1)} %copy-done.4), channel_id=1, source_target_pairs={{0,5},{1,6},{2,7},{3,0},{4,1},{5,2},{6,3},{7,4},{8,13},{9,14},{10,... | collective-permute-start | bytes 393224 | tf_op jit(solution)/shard_map/ppermute | solution.py:253
  62.2 0.0 collective-permute-done.refs_1_
  62.2 0.0 copy-start.5
  62.2 3.3 %collective-permute-start.5 = (bf16[32,2048]{1,0:T(8,128)(2,1)S(1)}, bf16[32,2048]{1,0:T(8,128)(2,1)S(1)}, u32[]{:S(2)}, u32[]{:S(2)}) collective-permute-start(bf16[32,2048]{1,0:T(8,128)(2,1)S(1)} %copy-done.4), channel_id=1, source_target_pairs={{0,6},{1,7},{2,0},{3,1},{4,2},{5,3},{6,4},{7,5},{8,14},{9,15},{10,... | collective-permute-start | bytes 393224 | tf_op jit(solution)/shard_map/ppermute | solution.py:253
  65.6 0.0 collective-permute-done.1.refs_2_
  65.6 0.0 collective-permute-start.6
  65.6 0.5 and_select_fusion.places
  66.1 0.0 collective-permute-done.2.refs_3_
  66.1 0.0 collective-permute-done.3.refs_4_
  66.2 0.2 collective-permute-done.4.refs_5_
  66.4 2.8 %collective-permute-done.5.refs_6_ = bf16[32,2048]{1,0:T(8,128)(2,1)S(1)} collective-permute-done((bf16[32,2048]{1,0:T(8,128)(2,1)S(1)}, bf16[32,2048]{1,0:T(8,128)(2,1)S(1)}, u32[]{:S(2)}, u32[]{:S(2)}) %collective-permute-start.5) | collective-permute-done | bytes 131104 | tf_op jit(solution)/shard_map/ppermute | solution.py:253
  69.2 0.2 collective-permute-done.6.refs_7_
  69.5 0.4 copy-done.10
  69.8 0.3 copy-done.11
  70.1 2.8 %shard_map.154 = (bf16[256,2048]{1,0:T(8,128)(2,1)}, bf16[32,2048]{1,0:T(8,128)(2,1)}) custom-call(s32[8]{0:T(128)} %and_select_fusion.places, f32[1,2048]{1,0:T(1,128)} %bitcast.17, bf16[32,2048]{1,0:T(8,128)(2,1)} %refs_0_.1, bf16[32,2048]{1,0:T(8,128)(2,1)} %copy-done.5, bf16[32,2048]{1,0:T(8,128)(2,1)} %copy-done.6, bf16[32,2048]{1,0:T(8,128)(2,1)} %copy-done.7, ...), custom_call_target="tpu_custom_call" | custom-call | tf_op jit(solution)/shard_map/pallas_call | solution.py:37
  72.8 3.5 %all-to-all-done.2 = bf16[64,32,256]{2,1,0:T(8,128)(2,1)S(1)} async-done(((bf16[64,32,256]{2,1,0:T(8,128)(2,1)}), bf16[64,32,256]{2,1,0:T(8,128)(2,1)S(1)}, u32[]{:S(2)}, u32[]{:S(2)}) %all-to-all-start.2) | async-done | bytes 1048608 | tf_op jit(solution)/shard_map/all_to_all | solution.py:246
  76.4 1.0 copy-done
  77.4 3.8 %shard_map.158 = (bf16[8,136,128]{2,1,0:T(8,128)(2,1)}, bf16[256,128]{1,0:T(8,128)(2,1)}, bf16[256,128]{1,0:T(8,128)(2,1)}, f32[256,128]{1,0:T(8,128)}, bf16[4,128,128]{2,1,0:T(8,128)(2,1)}, /*index=5*/f32[4,128]{1,0:T(4,128)}) custom-call(bf16[256,2048]{1,0:T(8,128)(2,1)} %get-tuple-element.21.normed, bf16[2048,256]{1,0:T(8,128)(2,1)} %bitcast.13, ...), custom_call_target="tpu_custom_call" | custom-call | tf_op jit(solution)/shard_map/pallas_call | solution.py:37
  81.2 7.0 %all-to-all-start.3 = ((bf16[8,136,128]{2,1,0:T(8,128)(2,1)}), bf16[8,136,128]{2,1,0:T(8,128)(2,1)S(1)}, u32[]{:S(2)}, u32[]{:S(2)}) async-start(bf16[8,136,128]{2,1,0:T(8,128)(2,1)} %get-tuple-element.24), calls=%async_computation.3 | async-start | bytes 557056 | tf_op jit(solution)/shard_map/all_to_all | solution.py:246
  88.2 7.2 %all-to-all-done.3.got = bf16[8,136,128]{2,1,0:T(8,128)(2,1)S(1)} async-done(((bf16[8,136,128]{2,1,0:T(8,128)(2,1)}), bf16[8,136,128]{2,1,0:T(8,128)(2,1)S(1)}, u32[]{:S(2)}, u32[]{:S(2)}) %all-to-all-start.3) | async-done | bytes 278560 | tf_op jit(solution)/shard_map/all_to_all | solution.py:246
  95.4 0.7 copy-done.2
  96.1 1.8 %shard_map.159 = (bf16[8,136,128]{2,1,0:T(8,128)(2,1)}, f32[128,128]{1,0:T(8,128)}, f32[8,128]{1,0:T(8,128)}) custom-call(s32[1]{0:T(128)} %bitcast.6.position, bf16[8,136,128]{2,1,0:T(8,128)(2,1)} %copy-done.2), custom_call_target="tpu_custom_call" | custom-call | tf_op jit(solution)/shard_map/pallas_call | solution.py:37
  97.9 5.9 %all-to-all-start.4 = ((bf16[8,136,128]{2,1,0:T(8,128)(2,1)}), bf16[8,136,128]{2,1,0:T(8,128)(2,1)S(1)}, u32[]{:S(2)}, u32[]{:S(2)}) async-start(bf16[8,136,128]{2,1,0:T(8,128)(2,1)} %get-tuple-element.25), calls=%async_computation.4 | async-start | bytes 557056 | tf_op jit(solution)/shard_map/all_to_all | solution.py:246
  103.8 3.0 %collective-permute-start.7 = (bf16[32,2048]{1,0:T(8,128)(2,1)}, bf16[32,2048]{1,0:T(8,128)(2,1)S(1)}, u32[]{:S(2)}, u32[]{:S(2)}) collective-permute-start(bf16[32,2048]{1,0:T(8,128)(2,1)} %get-tuple-element.20), channel_id=1, source_target_pairs={{0,8},{8,16},{16,24},{24,32},{32,40},{40,48},{48,56},{56,64},{64,7... | collective-permute-start | bytes 393224 | tf_op jit(solution)/shard_map/ppermute | solution.py:304
  106.9 4.3 %collective-permute-done.7.halo = bf16[32,2048]{1,0:T(8,128)(2,1)S(1)} collective-permute-done((bf16[32,2048]{1,0:T(8,128)(2,1)}, bf16[32,2048]{1,0:T(8,128)(2,1)S(1)}, u32[]{:S(2)}, u32[]{:S(2)}) %collective-permute-start.7) | collective-permute-done | bytes 131104 | tf_op jit(solution)/shard_map/ppermute | solution.py:304
  111.2 12.6 %all-gather.2.cloned.1.call-done.weights.w_rec.w_low.w_high = bf16[2048,1152]{1,0:T(8,128)(2,1)} async-done(((bf16[256,1152]{1,0:T(8,128)(2,1)}), bf16[2048,1152]{1,0:T(8,128)(2,1)}) %all-gather.2.cloned.1.call-update) | async-done | bytes 4718608 | tf_op jit(solution)/shard_map/all_gather | solution.py:287
  123.8 4.6 %shard_map.156 = (f32[256,256]{1,0:T(8,128)}, f32[8,2,256]{2,1,0:T(2,128)}) custom-call(bf16[32,2048]{1,0:T(8,128)(2,1)} %copy-done.3, bf16[256,2048]{1,0:T(8,128)(2,1)} %get-tuple-element.21.normed, bf16[2048,1152]{1,0:T(8,128)(2,1)} %all-gather.2.cloned.1.call-done.weights.w_rec.w_low.w_high, f32[31,256]{1,0:T(8,128)} %taps.1), custom_call_target="tpu_custom_call" | custom-call | tf_op jit(solution)/shard_map/pallas_call | solution.py:37
  128.3 0.0 all-to-all-done.4.got
  128.4 4.3 %all-to-all-start.1 = ((f32[8,2,256]{2,1,0:T(2,128)}), f32[8,2,256]{2,1,0:T(2,128)S(1)}, u32[]{:S(2)}, u32[]{:S(2)}) async-start(f32[8,2,256]{2,1,0:T(2,128)} %get-tuple-element.22), calls=%async_computation.1 | async-start | bytes 32768 | tf_op jit(solution)/shard_map/all_to_all | solution.py:246
  132.7 3.6 %shard_map.160.head_out = bf16[256,128]{1,0:T(8,128)(2,1)} custom-call(s32[1]{0:T(128)} %bitcast.5.position, bf16[8,136,128]{2,1,0:T(8,128)(2,1)} %copy-done.1, f32[128,128]{1,0:T(8,128)} %get-tuple-element.26.inner_state, f32[8,128]{1,0:T(8,128)} %get-tuple-element.27.inner_total, bf16[256,2048]{1,0:T(8,128)(2,1)} %get-tuple-element.21.normed, ...), custom_call_target="tpu_custom_call" | custom-call | tf_op jit(solution)/shard_map/pallas_call | solution.py:37
  136.3 1.7 %all-to-all-done.1.stats = f32[8,2,256]{2,1,0:T(2,128)S(1)} async-done(((f32[8,2,256]{2,1,0:T(2,128)}), f32[8,2,256]{2,1,0:T(2,128)S(1)}, u32[]{:S(2)}, u32[]{:S(2)}) %all-to-all-start.1) | async-done | bytes 16416 | tf_op jit(solution)/shard_map/all_to_all | solution.py:246
  138.0 0.6 copy-done.12
  138.6 3.6 %shard_map.161 = (bf16[2,128,384]{2,1,0:T(8,128)(2,1)}, bf16[128,2048]{1,0:T(8,128)(2,1)}) custom-call(s32[1]{0:T(128)} %bitcast.core, f32[8,2,256]{2,1,0:T(2,128)} %copy-done.12, f32[256,256]{1,0:T(8,128)} %get-tuple-element.23.conv, bf16[256,128]{1,0:T(8,128)(2,1)} %shard_map.160.head_out, f32[1,256]{1,0:T(1,128)} %bitcast.19, f32[1,256]{1,0:T(1,128)} %bitcast.20, ...), custom_call_target="tpu_custom_call" | custom-call | tf_op jit(solution)/shard_map/pallas_call | solution.py:37
  142.2 1.9 %collective-permute-start.8 = (bf16[128,2048]{1,0:T(8,128)(2,1)}, bf16[128,2048]{1,0:T(8,128)(2,1)S(1)}, u32[]{:S(2)}, u32[]{:S(2)}) collective-permute-start(bf16[128,2048]{1,0:T(8,128)(2,1)} %get-tuple-element.34), channel_id=1, source_target_pairs={{0,1},{1,0},{2,3},{3,2},{4,5},{5,4},{6,7},{7,6},{8,9},{9,8},{10,11... | collective-permute-start | bytes 1572872 | tf_op jit(solution)/shard_map/ppermute | solution.py:405
  144.1 2.8 %shard_map.162 = bf16[128,2048]{1,0:T(8,128)(2,1)} custom-call(s32[1]{0:T(128)} %bitcast.core, bf16[2,128,384]{2,1,0:T(8,128)(2,1)} %get-tuple-element.33.rows, bf16[2048,1152]{1,0:T(8,128)(2,1)} %all-gather.2.cloned.1.call-done.weights.w_rec.w_low.w_high, bf16[2048,1152]{1,0:T(8,128)(2,1)} %all-gather.2.cloned.1.call-done.weights.w_rec.w_low.w_high, ...), custom_call_target="tpu_custom_call" | custom-call | tf_op jit(solution)/shard_map/pallas_call | solution.py:37
  146.9 0.0 collective-permute-done.8
  146.9 1.2 add_convert_fusion
  148.1 13.0 %all_to_all.31 = bf16[4,32,2048]{2,1,0:T(8,128)(2,1)S(1)} all-to-all(bf16[4,32,2048]{2,1,0:T(8,128)(2,1)S(1)} %bitcast.15), channel_id=1, replica_groups=mesh['sp_0'=8,'sp_1'=8,'x'=4,'core'=2] {'x'}, dimensions={0} | all-to-all | bytes 1048576 | tf_op jit(solution)/shard_map/all_to_all | solution.py:246
  161.1 0.7 reduce_sum.12
  (21 shorter events, 0.0 us)
Async XLA Ops:
  6.5 40.8 %copy-start.4 = (bf16[32,2048]{1,0:T(8,128)(2,1)S(1)}, bf16[32,2048]{1,0:T(8,128)(2,1)}, u32[]{:S(2)}) copy-start(bf16[32,2048]{1,0:T(8,128)(2,1)} %refs_0_.1) | copy-start | bytes 393220
  6.5 117.3 %all-gather.2.cloned.1.call-start = ((), (), s32[]{:S(2)}) async-start(), calls=%async_computation.6 | async-start | bytes 5308416 | tf_op jit(solution)/shard_map/all_gather | solution.py:287
  33.0 43.4 %all-to-all-start.2 = ((bf16[64,32,256]{2,1,0:T(8,128)(2,1)}), bf16[64,32,256]{2,1,0:T(8,128)(2,1)S(1)}, u32[]{:S(2)}, u32[]{:S(2)}) async-start(bf16[64,32,256]{2,1,0:T(8,128)(2,1)} %shard_map.157), calls=%async_computation.2 | async-start | bytes 2097152 | tf_op jit(solution)/shard_map/all_to_all | solution.py:246
  47.3 14.9 %collective-permute-start = (bf16[32,2048]{1,0:T(8,128)(2,1)S(1)}, bf16[32,2048]{1,0:T(8,128)(2,1)S(1)}, u32[]{:S(2)}, u32[]{:S(2)}) collective-permute-start(bf16[32,2048]{1,0:T(8,128)(2,1)S(1)} %copy-done.4), channel_id=1, source_target_pairs={{0,1},{1,2},{2,3},{3,4},{4,5},{5,6},{6,7},{7,0},{8,9},{9,10},{10,1... | collective-permute-start | bytes 393224 | tf_op jit(solution)/shard_map/ppermute | solution.py:253
  47.3 18.2 %collective-permute-start.1 = (bf16[32,2048]{1,0:T(8,128)(2,1)S(1)}, bf16[32,2048]{1,0:T(8,128)(2,1)S(1)}, u32[]{:S(2)}, u32[]{:S(2)}) collective-permute-start(bf16[32,2048]{1,0:T(8,128)(2,1)S(1)} %copy-done.4), channel_id=1, source_target_pairs={{0,2},{1,3},{2,4},{3,5},{4,6},{5,7},{6,0},{7,1},{8,10},{9,11},{10,... | collective-permute-start | bytes 393224 | tf_op jit(solution)/shard_map/ppermute | solution.py:253
  50.7 15.4 %collective-permute-start.2 = (bf16[32,2048]{1,0:T(8,128)(2,1)S(1)}, bf16[32,2048]{1,0:T(8,128)(2,1)S(1)}, u32[]{:S(2)}, u32[]{:S(2)}) collective-permute-start(bf16[32,2048]{1,0:T(8,128)(2,1)S(1)} %copy-done.4), channel_id=1, source_target_pairs={{0,3},{1,4},{2,5},{3,6},{4,7},{5,0},{6,1},{7,2},{8,11},{9,12},{10,... | collective-permute-start | bytes 393224 | tf_op jit(solution)/shard_map/ppermute | solution.py:253
  54.8 11.4 %collective-permute-start.3 = (bf16[32,2048]{1,0:T(8,128)(2,1)S(1)}, bf16[32,2048]{1,0:T(8,128)(2,1)S(1)}, u32[]{:S(2)}, u32[]{:S(2)}) collective-permute-start(bf16[32,2048]{1,0:T(8,128)(2,1)S(1)} %copy-done.4), channel_id=1, source_target_pairs={{0,4},{1,5},{2,6},{3,7},{4,0},{5,1},{6,2},{7,3},{8,12},{9,13},{10,... | collective-permute-start | bytes 393224 | tf_op jit(solution)/shard_map/ppermute | solution.py:253
  58.7 7.7 %collective-permute-start.4 = (bf16[32,2048]{1,0:T(8,128)(2,1)S(1)}, bf16[32,2048]{1,0:T(8,128)(2,1)S(1)}, u32[]{:S(2)}, u32[]{:S(2)}) collective-permute-start(bf16[32,2048]{1,0:T(8,128)(2,1)S(1)} %copy-done.4), channel_id=1, source_target_pairs={{0,5},{1,6},{2,7},{3,0},{4,1},{5,2},{6,3},{7,4},{8,13},{9,14},{10,... | collective-permute-start | bytes 393224 | tf_op jit(solution)/shard_map/ppermute | solution.py:253
  62.2 7.2 %copy-start.5 = (bf16[32,2048]{1,0:T(8,128)(2,1)}, bf16[32,2048]{1,0:T(8,128)(2,1)S(1)}, u32[]{:S(2)}) copy-start(bf16[32,2048]{1,0:T(8,128)(2,1)S(1)} %collective-permute-done.refs_1_) | copy-start | bytes 393220
  62.2 7.0 %collective-permute-start.5 = (bf16[32,2048]{1,0:T(8,128)(2,1)S(1)}, bf16[32,2048]{1,0:T(8,128)(2,1)S(1)}, u32[]{:S(2)}, u32[]{:S(2)}) collective-permute-start(bf16[32,2048]{1,0:T(8,128)(2,1)S(1)} %copy-done.4), channel_id=1, source_target_pairs={{0,6},{1,7},{2,0},{3,1},{4,2},{5,3},{6,4},{7,5},{8,14},{9,15},{10,... | collective-permute-start | bytes 393224 | tf_op jit(solution)/shard_map/ppermute | solution.py:253
  65.6 3.9 %copy-start.6 = (bf16[32,2048]{1,0:T(8,128)(2,1)}, bf16[32,2048]{1,0:T(8,128)(2,1)S(1)}, u32[]{:S(2)}) copy-start(bf16[32,2048]{1,0:T(8,128)(2,1)S(1)} %collective-permute-done.1.refs_2_) | copy-start | bytes 393220
  65.6 3.8 %collective-permute-start.6 = (bf16[32,2048]{1,0:T(8,128)(2,1)S(1)}, bf16[32,2048]{1,0:T(8,128)(2,1)S(1)}, u32[]{:S(2)}, u32[]{:S(2)}) collective-permute-start(bf16[32,2048]{1,0:T(8,128)(2,1)S(1)} %copy-done.4), channel_id=1, source_target_pairs={{0,7},{1,0},{2,1},{3,2},{4,3},{5,4},{6,5},{7,6},{8,15},{9,8},{10,9... | collective-permute-start | bytes 393224 | tf_op jit(solution)/shard_map/ppermute | solution.py:253
  66.1 3.3 %copy-start.7 = (bf16[32,2048]{1,0:T(8,128)(2,1)}, bf16[32,2048]{1,0:T(8,128)(2,1)S(1)}, u32[]{:S(2)}) copy-start(bf16[32,2048]{1,0:T(8,128)(2,1)S(1)} %collective-permute-done.2.refs_3_) | copy-start | bytes 393220
  66.1 3.3 %copy-start.8 = (bf16[32,2048]{1,0:T(8,128)(2,1)}, bf16[32,2048]{1,0:T(8,128)(2,1)S(1)}, u32[]{:S(2)}) copy-start(bf16[32,2048]{1,0:T(8,128)(2,1)S(1)} %collective-permute-done.3.refs_4_) | copy-start | bytes 393220
  66.4 3.1 %copy-start.9 = (bf16[32,2048]{1,0:T(8,128)(2,1)}, bf16[32,2048]{1,0:T(8,128)(2,1)S(1)}, u32[]{:S(2)}) copy-start(bf16[32,2048]{1,0:T(8,128)(2,1)S(1)} %collective-permute-done.4.refs_5_) | copy-start | bytes 393220
  69.2 0.6 copy-start.10
  69.4 0.7 copy-start.11
  76.4 1.0 copy-start
  81.2 14.3 %all-to-all-start.3 = ((bf16[8,136,128]{2,1,0:T(8,128)(2,1)}), bf16[8,136,128]{2,1,0:T(8,128)(2,1)S(1)}, u32[]{:S(2)}, u32[]{:S(2)}) async-start(bf16[8,136,128]{2,1,0:T(8,128)(2,1)} %get-tuple-element.24), calls=%async_computation.3 | async-start | bytes 557056 | tf_op jit(solution)/shard_map/all_to_all | solution.py:246
  95.4 0.7 copy-start.2
  97.9 30.4 %all-to-all-start.4 = ((bf16[8,136,128]{2,1,0:T(8,128)(2,1)}), bf16[8,136,128]{2,1,0:T(8,128)(2,1)S(1)}, u32[]{:S(2)}, u32[]{:S(2)}) async-start(bf16[8,136,128]{2,1,0:T(8,128)(2,1)} %get-tuple-element.25), calls=%async_computation.4 | async-start | bytes 557056 | tf_op jit(solution)/shard_map/all_to_all | solution.py:246
  103.8 7.3 %collective-permute-start.7 = (bf16[32,2048]{1,0:T(8,128)(2,1)}, bf16[32,2048]{1,0:T(8,128)(2,1)S(1)}, u32[]{:S(2)}, u32[]{:S(2)}) collective-permute-start(bf16[32,2048]{1,0:T(8,128)(2,1)} %get-tuple-element.20), channel_id=1, source_target_pairs={{0,8},{8,16},{16,24},{24,32},{32,40},{40,48},{48,56},{56,64},{64,7... | collective-permute-start | bytes 393224 | tf_op jit(solution)/shard_map/ppermute | solution.py:304
  111.2 12.6 %copy-start.3 = (bf16[32,2048]{1,0:T(8,128)(2,1)}, bf16[32,2048]{1,0:T(8,128)(2,1)S(1)}, u32[]{:S(2)}) copy-start(bf16[32,2048]{1,0:T(8,128)(2,1)S(1)} %collective-permute-done.7.halo) | copy-start | bytes 393220
  128.3 4.3 %copy-start.1 = (bf16[8,136,128]{2,1,0:T(8,128)(2,1)}, bf16[8,136,128]{2,1,0:T(8,128)(2,1)S(1)}, u32[]{:S(2)}) copy-start(bf16[8,136,128]{2,1,0:T(8,128)(2,1)S(1)} %all-to-all-done.4.got) | copy-start | bytes 835588
  128.4 9.7 %all-to-all-start.1 = ((f32[8,2,256]{2,1,0:T(2,128)}), f32[8,2,256]{2,1,0:T(2,128)S(1)}, u32[]{:S(2)}, u32[]{:S(2)}) async-start(f32[8,2,256]{2,1,0:T(2,128)} %get-tuple-element.22), calls=%async_computation.1 | async-start | bytes 32768 | tf_op jit(solution)/shard_map/all_to_all | solution.py:246
  138.0 0.6 copy-start.12
  142.2 4.7 %collective-permute-start.8 = (bf16[128,2048]{1,0:T(8,128)(2,1)}, bf16[128,2048]{1,0:T(8,128)(2,1)S(1)}, u32[]{:S(2)}, u32[]{:S(2)}) collective-permute-start(bf16[128,2048]{1,0:T(8,128)(2,1)} %get-tuple-element.34), channel_id=1, source_target_pairs={{0,1},{1,0},{2,3},{3,2},{4,5},{5,4},{6,7},{7,6},{8,9},{9,8},{10,11... | collective-permute-start | bytes 1572872 | tf_op jit(solution)/shard_map/ppermute | solution.py:405
Sparse Core Ops, SparseCore 0:
  31.3 92.4 all-gather.1

commit v9 on v6

--- a/solution.py
+++ b/solution.py
@@ -204,7 +204,7 @@
         stats[k] = both
 
 
-def out_body(core, stats, conv, head_out, ln_gain, ln_bias, w_rec, w_low, w_high, rows_out, out):
+def out_body(core, stats, conv, head_out, ln_gain, ln_bias, w_rec, w_low, w_high, out, own, rows_out):
     channels = conv.shape[1]
     share = conv.shape[0] // stats.shape[0]
     both = stats[0]
@@ -234,6 +234,7 @@
         rows_out[k % 2, at, :HEAD_K] = head_out[piece]
         rows_out[k % 2, at, HEAD_K:] = conv_out[piece]
     out[...] = product(rows_out[1 - core[0]], w_rec, w_low, w_high)
+    own[...] = product(rows_out[core[0]], w_rec, w_low, w_high)
 
 
 def product(rows, w_rec, w_low, w_high):
@@ -241,10 +242,6 @@
     mixed = mixed + dot_nt(rows[:, HEAD_K : 2 * HEAD_K], w_low[...])
     mixed = mixed + dot_nt(rows[:, 2 * HEAD_K :], w_high[...])
     return mixed.astype(BF16)
-
-
-def own_body(core, rows, w_rec, w_low, w_high, out):
-    out[...] = product(rows[core[0]], w_rec, w_low, w_high)
 
 
 def swap(value, axis):
@@ -392,9 +389,9 @@
     core = lax.axis_index(TP[1]).reshape(1)
     weights = [gathered] * 3
     weight_specs = [part(HEAD_K, first + k) for k in range(3)]
-    mixed_rows, sent = call(
+    sent, own = call(
         out_body,
-        (shape((2, half, width), BF16), shape((half, features), BF16)),
+        (shape((half, features), BF16),) * 2,
         core,
         stats,
         conv,
@@ -412,19 +409,10 @@
             full(1, channels),
             *weight_specs,
         ],
-        out_specs=(full(2, half, width), full(half, features)),
+        out_specs=(full(half, features),) * 2,
+        scratch=(pltpu.VMEM((2, half, width), BF16),),
     )
     received = lax.ppermute(sent, TP[1], [(0, 1), (1, 0)])
-    own = call(
-        own_body,
-        shape((half, features), BF16),
-        core,
-        mixed_rows,
-        *weights,
-        grid=(1,),
-        in_specs=[smem, full(2, half, width), *weight_specs],
-        out_specs=full(half, features),
-    )
     pair = (own.astype(F32) + received.astype(F32)).astype(BF16)
     arrived = swap(pair.reshape(group // 2, share, features), TP[0])
     return arrived.astype(F32).sum(axis=0).astype(BF16)

time: 163 us -> 162 us (level)
  Pallas kernels: 26.3 us -> 23.8 us
  waiting for transfers between devices: 37.7 us -> 39.4 us
    pallas_call x9 -> x8, Pallas kernels: 26.3 us -> 23.8 us  [call(): pl.pallas_call(body, out_shape=outs, scratch_shapes=scratch, **specs)(*args)]
    ppermute x1, waiting for transfers between devices: 0.01 us -> 1.73 us  [on_device(): received = lax.ppermute(sent, TP[1], [(0, 1), (1, 0)])]
  transfers between devices with their start and end apart: 14 -> 14, of which waited for: 7 -> 8; matrix products, arithmetic and copies ran while one was open for 0% -> 0% of each run, Pallas kernels for 13% -> 11%
where the time goes in v9:
time: 162 us; the launch traced here: 161 us
  starting transfers between devices  48.8 us (30%)
  waiting for transfers between devices  39.4 us (24%)
  blocking collectives  29.9 us (18%)
  Pallas kernels  23.8 us (15%)
  between operations  13.6 us (8%)
  local copies, waits for them, and re-layouts  2.98 us (2%)
  other arithmetic  2.48 us (2%)
    all_to_all x2, blocking collectives, swap(): return lax.all_to_all(value, axis, split_axis=0, concat_axis=0, tiled=True)  29.9 us
    pallas_call x8, Pallas kernels, call(): pl.pallas_call(body, out_shape=outs, scratch_shapes=scratch, **specs)(*args)  23.8 us
    all_to_all x4, starting transfers between devices, swap(): return lax.all_to_all(value, axis, split_axis=0, concat_axis=0, tiled=True)  23.4 us
    ppermute x7, starting transfers between devices, shifted_around(): lax.ppermute(value, axis, [(n, (n + k) % count) for n in range(count)])  20.8 us
    all_to_all x4, waiting for transfers between devices, swap(): return lax.all_to_all(value, axis, split_axis=0, concat_axis=0, tiled=True)  18.8 us
    all_gather x1, waiting for transfers between devices, on_device(): gathered = lax.all_gather(operand, SP, axis=0, tiled=True)  8.62 us
    ppermute x1, waiting for transfers between devices, on_device(): halo = lax.ppermute(tail, SP, [(k, k + 1) for k in range(count - 1)])  5.93 us
    ppermute x7, waiting for transfers between devices, shifted_around(): lax.ppermute(value, axis, [(n, (n + k) % count) for n in range(count)])  4.31 us
  transfers between devices with their start and end apart: 14, of which 8 were waited for; matrix products, arithmetic and copies ran while one was open for 0% of the time, Pallas kernels for 11%

profile of v9, /device:TPU:1, one launch (start us, length us, event | category | flops | bytes accessed | tf_op | source)
XLA Modules:
  0.0 161.0 jit_solution(10341240073813311119)
XLA Ops:
  6.5 1.5 shard_map.155
  8.0 0.0 all-gather.2.cloned.1.call-update
  8.1 18.7 %all_to_all.30.value = bf16[8,32,256]{2,1,0:T(8,128)(2,1)} all-to-all(bf16[8,32,256]{2,1,0:T(8,128)(2,1)} %get-tuple-element.27), channel_id=1, replica_groups=mesh['sp_0'=8,'sp_1'=8,'x'=4,'core'=2] {'sp_0'}, dimensions={0} | all-to-all | bytes 262144 | tf_op jit(solution)/shard_map/all_to_all | solution.py:248
  26.8 2.0 %shard_map.157 = bf16[8,8,32,256]{3,2,1,0:T(8,128)(2,1)} custom-call(bf16[8,32,256]{2,1,0:T(8,128)(2,1)} %all_to_all.30.value), custom_call_target="tpu_custom_call" | custom-call | tf_op jit(solution)/shard_map/pallas_call | solution.py:37
  28.8 6.8 %all-to-all-start.2 = ((bf16[8,8,32,256]{3,2,1,0:T(8,128)(2,1)}), bf16[8,8,32,256]{3,2,1,0:T(8,128)(2,1)S(1)}, u32[]{:S(2)}, u32[]{:S(2)}) async-start(bf16[8,8,32,256]{3,2,1,0:T(8,128)(2,1)} %shard_map.157), calls=%async_computation.2 | async-start | bytes 2097152 | tf_op jit(solution)/shard_map/all_to_all | solution.py:248
  35.6 3.7 %collective-permute-start = (bf16[32,2048]{1,0:T(8,128)(2,1)}, bf16[32,2048]{1,0:T(8,128)(2,1)S(1)}, u32[]{:S(2)}, u32[]{:S(2)}) collective-permute-start(bf16[32,2048]{1,0:T(8,128)(2,1)} %refs_0_.1), channel_id=1, source_target_pairs={{0,1},{1,2},{2,3},{3,4},{4,5},{5,6},{6,7},{7,0},{8,9},{9,10},{10,1... | collective-permute-start | bytes 393224 | tf_op jit(solution)/shard_map/ppermute | solution.py:255
  39.3 3.1 %collective-permute-start.1 = (bf16[32,2048]{1,0:T(8,128)(2,1)}, bf16[32,2048]{1,0:T(8,128)(2,1)S(1)}, u32[]{:S(2)}, u32[]{:S(2)}) collective-permute-start(bf16[32,2048]{1,0:T(8,128)(2,1)} %refs_0_.1), channel_id=1, source_target_pairs={{0,2},{1,3},{2,4},{3,5},{4,6},{5,7},{6,0},{7,1},{8,10},{9,11},{10,... | collective-permute-start | bytes 393224 | tf_op jit(solution)/shard_map/ppermute | solution.py:255
  42.4 3.5 %collective-permute-start.2 = (bf16[32,2048]{1,0:T(8,128)(2,1)}, bf16[32,2048]{1,0:T(8,128)(2,1)S(1)}, u32[]{:S(2)}, u32[]{:S(2)}) collective-permute-start(bf16[32,2048]{1,0:T(8,128)(2,1)} %refs_0_.1), channel_id=1, source_target_pairs={{0,3},{1,4},{2,5},{3,6},{4,7},{5,0},{6,1},{7,2},{8,11},{9,12},{10,... | collective-permute-start | bytes 393224 | tf_op jit(solution)/shard_map/ppermute | solution.py:255
  45.8 2.4 %collective-permute-start.3 = (bf16[32,2048]{1,0:T(8,128)(2,1)}, bf16[32,2048]{1,0:T(8,128)(2,1)S(1)}, u32[]{:S(2)}, u32[]{:S(2)}) collective-permute-start(bf16[32,2048]{1,0:T(8,128)(2,1)} %refs_0_.1), channel_id=1, source_target_pairs={{0,4},{1,5},{2,6},{3,7},{4,0},{5,1},{6,2},{7,3},{8,12},{9,13},{10,... | collective-permute-start | bytes 393224 | tf_op jit(solution)/shard_map/ppermute | solution.py:255
  48.3 3.9 %collective-permute-start.4 = (bf16[32,2048]{1,0:T(8,128)(2,1)}, bf16[32,2048]{1,0:T(8,128)(2,1)S(1)}, u32[]{:S(2)}, u32[]{:S(2)}) collective-permute-start(bf16[32,2048]{1,0:T(8,128)(2,1)} %refs_0_.1), channel_id=1, source_target_pairs={{0,5},{1,6},{2,7},{3,0},{4,1},{5,2},{6,3},{7,4},{8,13},{9,14},{10,... | collective-permute-start | bytes 393224 | tf_op jit(solution)/shard_map/ppermute | solution.py:255
  52.2 0.0 collective-permute-done.refs_1_
  52.2 0.0 copy-start.4
  52.2 2.6 %collective-permute-start.5 = (bf16[32,2048]{1,0:T(8,128)(2,1)}, bf16[32,2048]{1,0:T(8,128)(2,1)S(1)}, u32[]{:S(2)}, u32[]{:S(2)}) collective-permute-start(bf16[32,2048]{1,0:T(8,128)(2,1)} %refs_0_.1), channel_id=1, source_target_pairs={{0,6},{1,7},{2,0},{3,1},{4,2},{5,3},{6,4},{7,5},{8,14},{9,15},{10,... | collective-permute-start | bytes 393224 | tf_op jit(solution)/shard_map/ppermute | solution.py:255
  54.8 0.0 collective-permute-done.1.refs_2_
  54.8 0.0 copy-start.5
  54.8 1.6 %collective-permute-start.6 = (bf16[32,2048]{1,0:T(8,128)(2,1)}, bf16[32,2048]{1,0:T(8,128)(2,1)S(1)}, u32[]{:S(2)}, u32[]{:S(2)}) collective-permute-start(bf16[32,2048]{1,0:T(8,128)(2,1)} %refs_0_.1), channel_id=1, source_target_pairs={{0,7},{1,0},{2,1},{3,2},{4,3},{5,4},{6,5},{7,6},{8,15},{9,8},{10,9... | collective-permute-start | bytes 393224 | tf_op jit(solution)/shard_map/ppermute | solution.py:255
  56.4 0.6 and_select_fusion.places
  57.0 0.0 collective-permute-done.2.refs_3_
  57.0 0.0 collective-permute-done.3.refs_4_
  57.0 0.0 collective-permute-done.4.refs_5_
  57.1 1.6 collective-permute-done.5.refs_6_
  58.7 2.7 %collective-permute-done.6.refs_7_ = bf16[32,2048]{1,0:T(8,128)(2,1)S(1)} collective-permute-done((bf16[32,2048]{1,0:T(8,128)(2,1)}, bf16[32,2048]{1,0:T(8,128)(2,1)S(1)}, u32[]{:S(2)}, u32[]{:S(2)}) %collective-permute-start.6) | collective-permute-done | bytes 131104 | tf_op jit(solution)/shard_map/ppermute | solution.py:255
  61.4 0.0 copy-done.5
  61.4 0.6 copy-done.10
  62.0 2.7 %shard_map.154 = (bf16[256,2048]{1,0:T(8,128)(2,1)}, bf16[32,2048]{1,0:T(8,128)(2,1)}) custom-call(s32[8]{0:T(128)} %and_select_fusion.places, f32[1,2048]{1,0:T(1,128)} %bitcast.13, bf16[32,2048]{1,0:T(8,128)(2,1)} %refs_0_.1, bf16[32,2048]{1,0:T(8,128)(2,1)} %copy-done.4, bf16[32,2048]{1,0:T(8,128)(2,1)} %copy-done.5, bf16[32,2048]{1,0:T(8,128)(2,1)} %copy-done.6, ...), custom_call_target="tpu_custom_call" | custom-call | tf_op jit(solution)/shard_map/pallas_call | solution.py:37
  64.8 2.1 %all-to-all-done.2.weights = bf16[8,8,32,256]{3,2,1,0:T(8,128)(2,1)S(1)} async-done(((bf16[8,8,32,256]{3,2,1,0:T(8,128)(2,1)}), bf16[8,8,32,256]{3,2,1,0:T(8,128)(2,1)S(1)}, u32[]{:S(2)}, u32[]{:S(2)}) %all-to-all-start.2) | async-done | bytes 1048608 | tf_op jit(solution)/shard_map/all_to_all | solution.py:248
  66.9 1.0 copy-done
  67.9 3.7 %shard_map.158 = (bf16[8,136,128]{2,1,0:T(8,128)(2,1)}, bf16[256,128]{1,0:T(8,128)(2,1)}, bf16[256,128]{1,0:T(8,128)(2,1)}, f32[256,128]{1,0:T(8,128)}, bf16[4,128,128]{2,1,0:T(8,128)(2,1)}, /*index=5*/f32[4,128]{1,0:T(4,128)}) custom-call(bf16[256,2048]{1,0:T(8,128)(2,1)} %get-tuple-element.23.normed, bf16[8,8,32,256]{3,2,1,0:T(8,128)(2,1)} %copy-done, ...), custom_call_target="tpu_custom_call" | custom-call | tf_op jit(solution)/shard_map/pallas_call | solution.py:37
  71.6 4.8 %all-to-all-start.3 = ((bf16[8,136,128]{2,1,0:T(8,128)(2,1)}), bf16[8,136,128]{2,1,0:T(8,128)(2,1)S(1)}, u32[]{:S(2)}, u32[]{:S(2)}) async-start(bf16[8,136,128]{2,1,0:T(8,128)(2,1)} %get-tuple-element.28), calls=%async_computation.3 | async-start | bytes 557056 | tf_op jit(solution)/shard_map/all_to_all | solution.py:248
  76.4 15.7 %all-to-all-done.3.got = bf16[8,136,128]{2,1,0:T(8,128)(2,1)S(1)} async-done(((bf16[8,136,128]{2,1,0:T(8,128)(2,1)}), bf16[8,136,128]{2,1,0:T(8,128)(2,1)S(1)}, u32[]{:S(2)}, u32[]{:S(2)}) %all-to-all-start.3) | async-done | bytes 278560 | tf_op jit(solution)/shard_map/all_to_all | solution.py:248
  92.1 0.7 copy-done.2
  92.8 1.8 %shard_map.159 = (bf16[8,136,128]{2,1,0:T(8,128)(2,1)}, f32[128,128]{1,0:T(8,128)}, f32[8,128]{1,0:T(8,128)}) custom-call(s32[1]{0:T(128)} %bitcast.5.position, bf16[8,136,128]{2,1,0:T(8,128)(2,1)} %copy-done.2), custom_call_target="tpu_custom_call" | custom-call | tf_op jit(solution)/shard_map/pallas_call | solution.py:37
  94.6 3.4 %all-to-all-start.4 = ((bf16[8,136,128]{2,1,0:T(8,128)(2,1)}), bf16[8,136,128]{2,1,0:T(8,128)(2,1)S(1)}, u32[]{:S(2)}, u32[]{:S(2)}) async-start(bf16[8,136,128]{2,1,0:T(8,128)(2,1)} %get-tuple-element.29), calls=%async_computation.4 | async-start | bytes 557056 | tf_op jit(solution)/shard_map/all_to_all | solution.py:248
  98.1 2.0 %collective-permute-start.7 = (bf16[32,2048]{1,0:T(8,128)(2,1)}, bf16[32,2048]{1,0:T(8,128)(2,1)S(1)}, u32[]{:S(2)}, u32[]{:S(2)}) collective-permute-start(bf16[32,2048]{1,0:T(8,128)(2,1)} %get-tuple-element.22), channel_id=1, source_target_pairs={{0,8},{8,16},{16,24},{24,32},{32,40},{40,48},{48,56},{56,64},{64,7... | collective-permute-start | bytes 393224 | tf_op jit(solution)/shard_map/ppermute | solution.py:313
  100.1 5.9 %collective-permute-done.7.halo = bf16[32,2048]{1,0:T(8,128)(2,1)S(1)} collective-permute-done((bf16[32,2048]{1,0:T(8,128)(2,1)}, bf16[32,2048]{1,0:T(8,128)(2,1)S(1)}, u32[]{:S(2)}, u32[]{:S(2)}) %collective-permute-start.7) | collective-permute-done | bytes 131104 | tf_op jit(solution)/shard_map/ppermute | solution.py:313
  106.0 8.6 %all-gather.2.cloned.1.call-done.weights.w_rec.w_low.w_high = bf16[2048,1152]{1,0:T(8,128)(2,1)} async-done(((bf16[32,1152]{1,0:T(8,128)(2,1)}), bf16[2048,1152]{1,0:T(8,128)(2,1)}) %all-gather.2.cloned.1.call-update) | async-done | bytes 4718608 | tf_op jit(solution)/shard_map/all_gather | solution.py:298
  114.6 4.6 %shard_map.156 = (f32[256,256]{1,0:T(8,128)}, f32[8,2,256]{2,1,0:T(2,128)}) custom-call(bf16[32,2048]{1,0:T(8,128)(2,1)} %copy-done.3, bf16[256,2048]{1,0:T(8,128)(2,1)} %get-tuple-element.23.normed, bf16[2048,1152]{1,0:T(8,128)(2,1)} %all-gather.2.cloned.1.call-done.weights.w_rec.w_low.w_high, f32[31,256]{1,0:T(8,128)} %taps.1), custom_call_target="tpu_custom_call" | custom-call | tf_op jit(solution)/shard_map/pallas_call | solution.py:37
  119.2 0.0 all-to-all-done.4.got
  119.2 8.3 %all-to-all-start = ((f32[8,2,256]{2,1,0:T(2,128)}), f32[8,2,256]{2,1,0:T(2,128)S(1)}, u32[]{:S(2)}, u32[]{:S(2)}) async-start(f32[8,2,256]{2,1,0:T(2,128)} %get-tuple-element.25), calls=%async_computation | async-start | bytes 32768 | tf_op jit(solution)/shard_map/all_to_all | solution.py:248
  127.5 3.6 %shard_map.160.head_out = bf16[256,128]{1,0:T(8,128)(2,1)} custom-call(s32[1]{0:T(128)} %bitcast.4.position, bf16[8,136,128]{2,1,0:T(8,128)(2,1)} %copy-done.1, f32[128,128]{1,0:T(8,128)} %get-tuple-element.30.inner_state, f32[8,128]{1,0:T(8,128)} %get-tuple-element.31.inner_total, bf16[256,2048]{1,0:T(8,128)(2,1)} %get-tuple-element.23.normed, ...), custom_call_target="tpu_custom_call" | custom-call | tf_op jit(solution)/shard_map/pallas_call | solution.py:37
  131.2 1.0 all-to-all-done.stats
  132.2 0.6 copy-done.11
  132.8 3.9 %shard_map.161 = (bf16[128,2048]{1,0:T(8,128)(2,1)}, bf16[128,2048]{1,0:T(8,128)(2,1)}) custom-call(s32[1]{0:T(128)} %bitcast.core, f32[8,2,256]{2,1,0:T(2,128)} %copy-done.11, f32[256,256]{1,0:T(8,128)} %get-tuple-element.26.conv, bf16[256,128]{1,0:T(8,128)(2,1)} %shard_map.160.head_out, f32[1,256]{1,0:T(1,128)} %bitcast.15, f32[1,256]{1,0:T(1,128)} %bitcast.16, ...), custom_call_target="tpu_custom_call" | custom-call | tf_op jit(solution)/shard_map/pallas_call | solution.py:37
  136.7 2.6 %collective-permute-start.8 = (bf16[128,2048]{1,0:T(8,128)(2,1)}, bf16[128,2048]{1,0:T(8,128)(2,1)S(1)}, u32[]{:S(2)}, u32[]{:S(2)}) collective-permute-start(bf16[128,2048]{1,0:T(8,128)(2,1)} %get-tuple-element.38), channel_id=1, source_target_pairs={{0,1},{1,0},{2,3},{3,2},{4,5},{5,4},{6,7},{7,6},{8,9},{9,8},{10,11... | collective-permute-start | bytes 1572872 | tf_op jit(solution)/shard_map/ppermute | solution.py:415
  139.3 1.7 %collective-permute-done.8 = bf16[128,2048]{1,0:T(8,128)(2,1)S(1)} collective-permute-done((bf16[128,2048]{1,0:T(8,128)(2,1)}, bf16[128,2048]{1,0:T(8,128)(2,1)S(1)}, u32[]{:S(2)}, u32[]{:S(2)}) %collective-permute-start.8) | collective-permute-done | bytes 524320 | tf_op jit(solution)/shard_map/ppermute | solution.py:415
  141.1 1.2 add_convert_fusion
  142.2 11.2 %all_to_all.31 = bf16[4,32,2048]{2,1,0:T(8,128)(2,1)S(1)} all-to-all(bf16[4,32,2048]{2,1,0:T(8,128)(2,1)S(1)} %bitcast.11), channel_id=1, replica_groups=mesh['sp_0'=8,'sp_1'=8,'x'=4,'core'=2] {'x'}, dimensions={0} | all-to-all | bytes 1048576 | tf_op jit(solution)/shard_map/all_to_all | solution.py:248
  153.4 0.7 reduce_sum.12
  (18 shorter events, 0.0 us)
Async XLA Ops:
  6.5 108.1 %all-gather.2.cloned.1.call-start = ((), (), s32[]{:S(2)}) async-start(), calls=%async_computation.6 | async-start | bytes 4792320 | tf_op jit(solution)/shard_map/all_gather | solution.py:298
  28.8 38.1 %all-to-all-start.2 = ((bf16[8,8,32,256]{3,2,1,0:T(8,128)(2,1)}), bf16[8,8,32,256]{3,2,1,0:T(8,128)(2,1)S(1)}, u32[]{:S(2)}, u32[]{:S(2)}) async-start(bf16[8,8,32,256]{3,2,1,0:T(8,128)(2,1)} %shard_map.157), calls=%async_computation.2 | async-start | bytes 2097152 | tf_op jit(solution)/shard_map/all_to_all | solution.py:248
  35.6 16.6 %collective-permute-start = (bf16[32,2048]{1,0:T(8,128)(2,1)}, bf16[32,2048]{1,0:T(8,128)(2,1)S(1)}, u32[]{:S(2)}, u32[]{:S(2)}) collective-permute-start(bf16[32,2048]{1,0:T(8,128)(2,1)} %refs_0_.1), channel_id=1, source_target_pairs={{0,1},{1,2},{2,3},{3,4},{4,5},{5,6},{6,7},{7,0},{8,9},{9,10},{10,1... | collective-permute-start | bytes 393224 | tf_op jit(solution)/shard_map/ppermute | solution.py:255
  39.3 15.5 %collective-permute-start.1 = (bf16[32,2048]{1,0:T(8,128)(2,1)}, bf16[32,2048]{1,0:T(8,128)(2,1)S(1)}, u32[]{:S(2)}, u32[]{:S(2)}) collective-permute-start(bf16[32,2048]{1,0:T(8,128)(2,1)} %refs_0_.1), channel_id=1, source_target_pairs={{0,2},{1,3},{2,4},{3,5},{4,6},{5,7},{6,0},{7,1},{8,10},{9,11},{10,... | collective-permute-start | bytes 393224 | tf_op jit(solution)/shard_map/ppermute | solution.py:255
  42.4 14.6 %collective-permute-start.2 = (bf16[32,2048]{1,0:T(8,128)(2,1)}, bf16[32,2048]{1,0:T(8,128)(2,1)S(1)}, u32[]{:S(2)}, u32[]{:S(2)}) collective-permute-start(bf16[32,2048]{1,0:T(8,128)(2,1)} %refs_0_.1), channel_id=1, source_target_pairs={{0,3},{1,4},{2,5},{3,6},{4,7},{5,0},{6,1},{7,2},{8,11},{9,12},{10,... | collective-permute-start | bytes 393224 | tf_op jit(solution)/shard_map/ppermute | solution.py:255
  45.8 11.2 %collective-permute-start.3 = (bf16[32,2048]{1,0:T(8,128)(2,1)}, bf16[32,2048]{1,0:T(8,128)(2,1)S(1)}, u32[]{:S(2)}, u32[]{:S(2)}) collective-permute-start(bf16[32,2048]{1,0:T(8,128)(2,1)} %refs_0_.1), channel_id=1, source_target_pairs={{0,4},{1,5},{2,6},{3,7},{4,0},{5,1},{6,2},{7,3},{8,12},{9,13},{10,... | collective-permute-start | bytes 393224 | tf_op jit(solution)/shard_map/ppermute | solution.py:255
  48.3 8.8 %collective-permute-start.4 = (bf16[32,2048]{1,0:T(8,128)(2,1)}, bf16[32,2048]{1,0:T(8,128)(2,1)S(1)}, u32[]{:S(2)}, u32[]{:S(2)}) collective-permute-start(bf16[32,2048]{1,0:T(8,128)(2,1)} %refs_0_.1), channel_id=1, source_target_pairs={{0,5},{1,6},{2,7},{3,0},{4,1},{5,2},{6,3},{7,4},{8,13},{9,14},{10,... | collective-permute-start | bytes 393224 | tf_op jit(solution)/shard_map/ppermute | solution.py:255
  52.2 9.2 %copy-start.4 = (bf16[32,2048]{1,0:T(8,128)(2,1)}, bf16[32,2048]{1,0:T(8,128)(2,1)S(1)}, u32[]{:S(2)}) copy-start(bf16[32,2048]{1,0:T(8,128)(2,1)S(1)} %collective-permute-done.refs_1_) | copy-start | bytes 393220
  52.2 6.4 %collective-permute-start.5 = (bf16[32,2048]{1,0:T(8,128)(2,1)}, bf16[32,2048]{1,0:T(8,128)(2,1)S(1)}, u32[]{:S(2)}, u32[]{:S(2)}) collective-permute-start(bf16[32,2048]{1,0:T(8,128)(2,1)} %refs_0_.1), channel_id=1, source_target_pairs={{0,6},{1,7},{2,0},{3,1},{4,2},{5,3},{6,4},{7,5},{8,14},{9,15},{10,... | collective-permute-start | bytes 393224 | tf_op jit(solution)/shard_map/ppermute | solution.py:255
  54.8 6.6 %copy-start.5 = (bf16[32,2048]{1,0:T(8,128)(2,1)}, bf16[32,2048]{1,0:T(8,128)(2,1)S(1)}, u32[]{:S(2)}) copy-start(bf16[32,2048]{1,0:T(8,128)(2,1)S(1)} %collective-permute-done.1.refs_2_) | copy-start | bytes 393220
  54.8 6.5 %collective-permute-start.6 = (bf16[32,2048]{1,0:T(8,128)(2,1)}, bf16[32,2048]{1,0:T(8,128)(2,1)S(1)}, u32[]{:S(2)}, u32[]{:S(2)}) collective-permute-start(bf16[32,2048]{1,0:T(8,128)(2,1)} %refs_0_.1), channel_id=1, source_target_pairs={{0,7},{1,0},{2,1},{3,2},{4,3},{5,4},{6,5},{7,6},{8,15},{9,8},{10,9... | collective-permute-start | bytes 393224 | tf_op jit(solution)/shard_map/ppermute | solution.py:255
  57.0 4.4 %copy-start.6 = (bf16[32,2048]{1,0:T(8,128)(2,1)}, bf16[32,2048]{1,0:T(8,128)(2,1)S(1)}, u32[]{:S(2)}) copy-start(bf16[32,2048]{1,0:T(8,128)(2,1)S(1)} %collective-permute-done.2.refs_3_) | copy-start | bytes 393220
  57.0 4.3 %copy-start.7 = (bf16[32,2048]{1,0:T(8,128)(2,1)}, bf16[32,2048]{1,0:T(8,128)(2,1)S(1)}, u32[]{:S(2)}) copy-start(bf16[32,2048]{1,0:T(8,128)(2,1)S(1)} %collective-permute-done.3.refs_4_) | copy-start | bytes 393220
  57.0 4.3 %copy-start.8 = (bf16[32,2048]{1,0:T(8,128)(2,1)}, bf16[32,2048]{1,0:T(8,128)(2,1)S(1)}, u32[]{:S(2)}) copy-start(bf16[32,2048]{1,0:T(8,128)(2,1)S(1)} %collective-permute-done.4.refs_5_) | copy-start | bytes 393220
  58.7 2.7 %copy-start.9 = (bf16[32,2048]{1,0:T(8,128)(2,1)}, bf16[32,2048]{1,0:T(8,128)(2,1)S(1)}, u32[]{:S(2)}) copy-start(bf16[32,2048]{1,0:T(8,128)(2,1)S(1)} %collective-permute-done.5.refs_6_) | copy-start | bytes 393220
  61.4 0.7 copy-start.10
  66.9 1.0 copy-start
  71.6 20.5 %all-to-all-start.3 = ((bf16[8,136,128]{2,1,0:T(8,128)(2,1)}), bf16[8,136,128]{2,1,0:T(8,128)(2,1)S(1)}, u32[]{:S(2)}, u32[]{:S(2)}) async-start(bf16[8,136,128]{2,1,0:T(8,128)(2,1)} %get-tuple-element.28), calls=%async_computation.3 | async-start | bytes 557056 | tf_op jit(solution)/shard_map/all_to_all | solution.py:248
  92.1 0.7 copy-start.2
  94.6 24.6 %all-to-all-start.4 = ((bf16[8,136,128]{2,1,0:T(8,128)(2,1)}), bf16[8,136,128]{2,1,0:T(8,128)(2,1)S(1)}, u32[]{:S(2)}, u32[]{:S(2)}) async-start(bf16[8,136,128]{2,1,0:T(8,128)(2,1)} %get-tuple-element.29), calls=%async_computation.4 | async-start | bytes 557056 | tf_op jit(solution)/shard_map/all_to_all | solution.py:248
  98.1 8.0 %collective-permute-start.7 = (bf16[32,2048]{1,0:T(8,128)(2,1)}, bf16[32,2048]{1,0:T(8,128)(2,1)S(1)}, u32[]{:S(2)}, u32[]{:S(2)}) collective-permute-start(bf16[32,2048]{1,0:T(8,128)(2,1)} %get-tuple-element.22), channel_id=1, source_target_pairs={{0,8},{8,16},{16,24},{24,32},{32,40},{40,48},{48,56},{56,64},{64,7... | collective-permute-start | bytes 393224 | tf_op jit(solution)/shard_map/ppermute | solution.py:313
  106.0 8.6 %copy-start.3 = (bf16[32,2048]{1,0:T(8,128)(2,1)}, bf16[32,2048]{1,0:T(8,128)(2,1)S(1)}, u32[]{:S(2)}) copy-start(bf16[32,2048]{1,0:T(8,128)(2,1)S(1)} %collective-permute-done.7.halo) | copy-start | bytes 393220
  119.2 8.3 %copy-start.1 = (bf16[8,136,128]{2,1,0:T(8,128)(2,1)}, bf16[8,136,128]{2,1,0:T(8,128)(2,1)S(1)}, u32[]{:S(2)}) copy-start(bf16[8,136,128]{2,1,0:T(8,128)(2,1)S(1)} %all-to-all-done.4.got) | copy-start | bytes 835588
  119.2 13.0 %all-to-all-start = ((f32[8,2,256]{2,1,0:T(2,128)}), f32[8,2,256]{2,1,0:T(2,128)S(1)}, u32[]{:S(2)}, u32[]{:S(2)}) async-start(f32[8,2,256]{2,1,0:T(2,128)} %get-tuple-element.25), calls=%async_computation | async-start | bytes 32768 | tf_op jit(solution)/shard_map/all_to_all | solution.py:248
  132.2 0.6 copy-start.11
  136.7 4.3 %collective-permute-start.8 = (bf16[128,2048]{1,0:T(8,128)(2,1)}, bf16[128,2048]{1,0:T(8,128)(2,1)S(1)}, u32[]{:S(2)}, u32[]{:S(2)}) collective-permute-start(bf16[128,2048]{1,0:T(8,128)(2,1)} %get-tuple-element.38), channel_id=1, source_target_pairs={{0,1},{1,0},{2,3},{3,2},{4,5},{5,4},{6,7},{7,6},{8,9},{9,8},{10,11... | collective-permute-start | bytes 1572872 | tf_op jit(solution)/shard_map/ppermute | solution.py:415
Sparse Core Ops, SparseCore 0:
  10.3 104.2 all-gather.1

commit v10 on v9

--- a/solution.py
+++ b/solution.py
@@ -83,12 +83,7 @@
 
 def state_body(normed, weights, leak, shift, sent, value_out, key, totals, starts, befores):
     rows = normed.shape[0]
-    peers = weights.shape[0]
-    ordered = jnp.concatenate(
-        [weights[inner, outer] for outer in range(weights.shape[1]) for inner in range(peers)],
-        axis=0,
-    )
-    projected = jnp.dot(normed[...], ordered, preferred_element_type=F32).astype(BF16)
+    projected = jnp.dot(normed[...], weights[...], preferred_element_type=F32).astype(BF16)
     value = projected[:, HEAD_K:]
     value_out[...] = value
     in_gate = leak[...] * jax.nn.sigmoid(-projected[:, :HEAD_K].astype(F32))
@@ -289,16 +284,16 @@
         first_body,
         (
             shape((depth, all_width), BF16),
-            shape((outer_count, depth, 2 * HEAD_K), BF16),
+            shape((inner_count, depth, 2 * HEAD_K), BF16),
         ),
         *columns,
         w_forget,
         w_value,
     )
     gathered = lax.all_gather(operand, SP, axis=0, tiled=True)
-    column = swap(copies, SP[0])
-    copies = call(again_body, shape((inner_count, *column.shape), BF16), column)
-    state_weights = swap(copies, SP[1])
+    column = swap(copies, SP[1])
+    copies = call(again_body, shape((outer_count, *column.shape), BF16), column)
+    state_weights = swap(copies, SP[0]).reshape(-1, 2 * HEAD_K)
     pieces, places = shifted_around(tokens, TP)
     rows = group * share
     normed, tail = call(

time: 162 us -> 161 us (level)
  blocking collectives: 29.9 us -> 27 us
  waiting for transfers between devices: 39.4 us -> 41.2 us
    all_to_all x2, blocking collectives: 29.9 us -> 27 us  [swap(): return lax.all_to_all(value, axis, split_axis=0, concat_axis=0, tiled=True)]
    all_gather x1, waiting for transfers between devices: 8.62 us -> 11.5 us  [on_device(): gathered = lax.all_gather(operand, SP, axis=0, tiled=True)]
where the time goes in v10:
time: 161 us; the launch traced here: 160 us
  starting transfers between devices  49.4 us (31%)
  waiting for transfers between devices  41.2 us (26%)
  blocking collectives  27 us (17%)
  Pallas kernels  23.8 us (15%)
  between operations  13.6 us (8%)
  local copies, waits for them, and re-layouts  2.98 us (2%)
  other arithmetic  2.48 us (2%)
    all_to_all x2, blocking collectives, swap(): return lax.all_to_all(value, axis, split_axis=0, concat_axis=0, tiled=True)  27 us
    all_to_all x4, starting transfers between devices, swap(): return lax.all_to_all(value, axis, split_axis=0, concat_axis=0, tiled=True)  24.1 us
    pallas_call x8, Pallas kernels, call(): pl.pallas_call(body, out_shape=outs, scratch_shapes=scratch, **specs)(*args)  23.8 us
    ppermute x7, starting transfers between devices, shifted_around(): lax.ppermute(value, axis, [(n, (n + k) % count) for n in range(count)])  20.8 us
    all_to_all x4, waiting for transfers between devices, swap(): return lax.all_to_all(value, axis, split_axis=0, concat_axis=0, tiled=True)  18.3 us
    all_gather x1, waiting for transfers between devices, on_device(): gathered = lax.all_gather(operand, SP, axis=0, tiled=True)  11.5 us
    ppermute x1, waiting for transfers between devices, on_device(): halo = lax.ppermute(tail, SP, [(k, k + 1) for k in range(count - 1)])  5.41 us
    ppermute x7, waiting for transfers between devices, shifted_around(): lax.ppermute(value, axis, [(n, (n + k) % count) for n in range(count)])  4.32 us
  transfers between devices with their start and end apart: 14, of which 8 were waited for; matrix products, arithmetic and copies ran while one was open for 0% of the time, Pallas kernels for 11%

profile of v10, /device:TPU:1, one launch (start us, length us, event | category | flops | bytes accessed | tf_op | source)
XLA Modules:
  0.0 160.4 jit_solution(385352306468368743)
XLA Ops:
  6.5 1.5 shard_map.155
  8.0 0.0 all-gather.2.cloned.1.call-update
  8.1 15.8 %all_to_all.30.value = bf16[8,32,256]{2,1,0:T(8,128)(2,1)} all-to-all(bf16[8,32,256]{2,1,0:T(8,128)(2,1)} %get-tuple-element.27), channel_id=1, replica_groups=mesh['sp_0'=8,'sp_1'=8,'x'=4,'core'=2] {'sp_1'}, dimensions={0} | all-to-all | bytes 262144 | tf_op jit(solution)/shard_map/all_to_all | solution.py:243
  23.8 2.0 %shard_map.157 = bf16[8,8,32,256]{3,2,1,0:T(8,128)(2,1)} custom-call(bf16[8,32,256]{2,1,0:T(8,128)(2,1)} %all_to_all.30.value), custom_call_target="tpu_custom_call" | custom-call | tf_op jit(solution)/shard_map/pallas_call | solution.py:37
  25.8 9.8 %all-to-all-start.2 = ((bf16[8,8,32,256]{3,2,1,0:T(8,128)(2,1)}), bf16[8,8,32,256]{3,2,1,0:T(8,128)(2,1)S(1)}, u32[]{:S(2)}, u32[]{:S(2)}) async-start(bf16[8,8,32,256]{3,2,1,0:T(8,128)(2,1)} %shard_map.157), calls=%async_computation.2 | async-start | bytes 2097152 | tf_op jit(solution)/shard_map/all_to_all | solution.py:243
  35.6 3.7 %collective-permute-start = (bf16[32,2048]{1,0:T(8,128)(2,1)}, bf16[32,2048]{1,0:T(8,128)(2,1)S(1)}, u32[]{:S(2)}, u32[]{:S(2)}) collective-permute-start(bf16[32,2048]{1,0:T(8,128)(2,1)} %refs_0_.1), channel_id=1, source_target_pairs={{0,1},{1,2},{2,3},{3,4},{4,5},{5,6},{6,7},{7,0},{8,9},{9,10},{10,1... | collective-permute-start | bytes 393224 | tf_op jit(solution)/shard_map/ppermute | solution.py:250
  39.3 3.1 %collective-permute-start.1 = (bf16[32,2048]{1,0:T(8,128)(2,1)}, bf16[32,2048]{1,0:T(8,128)(2,1)S(1)}, u32[]{:S(2)}, u32[]{:S(2)}) collective-permute-start(bf16[32,2048]{1,0:T(8,128)(2,1)} %refs_0_.1), channel_id=1, source_target_pairs={{0,2},{1,3},{2,4},{3,5},{4,6},{5,7},{6,0},{7,1},{8,10},{9,11},{10,... | collective-permute-start | bytes 393224 | tf_op jit(solution)/shard_map/ppermute | solution.py:250
  42.4 3.5 %collective-permute-start.2 = (bf16[32,2048]{1,0:T(8,128)(2,1)}, bf16[32,2048]{1,0:T(8,128)(2,1)S(1)}, u32[]{:S(2)}, u32[]{:S(2)}) collective-permute-start(bf16[32,2048]{1,0:T(8,128)(2,1)} %refs_0_.1), channel_id=1, source_target_pairs={{0,3},{1,4},{2,5},{3,6},{4,7},{5,0},{6,1},{7,2},{8,11},{9,12},{10,... | collective-permute-start | bytes 393224 | tf_op jit(solution)/shard_map/ppermute | solution.py:250
  45.8 2.4 %collective-permute-start.3 = (bf16[32,2048]{1,0:T(8,128)(2,1)}, bf16[32,2048]{1,0:T(8,128)(2,1)S(1)}, u32[]{:S(2)}, u32[]{:S(2)}) collective-permute-start(bf16[32,2048]{1,0:T(8,128)(2,1)} %refs_0_.1), channel_id=1, source_target_pairs={{0,4},{1,5},{2,6},{3,7},{4,0},{5,1},{6,2},{7,3},{8,12},{9,13},{10,... | collective-permute-start | bytes 393224 | tf_op jit(solution)/shard_map/ppermute | solution.py:250
  48.3 3.9 %collective-permute-start.4 = (bf16[32,2048]{1,0:T(8,128)(2,1)}, bf16[32,2048]{1,0:T(8,128)(2,1)S(1)}, u32[]{:S(2)}, u32[]{:S(2)}) collective-permute-start(bf16[32,2048]{1,0:T(8,128)(2,1)} %refs_0_.1), channel_id=1, source_target_pairs={{0,5},{1,6},{2,7},{3,0},{4,1},{5,2},{6,3},{7,4},{8,13},{9,14},{10,... | collective-permute-start | bytes 393224 | tf_op jit(solution)/shard_map/ppermute | solution.py:250
  52.2 0.0 collective-permute-done.refs_1_
  52.2 0.0 copy-start.4
  52.2 2.6 %collective-permute-start.5 = (bf16[32,2048]{1,0:T(8,128)(2,1)}, bf16[32,2048]{1,0:T(8,128)(2,1)S(1)}, u32[]{:S(2)}, u32[]{:S(2)}) collective-permute-start(bf16[32,2048]{1,0:T(8,128)(2,1)} %refs_0_.1), channel_id=1, source_target_pairs={{0,6},{1,7},{2,0},{3,1},{4,2},{5,3},{6,4},{7,5},{8,14},{9,15},{10,... | collective-permute-start | bytes 393224 | tf_op jit(solution)/shard_map/ppermute | solution.py:250
  54.8 0.0 collective-permute-done.1.refs_2_
  54.8 1.6 %collective-permute-start.6 = (bf16[32,2048]{1,0:T(8,128)(2,1)}, bf16[32,2048]{1,0:T(8,128)(2,1)S(1)}, u32[]{:S(2)}, u32[]{:S(2)}) collective-permute-start(bf16[32,2048]{1,0:T(8,128)(2,1)} %refs_0_.1), channel_id=1, source_target_pairs={{0,7},{1,0},{2,1},{3,2},{4,3},{5,4},{6,5},{7,6},{8,15},{9,8},{10,9... | collective-permute-start | bytes 393224 | tf_op jit(solution)/shard_map/ppermute | solution.py:250
  56.4 0.6 and_select_fusion.places
  57.0 0.0 collective-permute-done.2.refs_3_
  57.0 0.0 collective-permute-done.3.refs_4_
  57.0 0.0 collective-permute-done.4.refs_5_
  57.0 0.0 copy-start.8
  57.1 1.6 %collective-permute-done.5.refs_6_ = bf16[32,2048]{1,0:T(8,128)(2,1)S(1)} collective-permute-done((bf16[32,2048]{1,0:T(8,128)(2,1)}, bf16[32,2048]{1,0:T(8,128)(2,1)S(1)}, u32[]{:S(2)}, u32[]{:S(2)}) %collective-permute-start.5) | collective-permute-done | bytes 131104 | tf_op jit(solution)/shard_map/ppermute | solution.py:250
  58.7 2.7 %collective-permute-done.6.refs_7_ = bf16[32,2048]{1,0:T(8,128)(2,1)S(1)} collective-permute-done((bf16[32,2048]{1,0:T(8,128)(2,1)}, bf16[32,2048]{1,0:T(8,128)(2,1)S(1)}, u32[]{:S(2)}, u32[]{:S(2)}) %collective-permute-start.6) | collective-permute-done | bytes 131104 | tf_op jit(solution)/shard_map/ppermute | solution.py:250
  61.4 0.0 copy-done.5
  61.4 0.6 copy-done.10
  62.0 2.7 %shard_map.154 = (bf16[256,2048]{1,0:T(8,128)(2,1)}, bf16[32,2048]{1,0:T(8,128)(2,1)}) custom-call(s32[8]{0:T(128)} %and_select_fusion.places, f32[1,2048]{1,0:T(1,128)} %bitcast.15, bf16[32,2048]{1,0:T(8,128)(2,1)} %refs_0_.1, bf16[32,2048]{1,0:T(8,128)(2,1)} %copy-done.4, bf16[32,2048]{1,0:T(8,128)(2,1)} %copy-done.5, bf16[32,2048]{1,0:T(8,128)(2,1)} %copy-done.6, ...), custom_call_target="tpu_custom_call" | custom-call | tf_op jit(solution)/shard_map/pallas_call | solution.py:37
  64.8 2.2 %all-to-all-done.2 = bf16[8,8,32,256]{3,2,1,0:T(8,128)(2,1)S(1)} async-done(((bf16[8,8,32,256]{3,2,1,0:T(8,128)(2,1)}), bf16[8,8,32,256]{3,2,1,0:T(8,128)(2,1)S(1)}, u32[]{:S(2)}, u32[]{:S(2)}) %all-to-all-start.2) | async-done | bytes 1048608 | tf_op jit(solution)/shard_map/all_to_all | solution.py:243
  67.0 1.0 copy-done
  68.0 3.7 %shard_map.158 = (bf16[8,136,128]{2,1,0:T(8,128)(2,1)}, bf16[256,128]{1,0:T(8,128)(2,1)}, bf16[256,128]{1,0:T(8,128)(2,1)}, f32[256,128]{1,0:T(8,128)}, bf16[4,128,128]{2,1,0:T(8,128)(2,1)}, /*index=5*/f32[4,128]{1,0:T(4,128)}) custom-call(bf16[256,2048]{1,0:T(8,128)(2,1)} %get-tuple-element.23.normed, bf16[2048,256]{1,0:T(8,128)(2,1)} %bitcast.12, ...), custom_call_target="tpu_custom_call" | custom-call | tf_op jit(solution)/shard_map/pallas_call | solution.py:37
  71.7 3.4 %all-to-all-start.3 = ((bf16[8,136,128]{2,1,0:T(8,128)(2,1)}), bf16[8,136,128]{2,1,0:T(8,128)(2,1)S(1)}, u32[]{:S(2)}, u32[]{:S(2)}) async-start(bf16[8,136,128]{2,1,0:T(8,128)(2,1)} %get-tuple-element.28), calls=%async_computation.3 | async-start | bytes 557056 | tf_op jit(solution)/shard_map/all_to_all | solution.py:243
  75.1 15.0 %all-to-all-done.3.got = bf16[8,136,128]{2,1,0:T(8,128)(2,1)S(1)} async-done(((bf16[8,136,128]{2,1,0:T(8,128)(2,1)}), bf16[8,136,128]{2,1,0:T(8,128)(2,1)S(1)}, u32[]{:S(2)}, u32[]{:S(2)}) %all-to-all-start.3) | async-done | bytes 278560 | tf_op jit(solution)/shard_map/all_to_all | solution.py:243
  90.2 0.7 copy-done.2
  90.9 1.8 %shard_map.159 = (bf16[8,136,128]{2,1,0:T(8,128)(2,1)}, f32[128,128]{1,0:T(8,128)}, f32[8,128]{1,0:T(8,128)}) custom-call(s32[1]{0:T(128)} %bitcast.5.position, bf16[8,136,128]{2,1,0:T(8,128)(2,1)} %copy-done.2), custom_call_target="tpu_custom_call" | custom-call | tf_op jit(solution)/shard_map/pallas_call | solution.py:37
  92.7 3.5 %all-to-all-start.4 = ((bf16[8,136,128]{2,1,0:T(8,128)(2,1)}), bf16[8,136,128]{2,1,0:T(8,128)(2,1)S(1)}, u32[]{:S(2)}, u32[]{:S(2)}) async-start(bf16[8,136,128]{2,1,0:T(8,128)(2,1)} %get-tuple-element.29), calls=%async_computation.4 | async-start | bytes 557056 | tf_op jit(solution)/shard_map/all_to_all | solution.py:243
  96.2 1.9 %collective-permute-start.7 = (bf16[32,2048]{1,0:T(8,128)(2,1)}, bf16[32,2048]{1,0:T(8,128)(2,1)S(1)}, u32[]{:S(2)}, u32[]{:S(2)}) collective-permute-start(bf16[32,2048]{1,0:T(8,128)(2,1)} %get-tuple-element.22), channel_id=1, source_target_pairs={{0,8},{8,16},{16,24},{24,32},{32,40},{40,48},{48,56},{56,64},{64,7... | collective-permute-start | bytes 393224 | tf_op jit(solution)/shard_map/ppermute | solution.py:308
  98.1 5.4 %collective-permute-done.7.halo = bf16[32,2048]{1,0:T(8,128)(2,1)S(1)} collective-permute-done((bf16[32,2048]{1,0:T(8,128)(2,1)}, bf16[32,2048]{1,0:T(8,128)(2,1)S(1)}, u32[]{:S(2)}, u32[]{:S(2)}) %collective-permute-start.7) | collective-permute-done | bytes 131104 | tf_op jit(solution)/shard_map/ppermute | solution.py:308
  103.5 11.5 %all-gather.2.cloned.1.call-done.weights.w_rec.w_low.w_high = bf16[2048,1152]{1,0:T(8,128)(2,1)} async-done(((bf16[32,1152]{1,0:T(8,128)(2,1)}), bf16[2048,1152]{1,0:T(8,128)(2,1)}) %all-gather.2.cloned.1.call-update) | async-done | bytes 4718608 | tf_op jit(solution)/shard_map/all_gather | solution.py:293
  115.0 4.6 %shard_map.156 = (f32[256,256]{1,0:T(8,128)}, f32[8,2,256]{2,1,0:T(2,128)}) custom-call(bf16[32,2048]{1,0:T(8,128)(2,1)} %copy-done.3, bf16[256,2048]{1,0:T(8,128)(2,1)} %get-tuple-element.23.normed, bf16[2048,1152]{1,0:T(8,128)(2,1)} %all-gather.2.cloned.1.call-done.weights.w_rec.w_low.w_high, f32[31,256]{1,0:T(8,128)} %taps.1), custom_call_target="tpu_custom_call" | custom-call | tf_op jit(solution)/shard_map/pallas_call | solution.py:37
  119.5 0.0 all-to-all-done.4.got
  119.5 7.4 %all-to-all-start = ((f32[8,2,256]{2,1,0:T(2,128)}), f32[8,2,256]{2,1,0:T(2,128)S(1)}, u32[]{:S(2)}, u32[]{:S(2)}) async-start(f32[8,2,256]{2,1,0:T(2,128)} %get-tuple-element.25), calls=%async_computation | async-start | bytes 32768 | tf_op jit(solution)/shard_map/all_to_all | solution.py:243
  126.9 3.6 %shard_map.160.head_out = bf16[256,128]{1,0:T(8,128)(2,1)} custom-call(s32[1]{0:T(128)} %bitcast.4.position, bf16[8,136,128]{2,1,0:T(8,128)(2,1)} %copy-done.1, f32[128,128]{1,0:T(8,128)} %get-tuple-element.30.inner_state, f32[8,128]{1,0:T(8,128)} %get-tuple-element.31.inner_total, bf16[256,2048]{1,0:T(8,128)(2,1)} %get-tuple-element.23.normed, ...), custom_call_target="tpu_custom_call" | custom-call | tf_op jit(solution)/shard_map/pallas_call | solution.py:37
  130.6 1.0 all-to-all-done.stats
  131.6 0.6 copy-done.11
  132.2 3.9 %shard_map.161 = (bf16[128,2048]{1,0:T(8,128)(2,1)}, bf16[128,2048]{1,0:T(8,128)(2,1)}) custom-call(s32[1]{0:T(128)} %bitcast.core, f32[8,2,256]{2,1,0:T(2,128)} %copy-done.11, f32[256,256]{1,0:T(8,128)} %get-tuple-element.26.conv, bf16[256,128]{1,0:T(8,128)(2,1)} %shard_map.160.head_out, f32[1,256]{1,0:T(1,128)} %bitcast.17, f32[1,256]{1,0:T(1,128)} %bitcast.18, ...), custom_call_target="tpu_custom_call" | custom-call | tf_op jit(solution)/shard_map/pallas_call | solution.py:37
  136.1 2.6 %collective-permute-start.8 = (bf16[128,2048]{1,0:T(8,128)(2,1)}, bf16[128,2048]{1,0:T(8,128)(2,1)S(1)}, u32[]{:S(2)}, u32[]{:S(2)}) collective-permute-start(bf16[128,2048]{1,0:T(8,128)(2,1)} %get-tuple-element.38), channel_id=1, source_target_pairs={{0,1},{1,0},{2,3},{3,2},{4,5},{5,4},{6,7},{7,6},{8,9},{9,8},{10,11... | collective-permute-start | bytes 1572872 | tf_op jit(solution)/shard_map/ppermute | solution.py:410
  138.7 1.7 %collective-permute-done.8 = bf16[128,2048]{1,0:T(8,128)(2,1)S(1)} collective-permute-done((bf16[128,2048]{1,0:T(8,128)(2,1)}, bf16[128,2048]{1,0:T(8,128)(2,1)S(1)}, u32[]{:S(2)}, u32[]{:S(2)}) %collective-permute-start.8) | collective-permute-done | bytes 524320 | tf_op jit(solution)/shard_map/ppermute | solution.py:410
  140.5 1.2 add_convert_fusion
  141.6 11.2 %all_to_all.31 = bf16[4,32,2048]{2,1,0:T(8,128)(2,1)S(1)} all-to-all(bf16[4,32,2048]{2,1,0:T(8,128)(2,1)S(1)} %bitcast.13), channel_id=1, replica_groups=mesh['sp_0'=8,'sp_1'=8,'x'=4,'core'=2] {'x'}, dimensions={0} | all-to-all | bytes 1048576 | tf_op jit(solution)/shard_map/all_to_all | solution.py:243
  152.8 0.7 reduce_sum.12
  (18 shorter events, 0.0 us)
Async XLA Ops:
  6.5 108.4 %all-gather.2.cloned.1.call-start = ((), (), s32[]{:S(2)}) async-start(), calls=%async_computation.6 | async-start | bytes 4792320 | tf_op jit(solution)/shard_map/all_gather | solution.py:293
  25.8 41.2 %all-to-all-start.2 = ((bf16[8,8,32,256]{3,2,1,0:T(8,128)(2,1)}), bf16[8,8,32,256]{3,2,1,0:T(8,128)(2,1)S(1)}, u32[]{:S(2)}, u32[]{:S(2)}) async-start(bf16[8,8,32,256]{3,2,1,0:T(8,128)(2,1)} %shard_map.157), calls=%async_computation.2 | async-start | bytes 2097152 | tf_op jit(solution)/shard_map/all_to_all | solution.py:243
  35.6 16.6 %collective-permute-start = (bf16[32,2048]{1,0:T(8,128)(2,1)}, bf16[32,2048]{1,0:T(8,128)(2,1)S(1)}, u32[]{:S(2)}, u32[]{:S(2)}) collective-permute-start(bf16[32,2048]{1,0:T(8,128)(2,1)} %refs_0_.1), channel_id=1, source_target_pairs={{0,1},{1,2},{2,3},{3,4},{4,5},{5,6},{6,7},{7,0},{8,9},{9,10},{10,1... | collective-permute-start | bytes 393224 | tf_op jit(solution)/shard_map/ppermute | solution.py:250
  39.3 15.5 %collective-permute-start.1 = (bf16[32,2048]{1,0:T(8,128)(2,1)}, bf16[32,2048]{1,0:T(8,128)(2,1)S(1)}, u32[]{:S(2)}, u32[]{:S(2)}) collective-permute-start(bf16[32,2048]{1,0:T(8,128)(2,1)} %refs_0_.1), channel_id=1, source_target_pairs={{0,2},{1,3},{2,4},{3,5},{4,6},{5,7},{6,0},{7,1},{8,10},{9,11},{10,... | collective-permute-start | bytes 393224 | tf_op jit(solution)/shard_map/ppermute | solution.py:250
  42.4 14.6 %collective-permute-start.2 = (bf16[32,2048]{1,0:T(8,128)(2,1)}, bf16[32,2048]{1,0:T(8,128)(2,1)S(1)}, u32[]{:S(2)}, u32[]{:S(2)}) collective-permute-start(bf16[32,2048]{1,0:T(8,128)(2,1)} %refs_0_.1), channel_id=1, source_target_pairs={{0,3},{1,4},{2,5},{3,6},{4,7},{5,0},{6,1},{7,2},{8,11},{9,12},{10,... | collective-permute-start | bytes 393224 | tf_op jit(solution)/shard_map/ppermute | solution.py:250
  45.8 11.2 %collective-permute-start.3 = (bf16[32,2048]{1,0:T(8,128)(2,1)}, bf16[32,2048]{1,0:T(8,128)(2,1)S(1)}, u32[]{:S(2)}, u32[]{:S(2)}) collective-permute-start(bf16[32,2048]{1,0:T(8,128)(2,1)} %refs_0_.1), channel_id=1, source_target_pairs={{0,4},{1,5},{2,6},{3,7},{4,0},{5,1},{6,2},{7,3},{8,12},{9,13},{10,... | collective-permute-start | bytes 393224 | tf_op jit(solution)/shard_map/ppermute | solution.py:250
  48.3 8.8 %collective-permute-start.4 = (bf16[32,2048]{1,0:T(8,128)(2,1)}, bf16[32,2048]{1,0:T(8,128)(2,1)S(1)}, u32[]{:S(2)}, u32[]{:S(2)}) collective-permute-start(bf16[32,2048]{1,0:T(8,128)(2,1)} %refs_0_.1), channel_id=1, source_target_pairs={{0,5},{1,6},{2,7},{3,0},{4,1},{5,2},{6,3},{7,4},{8,13},{9,14},{10,... | collective-permute-start | bytes 393224 | tf_op jit(solution)/shard_map/ppermute | solution.py:250
  52.2 9.2 %copy-start.4 = (bf16[32,2048]{1,0:T(8,128)(2,1)}, bf16[32,2048]{1,0:T(8,128)(2,1)S(1)}, u32[]{:S(2)}) copy-start(bf16[32,2048]{1,0:T(8,128)(2,1)S(1)} %collective-permute-done.refs_1_) | copy-start | bytes 393220
  52.2 6.4 %collective-permute-start.5 = (bf16[32,2048]{1,0:T(8,128)(2,1)}, bf16[32,2048]{1,0:T(8,128)(2,1)S(1)}, u32[]{:S(2)}, u32[]{:S(2)}) collective-permute-start(bf16[32,2048]{1,0:T(8,128)(2,1)} %refs_0_.1), channel_id=1, source_target_pairs={{0,6},{1,7},{2,0},{3,1},{4,2},{5,3},{6,4},{7,5},{8,14},{9,15},{10,... | collective-permute-start | bytes 393224 | tf_op jit(solution)/shard_map/ppermute | solution.py:250
  54.8 6.6 %copy-start.5 = (bf16[32,2048]{1,0:T(8,128)(2,1)}, bf16[32,2048]{1,0:T(8,128)(2,1)S(1)}, u32[]{:S(2)}) copy-start(bf16[32,2048]{1,0:T(8,128)(2,1)S(1)} %collective-permute-done.1.refs_2_) | copy-start | bytes 393220
  54.8 6.5 %collective-permute-start.6 = (bf16[32,2048]{1,0:T(8,128)(2,1)}, bf16[32,2048]{1,0:T(8,128)(2,1)S(1)}, u32[]{:S(2)}, u32[]{:S(2)}) collective-permute-start(bf16[32,2048]{1,0:T(8,128)(2,1)} %refs_0_.1), channel_id=1, source_target_pairs={{0,7},{1,0},{2,1},{3,2},{4,3},{5,4},{6,5},{7,6},{8,15},{9,8},{10,9... | collective-permute-start | bytes 393224 | tf_op jit(solution)/shard_map/ppermute | solution.py:250
  57.0 4.4 %copy-start.6 = (bf16[32,2048]{1,0:T(8,128)(2,1)}, bf16[32,2048]{1,0:T(8,128)(2,1)S(1)}, u32[]{:S(2)}) copy-start(bf16[32,2048]{1,0:T(8,128)(2,1)S(1)} %collective-permute-done.2.refs_3_) | copy-start | bytes 393220
  57.0 4.4 %copy-start.7 = (bf16[32,2048]{1,0:T(8,128)(2,1)}, bf16[32,2048]{1,0:T(8,128)(2,1)S(1)}, u32[]{:S(2)}) copy-start(bf16[32,2048]{1,0:T(8,128)(2,1)S(1)} %collective-permute-done.3.refs_4_) | copy-start | bytes 393220
  57.0 4.3 %copy-start.8 = (bf16[32,2048]{1,0:T(8,128)(2,1)}, bf16[32,2048]{1,0:T(8,128)(2,1)S(1)}, u32[]{:S(2)}) copy-start(bf16[32,2048]{1,0:T(8,128)(2,1)S(1)} %collective-permute-done.4.refs_5_) | copy-start | bytes 393220
  58.7 2.7 %copy-start.9 = (bf16[32,2048]{1,0:T(8,128)(2,1)}, bf16[32,2048]{1,0:T(8,128)(2,1)S(1)}, u32[]{:S(2)}) copy-start(bf16[32,2048]{1,0:T(8,128)(2,1)S(1)} %collective-permute-done.5.refs_6_) | copy-start | bytes 393220
  61.4 0.7 copy-start.10
  67.0 1.0 copy-start
  71.7 18.4 %all-to-all-start.3 = ((bf16[8,136,128]{2,1,0:T(8,128)(2,1)}), bf16[8,136,128]{2,1,0:T(8,128)(2,1)S(1)}, u32[]{:S(2)}, u32[]{:S(2)}) async-start(bf16[8,136,128]{2,1,0:T(8,128)(2,1)} %get-tuple-element.28), calls=%async_computation.3 | async-start | bytes 557056 | tf_op jit(solution)/shard_map/all_to_all | solution.py:243
  90.2 0.7 copy-start.2
  92.7 26.8 %all-to-all-start.4 = ((bf16[8,136,128]{2,1,0:T(8,128)(2,1)}), bf16[8,136,128]{2,1,0:T(8,128)(2,1)S(1)}, u32[]{:S(2)}, u32[]{:S(2)}) async-start(bf16[8,136,128]{2,1,0:T(8,128)(2,1)} %get-tuple-element.29), calls=%async_computation.4 | async-start | bytes 557056 | tf_op jit(solution)/shard_map/all_to_all | solution.py:243
  96.2 7.3 %collective-permute-start.7 = (bf16[32,2048]{1,0:T(8,128)(2,1)}, bf16[32,2048]{1,0:T(8,128)(2,1)S(1)}, u32[]{:S(2)}, u32[]{:S(2)}) collective-permute-start(bf16[32,2048]{1,0:T(8,128)(2,1)} %get-tuple-element.22), channel_id=1, source_target_pairs={{0,8},{8,16},{16,24},{24,32},{32,40},{40,48},{48,56},{56,64},{64,7... | collective-permute-start | bytes 393224 | tf_op jit(solution)/shard_map/ppermute | solution.py:308
  103.5 11.5 %copy-start.3 = (bf16[32,2048]{1,0:T(8,128)(2,1)}, bf16[32,2048]{1,0:T(8,128)(2,1)S(1)}, u32[]{:S(2)}) copy-start(bf16[32,2048]{1,0:T(8,128)(2,1)S(1)} %collective-permute-done.7.halo) | copy-start | bytes 393220
  119.5 7.4 %copy-start.1 = (bf16[8,136,128]{2,1,0:T(8,128)(2,1)}, bf16[8,136,128]{2,1,0:T(8,128)(2,1)S(1)}, u32[]{:S(2)}) copy-start(bf16[8,136,128]{2,1,0:T(8,128)(2,1)S(1)} %all-to-all-done.4.got) | copy-start | bytes 835588
  119.5 12.1 %all-to-all-start = ((f32[8,2,256]{2,1,0:T(2,128)}), f32[8,2,256]{2,1,0:T(2,128)S(1)}, u32[]{:S(2)}, u32[]{:S(2)}) async-start(f32[8,2,256]{2,1,0:T(2,128)} %get-tuple-element.25), calls=%async_computation | async-start | bytes 32768 | tf_op jit(solution)/shard_map/all_to_all | solution.py:243
  131.6 0.6 copy-start.11
  136.1 4.3 %collective-permute-start.8 = (bf16[128,2048]{1,0:T(8,128)(2,1)}, bf16[128,2048]{1,0:T(8,128)(2,1)S(1)}, u32[]{:S(2)}, u32[]{:S(2)}) collective-permute-start(bf16[128,2048]{1,0:T(8,128)(2,1)} %get-tuple-element.38), channel_id=1, source_target_pairs={{0,1},{1,0},{2,3},{3,2},{4,5},{5,4},{6,7},{7,6},{8,9},{9,8},{10,11... | collective-permute-start | bytes 1572872 | tf_op jit(solution)/shard_map/ppermute | solution.py:410
Sparse Core Ops, SparseCore 0:
  10.3 104.5 all-gather.1

commit v11 on v10

--- a/solution.py
+++ b/solution.py
@@ -16,6 +16,7 @@
 F32 = jnp.float32
 BF16 = jnp.bfloat16
 EXACT = lax.Precision.HIGHEST
+ANY = pl.BlockSpec(memory_space=pl.ANY)
 
 
 def dot_nt(a, b):
@@ -165,12 +166,31 @@
         out[at] = (recur * scaling * gain[...] * gate_act[at]).astype(BF16)
 
 
-def conv_body(halo, normed, weights, taps, conv, stats, shifted):
+def conv_body(halo, normed, gathered, taps, conv, stats, shifted, extended, weights, sems):
     channels = conv.shape[1]
     rows = conv.shape[0]
     filled = HALO + rows
-    extended = jnp.concatenate([halo[...], normed[...]], axis=0)
-    projected = jnp.dot(extended, weights[...], preferred_element_type=F32)
+    depth, width = weights.shape
+    chunk = depth // 2
+    chunks = [slice(k * chunk, (k + 1) * chunk) for k in range(2)]
+    copies = [
+        pltpu.make_async_copy(halo, extended.at[0:HALO], sems.at[0]),
+        pltpu.make_async_copy(normed, extended.at[HALO:filled], sems.at[1]),
+        *[
+            pltpu.make_async_copy(gathered.at[at, 0:width], weights.at[at], sems.at[2 + k])
+            for k, at in enumerate(chunks)
+        ],
+    ]
+    for copy in copies:
+        copy.start()
+    for copy in copies[:3]:
+        copy.wait()
+    first_at, second_at = chunks
+    projected = jnp.dot(extended[:, first_at], weights[first_at], preferred_element_type=F32)
+    copies[3].wait()
+    projected = projected + jnp.dot(
+        extended[:, second_at], weights[second_at], preferred_element_type=F32
+    )
     projected = projected.astype(BF16).astype(F32)
     glu = projected[:, :channels] * jax.nn.sigmoid(projected[:, channels:])
     shifted[0, :filled] = glu.astype(BF16).astype(F32)
@@ -199,9 +219,15 @@
         stats[k] = both
 
 
-def out_body(core, stats, conv, head_out, ln_gain, ln_bias, w_rec, w_low, w_high, out, own, rows_out):
+def out_body(
+    core, stats, conv, head_out, ln_gain, ln_bias, gathered, out, own, rows_out, weights, sem
+):
     channels = conv.shape[1]
     share = conv.shape[0] // stats.shape[0]
+    used = weights.shape[1]
+    all_width = gathered.shape[1]
+    copy = pltpu.make_async_copy(gathered.at[:, all_width - used : all_width], weights, sem)
+    copy.start()
     both = stats[0]
     for k in range(1, stats.shape[0]):
         both = both + stats[k]
@@ -228,15 +254,9 @@
         at = slice(k // 2 * share, (k // 2 + 1) * share)
         rows_out[k % 2, at, :HEAD_K] = head_out[piece]
         rows_out[k % 2, at, HEAD_K:] = conv_out[piece]
-    out[...] = product(rows_out[1 - core[0]], w_rec, w_low, w_high)
-    own[...] = product(rows_out[core[0]], w_rec, w_low, w_high)
-
-
-def product(rows, w_rec, w_low, w_high):
-    mixed = dot_nt(rows[:, :HEAD_K], w_rec[...])
-    mixed = mixed + dot_nt(rows[:, HEAD_K : 2 * HEAD_K], w_low[...])
-    mixed = mixed + dot_nt(rows[:, 2 * HEAD_K :], w_high[...])
-    return mixed.astype(BF16)
+    copy.wait()
+    out[...] = dot_nt(rows_out[1 - core[0]], weights[...]).astype(BF16)
+    own[...] = dot_nt(rows_out[core[0]], weights[...]).astype(BF16)
 
 
 def swap(value, axis):
@@ -345,14 +365,14 @@
         gathered,
         conv_kernel,
         grid=(1,),
-        in_specs=[
-            full(*halo.shape),
-            full(*normed.shape),
-            part(glu_width, 0),
-            full(*conv_kernel.shape),
-        ],
+        in_specs=[ANY, ANY, ANY, full(*conv_kernel.shape)],
         out_specs=(full(rows, channels), full(group, 2, rows)),
-        scratch=(pltpu.VMEM((8, HALO + rows, channels), F32),),
+        scratch=(
+            pltpu.VMEM((8, HALO + rows, channels), F32),
+            pltpu.VMEM((HALO + rows, features), BF16),
+            pltpu.VMEM((features, glu_width), BF16),
+            pltpu.SemaphoreType.DMA((4,)),
+        ),
     )
     stats = swap(stats, TP)
     outer_sent = swap(sent, SP[0])
@@ -378,12 +398,9 @@
         ],
         out_specs=full(rows, HEAD_K),
     )
-    first = glu_width // HEAD_K + 2
     half = rows // 2
     width = HEAD_K + channels
     core = lax.axis_index(TP[1]).reshape(1)
-    weights = [gathered] * 3
-    weight_specs = [part(HEAD_K, first + k) for k in range(3)]
     sent, own = call(
         out_body,
         (shape((half, features), BF16),) * 2,
@@ -393,7 +410,7 @@
         head_out,
         ln_gain.reshape(1, -1),
         ln_bias.reshape(1, -1),
-        *weights,
+        gathered,
         grid=(1,),
         in_specs=[
             smem,
@@ -402,10 +419,14 @@
             full(rows, HEAD_K),
             full(1, channels),
             full(1, channels),
-            *weight_specs,
+            ANY,
         ],
         out_specs=(full(half, features),) * 2,
-        scratch=(pltpu.VMEM((2, half, width), BF16),),
+        scratch=(
+            pltpu.VMEM((2, half, width), BF16),
+            pltpu.VMEM((features, width), BF16),
+            pltpu.SemaphoreType.DMA,
+        ),
     )
     received = lax.ppermute(sent, TP[1], [(0, 1), (1, 0)])
     pair = (own.astype(F32) + received.astype(F32)).astype(BF16)

time: 161 us -> 163 us (1.012)
  transfers between devices with their start and end apart: 14 -> 14, of which waited for: 8 -> 8; matrix products, arithmetic and copies ran while one was open for 0% -> 0% of each run, Pallas kernels for 11% -> 12%
where the time goes in v11:
time: 163 us; the launch traced here: 162 us
  starting transfers between devices  49.4 us (30%)
  waiting for transfers between devices  41.2 us (25%)
  blocking collectives  27 us (17%)
  Pallas kernels  25 us (15%)
  between operations  13.6 us (8%)
  local copies, waits for them, and re-layouts  2.98 us (2%)
  other arithmetic  2.48 us (2%)
    all_to_all x2, blocking collectives, swap(): return lax.all_to_all(value, axis, split_axis=0, concat_axis=0, tiled=True)  27 us
    pallas_call x8, Pallas kernels, call(): pl.pallas_call(body, out_shape=outs, scratch_shapes=scratch, **specs)(*args)  25 us
    all_to_all x4, starting transfers between devices, swap(): return lax.all_to_all(value, axis, split_axis=0, concat_axis=0, tiled=True)  24.1 us
    ppermute x7, starting transfers between devices, shifted_around(): lax.ppermute(value, axis, [(n, (n + k) % count) for n in range(count)])  20.8 us
    all_to_all x4, waiting for transfers between devices, swap(): return lax.all_to_all(value, axis, split_axis=0, concat_axis=0, tiled=True)  18.3 us
    all_gather x1, waiting for transfers between devices, on_device(): gathered = lax.all_gather(operand, SP, axis=0, tiled=True)  11.5 us
    ppermute x1, waiting for transfers between devices, on_device(): halo = lax.ppermute(tail, SP, [(k, k + 1) for k in range(count - 1)])  5.41 us
    ppermute x7, waiting for transfers between devices, shifted_around(): lax.ppermute(value, axis, [(n, (n + k) % count) for n in range(count)])  4.32 us
  transfers between devices with their start and end apart: 14, of which 8 were waited for; matrix products, arithmetic and copies ran while one was open for 0% of the time, Pallas kernels for 12%

profile of v11, /device:TPU:1, one launch (start us, length us, event | category | flops | bytes accessed | tf_op | source)
XLA Modules:
  0.0 161.6 jit_solution(2145959623976694239)
XLA Ops:
  6.5 1.5 shard_map.155
  8.0 0.0 all-gather.2.cloned.1.call-update
  8.1 15.8 %all_to_all.30.value = bf16[8,32,256]{2,1,0:T(8,128)(2,1)} all-to-all(bf16[8,32,256]{2,1,0:T(8,128)(2,1)} %get-tuple-element.27), channel_id=1, replica_groups=mesh['sp_0'=8,'sp_1'=8,'x'=4,'core'=2] {'sp_1'}, dimensions={0} | all-to-all | bytes 262144 | tf_op jit(solution)/shard_map/all_to_all | solution.py:263
  23.8 2.0 %shard_map.157 = bf16[8,8,32,256]{3,2,1,0:T(8,128)(2,1)} custom-call(bf16[8,32,256]{2,1,0:T(8,128)(2,1)} %all_to_all.30.value), custom_call_target="tpu_custom_call" | custom-call | tf_op jit(solution)/shard_map/pallas_call | solution.py:38
  25.8 9.8 %all-to-all-start.2 = ((bf16[8,8,32,256]{3,2,1,0:T(8,128)(2,1)}), bf16[8,8,32,256]{3,2,1,0:T(8,128)(2,1)S(1)}, u32[]{:S(2)}, u32[]{:S(2)}) async-start(bf16[8,8,32,256]{3,2,1,0:T(8,128)(2,1)} %shard_map.157), calls=%async_computation.2 | async-start | bytes 2097152 | tf_op jit(solution)/shard_map/all_to_all | solution.py:263
  35.6 3.7 %collective-permute-start = (bf16[32,2048]{1,0:T(8,128)(2,1)}, bf16[32,2048]{1,0:T(8,128)(2,1)S(1)}, u32[]{:S(2)}, u32[]{:S(2)}) collective-permute-start(bf16[32,2048]{1,0:T(8,128)(2,1)} %refs_0_.1), channel_id=1, source_target_pairs={{0,1},{1,2},{2,3},{3,4},{4,5},{5,6},{6,7},{7,0},{8,9},{9,10},{10,1... | collective-permute-start | bytes 393224 | tf_op jit(solution)/shard_map/ppermute | solution.py:270
  39.3 3.1 %collective-permute-start.1 = (bf16[32,2048]{1,0:T(8,128)(2,1)}, bf16[32,2048]{1,0:T(8,128)(2,1)S(1)}, u32[]{:S(2)}, u32[]{:S(2)}) collective-permute-start(bf16[32,2048]{1,0:T(8,128)(2,1)} %refs_0_.1), channel_id=1, source_target_pairs={{0,2},{1,3},{2,4},{3,5},{4,6},{5,7},{6,0},{7,1},{8,10},{9,11},{10,... | collective-permute-start | bytes 393224 | tf_op jit(solution)/shard_map/ppermute | solution.py:270
  42.4 3.5 %collective-permute-start.2 = (bf16[32,2048]{1,0:T(8,128)(2,1)}, bf16[32,2048]{1,0:T(8,128)(2,1)S(1)}, u32[]{:S(2)}, u32[]{:S(2)}) collective-permute-start(bf16[32,2048]{1,0:T(8,128)(2,1)} %refs_0_.1), channel_id=1, source_target_pairs={{0,3},{1,4},{2,5},{3,6},{4,7},{5,0},{6,1},{7,2},{8,11},{9,12},{10,... | collective-permute-start | bytes 393224 | tf_op jit(solution)/shard_map/ppermute | solution.py:270
  45.8 2.4 %collective-permute-start.3 = (bf16[32,2048]{1,0:T(8,128)(2,1)}, bf16[32,2048]{1,0:T(8,128)(2,1)S(1)}, u32[]{:S(2)}, u32[]{:S(2)}) collective-permute-start(bf16[32,2048]{1,0:T(8,128)(2,1)} %refs_0_.1), channel_id=1, source_target_pairs={{0,4},{1,5},{2,6},{3,7},{4,0},{5,1},{6,2},{7,3},{8,12},{9,13},{10,... | collective-permute-start | bytes 393224 | tf_op jit(solution)/shard_map/ppermute | solution.py:270
  48.3 3.9 %collective-permute-start.4 = (bf16[32,2048]{1,0:T(8,128)(2,1)}, bf16[32,2048]{1,0:T(8,128)(2,1)S(1)}, u32[]{:S(2)}, u32[]{:S(2)}) collective-permute-start(bf16[32,2048]{1,0:T(8,128)(2,1)} %refs_0_.1), channel_id=1, source_target_pairs={{0,5},{1,6},{2,7},{3,0},{4,1},{5,2},{6,3},{7,4},{8,13},{9,14},{10,... | collective-permute-start | bytes 393224 | tf_op jit(solution)/shard_map/ppermute | solution.py:270
  52.2 0.0 collective-permute-done.refs_1_
  52.2 0.0 copy-start.4
  52.2 2.6 %collective-permute-start.5 = (bf16[32,2048]{1,0:T(8,128)(2,1)}, bf16[32,2048]{1,0:T(8,128)(2,1)S(1)}, u32[]{:S(2)}, u32[]{:S(2)}) collective-permute-start(bf16[32,2048]{1,0:T(8,128)(2,1)} %refs_0_.1), channel_id=1, source_target_pairs={{0,6},{1,7},{2,0},{3,1},{4,2},{5,3},{6,4},{7,5},{8,14},{9,15},{10,... | collective-permute-start | bytes 393224 | tf_op jit(solution)/shard_map/ppermute | solution.py:270
  54.8 0.0 collective-permute-done.1.refs_2_
  54.8 1.6 %collective-permute-start.6 = (bf16[32,2048]{1,0:T(8,128)(2,1)}, bf16[32,2048]{1,0:T(8,128)(2,1)S(1)}, u32[]{:S(2)}, u32[]{:S(2)}) collective-permute-start(bf16[32,2048]{1,0:T(8,128)(2,1)} %refs_0_.1), channel_id=1, source_target_pairs={{0,7},{1,0},{2,1},{3,2},{4,3},{5,4},{6,5},{7,6},{8,15},{9,8},{10,9... | collective-permute-start | bytes 393224 | tf_op jit(solution)/shard_map/ppermute | solution.py:270
  56.4 0.6 and_select_fusion.places
  57.0 0.0 collective-permute-done.2.refs_3_
  57.0 0.0 collective-permute-done.3.refs_4_
  57.0 0.0 collective-permute-done.4.refs_5_
  57.0 0.0 copy-start.8
  57.1 1.6 collective-permute-done.5.refs_6_
  58.7 2.7 %collective-permute-done.6.refs_7_ = bf16[32,2048]{1,0:T(8,128)(2,1)S(1)} collective-permute-done((bf16[32,2048]{1,0:T(8,128)(2,1)}, bf16[32,2048]{1,0:T(8,128)(2,1)S(1)}, u32[]{:S(2)}, u32[]{:S(2)}) %collective-permute-start.6) | collective-permute-done | bytes 131104 | tf_op jit(solution)/shard_map/ppermute | solution.py:270
  61.4 0.0 copy-done.5
  61.4 0.6 copy-done.10
  62.0 2.7 %shard_map.154 = (bf16[256,2048]{1,0:T(8,128)(2,1)}, bf16[32,2048]{1,0:T(8,128)(2,1)}) custom-call(s32[8]{0:T(128)} %and_select_fusion.places, f32[1,2048]{1,0:T(1,128)} %bitcast.15, bf16[32,2048]{1,0:T(8,128)(2,1)} %refs_0_.1, bf16[32,2048]{1,0:T(8,128)(2,1)} %copy-done.4, bf16[32,2048]{1,0:T(8,128)(2,1)} %copy-done.5, bf16[32,2048]{1,0:T(8,128)(2,1)} %copy-done.6, ...), custom_call_target="tpu_custom_call" | custom-call | tf_op jit(solution)/shard_map/pallas_call | solution.py:38
  64.8 2.2 %all-to-all-done.2 = bf16[8,8,32,256]{3,2,1,0:T(8,128)(2,1)S(1)} async-done(((bf16[8,8,32,256]{3,2,1,0:T(8,128)(2,1)}), bf16[8,8,32,256]{3,2,1,0:T(8,128)(2,1)S(1)}, u32[]{:S(2)}, u32[]{:S(2)}) %all-to-all-start.2) | async-done | bytes 1048608 | tf_op jit(solution)/shard_map/all_to_all | solution.py:263
  67.0 1.0 copy-done
  68.0 3.7 %shard_map.158 = (bf16[8,136,128]{2,1,0:T(8,128)(2,1)}, bf16[256,128]{1,0:T(8,128)(2,1)}, bf16[256,128]{1,0:T(8,128)(2,1)}, f32[256,128]{1,0:T(8,128)}, bf16[4,128,128]{2,1,0:T(8,128)(2,1)}, /*index=5*/f32[4,128]{1,0:T(4,128)}) custom-call(bf16[256,2048]{1,0:T(8,128)(2,1)} %get-tuple-element.23.normed, bf16[2048,256]{1,0:T(8,128)(2,1)} %bitcast.12, ...), custom_call_target="tpu_custom_call" | custom-call | tf_op jit(solution)/shard_map/pallas_call | solution.py:38
  71.7 3.4 %all-to-all-start.3 = ((bf16[8,136,128]{2,1,0:T(8,128)(2,1)}), bf16[8,136,128]{2,1,0:T(8,128)(2,1)S(1)}, u32[]{:S(2)}, u32[]{:S(2)}) async-start(bf16[8,136,128]{2,1,0:T(8,128)(2,1)} %get-tuple-element.28), calls=%async_computation.3 | async-start | bytes 557056 | tf_op jit(solution)/shard_map/all_to_all | solution.py:263
  75.1 15.0 %all-to-all-done.3.got = bf16[8,136,128]{2,1,0:T(8,128)(2,1)S(1)} async-done(((bf16[8,136,128]{2,1,0:T(8,128)(2,1)}), bf16[8,136,128]{2,1,0:T(8,128)(2,1)S(1)}, u32[]{:S(2)}, u32[]{:S(2)}) %all-to-all-start.3) | async-done | bytes 278560 | tf_op jit(solution)/shard_map/all_to_all | solution.py:263
  90.2 0.7 copy-done.2
  90.9 1.8 %shard_map.159 = (bf16[8,136,128]{2,1,0:T(8,128)(2,1)}, f32[128,128]{1,0:T(8,128)}, f32[8,128]{1,0:T(8,128)}) custom-call(s32[1]{0:T(128)} %bitcast.5.position, bf16[8,136,128]{2,1,0:T(8,128)(2,1)} %copy-done.2), custom_call_target="tpu_custom_call" | custom-call | tf_op jit(solution)/shard_map/pallas_call | solution.py:38
  92.7 3.5 %all-to-all-start.4 = ((bf16[8,136,128]{2,1,0:T(8,128)(2,1)}), bf16[8,136,128]{2,1,0:T(8,128)(2,1)S(1)}, u32[]{:S(2)}, u32[]{:S(2)}) async-start(bf16[8,136,128]{2,1,0:T(8,128)(2,1)} %get-tuple-element.29), calls=%async_computation.4 | async-start | bytes 557056 | tf_op jit(solution)/shard_map/all_to_all | solution.py:263
  96.2 1.9 %collective-permute-start.7 = (bf16[32,2048]{1,0:T(8,128)(2,1)}, bf16[32,2048]{1,0:T(8,128)(2,1)S(1)}, u32[]{:S(2)}, u32[]{:S(2)}) collective-permute-start(bf16[32,2048]{1,0:T(8,128)(2,1)} %get-tuple-element.22), channel_id=1, source_target_pairs={{0,8},{8,16},{16,24},{24,32},{32,40},{40,48},{48,56},{56,64},{64,7... | collective-permute-start | bytes 393224 | tf_op jit(solution)/shard_map/ppermute | solution.py:328
  98.1 5.4 %collective-permute-done.7.halo = bf16[32,2048]{1,0:T(8,128)(2,1)S(1)} collective-permute-done((bf16[32,2048]{1,0:T(8,128)(2,1)}, bf16[32,2048]{1,0:T(8,128)(2,1)S(1)}, u32[]{:S(2)}, u32[]{:S(2)}) %collective-permute-start.7) | collective-permute-done | bytes 131104 | tf_op jit(solution)/shard_map/ppermute | solution.py:328
  103.5 11.5 %all-gather.2.cloned.1.call-done.gathered.weights = bf16[2048,1152]{1,0:T(8,128)(2,1)} async-done(((bf16[32,1152]{1,0:T(8,128)(2,1)}), bf16[2048,1152]{1,0:T(8,128)(2,1)}) %all-gather.2.cloned.1.call-update) | async-done | bytes 4718608 | tf_op jit(solution)/shard_map/all_gather | solution.py:313
  115.0 5.3 %shard_map.156 = (f32[256,256]{1,0:T(8,128)}, f32[8,2,256]{2,1,0:T(2,128)}) custom-call(bf16[32,2048]{1,0:T(8,128)(2,1)} %copy-done.3, bf16[256,2048]{1,0:T(8,128)(2,1)} %get-tuple-element.23.normed, bf16[2048,1152]{1,0:T(8,128)(2,1)} %all-gather.2.cloned.1.call-done.gathered.weights, f32[31,256]{1,0:T(8,128)} %taps.1), custom_call_target="tpu_custom_call" | custom-call | tf_op jit(solution)/shard_map/pallas_call | solution.py:38
  120.3 0.0 all-to-all-done.4.got
  120.3 7.4 %all-to-all-start = ((f32[8,2,256]{2,1,0:T(2,128)}), f32[8,2,256]{2,1,0:T(2,128)S(1)}, u32[]{:S(2)}, u32[]{:S(2)}) async-start(f32[8,2,256]{2,1,0:T(2,128)} %get-tuple-element.25), calls=%async_computation | async-start | bytes 32768 | tf_op jit(solution)/shard_map/all_to_all | solution.py:263
  127.7 3.6 %shard_map.160.head_out = bf16[256,128]{1,0:T(8,128)(2,1)} custom-call(s32[1]{0:T(128)} %bitcast.4.position, bf16[8,136,128]{2,1,0:T(8,128)(2,1)} %copy-done.1, f32[128,128]{1,0:T(8,128)} %get-tuple-element.30.inner_state, f32[8,128]{1,0:T(8,128)} %get-tuple-element.31.inner_total, bf16[256,2048]{1,0:T(8,128)(2,1)} %get-tuple-element.23.normed, ...), custom_call_target="tpu_custom_call" | custom-call | tf_op jit(solution)/shard_map/pallas_call | solution.py:38
  131.4 1.0 all-to-all-done.stats
  132.4 0.6 copy-done.11
  133.0 4.3 %shard_map.161 = (bf16[128,2048]{1,0:T(8,128)(2,1)}, bf16[128,2048]{1,0:T(8,128)(2,1)}) custom-call(s32[1]{0:T(128)} %bitcast.core, f32[8,2,256]{2,1,0:T(2,128)} %copy-done.11, f32[256,256]{1,0:T(8,128)} %get-tuple-element.26.conv, bf16[256,128]{1,0:T(8,128)(2,1)} %shard_map.160.head_out, f32[1,256]{1,0:T(1,128)} %bitcast.17, f32[1,256]{1,0:T(1,128)} %bitcast.18, ...), custom_call_target="tpu_custom_call" | custom-call | tf_op jit(solution)/shard_map/pallas_call | solution.py:38
  137.3 2.6 %collective-permute-start.8 = (bf16[128,2048]{1,0:T(8,128)(2,1)}, bf16[128,2048]{1,0:T(8,128)(2,1)S(1)}, u32[]{:S(2)}, u32[]{:S(2)}) collective-permute-start(bf16[128,2048]{1,0:T(8,128)(2,1)} %get-tuple-element.38), channel_id=1, source_target_pairs={{0,1},{1,0},{2,3},{3,2},{4,5},{5,4},{6,7},{7,6},{8,9},{9,8},{10,11... | collective-permute-start | bytes 1572872 | tf_op jit(solution)/shard_map/ppermute | solution.py:431
  139.9 1.7 %collective-permute-done.8 = bf16[128,2048]{1,0:T(8,128)(2,1)S(1)} collective-permute-done((bf16[128,2048]{1,0:T(8,128)(2,1)}, bf16[128,2048]{1,0:T(8,128)(2,1)S(1)}, u32[]{:S(2)}, u32[]{:S(2)}) %collective-permute-start.8) | collective-permute-done | bytes 524320 | tf_op jit(solution)/shard_map/ppermute | solution.py:431
  141.6 1.2 add_convert_fusion
  142.8 11.2 %all_to_all.31 = bf16[4,32,2048]{2,1,0:T(8,128)(2,1)S(1)} all-to-all(bf16[4,32,2048]{2,1,0:T(8,128)(2,1)S(1)} %bitcast.13), channel_id=1, replica_groups=mesh['sp_0'=8,'sp_1'=8,'x'=4,'core'=2] {'x'}, dimensions={0} | all-to-all | bytes 1048576 | tf_op jit(solution)/shard_map/all_to_all | solution.py:263
  154.0 0.7 reduce_sum.12
  (18 shorter events, 0.0 us)
Async XLA Ops:
  6.5 108.4 %all-gather.2.cloned.1.call-start = ((), (), s32[]{:S(2)}) async-start(), calls=%async_computation.6 | async-start | bytes 4792320 | tf_op jit(solution)/shard_map/all_gather | solution.py:313
  25.8 41.2 %all-to-all-start.2 = ((bf16[8,8,32,256]{3,2,1,0:T(8,128)(2,1)}), bf16[8,8,32,256]{3,2,1,0:T(8,128)(2,1)S(1)}, u32[]{:S(2)}, u32[]{:S(2)}) async-start(bf16[8,8,32,256]{3,2,1,0:T(8,128)(2,1)} %shard_map.157), calls=%async_computation.2 | async-start | bytes 2097152 | tf_op jit(solution)/shard_map/all_to_all | solution.py:263
  35.6 16.6 %collective-permute-start = (bf16[32,2048]{1,0:T(8,128)(2,1)}, bf16[32,2048]{1,0:T(8,128)(2,1)S(1)}, u32[]{:S(2)}, u32[]{:S(2)}) collective-permute-start(bf16[32,2048]{1,0:T(8,128)(2,1)} %refs_0_.1), channel_id=1, source_target_pairs={{0,1},{1,2},{2,3},{3,4},{4,5},{5,6},{6,7},{7,0},{8,9},{9,10},{10,1... | collective-permute-start | bytes 393224 | tf_op jit(solution)/shard_map/ppermute | solution.py:270
  39.3 15.5 %collective-permute-start.1 = (bf16[32,2048]{1,0:T(8,128)(2,1)}, bf16[32,2048]{1,0:T(8,128)(2,1)S(1)}, u32[]{:S(2)}, u32[]{:S(2)}) collective-permute-start(bf16[32,2048]{1,0:T(8,128)(2,1)} %refs_0_.1), channel_id=1, source_target_pairs={{0,2},{1,3},{2,4},{3,5},{4,6},{5,7},{6,0},{7,1},{8,10},{9,11},{10,... | collective-permute-start | bytes 393224 | tf_op jit(solution)/shard_map/ppermute | solution.py:270
  42.4 14.6 %collective-permute-start.2 = (bf16[32,2048]{1,0:T(8,128)(2,1)}, bf16[32,2048]{1,0:T(8,128)(2,1)S(1)}, u32[]{:S(2)}, u32[]{:S(2)}) collective-permute-start(bf16[32,2048]{1,0:T(8,128)(2,1)} %refs_0_.1), channel_id=1, source_target_pairs={{0,3},{1,4},{2,5},{3,6},{4,7},{5,0},{6,1},{7,2},{8,11},{9,12},{10,... | collective-permute-start | bytes 393224 | tf_op jit(solution)/shard_map/ppermute | solution.py:270
  45.8 11.2 %collective-permute-start.3 = (bf16[32,2048]{1,0:T(8,128)(2,1)}, bf16[32,2048]{1,0:T(8,128)(2,1)S(1)}, u32[]{:S(2)}, u32[]{:S(2)}) collective-permute-start(bf16[32,2048]{1,0:T(8,128)(2,1)} %refs_0_.1), channel_id=1, source_target_pairs={{0,4},{1,5},{2,6},{3,7},{4,0},{5,1},{6,2},{7,3},{8,12},{9,13},{10,... | collective-permute-start | bytes 393224 | tf_op jit(solution)/shard_map/ppermute | solution.py:270
  48.3 8.8 %collective-permute-start.4 = (bf16[32,2048]{1,0:T(8,128)(2,1)}, bf16[32,2048]{1,0:T(8,128)(2,1)S(1)}, u32[]{:S(2)}, u32[]{:S(2)}) collective-permute-start(bf16[32,2048]{1,0:T(8,128)(2,1)} %refs_0_.1), channel_id=1, source_target_pairs={{0,5},{1,6},{2,7},{3,0},{4,1},{5,2},{6,3},{7,4},{8,13},{9,14},{10,... | collective-permute-start | bytes 393224 | tf_op jit(solution)/shard_map/ppermute | solution.py:270
  52.2 9.2 %copy-start.4 = (bf16[32,2048]{1,0:T(8,128)(2,1)}, bf16[32,2048]{1,0:T(8,128)(2,1)S(1)}, u32[]{:S(2)}) copy-start(bf16[32,2048]{1,0:T(8,128)(2,1)S(1)} %collective-permute-done.refs_1_) | copy-start | bytes 393220
  52.2 6.4 %collective-permute-start.5 = (bf16[32,2048]{1,0:T(8,128)(2,1)}, bf16[32,2048]{1,0:T(8,128)(2,1)S(1)}, u32[]{:S(2)}, u32[]{:S(2)}) collective-permute-start(bf16[32,2048]{1,0:T(8,128)(2,1)} %refs_0_.1), channel_id=1, source_target_pairs={{0,6},{1,7},{2,0},{3,1},{4,2},{5,3},{6,4},{7,5},{8,14},{9,15},{10,... | collective-permute-start | bytes 393224 | tf_op jit(solution)/shard_map/ppermute | solution.py:270
  54.8 6.6 %copy-start.5 = (bf16[32,2048]{1,0:T(8,128)(2,1)}, bf16[32,2048]{1,0:T(8,128)(2,1)S(1)}, u32[]{:S(2)}) copy-start(bf16[32,2048]{1,0:T(8,128)(2,1)S(1)} %collective-permute-done.1.refs_2_) | copy-start | bytes 393220
  54.8 6.5 %collective-permute-start.6 = (bf16[32,2048]{1,0:T(8,128)(2,1)}, bf16[32,2048]{1,0:T(8,128)(2,1)S(1)}, u32[]{:S(2)}, u32[]{:S(2)}) collective-permute-start(bf16[32,2048]{1,0:T(8,128)(2,1)} %refs_0_.1), channel_id=1, source_target_pairs={{0,7},{1,0},{2,1},{3,2},{4,3},{5,4},{6,5},{7,6},{8,15},{9,8},{10,9... | collective-permute-start | bytes 393224 | tf_op jit(solution)/shard_map/ppermute | solution.py:270
  57.0 4.4 %copy-start.6 = (bf16[32,2048]{1,0:T(8,128)(2,1)}, bf16[32,2048]{1,0:T(8,128)(2,1)S(1)}, u32[]{:S(2)}) copy-start(bf16[32,2048]{1,0:T(8,128)(2,1)S(1)} %collective-permute-done.2.refs_3_) | copy-start | bytes 393220
  57.0 4.4 %copy-start.7 = (bf16[32,2048]{1,0:T(8,128)(2,1)}, bf16[32,2048]{1,0:T(8,128)(2,1)S(1)}, u32[]{:S(2)}) copy-start(bf16[32,2048]{1,0:T(8,128)(2,1)S(1)} %collective-permute-done.3.refs_4_) | copy-start | bytes 393220
  57.0 4.3 %copy-start.8 = (bf16[32,2048]{1,0:T(8,128)(2,1)}, bf16[32,2048]{1,0:T(8,128)(2,1)S(1)}, u32[]{:S(2)}) copy-start(bf16[32,2048]{1,0:T(8,128)(2,1)S(1)} %collective-permute-done.4.refs_5_) | copy-start | bytes 393220
  58.7 2.7 %copy-start.9 = (bf16[32,2048]{1,0:T(8,128)(2,1)}, bf16[32,2048]{1,0:T(8,128)(2,1)S(1)}, u32[]{:S(2)}) copy-start(bf16[32,2048]{1,0:T(8,128)(2,1)S(1)} %collective-permute-done.5.refs_6_) | copy-start | bytes 393220
  61.4 0.7 copy-start.10
  67.0 1.0 copy-start
  71.7 18.4 %all-to-all-start.3 = ((bf16[8,136,128]{2,1,0:T(8,128)(2,1)}), bf16[8,136,128]{2,1,0:T(8,128)(2,1)S(1)}, u32[]{:S(2)}, u32[]{:S(2)}) async-start(bf16[8,136,128]{2,1,0:T(8,128)(2,1)} %get-tuple-element.28), calls=%async_computation.3 | async-start | bytes 557056 | tf_op jit(solution)/shard_map/all_to_all | solution.py:263
  90.2 0.7 copy-start.2
  92.7 27.6 %all-to-all-start.4 = ((bf16[8,136,128]{2,1,0:T(8,128)(2,1)}), bf16[8,136,128]{2,1,0:T(8,128)(2,1)S(1)}, u32[]{:S(2)}, u32[]{:S(2)}) async-start(bf16[8,136,128]{2,1,0:T(8,128)(2,1)} %get-tuple-element.29), calls=%async_computation.4 | async-start | bytes 557056 | tf_op jit(solution)/shard_map/all_to_all | solution.py:263
  96.2 7.3 %collective-permute-start.7 = (bf16[32,2048]{1,0:T(8,128)(2,1)}, bf16[32,2048]{1,0:T(8,128)(2,1)S(1)}, u32[]{:S(2)}, u32[]{:S(2)}) collective-permute-start(bf16[32,2048]{1,0:T(8,128)(2,1)} %get-tuple-element.22), channel_id=1, source_target_pairs={{0,8},{8,16},{16,24},{24,32},{32,40},{40,48},{48,56},{56,64},{64,7... | collective-permute-start | bytes 393224 | tf_op jit(solution)/shard_map/ppermute | solution.py:328
  103.5 11.5 %copy-start.3 = (bf16[32,2048]{1,0:T(8,128)(2,1)}, bf16[32,2048]{1,0:T(8,128)(2,1)S(1)}, u32[]{:S(2)}) copy-start(bf16[32,2048]{1,0:T(8,128)(2,1)S(1)} %collective-permute-done.7.halo) | copy-start | bytes 393220
  120.3 7.4 %copy-start.1 = (bf16[8,136,128]{2,1,0:T(8,128)(2,1)}, bf16[8,136,128]{2,1,0:T(8,128)(2,1)S(1)}, u32[]{:S(2)}) copy-start(bf16[8,136,128]{2,1,0:T(8,128)(2,1)S(1)} %all-to-all-done.4.got) | copy-start | bytes 835588
  120.3 12.1 %all-to-all-start = ((f32[8,2,256]{2,1,0:T(2,128)}), f32[8,2,256]{2,1,0:T(2,128)S(1)}, u32[]{:S(2)}, u32[]{:S(2)}) async-start(f32[8,2,256]{2,1,0:T(2,128)} %get-tuple-element.25), calls=%async_computation | async-start | bytes 32768 | tf_op jit(solution)/shard_map/all_to_all | solution.py:263
  132.4 0.6 copy-start.11
  137.3 4.3 %collective-permute-start.8 = (bf16[128,2048]{1,0:T(8,128)(2,1)}, bf16[128,2048]{1,0:T(8,128)(2,1)S(1)}, u32[]{:S(2)}, u32[]{:S(2)}) collective-permute-start(bf16[128,2048]{1,0:T(8,128)(2,1)} %get-tuple-element.38), channel_id=1, source_target_pairs={{0,1},{1,0},{2,3},{3,2},{4,5},{5,4},{6,7},{7,6},{8,9},{9,8},{10,11... | collective-permute-start | bytes 1572872 | tf_op jit(solution)/shard_map/ppermute | solution.py:431
Sparse Core Ops, SparseCore 0:
  10.3 104.5 all-gather.1

commit v12 on v10

--- a/solution.py
+++ b/solution.py
@@ -132,40 +132,31 @@
     pack_state(sent, state, total)
 
 
-def outer_body(
-    position,
-    got,
-    inner_state,
-    inner_total,
-    normed,
-    weights,
-    value,
-    key,
-    totals,
-    starts,
-    befores,
-    gain,
-    out,
-):
+def outer_body(position, got, inner_state, inner_total, starts, befores, states):
     outside_state = gathered_before(got, position[0])[0]
     incoming = jnp.exp(inner_total[0:1]) * outside_state + inner_state[...]
+    for n in range(starts.shape[0]):
+        state = jnp.exp(befores[n : n + 1]) * incoming + starts[n].astype(F32)
+        states[n] = state.astype(BF16)
+
+
+def head_body(normed, weights, value, key, totals, states, gain, out):
     projected = jnp.dot(normed[...], weights[...], preferred_element_type=F32)
     projected = projected.astype(BF16).astype(F32)
     queries = jax.nn.silu(projected[:, :HEAD_K])
     gate_act = jax.nn.silu(projected[:, HEAD_K:])
     causal = causal_mask()
-    for n in range(starts.shape[0]):
+    for n in range(states.shape[0]):
         at = slice(n * BLOCK, (n + 1) * BLOCK)
         query = (queries[at] * jnp.exp(totals[at])).astype(BF16)
         scores = jnp.where(causal, dot_nt(query, key[at]), 0.0).astype(BF16)
-        state = jnp.exp(befores[n : n + 1]) * incoming + starts[n].astype(F32)
         recur = jnp.dot(scores, value[at], preferred_element_type=F32)
-        recur = recur + dot_nt(query, state.astype(BF16))
+        recur = recur + dot_nt(query, states[n])
         scaling = lax.rsqrt(jnp.mean(recur * recur, axis=1, keepdims=True) + 1e-06)
         out[at] = (recur * scaling * gain[...] * gate_act[at]).astype(BF16)
 
 
-def conv_body(halo, normed, weights, taps, conv, stats, shifted):
+def conv_body(halo, normed, weights, taps, _, conv, stats, shifted):
     channels = conv.shape[1]
     rows = conv.shape[0]
     filled = HALO + rows
@@ -177,7 +168,7 @@
     for r in range(1, 8):
         shifted[r, : filled - 8] = shifted[0, r : filled - 8 + r]
     first = HALO - (KERNEL - 1)
-    step = 32
+    step = 64
     for row in range(0, rows, step):
         accum = jnp.zeros((step, channels), F32)
         for tap in range(KERNEL):
@@ -186,15 +177,10 @@
             accum = accum + taps[tap : tap + 1] * shifted[off - base, base : base + step]
         conv[row : row + step] = accum
     summed = conv[...]
-    ones = jnp.ones((8, channels), F32)
-
-    def over_channels(value):
-        return lax.dot_general(
-            ones, value, (((1,), (1,)), ((), ())), precision=EXACT, preferred_element_type=F32
-        )
-
-    row = lax.broadcasted_iota(jnp.int32, (8, rows), 0)
-    both = jnp.where(row == 0, over_channels(summed), over_channels(summed * summed))[0:2]
+    lane = lax.broadcasted_iota(jnp.int32, (rows, 128), 1)
+    sums = jnp.sum(summed, axis=1, keepdims=True)
+    squares = jnp.sum(summed * summed, axis=1, keepdims=True)
+    both = jnp.where(lane == 0, sums, squares).T[0:2]
     for k in range(stats.shape[0]):
         stats[k] = both
 
@@ -208,20 +194,9 @@
     both = both / (channels * stats.shape[0])
     mean = both[0:1]
     inverse = lax.rsqrt(both[1:2] - mean * mean + 1e-05)
-    row = lax.broadcasted_iota(jnp.int32, (8, both.shape[1]), 0)
-    paired = jnp.where(row == 0, mean, jnp.where(row == 1, inverse, 0.0))
-
-    def column(k):
-        chosen = jnp.where(lax.broadcasted_iota(jnp.int32, (8, channels), 0) == k, 1.0, 0.0)
-        return lax.dot_general(
-            paired,
-            chosen.astype(F32),
-            (((0,), (0,)), ((), ())),
-            precision=EXACT,
-            preferred_element_type=F32,
-        )
-
-    normal = (conv[...] - column(0)) * column(1) * ln_gain[...] + ln_bias[...]
+    row = lax.broadcasted_iota(jnp.int32, (128, both.shape[1]), 0)
+    turned = jnp.where(row == 0, mean, inverse).T
+    normal = (conv[...] - turned[:, 0:1]) * turned[:, 1:2] * ln_gain[...] + ln_bias[...]
     conv_out = jax.nn.silu(normal).astype(BF16)
     for k in range(stats.shape[0]):
         piece = slice(k * share, (k + 1) * share)
@@ -337,6 +312,18 @@
     def full(*lengths):
         return pl.BlockSpec(lengths, lambda k: (0,) * len(lengths))
 
+    *kept, starts, befores = kept
+    states = call(
+        outer_body,
+        shape(starts.shape, BF16),
+        lax.axis_index(SP[0]).reshape(1),
+        swap(sent, SP[0]),
+        inner_state,
+        inner_total,
+        starts,
+        befores,
+        in_specs=[smem] + whole(5),
+    )
     conv, stats = call(
         conv_body,
         (shape((rows, channels), F32), shape((group, 2, rows), F32)),
@@ -344,37 +331,32 @@
         normed,
         gathered,
         conv_kernel,
+        states,
         grid=(1,),
         in_specs=[
             full(*halo.shape),
             full(*normed.shape),
             part(glu_width, 0),
             full(*conv_kernel.shape),
+            pl.BlockSpec(memory_space=pl.ANY),
         ],
         out_specs=(full(rows, channels), full(group, 2, rows)),
         scratch=(pltpu.VMEM((8, HALO + rows, channels), F32),),
     )
     stats = swap(stats, TP)
-    outer_sent = swap(sent, SP[0])
     head_gain = head_gain.reshape(1, -1)
+    kept = (*kept, states, head_gain)
     head_out = call(
-        outer_body,
+        head_body,
         shape((rows, HEAD_K), BF16),
-        lax.axis_index(SP[0]).reshape(1),
-        outer_sent,
-        inner_state,
-        inner_total,
         normed,
         gathered,
         *kept,
-        head_gain,
         grid=(1,),
         in_specs=[
-            smem,
-            *[full(*a.shape) for a in (outer_sent, inner_state, inner_total, normed)],
+            full(*normed.shape),
             part(2 * HEAD_K, glu_width // (2 * HEAD_K)),
             *[full(*a.shape) for a in kept],
-            full(*head_gain.shape),
         ],
         out_specs=full(rows, HEAD_K),
     )

time: 161 us -> 161 us (level)
    all_to_all x4, waiting for transfers between devices: 18.3 us -> 33.7 us  [swap(): return lax.all_to_all(value, axis, split_axis=0, concat_axis=0, tiled=True)]
    all_gather x1, waiting for transfers between devices: 11.5 us -> 0.01 us  [on_device(): gathered = lax.all_gather(operand, SP, axis=0, tiled=True)]
    ppermute x1, waiting for transfers between devices: 5.41 us -> 0.01 us  [on_device(): halo = lax.ppermute(tail, SP, [(k, k + 1) for k in range(count - 1)])]
    pallas_call x8 -> x9, Pallas kernels: 23.8 us -> 24.8 us  [call(): pl.pallas_call(body, out_shape=outs, scratch_shapes=scratch, **specs)(*args)]
  transfers between devices with their start and end apart: 14 -> 14, of which waited for: 8 -> 7; matrix products, arithmetic and copies ran while one was open for 0% -> 0% of each run, Pallas kernels for 11% -> 10%
where the time goes in v12:
time: 161 us; the launch traced here: 160 us
  starting transfers between devices  48.6 us (30%)
  waiting for transfers between devices  39.8 us (25%)
  blocking collectives  26.9 us (17%)
  Pallas kernels  24.8 us (15%)
  between operations  13.6 us (8%)
  local copies, waits for them, and re-layouts  4.31 us (3%)
  other arithmetic  2.48 us (2%)
    all_to_all x4, waiting for transfers between devices, swap(): return lax.all_to_all(value, axis, split_axis=0, concat_axis=0, tiled=True)  33.7 us
    all_to_all x2, blocking collectives, swap(): return lax.all_to_all(value, axis, split_axis=0, concat_axis=0, tiled=True)  26.9 us
    pallas_call x9, Pallas kernels, call(): pl.pallas_call(body, out_shape=outs, scratch_shapes=scratch, **specs)(*args)  24.8 us
    all_to_all x4, starting transfers between devices, swap(): return lax.all_to_all(value, axis, split_axis=0, concat_axis=0, tiled=True)  23.3 us
    ppermute x7, starting transfers between devices, shifted_around(): lax.ppermute(value, axis, [(n, (n + k) % count) for n in range(count)])  20.8 us
    ppermute x7, waiting for transfers between devices, shifted_around(): lax.ppermute(value, axis, [(n, (n + k) % count) for n in range(count)])  4.32 us
    unnamed x24, local copies, waits for them, and re-layouts  4.31 us
  transfers between devices with their start and end apart: 14, of which 7 were waited for; matrix products, arithmetic and copies ran while one was open for 0% of the time, Pallas kernels for 10%

profile of v12, /device:TPU:1, one launch (start us, length us, event | category | flops | bytes accessed | tf_op | source)
XLA Modules:
  0.0 160.3 jit_solution(16453514993223792108)
XLA Ops:
  6.5 1.5 shard_map.155
  8.0 0.0 all-gather.2.cloned.1.call-update
  8.1 15.8 %all_to_all.30.value = bf16[8,32,256]{2,1,0:T(8,128)(2,1)} all-to-all(bf16[8,32,256]{2,1,0:T(8,128)(2,1)} %get-tuple-element.25), channel_id=1, replica_groups=mesh['sp_0'=8,'sp_1'=8,'x'=4,'core'=2] {'sp_1'}, dimensions={0} | all-to-all | bytes 262144 | tf_op jit(solution)/shard_map/all_to_all | solution.py:218
  23.8 2.0 %shard_map.156 = bf16[8,8,32,256]{3,2,1,0:T(8,128)(2,1)} custom-call(bf16[8,32,256]{2,1,0:T(8,128)(2,1)} %all_to_all.30.value), custom_call_target="tpu_custom_call" | custom-call | tf_op jit(solution)/shard_map/pallas_call | solution.py:37
  25.8 9.8 %all-to-all-start.1 = ((bf16[8,8,32,256]{3,2,1,0:T(8,128)(2,1)}), bf16[8,8,32,256]{3,2,1,0:T(8,128)(2,1)S(1)}, u32[]{:S(2)}, u32[]{:S(2)}) async-start(bf16[8,8,32,256]{3,2,1,0:T(8,128)(2,1)} %shard_map.156), calls=%async_computation.1 | async-start | bytes 2097152 | tf_op jit(solution)/shard_map/all_to_all | solution.py:218
  35.6 3.7 %collective-permute-start = (bf16[32,2048]{1,0:T(8,128)(2,1)}, bf16[32,2048]{1,0:T(8,128)(2,1)S(1)}, u32[]{:S(2)}, u32[]{:S(2)}) collective-permute-start(bf16[32,2048]{1,0:T(8,128)(2,1)} %refs_0_.1), channel_id=1, source_target_pairs={{0,1},{1,2},{2,3},{3,4},{4,5},{5,6},{6,7},{7,0},{8,9},{9,10},{10,1... | collective-permute-start | bytes 393224 | tf_op jit(solution)/shard_map/ppermute | solution.py:225
  39.3 3.1 %collective-permute-start.1 = (bf16[32,2048]{1,0:T(8,128)(2,1)}, bf16[32,2048]{1,0:T(8,128)(2,1)S(1)}, u32[]{:S(2)}, u32[]{:S(2)}) collective-permute-start(bf16[32,2048]{1,0:T(8,128)(2,1)} %refs_0_.1), channel_id=1, source_target_pairs={{0,2},{1,3},{2,4},{3,5},{4,6},{5,7},{6,0},{7,1},{8,10},{9,11},{10,... | collective-permute-start | bytes 393224 | tf_op jit(solution)/shard_map/ppermute | solution.py:225
  42.4 3.5 %collective-permute-start.2 = (bf16[32,2048]{1,0:T(8,128)(2,1)}, bf16[32,2048]{1,0:T(8,128)(2,1)S(1)}, u32[]{:S(2)}, u32[]{:S(2)}) collective-permute-start(bf16[32,2048]{1,0:T(8,128)(2,1)} %refs_0_.1), channel_id=1, source_target_pairs={{0,3},{1,4},{2,5},{3,6},{4,7},{5,0},{6,1},{7,2},{8,11},{9,12},{10,... | collective-permute-start | bytes 393224 | tf_op jit(solution)/shard_map/ppermute | solution.py:225
  45.8 2.4 %collective-permute-start.3 = (bf16[32,2048]{1,0:T(8,128)(2,1)}, bf16[32,2048]{1,0:T(8,128)(2,1)S(1)}, u32[]{:S(2)}, u32[]{:S(2)}) collective-permute-start(bf16[32,2048]{1,0:T(8,128)(2,1)} %refs_0_.1), channel_id=1, source_target_pairs={{0,4},{1,5},{2,6},{3,7},{4,0},{5,1},{6,2},{7,3},{8,12},{9,13},{10,... | collective-permute-start | bytes 393224 | tf_op jit(solution)/shard_map/ppermute | solution.py:225
  48.3 3.9 %collective-permute-start.4 = (bf16[32,2048]{1,0:T(8,128)(2,1)}, bf16[32,2048]{1,0:T(8,128)(2,1)S(1)}, u32[]{:S(2)}, u32[]{:S(2)}) collective-permute-start(bf16[32,2048]{1,0:T(8,128)(2,1)} %refs_0_.1), channel_id=1, source_target_pairs={{0,5},{1,6},{2,7},{3,0},{4,1},{5,2},{6,3},{7,4},{8,13},{9,14},{10,... | collective-permute-start | bytes 393224 | tf_op jit(solution)/shard_map/ppermute | solution.py:225
  52.2 0.0 collective-permute-done.refs_1_
  52.2 0.0 copy-start.4
  52.2 2.6 %collective-permute-start.5 = (bf16[32,2048]{1,0:T(8,128)(2,1)}, bf16[32,2048]{1,0:T(8,128)(2,1)S(1)}, u32[]{:S(2)}, u32[]{:S(2)}) collective-permute-start(bf16[32,2048]{1,0:T(8,128)(2,1)} %refs_0_.1), channel_id=1, source_target_pairs={{0,6},{1,7},{2,0},{3,1},{4,2},{5,3},{6,4},{7,5},{8,14},{9,15},{10,... | collective-permute-start | bytes 393224 | tf_op jit(solution)/shard_map/ppermute | solution.py:225
  54.8 0.0 collective-permute-done.1.refs_2_
  54.8 1.6 %collective-permute-start.6 = (bf16[32,2048]{1,0:T(8,128)(2,1)}, bf16[32,2048]{1,0:T(8,128)(2,1)S(1)}, u32[]{:S(2)}, u32[]{:S(2)}) collective-permute-start(bf16[32,2048]{1,0:T(8,128)(2,1)} %refs_0_.1), channel_id=1, source_target_pairs={{0,7},{1,0},{2,1},{3,2},{4,3},{5,4},{6,5},{7,6},{8,15},{9,8},{10,9... | collective-permute-start | bytes 393224 | tf_op jit(solution)/shard_map/ppermute | solution.py:225
  56.4 0.6 and_select_fusion.places
  57.0 0.0 collective-permute-done.2.refs_3_
  57.0 0.0 collective-permute-done.4.refs_5_
  57.1 1.6 %collective-permute-done.5.refs_6_ = bf16[32,2048]{1,0:T(8,128)(2,1)S(1)} collective-permute-done((bf16[32,2048]{1,0:T(8,128)(2,1)}, bf16[32,2048]{1,0:T(8,128)(2,1)S(1)}, u32[]{:S(2)}, u32[]{:S(2)}) %collective-permute-start.5) | collective-permute-done | bytes 131104 | tf_op jit(solution)/shard_map/ppermute | solution.py:225
  58.7 2.7 %collective-permute-done.6.refs_7_ = bf16[32,2048]{1,0:T(8,128)(2,1)S(1)} collective-permute-done((bf16[32,2048]{1,0:T(8,128)(2,1)}, bf16[32,2048]{1,0:T(8,128)(2,1)S(1)}, u32[]{:S(2)}, u32[]{:S(2)}) %collective-permute-start.6) | collective-permute-done | bytes 131104 | tf_op jit(solution)/shard_map/ppermute | solution.py:225
  61.4 0.6 copy-done.10
  62.0 2.7 %shard_map.154 = (bf16[256,2048]{1,0:T(8,128)(2,1)}, bf16[32,2048]{1,0:T(8,128)(2,1)}) custom-call(s32[8]{0:T(128)} %and_select_fusion.places, f32[1,2048]{1,0:T(1,128)} %bitcast.15, bf16[32,2048]{1,0:T(8,128)(2,1)} %refs_0_.1, bf16[32,2048]{1,0:T(8,128)(2,1)} %copy-done.4, bf16[32,2048]{1,0:T(8,128)(2,1)} %copy-done.5, bf16[32,2048]{1,0:T(8,128)(2,1)} %copy-done.6, ...), custom_call_target="tpu_custom_call" | custom-call | tf_op jit(solution)/shard_map/pallas_call | solution.py:37
  64.8 2.2 %all-to-all-done.1 = bf16[8,8,32,256]{3,2,1,0:T(8,128)(2,1)S(1)} async-done(((bf16[8,8,32,256]{3,2,1,0:T(8,128)(2,1)}), bf16[8,8,32,256]{3,2,1,0:T(8,128)(2,1)S(1)}, u32[]{:S(2)}, u32[]{:S(2)}) %all-to-all-start.1) | async-done | bytes 1048608 | tf_op jit(solution)/shard_map/all_to_all | solution.py:218
  67.0 1.0 copy-done
  68.0 3.7 %shard_map.157 = (bf16[8,136,128]{2,1,0:T(8,128)(2,1)}, bf16[256,128]{1,0:T(8,128)(2,1)}, bf16[256,128]{1,0:T(8,128)(2,1)}, f32[256,128]{1,0:T(8,128)}, bf16[4,128,128]{2,1,0:T(8,128)(2,1)}, /*index=5*/f32[4,128]{1,0:T(4,128)}) custom-call(bf16[256,2048]{1,0:T(8,128)(2,1)} %get-tuple-element.23.normed, bf16[2048,256]{1,0:T(8,128)(2,1)} %bitcast.12, ...), custom_call_target="tpu_custom_call" | custom-call | tf_op jit(solution)/shard_map/pallas_call | solution.py:37
  71.7 3.4 %all-to-all-start.2 = ((bf16[8,136,128]{2,1,0:T(8,128)(2,1)}), bf16[8,136,128]{2,1,0:T(8,128)(2,1)S(1)}, u32[]{:S(2)}, u32[]{:S(2)}) async-start(bf16[8,136,128]{2,1,0:T(8,128)(2,1)} %get-tuple-element.26), calls=%async_computation.2 | async-start | bytes 557056 | tf_op jit(solution)/shard_map/all_to_all | solution.py:218
  75.1 15.0 %all-to-all-done.2.got = bf16[8,136,128]{2,1,0:T(8,128)(2,1)S(1)} async-done(((bf16[8,136,128]{2,1,0:T(8,128)(2,1)}), bf16[8,136,128]{2,1,0:T(8,128)(2,1)S(1)}, u32[]{:S(2)}, u32[]{:S(2)}) %all-to-all-start.2) | async-done | bytes 278560 | tf_op jit(solution)/shard_map/all_to_all | solution.py:218
  90.2 0.7 copy-done.2
  90.9 1.8 %shard_map.158 = (bf16[8,136,128]{2,1,0:T(8,128)(2,1)}, f32[128,128]{1,0:T(8,128)}, f32[8,128]{1,0:T(8,128)}) custom-call(s32[1]{0:T(128)} %bitcast.5.position, bf16[8,136,128]{2,1,0:T(8,128)(2,1)} %copy-done.2), custom_call_target="tpu_custom_call" | custom-call | tf_op jit(solution)/shard_map/pallas_call | solution.py:37
  92.7 3.5 %all-to-all-start.3 = ((bf16[8,136,128]{2,1,0:T(8,128)(2,1)}), bf16[8,136,128]{2,1,0:T(8,128)(2,1)S(1)}, u32[]{:S(2)}, u32[]{:S(2)}) async-start(bf16[8,136,128]{2,1,0:T(8,128)(2,1)} %get-tuple-element.27), calls=%async_computation.3 | async-start | bytes 557056 | tf_op jit(solution)/shard_map/all_to_all | solution.py:218
  96.2 1.9 %collective-permute-start.7 = (bf16[32,2048]{1,0:T(8,128)(2,1)}, bf16[32,2048]{1,0:T(8,128)(2,1)S(1)}, u32[]{:S(2)}, u32[]{:S(2)}) collective-permute-start(bf16[32,2048]{1,0:T(8,128)(2,1)} %get-tuple-element.22), channel_id=1, source_target_pairs={{0,8},{8,16},{16,24},{24,32},{32,40},{40,48},{48,56},{56,64},{64,7... | collective-permute-start | bytes 393224 | tf_op jit(solution)/shard_map/ppermute | solution.py:283
  98.1 15.3 %all-to-all-done.3.got = bf16[8,136,128]{2,1,0:T(8,128)(2,1)S(1)} async-done(((bf16[8,136,128]{2,1,0:T(8,128)(2,1)}), bf16[8,136,128]{2,1,0:T(8,128)(2,1)S(1)}, u32[]{:S(2)}, u32[]{:S(2)}) %all-to-all-start.3) | async-done | bytes 278560 | tf_op jit(solution)/shard_map/all_to_all | solution.py:218
  113.4 0.7 copy-done.1
  114.1 1.8 %shard_map.159._.states = bf16[4,128,128]{2,1,0:T(8,128)(2,1)} custom-call(s32[1]{0:T(128)} %bitcast.4.position, bf16[8,136,128]{2,1,0:T(8,128)(2,1)} %copy-done.1, f32[128,128]{1,0:T(8,128)} %get-tuple-element.28.inner_state, f32[8,128]{1,0:T(8,128)} %get-tuple-element.29.inner_total, bf16[4,128,128]{2,1,0:T(8,128)(2,1)} %get-tuple-element.30.starts, ...), custom_call_target="tpu_custom_call" | custom-call | tf_op jit(solution)/shard_map/pallas_call | solution.py:37
  115.9 0.0 collective-permute-done.7.halo
  115.9 0.0 all-gather.2.cloned.1.call-done.weights.w_rec.w_low.w_high
  116.0 0.6 copy-done.3
  116.6 4.2 %shard_map.160 = (f32[256,256]{1,0:T(8,128)}, f32[8,2,256]{2,1,0:T(2,128)}) custom-call(bf16[32,2048]{1,0:T(8,128)(2,1)} %copy-done.3, bf16[256,2048]{1,0:T(8,128)(2,1)} %get-tuple-element.23.normed, bf16[2048,1152]{1,0:T(8,128)(2,1)} %all-gather.2.cloned.1.call-done.weights.w_rec.w_low.w_high, f32[31,256]{1,0:T(8,128)} %taps.1, ...), custom_call_target="tpu_custom_call" | custom-call | tf_op jit(solution)/shard_map/pallas_call | solution.py:37
  120.8 6.6 %all-to-all-start.4 = ((f32[8,2,256]{2,1,0:T(2,128)}), f32[8,2,256]{2,1,0:T(2,128)S(1)}, u32[]{:S(2)}, u32[]{:S(2)}) async-start(f32[8,2,256]{2,1,0:T(2,128)} %get-tuple-element.32), calls=%async_computation.4 | async-start | bytes 32768 | tf_op jit(solution)/shard_map/all_to_all | solution.py:218
  127.4 3.5 %shard_map.161.head_out = bf16[256,128]{1,0:T(8,128)(2,1)} custom-call(bf16[256,2048]{1,0:T(8,128)(2,1)} %get-tuple-element.23.normed, bf16[2048,1152]{1,0:T(8,128)(2,1)} %all-gather.2.cloned.1.call-done.weights.w_rec.w_low.w_high, bf16[256,128]{1,0:T(8,128)(2,1)} %get-tuple-element.34.value, bf16[256,128]{1,0:T(8,128)(2,1)} %get-tuple-element.35.key, ...), custom_call_target="tpu_custom_call" | custom-call | tf_op jit(solution)/shard_map/pallas_call | solution.py:37
  130.9 1.2 all-to-all-done.4.stats
  132.0 0.6 copy-done.11
  132.6 3.5 %shard_map.162 = (bf16[128,2048]{1,0:T(8,128)(2,1)}, bf16[128,2048]{1,0:T(8,128)(2,1)}) custom-call(s32[1]{0:T(128)} %bitcast.core, f32[8,2,256]{2,1,0:T(2,128)} %copy-done.11, f32[256,256]{1,0:T(8,128)} %get-tuple-element.33.conv, bf16[256,128]{1,0:T(8,128)(2,1)} %shard_map.161.head_out, f32[1,256]{1,0:T(1,128)} %bitcast.17, f32[1,256]{1,0:T(1,128)} %bitcast.18, ...), custom_call_target="tpu_custom_call" | custom-call | tf_op jit(solution)/shard_map/pallas_call | solution.py:37
  136.2 2.6 %collective-permute-start.8 = (bf16[128,2048]{1,0:T(8,128)(2,1)}, bf16[128,2048]{1,0:T(8,128)(2,1)S(1)}, u32[]{:S(2)}, u32[]{:S(2)}) collective-permute-start(bf16[128,2048]{1,0:T(8,128)(2,1)} %get-tuple-element.38), channel_id=1, source_target_pairs={{0,1},{1,0},{2,3},{3,2},{4,5},{5,4},{6,7},{7,6},{8,9},{9,8},{10,11... | collective-permute-start | bytes 1572872 | tf_op jit(solution)/shard_map/ppermute | solution.py:392
  138.8 1.7 %collective-permute-done.8 = bf16[128,2048]{1,0:T(8,128)(2,1)S(1)} collective-permute-done((bf16[128,2048]{1,0:T(8,128)(2,1)}, bf16[128,2048]{1,0:T(8,128)(2,1)S(1)}, u32[]{:S(2)}, u32[]{:S(2)}) %collective-permute-start.8) | collective-permute-done | bytes 524320 | tf_op jit(solution)/shard_map/ppermute | solution.py:392
  140.5 1.2 add_convert_fusion
  141.7 11.1 %all_to_all.31 = bf16[4,32,2048]{2,1,0:T(8,128)(2,1)S(1)} all-to-all(bf16[4,32,2048]{2,1,0:T(8,128)(2,1)S(1)} %bitcast.13), channel_id=1, replica_groups=mesh['sp_0'=8,'sp_1'=8,'x'=4,'core'=2] {'x'}, dimensions={0} | all-to-all | bytes 1048576 | tf_op jit(solution)/shard_map/all_to_all | solution.py:218
  152.7 0.7 reduce_sum.12
  (19 shorter events, 0.0 us)
Async XLA Ops:
  6.5 109.4 %all-gather.2.cloned.1.call-start = ((), (), s32[]{:S(2)}) async-start(), calls=%async_computation.6 | async-start | bytes 4792320 | tf_op jit(solution)/shard_map/all_gather | solution.py:268
  25.8 41.2 %all-to-all-start.1 = ((bf16[8,8,32,256]{3,2,1,0:T(8,128)(2,1)}), bf16[8,8,32,256]{3,2,1,0:T(8,128)(2,1)S(1)}, u32[]{:S(2)}, u32[]{:S(2)}) async-start(bf16[8,8,32,256]{3,2,1,0:T(8,128)(2,1)} %shard_map.156), calls=%async_computation.1 | async-start | bytes 2097152 | tf_op jit(solution)/shard_map/all_to_all | solution.py:218
  35.6 16.6 %collective-permute-start = (bf16[32,2048]{1,0:T(8,128)(2,1)}, bf16[32,2048]{1,0:T(8,128)(2,1)S(1)}, u32[]{:S(2)}, u32[]{:S(2)}) collective-permute-start(bf16[32,2048]{1,0:T(8,128)(2,1)} %refs_0_.1), channel_id=1, source_target_pairs={{0,1},{1,2},{2,3},{3,4},{4,5},{5,6},{6,7},{7,0},{8,9},{9,10},{10,1... | collective-permute-start | bytes 393224 | tf_op jit(solution)/shard_map/ppermute | solution.py:225
  39.3 15.5 %collective-permute-start.1 = (bf16[32,2048]{1,0:T(8,128)(2,1)}, bf16[32,2048]{1,0:T(8,128)(2,1)S(1)}, u32[]{:S(2)}, u32[]{:S(2)}) collective-permute-start(bf16[32,2048]{1,0:T(8,128)(2,1)} %refs_0_.1), channel_id=1, source_target_pairs={{0,2},{1,3},{2,4},{3,5},{4,6},{5,7},{6,0},{7,1},{8,10},{9,11},{10,... | collective-permute-start | bytes 393224 | tf_op jit(solution)/shard_map/ppermute | solution.py:225
  42.4 14.6 %collective-permute-start.2 = (bf16[32,2048]{1,0:T(8,128)(2,1)}, bf16[32,2048]{1,0:T(8,128)(2,1)S(1)}, u32[]{:S(2)}, u32[]{:S(2)}) collective-permute-start(bf16[32,2048]{1,0:T(8,128)(2,1)} %refs_0_.1), channel_id=1, source_target_pairs={{0,3},{1,4},{2,5},{3,6},{4,7},{5,0},{6,1},{7,2},{8,11},{9,12},{10,... | collective-permute-start | bytes 393224 | tf_op jit(solution)/shard_map/ppermute | solution.py:225
  45.8 11.2 %collective-permute-start.3 = (bf16[32,2048]{1,0:T(8,128)(2,1)}, bf16[32,2048]{1,0:T(8,128)(2,1)S(1)}, u32[]{:S(2)}, u32[]{:S(2)}) collective-permute-start(bf16[32,2048]{1,0:T(8,128)(2,1)} %refs_0_.1), channel_id=1, source_target_pairs={{0,4},{1,5},{2,6},{3,7},{4,0},{5,1},{6,2},{7,3},{8,12},{9,13},{10,... | collective-permute-start | bytes 393224 | tf_op jit(solution)/shard_map/ppermute | solution.py:225
  48.3 8.8 %collective-permute-start.4 = (bf16[32,2048]{1,0:T(8,128)(2,1)}, bf16[32,2048]{1,0:T(8,128)(2,1)S(1)}, u32[]{:S(2)}, u32[]{:S(2)}) collective-permute-start(bf16[32,2048]{1,0:T(8,128)(2,1)} %refs_0_.1), channel_id=1, source_target_pairs={{0,5},{1,6},{2,7},{3,0},{4,1},{5,2},{6,3},{7,4},{8,13},{9,14},{10,... | collective-permute-start | bytes 393224 | tf_op jit(solution)/shard_map/ppermute | solution.py:225
  52.2 9.2 %copy-start.4 = (bf16[32,2048]{1,0:T(8,128)(2,1)}, bf16[32,2048]{1,0:T(8,128)(2,1)S(1)}, u32[]{:S(2)}) copy-start(bf16[32,2048]{1,0:T(8,128)(2,1)S(1)} %collective-permute-done.refs_1_) | copy-start | bytes 393220
  52.2 6.4 %collective-permute-start.5 = (bf16[32,2048]{1,0:T(8,128)(2,1)}, bf16[32,2048]{1,0:T(8,128)(2,1)S(1)}, u32[]{:S(2)}, u32[]{:S(2)}) collective-permute-start(bf16[32,2048]{1,0:T(8,128)(2,1)} %refs_0_.1), channel_id=1, source_target_pairs={{0,6},{1,7},{2,0},{3,1},{4,2},{5,3},{6,4},{7,5},{8,14},{9,15},{10,... | collective-permute-start | bytes 393224 | tf_op jit(solution)/shard_map/ppermute | solution.py:225
  54.8 6.6 %copy-start.5 = (bf16[32,2048]{1,0:T(8,128)(2,1)}, bf16[32,2048]{1,0:T(8,128)(2,1)S(1)}, u32[]{:S(2)}) copy-start(bf16[32,2048]{1,0:T(8,128)(2,1)S(1)} %collective-permute-done.1.refs_2_) | copy-start | bytes 393220
  54.8 6.5 %collective-permute-start.6 = (bf16[32,2048]{1,0:T(8,128)(2,1)}, bf16[32,2048]{1,0:T(8,128)(2,1)S(1)}, u32[]{:S(2)}, u32[]{:S(2)}) collective-permute-start(bf16[32,2048]{1,0:T(8,128)(2,1)} %refs_0_.1), channel_id=1, source_target_pairs={{0,7},{1,0},{2,1},{3,2},{4,3},{5,4},{6,5},{7,6},{8,15},{9,8},{10,9... | collective-permute-start | bytes 393224 | tf_op jit(solution)/shard_map/ppermute | solution.py:225
  57.0 4.4 %copy-start.6 = (bf16[32,2048]{1,0:T(8,128)(2,1)}, bf16[32,2048]{1,0:T(8,128)(2,1)S(1)}, u32[]{:S(2)}) copy-start(bf16[32,2048]{1,0:T(8,128)(2,1)S(1)} %collective-permute-done.2.refs_3_) | copy-start | bytes 393220
  57.0 4.4 %copy-start.7 = (bf16[32,2048]{1,0:T(8,128)(2,1)}, bf16[32,2048]{1,0:T(8,128)(2,1)S(1)}, u32[]{:S(2)}) copy-start(bf16[32,2048]{1,0:T(8,128)(2,1)S(1)} %collective-permute-done.3.refs_4_) | copy-start | bytes 393220
  57.0 4.3 %copy-start.8 = (bf16[32,2048]{1,0:T(8,128)(2,1)}, bf16[32,2048]{1,0:T(8,128)(2,1)S(1)}, u32[]{:S(2)}) copy-start(bf16[32,2048]{1,0:T(8,128)(2,1)S(1)} %collective-permute-done.4.refs_5_) | copy-start | bytes 393220
  58.7 2.7 %copy-start.9 = (bf16[32,2048]{1,0:T(8,128)(2,1)}, bf16[32,2048]{1,0:T(8,128)(2,1)S(1)}, u32[]{:S(2)}) copy-start(bf16[32,2048]{1,0:T(8,128)(2,1)S(1)} %collective-permute-done.5.refs_6_) | copy-start | bytes 393220
  61.4 0.7 copy-start.10
  67.0 1.0 copy-start
  71.7 18.4 %all-to-all-start.2 = ((bf16[8,136,128]{2,1,0:T(8,128)(2,1)}), bf16[8,136,128]{2,1,0:T(8,128)(2,1)S(1)}, u32[]{:S(2)}, u32[]{:S(2)}) async-start(bf16[8,136,128]{2,1,0:T(8,128)(2,1)} %get-tuple-element.26), calls=%async_computation.2 | async-start | bytes 557056 | tf_op jit(solution)/shard_map/all_to_all | solution.py:218
  90.2 0.7 copy-start.2
  92.7 20.7 %all-to-all-start.3 = ((bf16[8,136,128]{2,1,0:T(8,128)(2,1)}), bf16[8,136,128]{2,1,0:T(8,128)(2,1)S(1)}, u32[]{:S(2)}, u32[]{:S(2)}) async-start(bf16[8,136,128]{2,1,0:T(8,128)(2,1)} %get-tuple-element.27), calls=%async_computation.3 | async-start | bytes 557056 | tf_op jit(solution)/shard_map/all_to_all | solution.py:218
  96.2 19.8 %collective-permute-start.7 = (bf16[32,2048]{1,0:T(8,128)(2,1)}, bf16[32,2048]{1,0:T(8,128)(2,1)S(1)}, u32[]{:S(2)}, u32[]{:S(2)}) collective-permute-start(bf16[32,2048]{1,0:T(8,128)(2,1)} %get-tuple-element.22), channel_id=1, source_target_pairs={{0,8},{8,16},{16,24},{24,32},{32,40},{40,48},{48,56},{56,64},{64,7... | collective-permute-start | bytes 393224 | tf_op jit(solution)/shard_map/ppermute | solution.py:283
  113.4 0.7 copy-start.1
  115.9 0.7 copy-start.3
  120.8 11.2 %all-to-all-start.4 = ((f32[8,2,256]{2,1,0:T(2,128)}), f32[8,2,256]{2,1,0:T(2,128)S(1)}, u32[]{:S(2)}, u32[]{:S(2)}) async-start(f32[8,2,256]{2,1,0:T(2,128)} %get-tuple-element.32), calls=%async_computation.4 | async-start | bytes 32768 | tf_op jit(solution)/shard_map/all_to_all | solution.py:218
  132.0 0.6 copy-start.11
  136.2 4.3 %collective-permute-start.8 = (bf16[128,2048]{1,0:T(8,128)(2,1)}, bf16[128,2048]{1,0:T(8,128)(2,1)S(1)}, u32[]{:S(2)}, u32[]{:S(2)}) collective-permute-start(bf16[128,2048]{1,0:T(8,128)(2,1)} %get-tuple-element.38), channel_id=1, source_target_pairs={{0,1},{1,0},{2,3},{3,2},{4,5},{5,4},{6,7},{7,6},{8,9},{9,8},{10,11... | collective-permute-start | bytes 1572872 | tf_op jit(solution)/shard_map/ppermute | solution.py:392
Sparse Core Ops, SparseCore 0:
  10.3 104.5 all-gather.1

commit v13 on v10

--- a/solution.py
+++ b/solution.py
@@ -177,7 +177,7 @@
     for r in range(1, 8):
         shifted[r, : filled - 8] = shifted[0, r : filled - 8 + r]
     first = HALO - (KERNEL - 1)
-    step = 32
+    step = 128
     for row in range(0, rows, step):
         accum = jnp.zeros((step, channels), F32)
         for tap in range(KERNEL):
@@ -186,15 +186,10 @@
             accum = accum + taps[tap : tap + 1] * shifted[off - base, base : base + step]
         conv[row : row + step] = accum
     summed = conv[...]
-    ones = jnp.ones((8, channels), F32)
-
-    def over_channels(value):
-        return lax.dot_general(
-            ones, value, (((1,), (1,)), ((), ())), precision=EXACT, preferred_element_type=F32
-        )
-
-    row = lax.broadcasted_iota(jnp.int32, (8, rows), 0)
-    both = jnp.where(row == 0, over_channels(summed), over_channels(summed * summed))[0:2]
+    lane = lax.broadcasted_iota(jnp.int32, (rows, 128), 1)
+    sums = jnp.sum(summed, axis=1, keepdims=True)
+    squares = jnp.sum(summed * summed, axis=1, keepdims=True)
+    both = jnp.where(lane == 0, sums, squares).T[0:2]
     for k in range(stats.shape[0]):
         stats[k] = both
 
@@ -208,20 +203,9 @@
     both = both / (channels * stats.shape[0])
     mean = both[0:1]
     inverse = lax.rsqrt(both[1:2] - mean * mean + 1e-05)
-    row = lax.broadcasted_iota(jnp.int32, (8, both.shape[1]), 0)
-    paired = jnp.where(row == 0, mean, jnp.where(row == 1, inverse, 0.0))
-
-    def column(k):
-        chosen = jnp.where(lax.broadcasted_iota(jnp.int32, (8, channels), 0) == k, 1.0, 0.0)
-        return lax.dot_general(
-            paired,
-            chosen.astype(F32),
-            (((0,), (0,)), ((), ())),
-            precision=EXACT,
-            preferred_element_type=F32,
-        )
-
-    normal = (conv[...] - column(0)) * column(1) * ln_gain[...] + ln_bias[...]
+    row = lax.broadcasted_iota(jnp.int32, (128, both.shape[1]), 0)
+    turned = jnp.where(row == 0, mean, inverse).T
+    normal = (conv[...] - turned[:, 0:1]) * turned[:, 1:2] * ln_gain[...] + ln_bias[...]
     conv_out = jax.nn.silu(normal).astype(BF16)
     for k in range(stats.shape[0]):
         piece = slice(k * share, (k + 1) * share)

time: 161 us -> 161 us (level)
  no operation moved by 1% of the time
where the time goes in v13:
time: 161 us; the launch traced here: 160 us
  starting transfers between devices  49.4 us (31%)
  waiting for transfers between devices  41.2 us (26%)
  blocking collectives  27 us (17%)
  Pallas kernels  23.1 us (14%)
  between operations  13.6 us (8%)
  local copies, waits for them, and re-layouts  2.98 us (2%)
  other arithmetic  2.48 us (2%)
    all_to_all x2, blocking collectives, swap(): return lax.all_to_all(value, axis, split_axis=0, concat_axis=0, tiled=True)  27 us
    all_to_all x4, starting transfers between devices, swap(): return lax.all_to_all(value, axis, split_axis=0, concat_axis=0, tiled=True)  24.1 us
    pallas_call x8, Pallas kernels, call(): pl.pallas_call(body, out_shape=outs, scratch_shapes=scratch, **specs)(*args)  23.1 us
    ppermute x7, starting transfers between devices, shifted_around(): lax.ppermute(value, axis, [(n, (n + k) % count) for n in range(count)])  20.8 us
    all_to_all x4, waiting for transfers between devices, swap(): return lax.all_to_all(value, axis, split_axis=0, concat_axis=0, tiled=True)  18.3 us
    all_gather x1, waiting for transfers between devices, on_device(): gathered = lax.all_gather(operand, SP, axis=0, tiled=True)  11.5 us
    ppermute x1, waiting for transfers between devices, on_device(): halo = lax.ppermute(tail, SP, [(k, k + 1) for k in range(count - 1)])  5.41 us
    ppermute x7, waiting for transfers between devices, shifted_around(): lax.ppermute(value, axis, [(n, (n + k) % count) for n in range(count)])  4.32 us
  transfers between devices with their start and end apart: 14, of which 8 were waited for; matrix products, arithmetic and copies ran while one was open for 0% of the time, Pallas kernels for 11%

profile of v13, /device:TPU:1, one launch (start us, length us, event | category | flops | bytes accessed | tf_op | source)
XLA Modules:
  0.0 159.7 jit_solution(6104850437806720315)
XLA Ops:
  6.5 1.5 shard_map.155
  8.0 0.0 all-gather.2.cloned.1.call-update
  8.1 15.8 %all_to_all.30.value = bf16[8,32,256]{2,1,0:T(8,128)(2,1)} all-to-all(bf16[8,32,256]{2,1,0:T(8,128)(2,1)} %get-tuple-element.27), channel_id=1, replica_groups=mesh['sp_0'=8,'sp_1'=8,'x'=4,'core'=2] {'sp_1'}, dimensions={0} | all-to-all | bytes 262144 | tf_op jit(solution)/shard_map/all_to_all | solution.py:227
  23.8 2.0 %shard_map.157 = bf16[8,8,32,256]{3,2,1,0:T(8,128)(2,1)} custom-call(bf16[8,32,256]{2,1,0:T(8,128)(2,1)} %all_to_all.30.value), custom_call_target="tpu_custom_call" | custom-call | tf_op jit(solution)/shard_map/pallas_call | solution.py:37
  25.8 9.8 %all-to-all-start.2 = ((bf16[8,8,32,256]{3,2,1,0:T(8,128)(2,1)}), bf16[8,8,32,256]{3,2,1,0:T(8,128)(2,1)S(1)}, u32[]{:S(2)}, u32[]{:S(2)}) async-start(bf16[8,8,32,256]{3,2,1,0:T(8,128)(2,1)} %shard_map.157), calls=%async_computation.2 | async-start | bytes 2097152 | tf_op jit(solution)/shard_map/all_to_all | solution.py:227
  35.6 3.7 %collective-permute-start = (bf16[32,2048]{1,0:T(8,128)(2,1)}, bf16[32,2048]{1,0:T(8,128)(2,1)S(1)}, u32[]{:S(2)}, u32[]{:S(2)}) collective-permute-start(bf16[32,2048]{1,0:T(8,128)(2,1)} %refs_0_.1), channel_id=1, source_target_pairs={{0,1},{1,2},{2,3},{3,4},{4,5},{5,6},{6,7},{7,0},{8,9},{9,10},{10,1... | collective-permute-start | bytes 393224 | tf_op jit(solution)/shard_map/ppermute | solution.py:234
  39.3 3.1 %collective-permute-start.1 = (bf16[32,2048]{1,0:T(8,128)(2,1)}, bf16[32,2048]{1,0:T(8,128)(2,1)S(1)}, u32[]{:S(2)}, u32[]{:S(2)}) collective-permute-start(bf16[32,2048]{1,0:T(8,128)(2,1)} %refs_0_.1), channel_id=1, source_target_pairs={{0,2},{1,3},{2,4},{3,5},{4,6},{5,7},{6,0},{7,1},{8,10},{9,11},{10,... | collective-permute-start | bytes 393224 | tf_op jit(solution)/shard_map/ppermute | solution.py:234
  42.4 3.5 %collective-permute-start.2 = (bf16[32,2048]{1,0:T(8,128)(2,1)}, bf16[32,2048]{1,0:T(8,128)(2,1)S(1)}, u32[]{:S(2)}, u32[]{:S(2)}) collective-permute-start(bf16[32,2048]{1,0:T(8,128)(2,1)} %refs_0_.1), channel_id=1, source_target_pairs={{0,3},{1,4},{2,5},{3,6},{4,7},{5,0},{6,1},{7,2},{8,11},{9,12},{10,... | collective-permute-start | bytes 393224 | tf_op jit(solution)/shard_map/ppermute | solution.py:234
  45.8 2.4 %collective-permute-start.3 = (bf16[32,2048]{1,0:T(8,128)(2,1)}, bf16[32,2048]{1,0:T(8,128)(2,1)S(1)}, u32[]{:S(2)}, u32[]{:S(2)}) collective-permute-start(bf16[32,2048]{1,0:T(8,128)(2,1)} %refs_0_.1), channel_id=1, source_target_pairs={{0,4},{1,5},{2,6},{3,7},{4,0},{5,1},{6,2},{7,3},{8,12},{9,13},{10,... | collective-permute-start | bytes 393224 | tf_op jit(solution)/shard_map/ppermute | solution.py:234
  48.3 3.9 %collective-permute-start.4 = (bf16[32,2048]{1,0:T(8,128)(2,1)}, bf16[32,2048]{1,0:T(8,128)(2,1)S(1)}, u32[]{:S(2)}, u32[]{:S(2)}) collective-permute-start(bf16[32,2048]{1,0:T(8,128)(2,1)} %refs_0_.1), channel_id=1, source_target_pairs={{0,5},{1,6},{2,7},{3,0},{4,1},{5,2},{6,3},{7,4},{8,13},{9,14},{10,... | collective-permute-start | bytes 393224 | tf_op jit(solution)/shard_map/ppermute | solution.py:234
  52.2 0.0 collective-permute-done.refs_1_
  52.2 0.0 copy-start.4
  52.2 2.6 %collective-permute-start.5 = (bf16[32,2048]{1,0:T(8,128)(2,1)}, bf16[32,2048]{1,0:T(8,128)(2,1)S(1)}, u32[]{:S(2)}, u32[]{:S(2)}) collective-permute-start(bf16[32,2048]{1,0:T(8,128)(2,1)} %refs_0_.1), channel_id=1, source_target_pairs={{0,6},{1,7},{2,0},{3,1},{4,2},{5,3},{6,4},{7,5},{8,14},{9,15},{10,... | collective-permute-start | bytes 393224 | tf_op jit(solution)/shard_map/ppermute | solution.py:234
  54.8 0.0 collective-permute-done.1.refs_2_
  54.8 1.6 %collective-permute-start.6 = (bf16[32,2048]{1,0:T(8,128)(2,1)}, bf16[32,2048]{1,0:T(8,128)(2,1)S(1)}, u32[]{:S(2)}, u32[]{:S(2)}) collective-permute-start(bf16[32,2048]{1,0:T(8,128)(2,1)} %refs_0_.1), channel_id=1, source_target_pairs={{0,7},{1,0},{2,1},{3,2},{4,3},{5,4},{6,5},{7,6},{8,15},{9,8},{10,9... | collective-permute-start | bytes 393224 | tf_op jit(solution)/shard_map/ppermute | solution.py:234
  56.4 0.6 and_select_fusion.places
  57.0 0.0 collective-permute-done.2.refs_3_
  57.0 0.0 collective-permute-done.3.refs_4_
  57.0 0.0 collective-permute-done.4.refs_5_
  57.0 0.0 copy-start.8
  57.1 1.6 %collective-permute-done.5.refs_6_ = bf16[32,2048]{1,0:T(8,128)(2,1)S(1)} collective-permute-done((bf16[32,2048]{1,0:T(8,128)(2,1)}, bf16[32,2048]{1,0:T(8,128)(2,1)S(1)}, u32[]{:S(2)}, u32[]{:S(2)}) %collective-permute-start.5) | collective-permute-done | bytes 131104 | tf_op jit(solution)/shard_map/ppermute | solution.py:234
  58.7 2.7 %collective-permute-done.6.refs_7_ = bf16[32,2048]{1,0:T(8,128)(2,1)S(1)} collective-permute-done((bf16[32,2048]{1,0:T(8,128)(2,1)}, bf16[32,2048]{1,0:T(8,128)(2,1)S(1)}, u32[]{:S(2)}, u32[]{:S(2)}) %collective-permute-start.6) | collective-permute-done | bytes 131104 | tf_op jit(solution)/shard_map/ppermute | solution.py:234
  61.4 0.0 copy-done.5
  61.4 0.6 copy-done.10
  62.0 2.7 %shard_map.154 = (bf16[256,2048]{1,0:T(8,128)(2,1)}, bf16[32,2048]{1,0:T(8,128)(2,1)}) custom-call(s32[8]{0:T(128)} %and_select_fusion.places, f32[1,2048]{1,0:T(1,128)} %bitcast.15, bf16[32,2048]{1,0:T(8,128)(2,1)} %refs_0_.1, bf16[32,2048]{1,0:T(8,128)(2,1)} %copy-done.4, bf16[32,2048]{1,0:T(8,128)(2,1)} %copy-done.5, bf16[32,2048]{1,0:T(8,128)(2,1)} %copy-done.6, ...), custom_call_target="tpu_custom_call" | custom-call | tf_op jit(solution)/shard_map/pallas_call | solution.py:37
  64.8 2.2 %all-to-all-done.2 = bf16[8,8,32,256]{3,2,1,0:T(8,128)(2,1)S(1)} async-done(((bf16[8,8,32,256]{3,2,1,0:T(8,128)(2,1)}), bf16[8,8,32,256]{3,2,1,0:T(8,128)(2,1)S(1)}, u32[]{:S(2)}, u32[]{:S(2)}) %all-to-all-start.2) | async-done | bytes 1048608 | tf_op jit(solution)/shard_map/all_to_all | solution.py:227
  67.0 1.0 copy-done
  68.0 3.7 %shard_map.158 = (bf16[8,136,128]{2,1,0:T(8,128)(2,1)}, bf16[256,128]{1,0:T(8,128)(2,1)}, bf16[256,128]{1,0:T(8,128)(2,1)}, f32[256,128]{1,0:T(8,128)}, bf16[4,128,128]{2,1,0:T(8,128)(2,1)}, /*index=5*/f32[4,128]{1,0:T(4,128)}) custom-call(bf16[256,2048]{1,0:T(8,128)(2,1)} %get-tuple-element.23.normed, bf16[2048,256]{1,0:T(8,128)(2,1)} %bitcast.12, ...), custom_call_target="tpu_custom_call" | custom-call | tf_op jit(solution)/shard_map/pallas_call | solution.py:37
  71.7 3.4 %all-to-all-start.3 = ((bf16[8,136,128]{2,1,0:T(8,128)(2,1)}), bf16[8,136,128]{2,1,0:T(8,128)(2,1)S(1)}, u32[]{:S(2)}, u32[]{:S(2)}) async-start(bf16[8,136,128]{2,1,0:T(8,128)(2,1)} %get-tuple-element.28), calls=%async_computation.3 | async-start | bytes 557056 | tf_op jit(solution)/shard_map/all_to_all | solution.py:227
  75.1 15.0 %all-to-all-done.3.got = bf16[8,136,128]{2,1,0:T(8,128)(2,1)S(1)} async-done(((bf16[8,136,128]{2,1,0:T(8,128)(2,1)}), bf16[8,136,128]{2,1,0:T(8,128)(2,1)S(1)}, u32[]{:S(2)}, u32[]{:S(2)}) %all-to-all-start.3) | async-done | bytes 278560 | tf_op jit(solution)/shard_map/all_to_all | solution.py:227
  90.2 0.7 copy-done.2
  90.9 1.8 %shard_map.159 = (bf16[8,136,128]{2,1,0:T(8,128)(2,1)}, f32[128,128]{1,0:T(8,128)}, f32[8,128]{1,0:T(8,128)}) custom-call(s32[1]{0:T(128)} %bitcast.5.position, bf16[8,136,128]{2,1,0:T(8,128)(2,1)} %copy-done.2), custom_call_target="tpu_custom_call" | custom-call | tf_op jit(solution)/shard_map/pallas_call | solution.py:37
  92.7 3.5 %all-to-all-start.4 = ((bf16[8,136,128]{2,1,0:T(8,128)(2,1)}), bf16[8,136,128]{2,1,0:T(8,128)(2,1)S(1)}, u32[]{:S(2)}, u32[]{:S(2)}) async-start(bf16[8,136,128]{2,1,0:T(8,128)(2,1)} %get-tuple-element.29), calls=%async_computation.4 | async-start | bytes 557056 | tf_op jit(solution)/shard_map/all_to_all | solution.py:227
  96.2 1.9 %collective-permute-start.7 = (bf16[32,2048]{1,0:T(8,128)(2,1)}, bf16[32,2048]{1,0:T(8,128)(2,1)S(1)}, u32[]{:S(2)}, u32[]{:S(2)}) collective-permute-start(bf16[32,2048]{1,0:T(8,128)(2,1)} %get-tuple-element.22), channel_id=1, source_target_pairs={{0,8},{8,16},{16,24},{24,32},{32,40},{40,48},{48,56},{56,64},{64,7... | collective-permute-start | bytes 393224 | tf_op jit(solution)/shard_map/ppermute | solution.py:292
  98.1 5.4 %collective-permute-done.7.halo = bf16[32,2048]{1,0:T(8,128)(2,1)S(1)} collective-permute-done((bf16[32,2048]{1,0:T(8,128)(2,1)}, bf16[32,2048]{1,0:T(8,128)(2,1)S(1)}, u32[]{:S(2)}, u32[]{:S(2)}) %collective-permute-start.7) | collective-permute-done | bytes 131104 | tf_op jit(solution)/shard_map/ppermute | solution.py:292
  103.5 11.5 %all-gather.2.cloned.1.call-done.weights.w_rec.w_low.w_high = bf16[2048,1152]{1,0:T(8,128)(2,1)} async-done(((bf16[32,1152]{1,0:T(8,128)(2,1)}), bf16[2048,1152]{1,0:T(8,128)(2,1)}) %all-gather.2.cloned.1.call-update) | async-done | bytes 4718608 | tf_op jit(solution)/shard_map/all_gather | solution.py:277
  115.0 4.2 %shard_map.156 = (f32[256,256]{1,0:T(8,128)}, f32[8,2,256]{2,1,0:T(2,128)}) custom-call(bf16[32,2048]{1,0:T(8,128)(2,1)} %copy-done.3, bf16[256,2048]{1,0:T(8,128)(2,1)} %get-tuple-element.23.normed, bf16[2048,1152]{1,0:T(8,128)(2,1)} %all-gather.2.cloned.1.call-done.weights.w_rec.w_low.w_high, f32[31,256]{1,0:T(8,128)} %taps.1), custom_call_target="tpu_custom_call" | custom-call | tf_op jit(solution)/shard_map/pallas_call | solution.py:37
  119.2 0.0 all-to-all-done.4.got
  119.2 7.4 %all-to-all-start = ((f32[8,2,256]{2,1,0:T(2,128)}), f32[8,2,256]{2,1,0:T(2,128)S(1)}, u32[]{:S(2)}, u32[]{:S(2)}) async-start(f32[8,2,256]{2,1,0:T(2,128)} %get-tuple-element.25), calls=%async_computation | async-start | bytes 32768 | tf_op jit(solution)/shard_map/all_to_all | solution.py:227
  126.6 3.6 %shard_map.160.head_out = bf16[256,128]{1,0:T(8,128)(2,1)} custom-call(s32[1]{0:T(128)} %bitcast.4.position, bf16[8,136,128]{2,1,0:T(8,128)(2,1)} %copy-done.1, f32[128,128]{1,0:T(8,128)} %get-tuple-element.30.inner_state, f32[8,128]{1,0:T(8,128)} %get-tuple-element.31.inner_total, bf16[256,2048]{1,0:T(8,128)(2,1)} %get-tuple-element.23.normed, ...), custom_call_target="tpu_custom_call" | custom-call | tf_op jit(solution)/shard_map/pallas_call | solution.py:37
  130.2 1.0 all-to-all-done.stats
  131.3 0.6 copy-done.11
  131.9 3.5 %shard_map.161 = (bf16[128,2048]{1,0:T(8,128)(2,1)}, bf16[128,2048]{1,0:T(8,128)(2,1)}) custom-call(s32[1]{0:T(128)} %bitcast.core, f32[8,2,256]{2,1,0:T(2,128)} %copy-done.11, f32[256,256]{1,0:T(8,128)} %get-tuple-element.26.conv, bf16[256,128]{1,0:T(8,128)(2,1)} %shard_map.160.head_out, f32[1,256]{1,0:T(1,128)} %bitcast.17, f32[1,256]{1,0:T(1,128)} %bitcast.18, ...), custom_call_target="tpu_custom_call" | custom-call | tf_op jit(solution)/shard_map/pallas_call | solution.py:37
  135.4 2.6 %collective-permute-start.8 = (bf16[128,2048]{1,0:T(8,128)(2,1)}, bf16[128,2048]{1,0:T(8,128)(2,1)S(1)}, u32[]{:S(2)}, u32[]{:S(2)}) collective-permute-start(bf16[128,2048]{1,0:T(8,128)(2,1)} %get-tuple-element.38), channel_id=1, source_target_pairs={{0,1},{1,0},{2,3},{3,2},{4,5},{5,4},{6,7},{7,6},{8,9},{9,8},{10,11... | collective-permute-start | bytes 1572872 | tf_op jit(solution)/shard_map/ppermute | solution.py:394
  138.0 1.7 %collective-permute-done.8 = bf16[128,2048]{1,0:T(8,128)(2,1)S(1)} collective-permute-done((bf16[128,2048]{1,0:T(8,128)(2,1)}, bf16[128,2048]{1,0:T(8,128)(2,1)S(1)}, u32[]{:S(2)}, u32[]{:S(2)}) %collective-permute-start.8) | collective-permute-done | bytes 524320 | tf_op jit(solution)/shard_map/ppermute | solution.py:394
  139.7 1.2 add_convert_fusion
  140.9 11.2 %all_to_all.31 = bf16[4,32,2048]{2,1,0:T(8,128)(2,1)S(1)} all-to-all(bf16[4,32,2048]{2,1,0:T(8,128)(2,1)S(1)} %bitcast.13), channel_id=1, replica_groups=mesh['sp_0'=8,'sp_1'=8,'x'=4,'core'=2] {'x'}, dimensions={0} | all-to-all | bytes 1048576 | tf_op jit(solution)/shard_map/all_to_all | solution.py:227
  152.1 0.7 reduce_sum.12
  (18 shorter events, 0.0 us)
Async XLA Ops:
  6.5 108.4 %all-gather.2.cloned.1.call-start = ((), (), s32[]{:S(2)}) async-start(), calls=%async_computation.6 | async-start | bytes 4792320 | tf_op jit(solution)/shard_map/all_gather | solution.py:277
  25.8 41.2 %all-to-all-start.2 = ((bf16[8,8,32,256]{3,2,1,0:T(8,128)(2,1)}), bf16[8,8,32,256]{3,2,1,0:T(8,128)(2,1)S(1)}, u32[]{:S(2)}, u32[]{:S(2)}) async-start(bf16[8,8,32,256]{3,2,1,0:T(8,128)(2,1)} %shard_map.157), calls=%async_computation.2 | async-start | bytes 2097152 | tf_op jit(solution)/shard_map/all_to_all | solution.py:227
  35.6 16.6 %collective-permute-start = (bf16[32,2048]{1,0:T(8,128)(2,1)}, bf16[32,2048]{1,0:T(8,128)(2,1)S(1)}, u32[]{:S(2)}, u32[]{:S(2)}) collective-permute-start(bf16[32,2048]{1,0:T(8,128)(2,1)} %refs_0_.1), channel_id=1, source_target_pairs={{0,1},{1,2},{2,3},{3,4},{4,5},{5,6},{6,7},{7,0},{8,9},{9,10},{10,1... | collective-permute-start | bytes 393224 | tf_op jit(solution)/shard_map/ppermute | solution.py:234
  39.3 15.5 %collective-permute-start.1 = (bf16[32,2048]{1,0:T(8,128)(2,1)}, bf16[32,2048]{1,0:T(8,128)(2,1)S(1)}, u32[]{:S(2)}, u32[]{:S(2)}) collective-permute-start(bf16[32,2048]{1,0:T(8,128)(2,1)} %refs_0_.1), channel_id=1, source_target_pairs={{0,2},{1,3},{2,4},{3,5},{4,6},{5,7},{6,0},{7,1},{8,10},{9,11},{10,... | collective-permute-start | bytes 393224 | tf_op jit(solution)/shard_map/ppermute | solution.py:234
  42.4 14.6 %collective-permute-start.2 = (bf16[32,2048]{1,0:T(8,128)(2,1)}, bf16[32,2048]{1,0:T(8,128)(2,1)S(1)}, u32[]{:S(2)}, u32[]{:S(2)}) collective-permute-start(bf16[32,2048]{1,0:T(8,128)(2,1)} %refs_0_.1), channel_id=1, source_target_pairs={{0,3},{1,4},{2,5},{3,6},{4,7},{5,0},{6,1},{7,2},{8,11},{9,12},{10,... | collective-permute-start | bytes 393224 | tf_op jit(solution)/shard_map/ppermute | solution.py:234
  45.8 11.2 %collective-permute-start.3 = (bf16[32,2048]{1,0:T(8,128)(2,1)}, bf16[32,2048]{1,0:T(8,128)(2,1)S(1)}, u32[]{:S(2)}, u32[]{:S(2)}) collective-permute-start(bf16[32,2048]{1,0:T(8,128)(2,1)} %refs_0_.1), channel_id=1, source_target_pairs={{0,4},{1,5},{2,6},{3,7},{4,0},{5,1},{6,2},{7,3},{8,12},{9,13},{10,... | collective-permute-start | bytes 393224 | tf_op jit(solution)/shard_map/ppermute | solution.py:234
  48.3 8.8 %collective-permute-start.4 = (bf16[32,2048]{1,0:T(8,128)(2,1)}, bf16[32,2048]{1,0:T(8,128)(2,1)S(1)}, u32[]{:S(2)}, u32[]{:S(2)}) collective-permute-start(bf16[32,2048]{1,0:T(8,128)(2,1)} %refs_0_.1), channel_id=1, source_target_pairs={{0,5},{1,6},{2,7},{3,0},{4,1},{5,2},{6,3},{7,4},{8,13},{9,14},{10,... | collective-permute-start | bytes 393224 | tf_op jit(solution)/shard_map/ppermute | solution.py:234
  52.2 9.2 %copy-start.4 = (bf16[32,2048]{1,0:T(8,128)(2,1)}, bf16[32,2048]{1,0:T(8,128)(2,1)S(1)}, u32[]{:S(2)}) copy-start(bf16[32,2048]{1,0:T(8,128)(2,1)S(1)} %collective-permute-done.refs_1_) | copy-start | bytes 393220
  52.2 6.4 %collective-permute-start.5 = (bf16[32,2048]{1,0:T(8,128)(2,1)}, bf16[32,2048]{1,0:T(8,128)(2,1)S(1)}, u32[]{:S(2)}, u32[]{:S(2)}) collective-permute-start(bf16[32,2048]{1,0:T(8,128)(2,1)} %refs_0_.1), channel_id=1, source_target_pairs={{0,6},{1,7},{2,0},{3,1},{4,2},{5,3},{6,4},{7,5},{8,14},{9,15},{10,... | collective-permute-start | bytes 393224 | tf_op jit(solution)/shard_map/ppermute | solution.py:234
  54.8 6.6 %copy-start.5 = (bf16[32,2048]{1,0:T(8,128)(2,1)}, bf16[32,2048]{1,0:T(8,128)(2,1)S(1)}, u32[]{:S(2)}) copy-start(bf16[32,2048]{1,0:T(8,128)(2,1)S(1)} %collective-permute-done.1.refs_2_) | copy-start | bytes 393220
  54.8 6.5 %collective-permute-start.6 = (bf16[32,2048]{1,0:T(8,128)(2,1)}, bf16[32,2048]{1,0:T(8,128)(2,1)S(1)}, u32[]{:S(2)}, u32[]{:S(2)}) collective-permute-start(bf16[32,2048]{1,0:T(8,128)(2,1)} %refs_0_.1), channel_id=1, source_target_pairs={{0,7},{1,0},{2,1},{3,2},{4,3},{5,4},{6,5},{7,6},{8,15},{9,8},{10,9... | collective-permute-start | bytes 393224 | tf_op jit(solution)/shard_map/ppermute | solution.py:234
  57.0 4.4 %copy-start.6 = (bf16[32,2048]{1,0:T(8,128)(2,1)}, bf16[32,2048]{1,0:T(8,128)(2,1)S(1)}, u32[]{:S(2)}) copy-start(bf16[32,2048]{1,0:T(8,128)(2,1)S(1)} %collective-permute-done.2.refs_3_) | copy-start | bytes 393220
  57.0 4.4 %copy-start.7 = (bf16[32,2048]{1,0:T(8,128)(2,1)}, bf16[32,2048]{1,0:T(8,128)(2,1)S(1)}, u32[]{:S(2)}) copy-start(bf16[32,2048]{1,0:T(8,128)(2,1)S(1)} %collective-permute-done.3.refs_4_) | copy-start | bytes 393220
  57.0 4.3 %copy-start.8 = (bf16[32,2048]{1,0:T(8,128)(2,1)}, bf16[32,2048]{1,0:T(8,128)(2,1)S(1)}, u32[]{:S(2)}) copy-start(bf16[32,2048]{1,0:T(8,128)(2,1)S(1)} %collective-permute-done.4.refs_5_) | copy-start | bytes 393220
  58.7 2.7 %copy-start.9 = (bf16[32,2048]{1,0:T(8,128)(2,1)}, bf16[32,2048]{1,0:T(8,128)(2,1)S(1)}, u32[]{:S(2)}) copy-start(bf16[32,2048]{1,0:T(8,128)(2,1)S(1)} %collective-permute-done.5.refs_6_) | copy-start | bytes 393220
  61.4 0.7 copy-start.10
  67.0 1.0 copy-start
  71.7 18.4 %all-to-all-start.3 = ((bf16[8,136,128]{2,1,0:T(8,128)(2,1)}), bf16[8,136,128]{2,1,0:T(8,128)(2,1)S(1)}, u32[]{:S(2)}, u32[]{:S(2)}) async-start(bf16[8,136,128]{2,1,0:T(8,128)(2,1)} %get-tuple-element.28), calls=%async_computation.3 | async-start | bytes 557056 | tf_op jit(solution)/shard_map/all_to_all | solution.py:227
  90.2 0.7 copy-start.2
  92.7 26.5 %all-to-all-start.4 = ((bf16[8,136,128]{2,1,0:T(8,128)(2,1)}), bf16[8,136,128]{2,1,0:T(8,128)(2,1)S(1)}, u32[]{:S(2)}, u32[]{:S(2)}) async-start(bf16[8,136,128]{2,1,0:T(8,128)(2,1)} %get-tuple-element.29), calls=%async_computation.4 | async-start | bytes 557056 | tf_op jit(solution)/shard_map/all_to_all | solution.py:227
  96.2 7.3 %collective-permute-start.7 = (bf16[32,2048]{1,0:T(8,128)(2,1)}, bf16[32,2048]{1,0:T(8,128)(2,1)S(1)}, u32[]{:S(2)}, u32[]{:S(2)}) collective-permute-start(bf16[32,2048]{1,0:T(8,128)(2,1)} %get-tuple-element.22), channel_id=1, source_target_pairs={{0,8},{8,16},{16,24},{24,32},{32,40},{40,48},{48,56},{56,64},{64,7... | collective-permute-start | bytes 393224 | tf_op jit(solution)/shard_map/ppermute | solution.py:292
  103.5 11.5 %copy-start.3 = (bf16[32,2048]{1,0:T(8,128)(2,1)}, bf16[32,2048]{1,0:T(8,128)(2,1)S(1)}, u32[]{:S(2)}) copy-start(bf16[32,2048]{1,0:T(8,128)(2,1)S(1)} %collective-permute-done.7.halo) | copy-start | bytes 393220
  119.2 7.4 %copy-start.1 = (bf16[8,136,128]{2,1,0:T(8,128)(2,1)}, bf16[8,136,128]{2,1,0:T(8,128)(2,1)S(1)}, u32[]{:S(2)}) copy-start(bf16[8,136,128]{2,1,0:T(8,128)(2,1)S(1)} %all-to-all-done.4.got) | copy-start | bytes 835588
  119.2 12.1 %all-to-all-start = ((f32[8,2,256]{2,1,0:T(2,128)}), f32[8,2,256]{2,1,0:T(2,128)S(1)}, u32[]{:S(2)}, u32[]{:S(2)}) async-start(f32[8,2,256]{2,1,0:T(2,128)} %get-tuple-element.25), calls=%async_computation | async-start | bytes 32768 | tf_op jit(solution)/shard_map/all_to_all | solution.py:227
  131.3 0.6 copy-start.11
  135.4 4.3 %collective-permute-start.8 = (bf16[128,2048]{1,0:T(8,128)(2,1)}, bf16[128,2048]{1,0:T(8,128)(2,1)S(1)}, u32[]{:S(2)}, u32[]{:S(2)}) collective-permute-start(bf16[128,2048]{1,0:T(8,128)(2,1)} %get-tuple-element.38), channel_id=1, source_target_pairs={{0,1},{1,0},{2,3},{3,2},{4,5},{5,4},{6,7},{7,6},{8,9},{9,8},{10,11... | collective-permute-start | bytes 1572872 | tf_op jit(solution)/shard_map/ppermute | solution.py:394
Sparse Core Ops, SparseCore 0:
  10.3 104.5 all-gather.1
